TPU v7x, 32 devices: a whole 2x2x4 slice. The times are simulated.
32 devices in a mesh: sp: 4 (over z), dp: 8 (over y, x, core).
Axes of the slice: x: 2, y: 2, z: 4, core: 2. Of those that a mesh axis runs over, the one named last changes fastest.
Arguments:
- queries: bfloat16 [8, 512, 1024], P('dp', 'sp'), may hold values from -6 to 6
- key_rows: bfloat16 [8, 512, 1024], P('dp', 'sp'), may hold values from -6 to 6
- values: bfloat16 [8, 512, 2048], P('dp', 'sp'), may hold values from -6 to 6
- out_gate: bfloat16 [8, 512, 2048], P('dp', 'sp'), may hold values from -6 to 6
- input_gate: bfloat16 [8, 4, 512], P('dp', None, 'sp'), may hold values from -6 to 205
- forget_gate: bfloat16 [8, 4, 512], P('dp', None, 'sp'), may hold values from 0.5 to 13
- out_weight: bfloat16 [2048, 2048], P(None, 'dp'), may hold values from -0.125 to 0.125
Outputs:
- layer_out: bfloat16 [8, 512, 2048], P('dp', 'sp')
All inputs are finite; a program needn't handle non-finite values.
Results may differ from a plain program's by a relative error of at most 0.0057.
Values may be sent and summed in bfloat16 or wider, within the bound.
No kernel may reach another device: no remote copies, remote signals or barrier semaphores. Data moves between devices by JAX's collectives and lax.ppermute only.
A program may use at most 64 MiB of HBM per device.

v0:
```python
import jax
import jax.numpy as jnp
from jax import lax
from jax.sharding import PartitionSpec as P

BLOCK = 128


def memory_cell(query_rows, key_in, value_rows, input_log, forget_log):
    block_count = query_rows.shape[0] // BLOCK
    key_width = query_rows.shape[1]
    value_width = value_rows.shape[1]
    key_scale = key_width ** (-0.5)
    causal = lax.broadcasted_iota(jnp.int32, (BLOCK, BLOCK), 0) >= lax.broadcasted_iota(
        jnp.int32, (BLOCK, BLOCK), 1
    )
    highest = lax.Precision.HIGHEST

    def block_step(state_in, inputs):
        memory, normer, stabil = state_in
        query_part, key_part, value_part, gain_part, decay_part = inputs
        query_part = query_part.astype(jnp.float32)
        key_part = key_part.astype(jnp.float32) * key_scale
        value_part = value_part.astype(jnp.float32)
        running = jnp.cumsum(decay_part)
        log_weight = running[:, None] - running[None, :] + gain_part[None, :]
        log_weight = jnp.where(causal, log_weight, -jnp.inf)
        carried_log = running + stabil
        row_top = jnp.maximum(carried_log, jnp.max(log_weight, axis=1))
        scores = jnp.dot(query_part, key_part.T, precision=highest) * jnp.exp(
            log_weight - row_top[:, None]
        )
        carried = jnp.exp(carried_log - row_top)
        numerator = jnp.dot(scores, value_part, precision=highest) + carried[:, None] * jnp.dot(
            query_part, memory, precision=highest
        )
        denominator = jnp.sum(scores, axis=1) + carried * jnp.dot(
            query_part, normer, precision=highest
        )
        output = numerator / jnp.maximum(jnp.abs(denominator), 1.0)[:, None]
        block_end = running[-1]
        weight_log = block_end - running + gain_part
        new_top = jnp.maximum(block_end + stabil, jnp.max(weight_log))
        weights = jnp.exp(weight_log - new_top)
        retain = jnp.exp(block_end + stabil - new_top)
        memory = retain * memory + jnp.dot(
            (key_part * weights[:, None]).T, value_part, precision=highest
        )
        normer = retain * normer + jnp.dot(weights, key_part, precision=highest)
        return ((memory, normer, new_top), output)

    start_state = (
        jnp.zeros((key_width, value_width), jnp.float32),
        jnp.zeros((key_width,), jnp.float32),
        jnp.zeros((), jnp.float32),
    )
    blocks = tuple(
        (
            source.reshape((block_count, BLOCK) + source.shape[1:])
            for source in (query_rows, key_in, value_rows, input_log, forget_log)
        )
    )
    _, outputs = lax.scan(block_step, start_state, blocks)
    return outputs.reshape(block_count * BLOCK, value_width)


def body(queries, key_rows, values, out_gate, input_gate, forget_gate, out_weight):
    group_count = lax.axis_size("sp")
    token_count = queries.shape[1]
    head_count = input_gate.shape[1]
    copies = group_count // head_count
    head_key = queries.shape[2] // head_count
    slice_width = values.shape[2] // group_count

    def spread(source):
        widened = jnp.broadcast_to(
            source[0].reshape(token_count, head_count, 1, head_key),
            (token_count, head_count, copies, head_key),
        )
        return widened.reshape(token_count, group_count, head_key)

    def spread_gate(source):
        return jnp.repeat(source[0].T, copies, axis=1)

    query_all, key_all = (
        lax.all_to_all(spread(queries), "sp", split_axis=1, concat_axis=0, tiled=True),
        lax.all_to_all(spread(key_rows), "sp", split_axis=1, concat_axis=0, tiled=True),
    )
    value_all, input_all, forget_all = (
        lax.all_to_all(
            values[0].reshape(token_count, group_count, slice_width),
            "sp",
            split_axis=1,
            concat_axis=0,
            tiled=True,
        ),
        lax.all_to_all(spread_gate(input_gate), "sp", split_axis=1, concat_axis=0, tiled=True),
        lax.all_to_all(spread_gate(forget_gate), "sp", split_axis=1, concat_axis=0, tiled=True),
    )
    output = memory_cell(
        query_all[:, 0],
        key_all[:, 0],
        value_all[:, 0],
        input_all[:, 0].astype(jnp.float32),
        jax.nn.log_sigmoid(forget_all[:, 0].astype(jnp.float32)),
    )
    hidden = output.astype(jnp.bfloat16)
    token_rows = lax.all_to_all(hidden, "sp", split_axis=0, concat_axis=1, tiled=True)
    gated_rows = (
        token_rows.astype(jnp.float32) * jax.nn.sigmoid(out_gate[0].astype(jnp.float32))
    ).astype(jnp.bfloat16)
    projected = jnp.dot(
        gated_rows,
        lax.all_gather(out_weight, "dp", axis=1, tiled=True),
        preferred_element_type=jnp.float32,
    )
    return projected.astype(jnp.bfloat16)[None]


def solution(mesh):
    return jax.shard_map(
        body,
        mesh=mesh,
        in_specs=(
            P("dp", "sp", None),
            P("dp", "sp", None),
            P("dp", "sp", None),
            P("dp", "sp", None),
            P("dp", None, "sp"),
            P("dp", None, "sp"),
            P(None, "dp"),
        ),
        out_specs=P("dp", "sp", None),
        check_vma=False,
    )
```

profile of v0, /device:TPU:0, one launch (start us, length us, event | category | flops | bytes accessed | tf_op | source)
XLA Modules:
  0.0 121.6 jit_solution(9997319030571958665)
XLA Ops:
  6.5 0.7 all-gather.2.cloned.1.call-update
  7.3 1.3 %copy.28 = bf16[128,4,1]{0,2,1:T(2,128)(2,1)} copy(bf16[128,4,1]{0,1,2:T(4,128)(2,1)} %bitcast.152) | data formatting | bytes 2048 | tf_op jit(solution)/shard_map/all_to_all | solution.py:98
  8.5 6.3 %all-to-all-start = ((bf16[128,4,1]{0,2,1:T(2,128)(2,1)}), bf16[128,4,1]{0,2,1:T(2,128)(2,1)S(1)}, u32[]{:S(2)}, u32[]{:S(2)}) async-start(bf16[128,4,1]{0,2,1:T(2,128)(2,1)} %copy.28), calls=%async_computation | async-start | bytes 4096 | tf_op jit(solution)/shard_map/all_to_all | solution.py:98
  14.9 1.3 %copy.29 = bf16[128,4,1]{0,2,1:T(2,128)(2,1)} copy(bf16[128,4,1]{0,1,2:T(4,128)(2,1)} %bitcast.153) | data formatting | bytes 2048 | tf_op jit(solution)/shard_map/all_to_all | solution.py:97
  16.1 4.2 %all-to-all-done = bf16[128,4,1]{0,2,1:T(2,128)(2,1)S(1)} async-done(((bf16[128,4,1]{0,2,1:T(2,128)(2,1)}), bf16[128,4,1]{0,2,1:T(2,128)(2,1)S(1)}, u32[]{:S(2)}, u32[]{:S(2)}) %all-to-all-start) | async-done | bytes 1056 | tf_op jit(solution)/shard_map/all_to_all | solution.py:98
  20.4 3.2 %all-to-all-start.1 = ((bf16[128,4,1]{0,2,1:T(2,128)(2,1)}), bf16[128,4,1]{0,2,1:T(2,128)(2,1)S(1)}, u32[]{:S(2)}, u32[]{:S(2)}) async-start(bf16[128,4,1]{0,2,1:T(2,128)(2,1)} %copy.29), calls=%async_computation.1 | async-start | bytes 4096 | tf_op jit(solution)/shard_map/all_to_all | solution.py:97
  23.6 1.8 %copy.30 = bf16[1,128,1024]{1,2,0:T(8,128)(2,1)} copy(bf16[1,128,1024]{2,1,0:T(8,128)(2,1)} %param.10) | data formatting | bytes 524288 | tf_op args[1]
  25.4 3.6 %all-to-all-done.1 = bf16[128,4,1]{0,2,1:T(2,128)(2,1)S(1)} async-done(((bf16[128,4,1]{0,2,1:T(2,128)(2,1)}), bf16[128,4,1]{0,2,1:T(2,128)(2,1)S(1)}, u32[]{:S(2)}, u32[]{:S(2)}) %all-to-all-start.1) | async-done | bytes 1056 | tf_op jit(solution)/shard_map/all_to_all | solution.py:97
  29.0 3.4 %all-to-all-start.2 = ((bf16[128,4,256]{0,2,1:T(8,128)(2,1)}), bf16[128,4,256]{0,2,1:T(8,128)(2,1)S(1)}, u32[]{:S(2)}, u32[]{:S(2)}) async-start(bf16[128,4,256]{0,2,1:T(8,128)(2,1)} %bitcast.11), calls=%async_computation.2 | async-start | bytes 524288 | tf_op jit(solution)/shard_map/all_to_all | solution.py:87
  32.4 1.8 %copy.32 = bf16[1,128,1024]{1,2,0:T(8,128)(2,1)} copy(bf16[1,128,1024]{2,1,0:T(8,128)(2,1)} %param.9) | data formatting | bytes 524288 | tf_op args[0]
  34.2 4.9 %all-to-all-done.2 = bf16[128,4,256]{0,2,1:T(8,128)(2,1)S(1)} async-done(((bf16[128,4,256]{0,2,1:T(8,128)(2,1)}), bf16[128,4,256]{0,2,1:T(8,128)(2,1)S(1)}, u32[]{:S(2)}, u32[]{:S(2)}) %all-to-all-start.2) | async-done | bytes 262176 | tf_op jit(solution)/shard_map/all_to_all | solution.py:87
  39.1 3.4 %all-to-all-start.4 = ((bf16[128,4,256]{0,2,1:T(8,128)(2,1)}), bf16[128,4,256]{0,2,1:T(8,128)(2,1)S(1)}, u32[]{:S(2)}, u32[]{:S(2)}) async-start(bf16[128,4,256]{0,2,1:T(8,128)(2,1)} %bitcast.19), calls=%async_computation.4 | async-start | bytes 524288 | tf_op jit(solution)/shard_map/all_to_all | solution.py:86
  42.6 2.1 %copy.31 = bf16[1,128,2048]{1,2,0:T(8,128)(2,1)} copy(bf16[1,128,2048]{2,1,0:T(8,128)(2,1)} %param.11) | data formatting | bytes 1048576 | tf_op args[2]
  44.7 4.7 %all-to-all-done.4 = bf16[128,4,256]{0,2,1:T(8,128)(2,1)S(1)} async-done(((bf16[128,4,256]{0,2,1:T(8,128)(2,1)}), bf16[128,4,256]{0,2,1:T(8,128)(2,1)S(1)}, u32[]{:S(2)}, u32[]{:S(2)}) %all-to-all-start.4) | async-done | bytes 262176 | tf_op jit(solution)/shard_map/all_to_all | solution.py:86
  49.4 3.5 %all-to-all-start.3 = ((bf16[128,4,512]{0,2,1:T(8,128)(2,1)}), bf16[128,4,512]{0,2,1:T(8,128)(2,1)S(1)}, u32[]{:S(2)}, u32[]{:S(2)}) async-start(bf16[128,4,512]{0,2,1:T(8,128)(2,1)} %bitcast.15), calls=%async_computation.3 | async-start | bytes 1048576 | tf_op jit(solution)/shard_map/all_to_all | solution.py:90
  52.9 10.2 %all-to-all-done.3 = bf16[128,4,512]{0,2,1:T(8,128)(2,1)S(1)} async-done(((bf16[128,4,512]{0,2,1:T(8,128)(2,1)}), bf16[128,4,512]{0,2,1:T(8,128)(2,1)S(1)}, u32[]{:S(2)}, u32[]{:S(2)}) %all-to-all-start.3) | async-done | bytes 524320 | tf_op jit(solution)/shard_map/all_to_all | solution.py:90
  63.1 32.2 %while.17 = (s32[]{:T(128)}, f32[256,512]{1,0:T(8,128)S(1)}, f32[256]{0:T(256)S(1)}, f32[]{:T(128)}, bf16[4,128,512]{1,2,0:T(8,128)(2,1)}, /*index=5*/f32[4,128]...) while((s32[]{:T(128)}, f32[256,512]{1,0:T(8,128)S(1)}, ...), condition=%wide.region_5.6_spmd.clone, body=%wide.region_0.5_spmd.clone.sunk | while | flops 555633152 | bytes 3825425 | solution.py:63
  63.2 0.2 broadcast_in_dim.43
  63.4 0.6 slice.7
  64.0 0.8 subtract_reduce_fusion.2
  64.7 1.3 %fusion.87 = (f32[]{:T(128)}, f32[128]{0:T(128)S(1)}) fusion(f32[128]{0:T(128)S(1)} %get-tuple-element.231, f32[]{:T(128)} %bitcast.142, f32[4,128]{1,0:T(4,128)S(1)} %get-tuple-element.274, s32[]{:T(128)} %get-tuple-element.255), kind=kLoop, calls=%fused_computation.63.clone.1 | loop fusion | flops 383 | bytes 1548 | tf_op jit(solution)/shard_map/while/body/eval_jaxpr/reduce_max | solution.py:43
  67.5 0.2 fusion.89
  67.9 0.7 subtract_exponential_fusion.2
  68.6 0.2 fusion.90
  69.0 0.3 fusion.91
  69.3 0.4 fusion.93
  69.8 0.7 constant_dynamic-update-slice_fusion.2
  70.5 0.6 convolution_add_fusion.2
  71.4 0.6 slice.7
  72.0 0.8 subtract_reduce_fusion.2
  72.8 1.3 %fusion.87 = (f32[]{:T(128)}, f32[128]{0:T(128)S(1)}) fusion(f32[128]{0:T(128)S(1)} %get-tuple-element.231, f32[]{:T(128)} %bitcast.142, f32[4,128]{1,0:T(4,128)S(1)} %get-tuple-element.274, s32[]{:T(128)} %get-tuple-element.255), kind=kLoop, calls=%fused_computation.63.clone.1 | loop fusion | flops 383 | bytes 1548 | tf_op jit(solution)/shard_map/while/body/eval_jaxpr/reduce_max | solution.py:43
  75.6 0.2 fusion.89
  76.0 0.7 subtract_exponential_fusion.2
  76.6 0.2 fusion.90
  77.0 0.3 fusion.91
  77.4 0.4 fusion.93
  77.9 0.7 constant_dynamic-update-slice_fusion.2
  78.5 0.6 convolution_add_fusion.2
  79.3 0.2 broadcast_in_dim.43
  79.5 0.6 slice.7
  80.0 0.8 subtract_reduce_fusion.2
  80.8 1.3 %fusion.87 = (f32[]{:T(128)}, f32[128]{0:T(128)S(1)}) fusion(f32[128]{0:T(128)S(1)} %get-tuple-element.231, f32[]{:T(128)} %bitcast.142, f32[4,128]{1,0:T(4,128)S(1)} %get-tuple-element.274, s32[]{:T(128)} %get-tuple-element.255), kind=kLoop, calls=%fused_computation.63.clone.1 | loop fusion | flops 383 | bytes 1548 | tf_op jit(solution)/shard_map/while/body/eval_jaxpr/reduce_max | solution.py:43
  83.6 0.2 fusion.89
  84.0 0.7 subtract_exponential_fusion.2
  84.7 0.2 fusion.90
  85.1 0.3 fusion.91
  85.4 0.4 fusion.93
  85.9 0.7 constant_dynamic-update-slice_fusion.2
  86.6 0.6 convolution_add_fusion.2
  87.5 0.6 slice.7
  88.1 0.8 subtract_reduce_fusion.2
  88.9 1.3 %fusion.87 = (f32[]{:T(128)}, f32[128]{0:T(128)S(1)}) fusion(f32[128]{0:T(128)S(1)} %get-tuple-element.231, f32[]{:T(128)} %bitcast.142, f32[4,128]{1,0:T(4,128)S(1)} %get-tuple-element.274, s32[]{:T(128)} %get-tuple-element.255), kind=kLoop, calls=%fused_computation.63.clone.1 | loop fusion | flops 383 | bytes 1548 | tf_op jit(solution)/shard_map/while/body/eval_jaxpr/reduce_max | solution.py:43
  91.7 0.2 fusion.89
  92.0 0.7 subtract_exponential_fusion.2
  92.7 0.2 fusion.90
  93.1 0.3 fusion.91
  93.4 0.4 fusion.93
  94.0 0.7 constant_dynamic-update-slice_fusion.2
  94.6 0.6 convolution_add_fusion.2
  95.2 3.5 %all-to-all-start.5 = ((bf16[4,128,512]{1,2,0:T(8,128)(2,1)}), bf16[4,128,512]{1,2,0:T(8,128)(2,1)S(1)}, u32[]{:S(2)}, u32[]{:S(2)}) async-start(bf16[4,128,512]{1,2,0:T(8,128)(2,1)} %get-tuple-element.62), calls=%async_computation.5 | async-start | bytes 1048576 | tf_op jit(solution)/shard_map/all_to_all | solution.py:108
  98.7 0.3 copy.37
  99.0 10.0 %all-to-all-done.5 = bf16[4,128,512]{1,2,0:T(8,128)(2,1)S(1)} async-done(((bf16[4,128,512]{1,2,0:T(8,128)(2,1)}), bf16[4,128,512]{1,2,0:T(8,128)(2,1)S(1)}, u32[]{:S(2)}, u32[]{:S(2)}) %all-to-all-start.5) | async-done | bytes 524320 | tf_op jit(solution)/shard_map/all_to_all | solution.py:108
  109.0 0.3 fusion.50
  109.3 5.5 %fusion.49 = bf16[1,128,2048]{2,1,0:T(8,128)(2,1)} fusion(bf16[128,2048]{0,1:T(8,128)(2,1)S(1)} %fusion.50, bf16[2048,2048]{1,0:T(8,128)(2,1)} %all-gather.2.cloned.1.call-done), kind=kOutput, calls=%fused_computation.65 | convolution fusion | flops 1074003968 | bytes 9437184 | tf_op jit(solution)/shard_map/dot_general | solution.py:112
  (44 shorter events, 2.9 us)
Async XLA Ops:
  6.5 102.8 %all-gather.2.cloned.1.call-start = ((), (), s32[]{:S(2)}) async-start(), calls=%async_computation.6 | async-start | bytes 9437184 | tf_op jit(solution)/shard_map/all_gather | solution.py:114
  8.5 11.8 %all-to-all-start = ((bf16[128,4,1]{0,2,1:T(2,128)(2,1)}), bf16[128,4,1]{0,2,1:T(2,128)(2,1)S(1)}, u32[]{:S(2)}, u32[]{:S(2)}) async-start(bf16[128,4,1]{0,2,1:T(2,128)(2,1)} %copy.28), calls=%async_computation | async-start | bytes 4096 | tf_op jit(solution)/shard_map/all_to_all | solution.py:98
  20.4 8.6 %all-to-all-start.1 = ((bf16[128,4,1]{0,2,1:T(2,128)(2,1)}), bf16[128,4,1]{0,2,1:T(2,128)(2,1)S(1)}, u32[]{:S(2)}, u32[]{:S(2)}) async-start(bf16[128,4,1]{0,2,1:T(2,128)(2,1)} %copy.29), calls=%async_computation.1 | async-start | bytes 4096 | tf_op jit(solution)/shard_map/all_to_all | solution.py:97
  29.0 10.2 %all-to-all-start.2 = ((bf16[128,4,256]{0,2,1:T(8,128)(2,1)}), bf16[128,4,256]{0,2,1:T(8,128)(2,1)S(1)}, u32[]{:S(2)}, u32[]{:S(2)}) async-start(bf16[128,4,256]{0,2,1:T(8,128)(2,1)} %bitcast.11), calls=%async_computation.2 | async-start | bytes 524288 | tf_op jit(solution)/shard_map/all_to_all | solution.py:87
  39.1 10.2 %all-to-all-start.4 = ((bf16[128,4,256]{0,2,1:T(8,128)(2,1)}), bf16[128,4,256]{0,2,1:T(8,128)(2,1)S(1)}, u32[]{:S(2)}, u32[]{:S(2)}) async-start(bf16[128,4,256]{0,2,1:T(8,128)(2,1)} %bitcast.19), calls=%async_computation.4 | async-start | bytes 524288 | tf_op jit(solution)/shard_map/all_to_all | solution.py:86
  49.4 13.7 %all-to-all-start.3 = ((bf16[128,4,512]{0,2,1:T(8,128)(2,1)}), bf16[128,4,512]{0,2,1:T(8,128)(2,1)S(1)}, u32[]{:S(2)}, u32[]{:S(2)}) async-start(bf16[128,4,512]{0,2,1:T(8,128)(2,1)} %bitcast.15), calls=%async_computation.3 | async-start | bytes 1048576 | tf_op jit(solution)/shard_map/all_to_all | solution.py:90
  63.1 35.7 %copy-start = (bf16[1,128,2048]{2,1,0:T(8,128)(2,1)S(1)}, bf16[1,128,2048]{2,1,0:T(8,128)(2,1)}, u32[]{:S(2)}) copy-start(bf16[1,128,2048]{2,1,0:T(8,128)(2,1)} %param.12) | copy-start | bytes 1572868
  95.2 13.7 %all-to-all-start.5 = ((bf16[4,128,512]{1,2,0:T(8,128)(2,1)}), bf16[4,128,512]{1,2,0:T(8,128)(2,1)S(1)}, u32[]{:S(2)}, u32[]{:S(2)}) async-start(bf16[4,128,512]{1,2,0:T(8,128)(2,1)} %get-tuple-element.62), calls=%async_computation.5 | async-start | bytes 1048576 | tf_op jit(solution)/shard_map/all_to_all | solution.py:108
Sparse Core Ops, SparseCore 0:
  9.2 58.5 all-gather.1
where the time goes:
time: 122 us
  waiting for transfers between devices  38.3 us (31%)
  starting transfers between devices  23.4 us (19%)
  local copies, waits for them, and re-layouts  15 us (12%)
  between operations  13.5 us (11%)
  matrix products  12.9 us (11%)
  other arithmetic  12.7 us (10%)
  loops' own time  5.83 us (5%)
    all_to_all x1, waiting for transfers between devices, body(): lax.all_to_all(values[0].reshape(token_count, group_count, slice_width),...  10.2 us
    all_to_all x1, waiting for transfers between devices, body(): lax.all_to_all(hidden, 'sp', split_axis=0, concat_axis=1, tiled=True)  9.97 us
    all_to_all x1, starting transfers between devices, body(): lax.all_to_all(spread_gate(forget_gate), 'sp', split_axis=1, concat_axis=...  6.35 us
    unnamed x6, local copies, waits for them, and re-layouts  6 us
    another operation x1, loops' own time, memory_cell(): _, outputs = lax.scan(block_step, start_state, blocks)  5.83 us
    dot_general x1, matrix products, body(): jnp.dot(gated_rows, lax.all_gather(out_weight, 'dp', axis=1, tiled=True),...  5.46 us
    reduce_max x4, other arithmetic, block_step(): new_top = jnp.maximum(block_end + stabil, jnp.max(weight_log))  5.38 us
    all_to_all x1, waiting for transfers between devices, body(): lax.all_to_all(spread(key_rows), 'sp', split_axis=1, concat_axis=0, tiled...  4.92 us
  transfers between devices with their start and end apart: 7, of which 6 were waited for; matrix products, arithmetic and copies ran while one was open for 29% of the time, Pallas kernels for 0%

commit v1 on v0

--- a/solution.py
+++ b/solution.py
@@ -1,6 +1,10 @@
+import functools
+
 import jax
 import jax.numpy as jnp
 from jax import lax
+from jax.experimental import pallas as pl
+from jax.experimental.pallas import tpu as pltpu
 from jax.sharding import PartitionSpec as P
 
 BLOCK = 128
@@ -64,6 +68,72 @@
     return outputs.reshape(block_count * BLOCK, value_width)
 
 
+CORE, XBIT, YBIT = 1, 2, 4
+
+
+def gather_weight(shard):
+    rows = shard.shape[0]
+    half = rows // 2
+
+    def swap(piece, bit):
+        pairs = [(i, i ^ bit) for i in range(lax.axis_size("dp"))]
+        return lax.ppermute(piece, "dp", pairs)
+
+    from_x = swap(shard, XBIT)
+    from_y = swap(shard, YBIT)
+    from_core = swap(shard, CORE)
+    top = swap(from_x[:half], YBIT)
+    bottom = swap(from_y[half:], XBIT)
+    x_core = swap(from_x, CORE)
+    y_core = swap(from_y, CORE)
+    top_core = swap(top, CORE)
+    bottom_core = swap(bottom, CORE)
+    return [
+        (0, 0, shard),
+        (CORE, 0, from_core),
+        (XBIT, 0, from_x),
+        (XBIT | CORE, 0, x_core),
+        (YBIT, 0, from_y),
+        (YBIT | CORE, 0, y_core),
+        (XBIT | YBIT, 0, top),
+        (XBIT | YBIT, half, bottom),
+        (XBIT | YBIT | CORE, 0, top_core),
+        (XBIT | YBIT | CORE, half, bottom_core),
+    ]
+
+
+def project_kernel(plan, place_ref, hidden_ref, gate_ref, *refs):
+    pieces, out_ref = refs[:-1], refs[-1]
+    gated = (
+        hidden_ref[...].astype(jnp.float32) * jax.nn.sigmoid(gate_ref[...].astype(jnp.float32))
+    ).astype(jnp.bfloat16)
+    totals = {}
+    for (mask, start), piece in zip(plan, pieces):
+        part = jnp.dot(
+            gated[:, start : start + piece.shape[0]], piece[...], preferred_element_type=jnp.float32
+        )
+        totals[mask] = totals[mask] + part if mask in totals else part
+    width = pieces[0].shape[1]
+    for mask, total in totals.items():
+        place = pl.multiple_of((place_ref[0] ^ mask) * width, width)
+        out_ref[:, pl.ds(place, width)] = total.astype(out_ref.dtype)
+
+
+def project(hidden, gate, pieces):
+    place = lax.axis_index("dp").astype(jnp.int32).reshape(1)
+    plan = tuple((mask, start) for mask, start, _ in pieces)
+    arrays = [piece for _, _, piece in pieces]
+    columns = arrays[0].shape[1] * lax.axis_size("dp")
+    vmem = pl.BlockSpec(memory_space=pltpu.VMEM)
+    return pl.pallas_call(
+        functools.partial(project_kernel, plan),
+        out_shape=jax.ShapeDtypeStruct((hidden.shape[0], columns), jnp.bfloat16),
+        in_specs=[pl.BlockSpec(memory_space=pltpu.SMEM)] + [vmem] * (2 + len(arrays)),
+        out_specs=vmem,
+        name="project",
+    )(place, hidden, gate, *arrays)
+
+
 def body(queries, key_rows, values, out_gate, input_gate, forget_gate, out_weight):
     group_count = lax.axis_size("sp")
     token_count = queries.shape[1]
@@ -106,6 +176,8 @@
     )
     hidden = output.astype(jnp.bfloat16)
     token_rows = lax.all_to_all(hidden, "sp", split_axis=0, concat_axis=1, tiled=True)
+    if lax.axis_size("dp") == 8:
+        return project(token_rows, out_gate[0], gather_weight(out_weight))[None]
     gated_rows = (
         token_rows.astype(jnp.float32) * jax.nn.sigmoid(out_gate[0].astype(jnp.float32))
     ).astype(jnp.bfloat16)

time: 122 us -> 144 us (1.18)
  between operations: 13.5 us -> 0.14 us
  other arithmetic: 12.7 us -> 22.3 us
  starting transfers between devices: 23.4 us -> 31.1 us
  local copies, waits for them, and re-layouts: 15 us -> 21.3 us
  Pallas kernels: 0 us -> 5.73 us
  waiting for transfers between devices: 38.3 us -> 41.4 us
  matrix products: 12.9 us -> 15.3 us
    ppermute x0 -> x9, waiting for transfers between devices: none -> 10.7 us  [swap(): return lax.ppermute(piece, 'dp', pairs)]
    all_to_all x1, waiting for transfers between devices: 10.2 us -> 0.01 us  [body(): lax.all_to_all(values[0].reshape(token_count, group_count, slice_width),...]
    ppermute x0 -> x9, starting transfers between devices: none -> 6.08 us  [swap(): return lax.ppermute(piece, 'dp', pairs)]
    pallas_call x0 -> x1, Pallas kernels: none -> 5.73 us  [project(): pl.pallas_call(functools.partial(project_kernel, plan), out_shape=jax.Sha...]
    dot_general x1 -> x0, matrix products: 5.46 us -> none  [body(): jnp.dot(gated_rows, lax.all_gather(out_weight, 'dp', axis=1, tiled=True),...]
    add x4, other arithmetic: 0.05 us -> 4.37 us  [block_step(): normer = retain * normer + jnp.dot(weights, key_part, precision=highest)]
    while x0 -> x40, local copies, waits for them, and re-layouts: none -> 4.29 us
    all_to_all x1, waiting for transfers between devices: 9.97 us -> 14.1 us  [body(): lax.all_to_all(hidden, 'sp', split_axis=0, concat_axis=1, tiled=True)]
  transfers between devices with their start and end apart: 7 -> 15, of which waited for: 6 -> 7; matrix products, arithmetic and copies ran while one was open for 29% -> 36% of each run, Pallas kernels for 0% -> 0%
where the time goes in v1:
time: 144 us; the launch traced here: 143 us
  waiting for transfers between devices  41.4 us (29%)
  starting transfers between devices  31.1 us (22%)
  other arithmetic  22.3 us (15%)
  local copies, waits for them, and re-layouts  21.3 us (15%)
  matrix products  15.3 us (11%)
  loops' own time  5.73 us (4%)
  Pallas kernels  5.73 us (4%)
    all_to_all x1, waiting for transfers between devices, body(): lax.all_to_all(hidden, 'sp', split_axis=0, concat_axis=1, tiled=True)  14.1 us
    ppermute x9, waiting for transfers between devices, swap(): return lax.ppermute(piece, 'dp', pairs)  10.7 us
    reduce_max x4, other arithmetic, block_step(): new_top = jnp.maximum(block_end + stabil, jnp.max(weight_log))  8.04 us
    unnamed x19, local copies, waits for them, and re-layouts  6.51 us
    all_to_all x1, starting transfers between devices, body(): lax.all_to_all(spread_gate(forget_gate), 'sp', split_axis=1, concat_axis=...  6.35 us
    ppermute x9, starting transfers between devices, swap(): return lax.ppermute(piece, 'dp', pairs)  6.08 us
    all_to_all x1, waiting for transfers between devices, body(): lax.all_to_all(spread(queries), 'sp', split_axis=1, concat_axis=0, tiled=...  5.88 us
    pallas_call x1, Pallas kernels, project(): pl.pallas_call(functools.partial(project_kernel, plan), out_shape=jax.Sha...  5.73 us
  transfers between devices with their start and end apart: 15, of which 7 were waited for; matrix products, arithmetic and copies ran while one was open for 36% of the time, Pallas kernels for 0%

profile of v1, /device:TPU:0, one launch (start us, length us, event | category | flops | bytes accessed | tf_op | source)
XLA Modules:
  0.0 143.0 jit_solution(7364858333431190329)
XLA Ops:
  0.0 0.7 copy-done.11
  1.3 6.3 %all-to-all-start = ((bf16[128,4,1]{0,2,1:T(2,128)(2,1)}), bf16[128,4,1]{0,2,1:T(2,128)(2,1)S(1)}, u32[]{:S(2)}, u32[]{:S(2)}) async-start(bf16[128,4,1]{0,2,1:T(2,128)(2,1)} %copy.27), calls=%async_computation | async-start | bytes 4096 | tf_op jit(solution)/shard_map/all_to_all | solution.py:168
  7.6 0.7 copy-done.12
  8.9 4.2 %all-to-all-done = bf16[128,4,1]{0,2,1:T(2,128)(2,1)S(1)} async-done(((bf16[128,4,1]{0,2,1:T(2,128)(2,1)}), bf16[128,4,1]{0,2,1:T(2,128)(2,1)S(1)}, u32[]{:S(2)}, u32[]{:S(2)}) %all-to-all-start) | async-done | bytes 1056 | tf_op jit(solution)/shard_map/all_to_all | solution.py:168
  13.1 3.2 %all-to-all-start.1 = ((bf16[128,4,1]{0,2,1:T(2,128)(2,1)}), bf16[128,4,1]{0,2,1:T(2,128)(2,1)S(1)}, u32[]{:S(2)}, u32[]{:S(2)}) async-start(bf16[128,4,1]{0,2,1:T(2,128)(2,1)} %copy.28), calls=%async_computation.1 | async-start | bytes 4096 | tf_op jit(solution)/shard_map/all_to_all | solution.py:167
  16.3 1.8 %copy.31 = bf16[1,128,1024]{1,2,0:T(8,128)(2,1)} copy(bf16[1,128,1024]{2,1,0:T(8,128)(2,1)} %param.9) | data formatting | bytes 524288 | tf_op args[0]
  18.1 3.8 %all-to-all-done.1 = bf16[128,4,1]{0,2,1:T(2,128)(2,1)S(1)} async-done(((bf16[128,4,1]{0,2,1:T(2,128)(2,1)}), bf16[128,4,1]{0,2,1:T(2,128)(2,1)S(1)}, u32[]{:S(2)}, u32[]{:S(2)}) %all-to-all-start.1) | async-done | bytes 1056 | tf_op jit(solution)/shard_map/all_to_all | solution.py:167
  21.8 3.5 %all-to-all-start.4 = ((bf16[128,4,256]{0,2,1:T(8,128)(2,1)}), bf16[128,4,256]{0,2,1:T(8,128)(2,1)S(1)}, u32[]{:S(2)}, u32[]{:S(2)}) async-start(bf16[128,4,256]{0,2,1:T(8,128)(2,1)} %bitcast.20), calls=%async_computation.4 | async-start | bytes 524288 | tf_op jit(solution)/shard_map/all_to_all | solution.py:156
  25.4 0.8 copy.29
  26.2 5.9 %all-to-all-done.4 = bf16[128,4,256]{0,2,1:T(8,128)(2,1)S(1)} async-done(((bf16[128,4,256]{0,2,1:T(8,128)(2,1)}), bf16[128,4,256]{0,2,1:T(8,128)(2,1)S(1)}, u32[]{:S(2)}, u32[]{:S(2)}) %all-to-all-start.4) | async-done | bytes 262176 | tf_op jit(solution)/shard_map/all_to_all | solution.py:156
  32.1 3.4 %all-to-all-start.2 = ((bf16[128,4,256]{0,2,1:T(8,128)(2,1)}), bf16[128,4,256]{0,2,1:T(8,128)(2,1)S(1)}, u32[]{:S(2)}, u32[]{:S(2)}) async-start(bf16[128,4,256]{0,2,1:T(8,128)(2,1)} %bitcast.12), calls=%async_computation.2 | async-start | bytes 524288 | tf_op jit(solution)/shard_map/all_to_all | solution.py:157
  35.5 1.5 %collective-permute-start.1 = (bf16[2048,256]{1,0:T(8,128)(2,1)}, bf16[2048,256]{1,0:T(8,128)(2,1)S(1)}, u32[]{:S(2)}, u32[]{:S(2)}) collective-permute-start(bf16[2048,256]{1,0:T(8,128)(2,1)} %refs_0_.1), channel_id=1, source_target_pairs={{0,2},{1,3},{2,0},{3,1},{4,6},{5,7},{6,4},{7,5},{8,10},{9,11},{10,... | collective-permute-start | bytes 3145736 | tf_op jit(solution)/shard_map/ppermute | solution.py:80
  37.1 1.5 %collective-permute-start.3 = (bf16[2048,256]{1,0:T(8,128)(2,1)}, bf16[2048,256]{1,0:T(8,128)(2,1)S(1)}, u32[]{:S(2)}, u32[]{:S(2)}) collective-permute-start(bf16[2048,256]{1,0:T(8,128)(2,1)} %refs_0_.1), channel_id=1, source_target_pairs={{0,4},{1,5},{2,6},{3,7},{4,0},{5,1},{6,2},{7,3},{8,12},{9,13},{10,... | collective-permute-start | bytes 3145736 | tf_op jit(solution)/shard_map/ppermute | solution.py:80
  38.6 1.0 copy.30
  39.6 2.7 %all-to-all-done.2 = bf16[128,4,256]{0,2,1:T(8,128)(2,1)S(1)} async-done(((bf16[128,4,256]{0,2,1:T(8,128)(2,1)}), bf16[128,4,256]{0,2,1:T(8,128)(2,1)S(1)}, u32[]{:S(2)}, u32[]{:S(2)}) %all-to-all-start.2) | async-done | bytes 262176 | tf_op jit(solution)/shard_map/all_to_all | solution.py:157
  42.3 0.7 copy-done.2
  43.1 3.5 %all-to-all-start.3 = ((bf16[128,4,512]{0,2,1:T(8,128)(2,1)}), bf16[128,4,512]{0,2,1:T(8,128)(2,1)S(1)}, u32[]{:S(2)}, u32[]{:S(2)}) async-start(bf16[128,4,512]{0,2,1:T(8,128)(2,1)} %bitcast.16), calls=%async_computation.3 | async-start | bytes 1048576 | tf_op jit(solution)/shard_map/all_to_all | solution.py:160
  47.3 9.5 %collective-permute-done.1.refs_2_ = bf16[2048,256]{1,0:T(8,128)(2,1)S(1)} collective-permute-done((bf16[2048,256]{1,0:T(8,128)(2,1)}, bf16[2048,256]{1,0:T(8,128)(2,1)S(1)}, u32[]{:S(2)}, u32[]{:S(2)}) %collective-permute-start.1) | collective-permute-done | bytes 1048608 | tf_op jit(solution)/shard_map/ppermute | solution.py:80
  56.8 0.9 slice.14
  57.7 1.6 %collective-permute-start.5 = (bf16[1024,256]{1,0:T(8,128)(2,1)}, bf16[1024,256]{1,0:T(8,128)(2,1)}, u32[]{:S(2)}, u32[]{:S(2)}) collective-permute-start(bf16[1024,256]{1,0:T(8,128)(2,1)} %slice.14), channel_id=1, source_target_pairs={{0,4},{1,5},{2,6},{3,7},{4,0},{5,1},{6,2},{7,3},{8,12},{9,13},{10,... | collective-permute-start | bytes 1572872 | tf_op jit(solution)/shard_map/ppermute | solution.py:80
  59.3 1.1 collective-permute-done.3.refs_4_
  60.4 0.9 slice.15
  62.2 53.7 %while.17 = (s32[]{:T(128)}, f32[256,512]{1,0:T(8,128)S(1)}, f32[256]{0:T(256)}, f32[]{:T(128)}, bf16[4,128,512]{2,1,0:T(8,128)(2,1)}, /*index=5*/f32[4,128]{1,0...) while((s32[]{:T(128)}, f32[256,512]{1,0:T(8,128)S(1)}, ...), condition=%wide.region_5.6_spmd.clone, body=%wide.region_0.5_spmd.clone.sunk | while | flops 555567616 | bytes 7646620 | solution.py:67
  64.4 0.8 subtract_reduce_fusion.2
  65.2 2.0 %fusion.84 = (f32[]{:T(128)}, f32[128]{0:T(128)S(1)}) fusion(f32[128]{0:T(128)S(1)} %get-tuple-element.231, f32[]{:T(128)} %bitcast.138, f32[4,128]{1,0:T(4,128)} %get-tuple-element.274, s32[]{:T(128)S(6)} %copy.50), kind=kLoop, calls=%fused_computation.63.clone.1 | loop fusion | flops 383 | bytes 1548 | tf_op jit(solution)/shard_map/while/body/eval_jaxpr/reduce_max | solution.py:47
  68.0 1.2 subtract_exponential_fusion.2
  69.2 0.8 constant_dynamic-slice_fusion.5
  70.2 0.9 fusion.86
  71.1 0.6 multiply_add_fusion.2
  71.7 0.8 fusion.87
  72.6 0.8 fusion.89
  74.4 0.6 convolution_add_fusion.2
  77.3 0.8 subtract_reduce_fusion.2
  78.1 2.0 %fusion.84 = (f32[]{:T(128)}, f32[128]{0:T(128)S(1)}) fusion(f32[128]{0:T(128)S(1)} %get-tuple-element.231, f32[]{:T(128)} %bitcast.138, f32[4,128]{1,0:T(4,128)} %get-tuple-element.274, s32[]{:T(128)S(6)} %copy.50), kind=kLoop, calls=%fused_computation.63.clone.1 | loop fusion | flops 383 | bytes 1548 | tf_op jit(solution)/shard_map/while/body/eval_jaxpr/reduce_max | solution.py:47
  80.9 1.2 subtract_exponential_fusion.2
  82.2 0.8 constant_dynamic-slice_fusion.5
  83.1 0.9 fusion.86
  84.0 1.3 multiply_add_fusion.2
  85.3 0.8 fusion.87
  86.2 0.8 fusion.89
  88.0 0.6 convolution_add_fusion.2
  90.9 0.8 subtract_reduce_fusion.2
  91.7 2.0 %fusion.84 = (f32[]{:T(128)}, f32[128]{0:T(128)S(1)}) fusion(f32[128]{0:T(128)S(1)} %get-tuple-element.231, f32[]{:T(128)} %bitcast.138, f32[4,128]{1,0:T(4,128)} %get-tuple-element.274, s32[]{:T(128)S(6)} %copy.50), kind=kLoop, calls=%fused_computation.63.clone.1 | loop fusion | flops 383 | bytes 1548 | tf_op jit(solution)/shard_map/while/body/eval_jaxpr/reduce_max | solution.py:47
  94.5 1.2 subtract_exponential_fusion.2
  95.8 0.8 constant_dynamic-slice_fusion.5
  96.7 0.9 fusion.86
  97.6 1.3 multiply_add_fusion.2
  98.9 0.8 fusion.87
  99.7 0.8 fusion.89
  101.6 0.6 convolution_add_fusion.2
  104.5 0.8 subtract_reduce_fusion.2
  105.3 2.0 %fusion.84 = (f32[]{:T(128)}, f32[128]{0:T(128)S(1)}) fusion(f32[128]{0:T(128)S(1)} %get-tuple-element.231, f32[]{:T(128)} %bitcast.138, f32[4,128]{1,0:T(4,128)} %get-tuple-element.274, s32[]{:T(128)S(6)} %copy.50), kind=kLoop, calls=%fused_computation.63.clone.1 | loop fusion | flops 383 | bytes 1548 | tf_op jit(solution)/shard_map/while/body/eval_jaxpr/reduce_max | solution.py:47
  108.1 1.2 subtract_exponential_fusion.2
  109.3 0.8 constant_dynamic-slice_fusion.5
  110.3 0.9 fusion.86
  111.2 1.3 multiply_add_fusion.2
  112.5 0.8 fusion.87
  113.3 0.8 fusion.89
  115.2 0.6 convolution_add_fusion.2
  115.9 5.1 %all-to-all-start.5 = ((bf16[4,128,512]{2,1,0:T(8,128)(2,1)}), bf16[4,128,512]{2,1,0:T(8,128)(2,1)S(1)}, u32[]{:S(2)}, u32[]{:S(2)}) async-start(bf16[4,128,512]{2,1,0:T(8,128)(2,1)} %get-tuple-element.62), calls=%async_computation.5 | async-start | bytes 1048576 | tf_op jit(solution)/shard_map/all_to_all | solution.py:178
  121.5 14.1 %all-to-all-done.5 = bf16[4,128,512]{2,1,0:T(8,128)(2,1)S(1)} async-done(((bf16[4,128,512]{2,1,0:T(8,128)(2,1)}), bf16[4,128,512]{2,1,0:T(8,128)(2,1)S(1)}, u32[]{:S(2)}, u32[]{:S(2)}) %all-to-all-start.5) | async-done | bytes 524320 | tf_op jit(solution)/shard_map/all_to_all | solution.py:178
  135.6 0.9 copy.39
  136.5 0.8 copy-done.3
  137.3 5.7 %project.1 = bf16[128,2048]{1,0:T(8,128)(2,1)} custom-call(s32[1]{0:T(128)} %bitcast.place_ref, bf16[128,2048]{1,0:T(8,128)(2,1)} %bitcast.142, bf16[128,2048]{1,0:T(8,128)(2,1)} %bitcast.146, bf16[2048,256]{1,0:T(8,128)(2,1)} %refs_0_.1, bf16[2048,256]{1,0:T(8,128)(2,1)} %collective-permute-done.refs_1_, bf16[2048,256]{1,0:T(8,128)(2,1)} %copy-done, ...), custom_call_target="tpu_custom_call" | custom-call | tf_op jit(solution)/shard_map/project/pallas_call | solution.py:128
  (106 shorter events, 14.8 us)
Async XLA Ops:
  0.0 0.7 copy-start.11
  1.3 11.8 %all-to-all-start = ((bf16[128,4,1]{0,2,1:T(2,128)(2,1)}), bf16[128,4,1]{0,2,1:T(2,128)(2,1)S(1)}, u32[]{:S(2)}, u32[]{:S(2)}) async-start(bf16[128,4,1]{0,2,1:T(2,128)(2,1)} %copy.27), calls=%async_computation | async-start | bytes 4096 | tf_op jit(solution)/shard_map/all_to_all | solution.py:168
  7.6 0.7 copy-start.12
  13.1 8.7 %all-to-all-start.1 = ((bf16[128,4,1]{0,2,1:T(2,128)(2,1)}), bf16[128,4,1]{0,2,1:T(2,128)(2,1)S(1)}, u32[]{:S(2)}, u32[]{:S(2)}) async-start(bf16[128,4,1]{0,2,1:T(2,128)(2,1)} %copy.28), calls=%async_computation.1 | async-start | bytes 4096 | tf_op jit(solution)/shard_map/all_to_all | solution.py:167
  21.8 3.5 %copy-start.7 = (bf16[1,128,1024]{2,1,0:T(8,128)(2,1)S(1)}, bf16[1,128,1024]{2,1,0:T(8,128)(2,1)}, u32[]{:S(2)}) copy-start(bf16[1,128,1024]{2,1,0:T(8,128)(2,1)} %param.10) | copy-start | bytes 786436
  21.8 10.3 %all-to-all-start.4 = ((bf16[128,4,256]{0,2,1:T(8,128)(2,1)}), bf16[128,4,256]{0,2,1:T(8,128)(2,1)S(1)}, u32[]{:S(2)}, u32[]{:S(2)}) async-start(bf16[128,4,256]{0,2,1:T(8,128)(2,1)} %bitcast.20), calls=%async_computation.4 | async-start | bytes 524288 | tf_op jit(solution)/shard_map/all_to_all | solution.py:156
  25.4 13.2 %copy-start.4 = (bf16[1,128,2048]{2,1,0:T(8,128)(2,1)S(1)}, bf16[1,128,2048]{2,1,0:T(8,128)(2,1)}, u32[]{:S(2)}) copy-start(bf16[1,128,2048]{2,1,0:T(8,128)(2,1)} %param.11) | copy-start | bytes 1572868
  32.1 10.2 %all-to-all-start.2 = ((bf16[128,4,256]{0,2,1:T(8,128)(2,1)}), bf16[128,4,256]{0,2,1:T(8,128)(2,1)S(1)}, u32[]{:S(2)}, u32[]{:S(2)}) async-start(bf16[128,4,256]{0,2,1:T(8,128)(2,1)} %bitcast.12), calls=%async_computation.2 | async-start | bytes 524288 | tf_op jit(solution)/shard_map/all_to_all | solution.py:157
  35.5 21.3 %collective-permute-start.1 = (bf16[2048,256]{1,0:T(8,128)(2,1)}, bf16[2048,256]{1,0:T(8,128)(2,1)S(1)}, u32[]{:S(2)}, u32[]{:S(2)}) collective-permute-start(bf16[2048,256]{1,0:T(8,128)(2,1)} %refs_0_.1), channel_id=1, source_target_pairs={{0,2},{1,3},{2,0},{3,1},{4,6},{5,7},{6,4},{7,5},{8,10},{9,11},{10,... | collective-permute-start | bytes 3145736 | tf_op jit(solution)/shard_map/ppermute | solution.py:80
  37.1 23.4 %collective-permute-start.3 = (bf16[2048,256]{1,0:T(8,128)(2,1)}, bf16[2048,256]{1,0:T(8,128)(2,1)S(1)}, u32[]{:S(2)}, u32[]{:S(2)}) collective-permute-start(bf16[2048,256]{1,0:T(8,128)(2,1)} %refs_0_.1), channel_id=1, source_target_pairs={{0,4},{1,5},{2,6},{3,7},{4,0},{5,1},{6,2},{7,3},{8,12},{9,13},{10,... | collective-permute-start | bytes 3145736 | tf_op jit(solution)/shard_map/ppermute | solution.py:80
  42.3 0.8 copy-start.2
  43.1 19.1 %all-to-all-start.3 = ((bf16[128,4,512]{0,2,1:T(8,128)(2,1)}), bf16[128,4,512]{0,2,1:T(8,128)(2,1)S(1)}, u32[]{:S(2)}, u32[]{:S(2)}) async-start(bf16[128,4,512]{0,2,1:T(8,128)(2,1)} %bitcast.16), calls=%async_computation.3 | async-start | bytes 1048576 | tf_op jit(solution)/shard_map/all_to_all | solution.py:160
  46.5 90.0 %collective-permute-start = (bf16[2048,256]{1,0:T(8,128)(2,1)}, bf16[2048,256]{1,0:T(8,128)(2,1)}, u32[]{:S(2)}, u32[]{:S(2)}) collective-permute-start(bf16[2048,256]{1,0:T(8,128)(2,1)} %refs_0_.1), channel_id=1, source_target_pairs={{0,1},{1,0},{2,3},{3,2},{4,5},{5,4},{6,7},{7,6},{8,9},{9,8},{10,11... | collective-permute-start | bytes 3145736 | tf_op jit(solution)/shard_map/ppermute | solution.py:80
  56.8 5.4 %copy-start = (bf16[2048,256]{1,0:T(8,128)(2,1)}, bf16[2048,256]{1,0:T(8,128)(2,1)S(1)}, u32[]{:S(2)}) copy-start(bf16[2048,256]{1,0:T(8,128)(2,1)S(1)} %collective-permute-done.1.refs_2_) | copy-start | bytes 3145732
  57.7 63.3 %collective-permute-start.5 = (bf16[1024,256]{1,0:T(8,128)(2,1)}, bf16[1024,256]{1,0:T(8,128)(2,1)}, u32[]{:S(2)}, u32[]{:S(2)}) collective-permute-start(bf16[1024,256]{1,0:T(8,128)(2,1)} %slice.14), channel_id=1, source_target_pairs={{0,4},{1,5},{2,6},{3,7},{4,0},{5,1},{6,2},{7,3},{8,12},{9,13},{10,... | collective-permute-start | bytes 1572872 | tf_op jit(solution)/shard_map/ppermute | solution.py:80
  60.4 1.8 %copy-start.1 = (bf16[2048,256]{1,0:T(8,128)(2,1)}, bf16[2048,256]{1,0:T(8,128)(2,1)S(1)}, u32[]{:S(2)}) copy-start(bf16[2048,256]{1,0:T(8,128)(2,1)S(1)} %collective-permute-done.3.refs_4_) | copy-start | bytes 3145732
  61.3 59.7 %collective-permute-start.6 = (bf16[1024,256]{1,0:T(8,128)(2,1)}, bf16[1024,256]{1,0:T(8,128)(2,1)}, u32[]{:S(2)}, u32[]{:S(2)}) collective-permute-start(bf16[1024,256]{1,0:T(8,128)(2,1)} %slice.15), channel_id=1, source_target_pairs={{0,2},{1,3},{2,0},{3,1},{4,6},{5,7},{6,4},{7,5},{8,10},{9,11},{10,... | collective-permute-start | bytes 1572872 | tf_op jit(solution)/shard_map/ppermute | solution.py:80
  61.7 74.8 %collective-permute-start.2 = (bf16[2048,256]{1,0:T(8,128)(2,1)S(1)}, bf16[2048,256]{1,0:T(8,128)(2,1)}, u32[]{:S(2)}, u32[]{:S(2)}) collective-permute-start(bf16[2048,256]{1,0:T(8,128)(2,1)S(1)} %collective-permute-done.1.refs_2_), channel_id=1, source_target_pairs={{0,1},{1,0},{2,3},{3,2},{4,5},{5,4},{6,7},{7,6},{8,9},{9,8},{10,11... | collective-permute-start | bytes 3145736 | tf_op jit(solution)/shard_map/ppermute | solution.py:80
  61.7 74.8 %collective-permute-start.4 = (bf16[2048,256]{1,0:T(8,128)(2,1)S(1)}, bf16[2048,256]{1,0:T(8,128)(2,1)}, u32[]{:S(2)}, u32[]{:S(2)}) collective-permute-start(bf16[2048,256]{1,0:T(8,128)(2,1)S(1)} %collective-permute-done.3.refs_4_), channel_id=1, source_target_pairs={{0,1},{1,0},{2,3},{3,2},{4,5},{5,4},{6,7},{7,6},{8,9},{9,8},{10,11... | collective-permute-start | bytes 3145736 | tf_op jit(solution)/shard_map/ppermute | solution.py:80
  62.2 0.6 copy-start.9
  70.2 3.5 %copy-start.5 = (bf16[4,128,512]{2,1,0:T(8,128)(2,1)S(1)}, bf16[4,128,512]{2,1,0:T(8,128)(2,1)}, u32[]{:S(2)}) copy-start(bf16[4,128,512]{2,1,0:T(8,128)(2,1)} %get-tuple-element.259) | copy-start | bytes 1572868 | tf_op jit(solution)/shard_map/while
  73.3 0.6 copy-start.8
  74.4 0.8 copy-start.6
  74.4 0.8 copy-start.10
  75.2 0.6 copy-start.9
  83.1 4.1 %copy-start.5 = (bf16[4,128,512]{2,1,0:T(8,128)(2,1)S(1)}, bf16[4,128,512]{2,1,0:T(8,128)(2,1)}, u32[]{:S(2)}) copy-start(bf16[4,128,512]{2,1,0:T(8,128)(2,1)} %get-tuple-element.259) | copy-start | bytes 1572868 | tf_op jit(solution)/shard_map/while
  86.9 0.6 copy-start.8
  88.0 0.8 copy-start.6
  88.0 0.8 copy-start.10
  88.8 0.6 copy-start.9
  96.7 4.1 %copy-start.5 = (bf16[4,128,512]{2,1,0:T(8,128)(2,1)S(1)}, bf16[4,128,512]{2,1,0:T(8,128)(2,1)}, u32[]{:S(2)}) copy-start(bf16[4,128,512]{2,1,0:T(8,128)(2,1)} %get-tuple-element.259) | copy-start | bytes 1572868 | tf_op jit(solution)/shard_map/while
  100.5 0.6 copy-start.8
  101.5 0.8 copy-start.6
  101.6 0.8 copy-start.10
  102.3 0.6 copy-start.9
  110.3 4.1 %copy-start.5 = (bf16[4,128,512]{2,1,0:T(8,128)(2,1)S(1)}, bf16[4,128,512]{2,1,0:T(8,128)(2,1)}, u32[]{:S(2)}) copy-start(bf16[4,128,512]{2,1,0:T(8,128)(2,1)} %get-tuple-element.259) | copy-start | bytes 1572868 | tf_op jit(solution)/shard_map/while
  114.1 0.6 copy-start.8
  115.1 0.8 copy-start.6
  115.1 0.8 copy-start.10
  115.9 19.7 %all-to-all-start.5 = ((bf16[4,128,512]{2,1,0:T(8,128)(2,1)}), bf16[4,128,512]{2,1,0:T(8,128)(2,1)S(1)}, u32[]{:S(2)}, u32[]{:S(2)}) async-start(bf16[4,128,512]{2,1,0:T(8,128)(2,1)} %get-tuple-element.62), calls=%async_computation.5 | async-start | bytes 1048576 | tf_op jit(solution)/shard_map/all_to_all | solution.py:178
  121.0 15.5 %collective-permute-start.7 = (bf16[1024,256]{1,0:T(8,128)(2,1)}, bf16[1024,256]{1,0:T(8,128)(2,1)S(1)}, u32[]{:S(2)}, u32[]{:S(2)}) collective-permute-start(bf16[1024,256]{1,0:T(8,128)(2,1)} %collective-permute-done.5.refs_6_), channel_id=1, source_target_pairs={{0,1},{1,0},{2,3},{3,2},{4,5},{5,4},{6,7},{7,6},{8,9},{9,8},{10,11... | collective-permute-start | bytes 1572872 | tf_op jit(solution)/shard_map/ppermute | solution.py:80
  121.0 15.5 %collective-permute-start.8 = (bf16[1024,256]{1,0:T(8,128)(2,1)}, bf16[1024,256]{1,0:T(8,128)(2,1)}, u32[]{:S(2)}, u32[]{:S(2)}) collective-permute-start(bf16[1024,256]{1,0:T(8,128)(2,1)} %collective-permute-done.6.refs_7_), channel_id=1, source_target_pairs={{0,1},{1,0},{2,3},{3,2},{4,5},{5,4},{6,7},{7,6},{8,9},{9,8},{10,11... | collective-permute-start | bytes 1572872 | tf_op jit(solution)/shard_map/ppermute | solution.py:80
  136.5 0.8 copy-start.3

commit v2 on v1

--- a/solution.py
+++ b/solution.py
@@ -102,11 +102,197 @@
     ]
 
 
-def project_kernel(plan, place_ref, hidden_ref, gate_ref, *refs):
-    pieces, out_ref = refs[:-1], refs[-1]
-    gated = (
-        hidden_ref[...].astype(jnp.float32) * jax.nn.sigmoid(gate_ref[...].astype(jnp.float32))
+LANES = 128
+
+
+def log_forget(gates):
+    return -jnp.log1p(jnp.exp(-gates))
+
+
+def running_sum(rows):
+    width = rows.shape[1]
+    upto = lax.broadcasted_iota(jnp.int32, (width, width), 0) <= lax.broadcasted_iota(
+        jnp.int32, (width, width), 1
+    )
+    return jnp.dot(
+        rows,
+        upto.astype(jnp.float32),
+        precision=lax.Precision.HIGHEST,
+        preferred_element_type=jnp.float32,
+    )
+
+
+def times_transpose(left, right):
+    return lax.dot_general(
+        left, right, (((1,), (1,)), ((), ())), preferred_element_type=jnp.float32
+    )
+
+
+def three_terms(value):
+    high = value.astype(jnp.bfloat16).astype(jnp.float32)
+    middle = (value - high).astype(jnp.bfloat16).astype(jnp.float32)
+    return [high, middle, value - high - middle]
+
+
+def to_lanes(columns, rows):
+    lane = lax.broadcasted_iota(jnp.int32, (rows, LANES), 1)
+    tile = jnp.zeros((rows, LANES), jnp.float32)
+    for place, column in enumerate(columns):
+        tile = jnp.where(lane == place, column, tile)
+    return tile
+
+
+def pack_kernel(key_ref, value_ref, input_ref, forget_ref, *payload_refs):
+    tokens = key_ref.shape[0]
+    key_width = key_ref.shape[1] // len(payload_refs)
+    value_width = value_ref.shape[1] // len(payload_refs)
+    gates = jnp.concatenate(
+        [input_ref[...].astype(jnp.float32), forget_ref[...].astype(jnp.float32)], axis=0
     ).astype(jnp.bfloat16)
+    for place, payload in enumerate(payload_refs):
+        payload[:tokens, :key_width] = key_ref[:, place * key_width : (place + 1) * key_width]
+        payload[:tokens, key_width:] = value_ref[
+            :, place * value_width : (place + 1) * value_width
+        ]
+        payload[tokens:, : gates.shape[1]] = gates
+        payload[tokens:, gates.shape[1] :] = jnp.zeros(
+            (gates.shape[0], payload.shape[1] - gates.shape[1]), jnp.bfloat16
+        )
+
+
+def local_kernel(heads, query_ref, key_ref, value_ref, input_ref, forget_ref, total_ref, note_ref):
+    tokens = query_ref.shape[0]
+    key_width = query_ref.shape[1] // heads
+    value_width = value_ref.shape[1] // heads
+    running = running_sum(log_forget(forget_ref[...].astype(jnp.float32)))
+    level = input_ref[...].astype(jnp.float32) - running
+    causal = lax.broadcasted_iota(jnp.int32, (tokens, tokens), 0) >= lax.broadcasted_iota(
+        jnp.int32, (tokens, tokens), 1
+    )
+    notes = []
+    for head in range(heads):
+        keys = slice(head * key_width, (head + 1) * key_width)
+        channels = slice(head * value_width, (head + 1) * value_width)
+        masked = jnp.where(causal, level[head : head + 1, :], -jnp.inf)
+        top = jnp.max(masked, axis=1, keepdims=True)
+        scores = times_transpose(query_ref[:, keys], key_ref[:, keys])
+        scores = scores * (key_width ** (-0.5)) * jnp.exp(masked - top)
+        notes += [jnp.sum(scores, axis=1, keepdims=True), top]
+        total_ref[:, channels] = jnp.dot(
+            scores.astype(jnp.bfloat16), value_ref[:, channels], preferred_element_type=jnp.float32
+        )
+    note_ref[...] = to_lanes(notes, tokens)
+
+
+def serve_kernel(
+    heads, first, count, leads_ref, earlier_ref, here_ref, query_ref, near_ref, far_ref,
+    own_ref, next_ref, later_ref,
+):
+    tokens = query_ref.shape[0]
+    key_width = query_ref.shape[1] // heads
+    value_width = (here_ref.shape[1] - count * key_width) // count
+    leads = leads_ref[0] != 0
+    gates0 = earlier_ref[tokens:, :tokens].astype(jnp.float32)
+    gates1 = here_ref[tokens:, :tokens].astype(jnp.float32)
+    running0 = running_sum(log_forget(gates0[heads:]))
+    running1 = running_sum(log_forget(gates1[heads:]))
+    end0, end1 = running0[:, tokens - 1 :], running1[:, tokens - 1 :]
+    shift = jnp.where(leads, end0, 0.0)
+    level0 = gates0[:heads] - running0
+    level1 = gates1[:heads] - running1 - shift
+    top0 = jnp.maximum(jnp.max(level0, axis=1, keepdims=True), 0.0)
+    top = jnp.max(level1, axis=1, keepdims=True)
+    top = jnp.where(leads, jnp.maximum(top, top0), top)
+    weight_own = jnp.exp(level0 - top0)
+    weight0 = jnp.where(leads, jnp.exp(level0 - top), 0.0)
+    weight1 = jnp.exp(level1 - top)
+    weight = jnp.concatenate([weight0, weight1], axis=1)
+    reach, reach_own = top + shift + end1, top0 + end0
+    key_scale = key_width ** (-0.5)
+    own_notes, next_notes, later_notes = [], [], []
+    for place in range(count):
+        head = first + place
+        pick = slice(head, head + 1)
+        columns = slice(head * key_width, (head + 1) * key_width)
+        keys = slice(place * key_width, (place + 1) * key_width)
+        start = count * key_width + place * value_width
+        channels = slice(start, start + value_width)
+        out = slice(place * value_width, (place + 1) * value_width)
+        key0, value0 = earlier_ref[:tokens, keys], earlier_ref[:tokens, channels]
+        key_both = jnp.concatenate([key0, here_ref[:tokens, keys]], axis=0)
+        value_both = jnp.concatenate([value0, here_ref[:tokens, channels]], axis=0)
+        rows = jnp.concatenate([near_ref[:, columns], far_ref[:, columns]], axis=0)
+        scores = times_transpose(rows, key_both) * key_scale * weight[pick]
+        sums = jnp.sum(scores, axis=1, keepdims=True)
+        given = jnp.dot(
+            scores.astype(jnp.bfloat16), value_both, preferred_element_type=jnp.float32
+        ).astype(jnp.bfloat16)
+        next_ref[:, out] = given[:tokens]
+        later_ref[:, out] = given[tokens:]
+        scores = times_transpose(query_ref[:, columns], key0) * key_scale * weight_own[pick]
+        own_ref[:, out] = jnp.dot(
+            scores.astype(jnp.bfloat16), value0, preferred_element_type=jnp.float32
+        ).astype(jnp.bfloat16)
+        tail = three_terms(end1[pick])
+        next_notes += three_terms(sums[:tokens]) + three_terms(reach[pick]) + tail
+        later_notes += three_terms(sums[tokens:]) + three_terms(reach[pick]) + tail
+        own_notes += (
+            three_terms(jnp.sum(scores, axis=1, keepdims=True))
+            + three_terms(reach_own[pick])
+            + tail
+        )
+    for ref, notes in ((own_ref, own_notes), (next_ref, next_notes), (later_ref, later_notes)):
+        ref[:, count * value_width :] = to_lanes(notes, tokens).astype(jnp.bfloat16)
+
+
+def finish_kernel(plan, heads, place_ref, total_ref, note_ref, gate_ref, *refs):
+    out_ref, pieces, messages = refs[-1], refs[-1 - len(plan) : -1], refs[: -1 - len(plan)]
+    chunks = len(messages) // 3
+    owns, nears, fars = messages[:chunks], messages[chunks : 2 * chunks], messages[2 * chunks :]
+    count = heads // chunks
+    value_width = total_ref.shape[1] // heads
+    block = place_ref[1]
+    from_own, from_near, from_far = block == 1, block >= 2, block >= 3
+    notes = note_ref[...]
+    gated = []
+    for head in range(heads):
+        chunk, place = divmod(head, count)
+        channels = slice(head * value_width, (head + 1) * value_width)
+        out = slice(place * value_width, (place + 1) * value_width)
+
+        def note(ref, entry):
+            tile = ref[:, count * value_width :].astype(jnp.float32)
+            at = (place * 3 + entry) * 3
+            return tile[:, at : at + 1] + tile[:, at + 1 : at + 2] + tile[:, at + 2 : at + 3]
+
+        own, near, far = owns[chunk], nears[chunk], fars[chunk]
+        top = notes[:, 2 * head + 1 : 2 * head + 2]
+        reach_own, reach_near = note(own, 1), note(near, 1)
+        reach_far = note(far, 1) + note(near, 2)
+        state = jnp.where(from_own, reach_own, jnp.where(from_near, reach_near, 0.0))
+        state = jnp.where(from_far, jnp.maximum(state, reach_far), state)
+        peak = jnp.maximum(top, state)
+        scale = jnp.exp(top - peak)
+        scale_own = jnp.where(from_own, jnp.exp(reach_own - peak), 0.0)
+        scale_near = jnp.where(from_near, jnp.exp(reach_near - peak), 0.0)
+        scale_far = jnp.where(from_far, jnp.exp(reach_far - peak), 0.0)
+        weight = (
+            scale * notes[:, 2 * head : 2 * head + 1]
+            + scale_own * note(own, 0)
+            + scale_near * note(near, 0)
+            + scale_far * note(far, 0)
+        )
+        inverse = 1.0 / jnp.maximum(jnp.abs(weight), 1.0)
+        cell = (
+            scale * total_ref[:, channels]
+            + scale_own * own[:, out].astype(jnp.float32)
+            + scale_near * near[:, out].astype(jnp.float32)
+            + scale_far * far[:, out].astype(jnp.float32)
+        ) * inverse
+        hidden = cell.astype(jnp.bfloat16).astype(jnp.float32)
+        gate = jax.nn.sigmoid(gate_ref[:, channels].astype(jnp.float32))
+        gated.append((hidden * gate).astype(jnp.bfloat16))
+    gated = jnp.concatenate(gated, axis=1)
     totals = {}
     for (mask, start), piece in zip(plan, pieces):
         part = jnp.dot(
@@ -115,23 +301,88 @@
         totals[mask] = totals[mask] + part if mask in totals else part
     width = pieces[0].shape[1]
     for mask, total in totals.items():
-        place = pl.multiple_of((place_ref[0] ^ mask) * width, width)
-        out_ref[:, pl.ds(place, width)] = total.astype(out_ref.dtype)
-
-
-def project(hidden, gate, pieces):
-    place = lax.axis_index("dp").astype(jnp.int32).reshape(1)
+        start = pl.multiple_of((place_ref[0] ^ mask) * width, width)
+        out_ref[:, pl.ds(start, width)] = total.astype(out_ref.dtype)
+
+
+MIB = 1 << 20
+CHUNKS = 2
+
+
+def kernel_call(kernel, name, scalars, operands, outs, flops, limit):
+    vmem = pl.BlockSpec(memory_space=pltpu.VMEM)
+    size = sum(x.size * x.dtype.itemsize for x in operands + outs)
+    return pl.pallas_call(
+        kernel,
+        out_shape=outs,
+        in_specs=[pl.BlockSpec(memory_space=pltpu.SMEM)] * len(scalars) + [vmem] * len(operands),
+        out_specs=[vmem] * len(outs),
+        compiler_params=pltpu.CompilerParams(vmem_limit_bytes=limit * MIB),
+        cost_estimate=pl.CostEstimate(flops=flops, bytes_accessed=size, transcendentals=0),
+        name=name,
+    )(*scalars, *operands)
+
+
+def block_body(queries, key_rows, values, out_gate, input_gate, forget_gate, out_weight):
+    query, key, value, gate = queries[0], key_rows[0], values[0], out_gate[0]
+    input_log, forget = input_gate[0], forget_gate[0]
+    tokens, heads = query.shape[0], input_log.shape[0]
+    key_width, value_width = query.shape[1] // heads, value.shape[1] // heads
+    count = heads // CHUNKS
+    position = lax.axis_index("sp").astype(jnp.int32)
+    shape = jax.ShapeDtypeStruct
+
+    payloads = kernel_call(
+        pack_kernel,
+        "pack",
+        [],
+        [key, value, input_log, forget],
+        [shape((tokens + 2 * heads, count * (key_width + value_width)), jnp.bfloat16)] * CHUNKS,
+        0,
+        8,
+    )
+    earlier = [lax.ppermute(payload, "sp", [(0, 1)]) for payload in payloads]
+    near = lax.ppermute(query, "sp", [(2, 1), (3, 2)])
+    far = lax.ppermute(query, "sp", [(3, 1)])
+    pieces = gather_weight(out_weight)
+    total, notes = kernel_call(
+        functools.partial(local_kernel, heads),
+        "local",
+        [],
+        [query, key, value, input_log, forget],
+        [shape(value.shape, jnp.float32), shape((tokens, LANES), jnp.float32)],
+        2 * heads * tokens * tokens * (key_width + value_width),
+        12,
+    )
+    leads = (position == 1).astype(jnp.int32).reshape(1)
+    message = shape((tokens, count * value_width + LANES), jnp.bfloat16)
+    owns, nears, fars = [], [], []
+    for chunk in range(CHUNKS):
+        own, given_next, given_later = kernel_call(
+            functools.partial(serve_kernel, heads, chunk * count, count),
+            "serve",
+            [leads],
+            [earlier[chunk], payloads[chunk], query, near, far],
+            [message] * 3,
+            2 * count * 5 * tokens * tokens * (key_width + value_width),
+            12,
+        )
+        owns.append(own)
+        nears.append(lax.ppermute(given_next, "sp", [(1, 2), (2, 3)]))
+        fars.append(lax.ppermute(given_later, "sp", [(1, 3)]))
+    place = jnp.stack([lax.axis_index("dp").astype(jnp.int32), position])
     plan = tuple((mask, start) for mask, start, _ in pieces)
-    arrays = [piece for _, _, piece in pieces]
-    columns = arrays[0].shape[1] * lax.axis_size("dp")
-    vmem = pl.BlockSpec(memory_space=pltpu.VMEM)
-    return pl.pallas_call(
-        functools.partial(project_kernel, plan),
-        out_shape=jax.ShapeDtypeStruct((hidden.shape[0], columns), jnp.bfloat16),
-        in_specs=[pl.BlockSpec(memory_space=pltpu.SMEM)] + [vmem] * (2 + len(arrays)),
-        out_specs=vmem,
-        name="project",
-    )(place, hidden, gate, *arrays)
+    columns = out_weight.shape[1] * lax.axis_size("dp")
+    (out,) = kernel_call(
+        functools.partial(finish_kernel, plan, heads),
+        "finish",
+        [place],
+        [total, notes, gate, *owns, *nears, *fars, *(piece for _, _, piece in pieces)],
+        [shape((tokens, columns), jnp.bfloat16)],
+        2 * tokens * value.shape[1] * columns,
+        24,
+    )
+    return out[None]
 
 
 def body(queries, key_rows, values, out_gate, input_gate, forget_gate, out_weight):
@@ -176,8 +427,6 @@
     )
     hidden = output.astype(jnp.bfloat16)
     token_rows = lax.all_to_all(hidden, "sp", split_axis=0, concat_axis=1, tiled=True)
-    if lax.axis_size("dp") == 8:
-        return project(token_rows, out_gate[0], gather_weight(out_weight))[None]
     gated_rows = (
         token_rows.astype(jnp.float32) * jax.nn.sigmoid(out_gate[0].astype(jnp.float32))
     ).astype(jnp.bfloat16)
@@ -190,8 +439,9 @@
 
 
 def solution(mesh):
+    blocks = mesh.shape["sp"] == 4 and mesh.shape["dp"] == 8
     return jax.shard_map(
-        body,
+        block_body if blocks else body,
         mesh=mesh,
         in_specs=(
             P("dp", "sp", None),

time: 144 us -> 66.6 us (0.46)
  the two profiles are of different devices: /device:TPU:0 before, /device:TPU:25 now
where the time goes in v2:
time: 66.6 us; the launch traced here: 66.1 us
  starting transfers between devices  24.1 us (36%)
  waiting for transfers between devices  19.8 us (30%)
  Pallas kernels  11.7 us (18%)
  local copies, waits for them, and re-layouts  10.2 us (15%)
    ppermute x9, starting transfers between devices, swap(): return lax.ppermute(piece, 'dp', pairs)  12.8 us
    pallas_call x5, Pallas kernels, kernel_call(): pl.pallas_call(kernel, out_shape=outs, in_specs=[pl.BlockSpec(memory_spac...  11.7 us
    unnamed x40, local copies, waits for them, and re-layouts  10.1 us
    ppermute x2, waiting for transfers between devices, block_body(): fars.append(lax.ppermute(given_later, 'sp', [(1, 3)]))  7.5 us
    ppermute x2, waiting for transfers between devices, block_body(): nears.append(lax.ppermute(given_next, 'sp', [(1, 2), (2, 3)]))  5.45 us
    ppermute x1, waiting for transfers between devices, block_body(): near = lax.ppermute(query, 'sp', [(2, 1), (3, 2)])  4.38 us
    ppermute x2, starting transfers between devices, block_body(): earlier = [lax.ppermute(payload, 'sp', [(0, 1)]) for payload in payloads]  2.86 us
    ppermute x2, starting transfers between devices, block_body(): fars.append(lax.ppermute(given_later, 'sp', [(1, 3)]))  2.58 us
  transfers between devices with their start and end apart: 17, of which 6 were waited for; matrix products, arithmetic and copies ran while one was open for 0% of the time, Pallas kernels for 8%

profile of v2, /device:TPU:25, one launch (start us, length us, event | category | flops | bytes accessed | tf_op | source)
XLA Modules:
  0.0 66.1 jit_solution(2429355437471344011)
XLA Ops:
  0.0 1.2 %collective-permute-start.9 = (bf16[2048,256]{1,0:T(8,128)(2,1)}, bf16[2048,256]{1,0:T(8,128)(2,1)S(1)}, u32[]{:S(2)}, u32[]{:S(2)}) collective-permute-start(bf16[2048,256]{1,0:T(8,128)(2,1)} %refs_6_.1), channel_id=1, source_target_pairs={{0,2},{1,3},{2,0},{3,1},{4,6},{5,7},{6,4},{7,5},{8,10},{9,11},{10,... | collective-permute-start | bytes 3145736 | tf_op jit(solution)/shard_map/ppermute | solution.py:80
  1.2 1.2 %collective-permute-start.11 = (bf16[2048,256]{1,0:T(8,128)(2,1)}, bf16[2048,256]{1,0:T(8,128)(2,1)S(1)}, u32[]{:S(2)}, u32[]{:S(2)}) collective-permute-start(bf16[2048,256]{1,0:T(8,128)(2,1)} %refs_6_.1), channel_id=1, source_target_pairs={{0,4},{1,5},{2,6},{3,7},{4,0},{5,1},{6,2},{7,3},{8,12},{9,13},{10,... | collective-permute-start | bytes 3145736 | tf_op jit(solution)/shard_map/ppermute | solution.py:80
  2.5 2.0 %collective-permute-start.2 = (bf16[128,1024]{1,0:T(8,128)(2,1)}, bf16[128,1024]{1,0:T(8,128)(2,1)S(1)}, u32[]{:S(2)}, u32[]{:S(2)}) collective-permute-start(bf16[128,1024]{1,0:T(8,128)(2,1)} %bitcast.10), channel_id=1, source_target_pairs={{24,8},{25,9},{26,10},{27,11},{28,12},{29,13},{30,14},{31,15}} | collective-permute-start | bytes 786440 | tf_op jit(solution)/shard_map/ppermute | solution.py:346
  4.4 0.0 copy-start.19
  4.4 0.0 copy-start.18
  4.4 0.7 copy-done.19
  5.1 0.0 copy-done.18
  5.1 1.0 %copy-done.1 = bf16[1,128,2048]{2,1,0:T(8,128)(2,1)S(1)} copy-done((bf16[1,128,2048]{2,1,0:T(8,128)(2,1)S(1)}, bf16[1,128,2048]{2,1,0:T(8,128)(2,1)}, u32[]{:S(2)}) %copy-start.1) | copy-done | bytes 524312
  6.2 0.9 %copy-done.3 = bf16[1,128,1024]{2,1,0:T(8,128)(2,1)S(1)} copy-done((bf16[1,128,1024]{2,1,0:T(8,128)(2,1)S(1)}, bf16[1,128,1024]{2,1,0:T(8,128)(2,1)}, u32[]{:S(2)}) %copy-start.3) | copy-done | bytes 262168
  7.1 0.8 %pack.1 = (bf16[136,1536]{1,0:T(8,128)(2,1)}, bf16[136,1536]{1,0:T(8,128)(2,1)S(1)}) custom-call(bf16[128,1024]{1,0:T(8,128)(2,1)S(1)} %bitcast.17, bf16[128,2048]{1,0:T(8,128)(2,1)S(1)} %bitcast.15, bf16[4,128]{1,0:T(4,128)(2,1)S(1)} %bitcast.20, bf16[4,128]{1,0:T(4,128)(2,1)S(1)} %bitcast.22), custom_call_target="tpu_custom_call" | custom-call | bytes 1624064 | tf_op jit(solution)/shard_map/pack/pallas_call | solution.py:315
  7.9 1.4 %collective-permute-start = (bf16[136,1536]{1,0:T(8,128)(2,1)}, bf16[136,1536]{1,0:T(8,128)(2,1)}, u32[]{:S(2)}, u32[]{:S(2)}) collective-permute-start(bf16[136,1536]{1,0:T(8,128)(2,1)} %get-tuple-element.17.here_ref), channel_id=1, source_target_pairs={{0,8},{1,9},{2,10},{3,11},{4,12},{5,13},{6,14},{7,15}} | collective-permute-start | bytes 1253384 | tf_op jit(solution)/shard_map/ppermute | solution.py:344
  9.3 1.4 %collective-permute-start.3 = (bf16[136,1536]{1,0:T(8,128)(2,1)S(1)}, bf16[136,1536]{1,0:T(8,128)(2,1)}, u32[]{:S(2)}, u32[]{:S(2)}) collective-permute-start(bf16[136,1536]{1,0:T(8,128)(2,1)S(1)} %get-tuple-element.19.here_ref), channel_id=1, source_target_pairs={{0,8},{1,9},{2,10},{3,11},{4,12},{5,13},{6,14},{7,15}} | collective-permute-start | bytes 1253384 | tf_op jit(solution)/shard_map/ppermute | solution.py:344
  10.8 0.0 collective-permute-done.2.far_ref
  10.8 0.0 copy-done
  10.8 1.3 %collective-permute-start.1 = (bf16[128,1024]{1,0:T(8,128)(2,1)S(1)}, bf16[128,1024]{1,0:T(8,128)(2,1)S(1)}, u32[]{:S(2)}, u32[]{:S(2)}) collective-permute-start(bf16[128,1024]{1,0:T(8,128)(2,1)S(1)} %bitcast.11), channel_id=1, source_target_pairs={{16,8},{24,16},{17,9},{25,17},{18,10},{26,18},{19,11},{27,19},{20,... | collective-permute-start | bytes 786440 | tf_op jit(solution)/shard_map/ppermute | solution.py:345
  12.1 4.4 %collective-permute-done.1.near_ref = bf16[128,1024]{1,0:T(8,128)(2,1)S(1)} collective-permute-done((bf16[128,1024]{1,0:T(8,128)(2,1)S(1)}, bf16[128,1024]{1,0:T(8,128)(2,1)S(1)}, u32[]{:S(2)}, u32[]{:S(2)}) %collective-permute-start.1) | collective-permute-done | bytes 262176 | tf_op jit(solution)/shard_map/ppermute | solution.py:345
  16.5 0.0 collective-permute-done.earlier_ref
  16.5 2.0 %serve.2 = (bf16[128,1152]{1,0:T(8,128)(2,1)S(1)}, bf16[128,1152]{1,0:T(8,128)(2,1)S(1)}, bf16[128,1152]{1,0:T(8,128)(2,1)S(1)}) custom-call(s32[1]{0:T(128)} %bitcast.8.leads_ref, bf16[136,1536]{1,0:T(8,128)(2,1)} %collective-permute-done.earlier_ref, bf16[136,1536]{1,0:T(8,128)(2,1)} %get-tuple-element.17.here_ref, bf16[128,1024]{1,0:T(8,128)(2,1)S(1)} %bitcast.12, ...), custom_call_target="tpu_custom_call" | custom-call | flops 251658240 | bytes 2506752 | tf_op jit(solution)/shard_map/serve/pallas_call | solution.py:315
  18.5 0.0 copy-start.6
  18.5 0.7 %copy-done.6 = bf16[128,1152]{1,0:T(8,128)(2,1)} copy-done((bf16[128,1152]{1,0:T(8,128)(2,1)}, bf16[128,1152]{1,0:T(8,128)(2,1)S(1)}, u32[]{:S(2)}) %copy-start.6) | copy-done | bytes 294936
  19.2 1.3 %collective-permute-start.4 = (bf16[128,1152]{1,0:T(8,128)(2,1)S(1)}, bf16[128,1152]{1,0:T(8,128)(2,1)S(1)}, u32[]{:S(2)}, u32[]{:S(2)}) collective-permute-start(bf16[128,1152]{1,0:T(8,128)(2,1)S(1)} %get-tuple-element.21), channel_id=1, source_target_pairs={{8,16},{16,24},{9,17},{17,25},{10,18},{18,26},{11,19},{19,27},{12,... | collective-permute-start | bytes 884744 | tf_op jit(solution)/shard_map/ppermute | solution.py:371
  20.5 1.3 %collective-permute-start.6 = (bf16[128,1152]{1,0:T(8,128)(2,1)S(1)}, bf16[128,1152]{1,0:T(8,128)(2,1)S(1)}, u32[]{:S(2)}, u32[]{:S(2)}) collective-permute-start(bf16[128,1152]{1,0:T(8,128)(2,1)S(1)} %get-tuple-element.23), channel_id=1, source_target_pairs={{8,24},{9,25},{10,26},{11,27},{12,28},{13,29},{14,30},{15,31}} | collective-permute-start | bytes 884744 | tf_op jit(solution)/shard_map/ppermute | solution.py:372
  21.8 0.0 collective-permute-done.3.earlier_ref
  21.8 1.9 %serve.3 = (bf16[128,1152]{1,0:T(8,128)(2,1)S(1)}, bf16[128,1152]{1,0:T(8,128)(2,1)S(1)}, bf16[128,1152]{1,0:T(8,128)(2,1)S(1)}) custom-call(s32[1]{0:T(128)} %bitcast.8.leads_ref, bf16[136,1536]{1,0:T(8,128)(2,1)} %collective-permute-done.3.earlier_ref, bf16[136,1536]{1,0:T(8,128)(2,1)S(1)} %get-tuple-element.19.here_ref, bf16[128,1024]{1,0:T(8,128)(2,1)S(1)} %bitcast.13, ...), custom_call_target="tpu_custom_call" | custom-call | flops 251658240 | bytes 2506752 | tf_op jit(solution)/shard_map/serve/pallas_call | solution.py:315
  23.7 0.0 copy-start.12
  23.7 1.3 %collective-permute-start.5 = (bf16[128,1152]{1,0:T(8,128)(2,1)S(1)}, bf16[128,1152]{1,0:T(8,128)(2,1)S(1)}, u32[]{:S(2)}, u32[]{:S(2)}) collective-permute-start(bf16[128,1152]{1,0:T(8,128)(2,1)S(1)} %get-tuple-element.22), channel_id=1, source_target_pairs={{8,16},{16,24},{9,17},{17,25},{10,18},{18,26},{11,19},{19,27},{12,... | collective-permute-start | bytes 884744 | tf_op jit(solution)/shard_map/ppermute | solution.py:371
  25.0 0.0 collective-permute-done.9.refs_8_
  25.1 1.3 %collective-permute-start.7 = (bf16[128,1152]{1,0:T(8,128)(2,1)S(1)}, bf16[128,1152]{1,0:T(8,128)(2,1)S(1)}, u32[]{:S(2)}, u32[]{:S(2)}) collective-permute-start(bf16[128,1152]{1,0:T(8,128)(2,1)S(1)} %get-tuple-element.24), channel_id=1, source_target_pairs={{8,24},{9,25},{10,26},{11,27},{12,28},{13,29},{14,30},{15,31}} | collective-permute-start | bytes 884744 | tf_op jit(solution)/shard_map/ppermute | solution.py:372
  26.4 0.0 copy-done.12
  26.4 0.0 copy-start.2
  26.4 0.0 copy-start.4
  26.4 0.0 collective-permute-done.11.refs_10_
  26.4 2.2 %collective-permute-start.8 = (bf16[2048,256]{1,0:T(8,128)(2,1)}, bf16[2048,256]{1,0:T(8,128)(2,1)}, u32[]{:S(2)}, u32[]{:S(2)}) collective-permute-start(bf16[2048,256]{1,0:T(8,128)(2,1)} %refs_6_.1), channel_id=1, source_target_pairs={{0,1},{1,0},{2,3},{3,2},{4,5},{5,4},{6,7},{7,6},{8,9},{9,8},{10,11... | collective-permute-start | bytes 3145736 | tf_op jit(solution)/shard_map/ppermute | solution.py:80
  28.6 0.0 collective-permute-done.4.refs_2_
  28.7 0.0 copy-start.8
  28.7 0.7 %copy-done.8 = bf16[128,1152]{1,0:T(8,128)(2,1)} copy-done((bf16[128,1152]{1,0:T(8,128)(2,1)}, bf16[128,1152]{1,0:T(8,128)(2,1)S(1)}, u32[]{:S(2)}) %copy-start.8) | copy-done | bytes 294936
  29.4 0.2 collective-permute-start.13
  29.6 5.9 %collective-permute-done.6.refs_4_ = bf16[128,1152]{1,0:T(8,128)(2,1)S(1)} collective-permute-done((bf16[128,1152]{1,0:T(8,128)(2,1)S(1)}, bf16[128,1152]{1,0:T(8,128)(2,1)S(1)}, u32[]{:S(2)}, u32[]{:S(2)}) %collective-permute-start.6) | collective-permute-done | bytes 294944 | tf_op jit(solution)/shard_map/ppermute | solution.py:372
  35.4 0.7 %copy-done.10 = bf16[128,1152]{1,0:T(8,128)(2,1)} copy-done((bf16[128,1152]{1,0:T(8,128)(2,1)}, bf16[128,1152]{1,0:T(8,128)(2,1)S(1)}, u32[]{:S(2)}) %copy-start.10) | copy-done | bytes 294936
  36.2 0.3 collective-permute-start.14
  36.4 5.4 %collective-permute-done.5.refs_3_ = bf16[128,1152]{1,0:T(8,128)(2,1)S(1)} collective-permute-done((bf16[128,1152]{1,0:T(8,128)(2,1)S(1)}, bf16[128,1152]{1,0:T(8,128)(2,1)S(1)}, u32[]{:S(2)}, u32[]{:S(2)}) %collective-permute-start.5) | collective-permute-done | bytes 294944 | tf_op jit(solution)/shard_map/ppermute | solution.py:371
  41.9 0.7 %copy-done.14 = bf16[128,1152]{1,0:T(8,128)(2,1)} copy-done((bf16[128,1152]{1,0:T(8,128)(2,1)}, bf16[128,1152]{1,0:T(8,128)(2,1)S(1)}, u32[]{:S(2)}) %copy-start.14) | copy-done | bytes 294936
  42.6 3.8 %collective-permute-start.10 = (bf16[2048,256]{1,0:T(8,128)(2,1)S(1)}, bf16[2048,256]{1,0:T(8,128)(2,1)}, u32[]{:S(2)}, u32[]{:S(2)}) collective-permute-start(bf16[2048,256]{1,0:T(8,128)(2,1)S(1)} %collective-permute-done.9.refs_8_), channel_id=1, source_target_pairs={{0,1},{1,0},{2,3},{3,2},{4,5},{5,4},{6,7},{7,6},{8,9},{9,8},{10,11... | collective-permute-start | bytes 3145736 | tf_op jit(solution)/shard_map/ppermute | solution.py:80
  46.4 1.6 %collective-permute-done.7.refs_5_ = bf16[128,1152]{1,0:T(8,128)(2,1)S(1)} collective-permute-done((bf16[128,1152]{1,0:T(8,128)(2,1)S(1)}, bf16[128,1152]{1,0:T(8,128)(2,1)S(1)}, u32[]{:S(2)}, u32[]{:S(2)}) %collective-permute-start.7) | collective-permute-done | bytes 294944 | tf_op jit(solution)/shard_map/ppermute | solution.py:372
  48.1 0.7 %copy-done.16 = bf16[128,1152]{1,0:T(8,128)(2,1)} copy-done((bf16[128,1152]{1,0:T(8,128)(2,1)}, bf16[128,1152]{1,0:T(8,128)(2,1)S(1)}, u32[]{:S(2)}) %copy-start.16) | copy-done | bytes 294936
  48.8 3.3 %collective-permute-start.12 = (bf16[2048,256]{1,0:T(8,128)(2,1)S(1)}, bf16[2048,256]{1,0:T(8,128)(2,1)}, u32[]{:S(2)}, u32[]{:S(2)}) collective-permute-start(bf16[2048,256]{1,0:T(8,128)(2,1)S(1)} %collective-permute-done.11.refs_10_), channel_id=1, source_target_pairs={{0,1},{1,0},{2,3},{3,2},{4,5},{5,4},{6,7},{7,6},{8,9},{9,8},{10,11... | collective-permute-start | bytes 3145736 | tf_op jit(solution)/shard_map/ppermute | solution.py:80
  52.2 0.0 collective-permute-done.13.refs_12_
  52.2 0.0 collective-permute-start.15
  52.2 0.0 collective-permute-done.14.refs_13_
  52.2 0.5 collective-permute-start.16
  52.7 0.0 copy-done.2
  52.7 0.9 %local.1 = (f32[128,2048]{1,0:T(8,128)S(1)}, f32[128,128]{1,0:T(8,128)S(1)}) custom-call(bf16[128,1024]{1,0:T(8,128)(2,1)S(1)} %bitcast.14, bf16[128,1024]{1,0:T(8,128)(2,1)S(1)} %bitcast.18, bf16[128,2048]{1,0:T(8,128)(2,1)S(1)} %bitcast.16, bf16[4,128]{1,0:T(4,128)(2,1)S(1)} %bitcast.21, bf16[4,128]{1,0:T(4,128)(2,1)S(1)} %bitcast.23), custom_call_target="tpu_custom_call" | custom-call | flops 100663296 | bytes 2164736 | tf_op jit(solution)/shard_map/local/pallas_call | solution.py:315
  53.6 0.1 pad_add_fusion.place_ref
  53.6 0.0 collective-permute-done.8.refs_7_
  53.6 1.7 %collective-permute-done.15.refs_14_ = bf16[1024,256]{1,0:T(8,128)(2,1)} collective-permute-done((bf16[1024,256]{1,0:T(8,128)(2,1)}, bf16[1024,256]{1,0:T(8,128)(2,1)}, u32[]{:S(2)}, u32[]{:S(2)}) %collective-permute-start.15) | collective-permute-done | bytes 524320 | tf_op jit(solution)/shard_map/ppermute | solution.py:80
  55.3 0.0 collective-permute-done.10.refs_9_
  55.3 0.7 %collective-permute-done.16.refs_15_ = bf16[1024,256]{1,0:T(8,128)(2,1)} collective-permute-done((bf16[1024,256]{1,0:T(8,128)(2,1)}, bf16[1024,256]{1,0:T(8,128)(2,1)}, u32[]{:S(2)}, u32[]{:S(2)}) %collective-permute-start.16) | collective-permute-done | bytes 524320 | tf_op jit(solution)/shard_map/ppermute | solution.py:80
  56.1 0.0 collective-permute-done.12.refs_11_
  56.1 0.0 copy-done.13
  56.1 1.0 %copy-done.9 = bf16[128,1152]{1,0:T(8,128)(2,1)S(1)} copy-done((bf16[128,1152]{1,0:T(8,128)(2,1)S(1)}, bf16[128,1152]{1,0:T(8,128)(2,1)}, u32[]{:S(2)}) %copy-start.9) | copy-done | bytes 294936
  57.1 1.0 %copy-done.11 = bf16[128,1152]{1,0:T(8,128)(2,1)S(1)} copy-done((bf16[128,1152]{1,0:T(8,128)(2,1)S(1)}, bf16[128,1152]{1,0:T(8,128)(2,1)}, u32[]{:S(2)}) %copy-start.11) | copy-done | bytes 294936
  58.0 1.0 %copy-done.15 = bf16[128,1152]{1,0:T(8,128)(2,1)S(1)} copy-done((bf16[128,1152]{1,0:T(8,128)(2,1)S(1)}, bf16[128,1152]{1,0:T(8,128)(2,1)}, u32[]{:S(2)}) %copy-start.15) | copy-done | bytes 294936
  59.0 1.0 %copy-done.17 = bf16[128,1152]{1,0:T(8,128)(2,1)S(1)} copy-done((bf16[128,1152]{1,0:T(8,128)(2,1)S(1)}, bf16[128,1152]{1,0:T(8,128)(2,1)}, u32[]{:S(2)}) %copy-start.17) | copy-done | bytes 294936
  59.9 6.1 %finish.1 = bf16[128,2048]{1,0:T(8,128)(2,1)} custom-call(s32[2]{0:T(128)S(1)} %pad_add_fusion.place_ref, f32[128,2048]{1,0:T(8,128)S(1)} %get-tuple-element.15.total_ref, f32[128,128]{1,0:T(8,128)S(1)} %get-tuple-element.16.note_ref, bf16[128,2048]{1,0:T(8,128)(2,1)S(1)} %bitcast.19, bf16[128,1152]{1,0:T(8,128)(2,1)S(1)} %copy-done.7, ...), custom_call_target="tpu_custom_call" | custom-call | flops 1073741824 | bytes 12320768 | tf_op jit(solution)/shard_map/finish/pallas_call | solution.py:315
  (18 shorter events, 0.1 us)
Async XLA Ops:
  0.0 25.0 %collective-permute-start.9 = (bf16[2048,256]{1,0:T(8,128)(2,1)}, bf16[2048,256]{1,0:T(8,128)(2,1)S(1)}, u32[]{:S(2)}, u32[]{:S(2)}) collective-permute-start(bf16[2048,256]{1,0:T(8,128)(2,1)} %refs_6_.1), channel_id=1, source_target_pairs={{0,2},{1,3},{2,0},{3,1},{4,6},{5,7},{6,4},{7,5},{8,10},{9,11},{10,... | collective-permute-start | bytes 3145736 | tf_op jit(solution)/shard_map/ppermute | solution.py:80
  1.2 25.2 %collective-permute-start.11 = (bf16[2048,256]{1,0:T(8,128)(2,1)}, bf16[2048,256]{1,0:T(8,128)(2,1)S(1)}, u32[]{:S(2)}, u32[]{:S(2)}) collective-permute-start(bf16[2048,256]{1,0:T(8,128)(2,1)} %refs_6_.1), channel_id=1, source_target_pairs={{0,4},{1,5},{2,6},{3,7},{4,0},{5,1},{6,2},{7,3},{8,12},{9,13},{10,... | collective-permute-start | bytes 3145736 | tf_op jit(solution)/shard_map/ppermute | solution.py:80
  2.5 8.3 %collective-permute-start.2 = (bf16[128,1024]{1,0:T(8,128)(2,1)}, bf16[128,1024]{1,0:T(8,128)(2,1)S(1)}, u32[]{:S(2)}, u32[]{:S(2)}) collective-permute-start(bf16[128,1024]{1,0:T(8,128)(2,1)} %bitcast.10), channel_id=1, source_target_pairs={{24,8},{25,9},{26,10},{27,11},{28,12},{29,13},{30,14},{31,15}} | collective-permute-start | bytes 786440 | tf_op jit(solution)/shard_map/ppermute | solution.py:346
  4.4 0.7 %copy-start.19 = (bf16[1,4,128]{2,1,0:T(4,128)(2,1)S(1)}, bf16[1,4,128]{2,1,0:T(4,128)(2,1)}, u32[]{:S(2)}) copy-start(bf16[1,4,128]{2,1,0:T(4,128)(2,1)} %param.12) | copy-start | bytes 3076
  4.4 0.7 %copy-start.18 = (bf16[1,4,128]{2,1,0:T(4,128)(2,1)S(1)}, bf16[1,4,128]{2,1,0:T(4,128)(2,1)}, u32[]{:S(2)}) copy-start(bf16[1,4,128]{2,1,0:T(4,128)(2,1)} %param.11) | copy-start | bytes 3076
  5.1 1.0 %copy-start.1 = (bf16[1,128,2048]{2,1,0:T(8,128)(2,1)S(1)}, bf16[1,128,2048]{2,1,0:T(8,128)(2,1)}, u32[]{:S(2)}) copy-start(bf16[1,128,2048]{2,1,0:T(8,128)(2,1)} %param.9) | copy-start | bytes 1572868
  6.2 0.9 %copy-start.3 = (bf16[1,128,1024]{2,1,0:T(8,128)(2,1)S(1)}, bf16[1,128,1024]{2,1,0:T(8,128)(2,1)}, u32[]{:S(2)}) copy-start(bf16[1,128,1024]{2,1,0:T(8,128)(2,1)} %param.8) | copy-start | bytes 786436
  7.1 3.7 %copy-start = (bf16[1,128,1024]{2,1,0:T(8,128)(2,1)S(1)}, bf16[1,128,1024]{2,1,0:T(8,128)(2,1)}, u32[]{:S(2)}) copy-start(bf16[1,128,1024]{2,1,0:T(8,128)(2,1)} %param.7) | copy-start | bytes 786436
  7.9 8.6 %collective-permute-start = (bf16[136,1536]{1,0:T(8,128)(2,1)}, bf16[136,1536]{1,0:T(8,128)(2,1)}, u32[]{:S(2)}, u32[]{:S(2)}) collective-permute-start(bf16[136,1536]{1,0:T(8,128)(2,1)} %get-tuple-element.17.here_ref), channel_id=1, source_target_pairs={{0,8},{1,9},{2,10},{3,11},{4,12},{5,13},{6,14},{7,15}} | collective-permute-start | bytes 1253384 | tf_op jit(solution)/shard_map/ppermute | solution.py:344
  9.3 12.5 %collective-permute-start.3 = (bf16[136,1536]{1,0:T(8,128)(2,1)S(1)}, bf16[136,1536]{1,0:T(8,128)(2,1)}, u32[]{:S(2)}, u32[]{:S(2)}) collective-permute-start(bf16[136,1536]{1,0:T(8,128)(2,1)S(1)} %get-tuple-element.19.here_ref), channel_id=1, source_target_pairs={{0,8},{1,9},{2,10},{3,11},{4,12},{5,13},{6,14},{7,15}} | collective-permute-start | bytes 1253384 | tf_op jit(solution)/shard_map/ppermute | solution.py:344
  10.8 5.7 %collective-permute-start.1 = (bf16[128,1024]{1,0:T(8,128)(2,1)S(1)}, bf16[128,1024]{1,0:T(8,128)(2,1)S(1)}, u32[]{:S(2)}, u32[]{:S(2)}) collective-permute-start(bf16[128,1024]{1,0:T(8,128)(2,1)S(1)} %bitcast.11), channel_id=1, source_target_pairs={{16,8},{24,16},{17,9},{25,17},{18,10},{26,18},{19,11},{27,19},{20,... | collective-permute-start | bytes 786440 | tf_op jit(solution)/shard_map/ppermute | solution.py:345
  18.5 0.7 %copy-start.6 = (bf16[128,1152]{1,0:T(8,128)(2,1)}, bf16[128,1152]{1,0:T(8,128)(2,1)S(1)}, u32[]{:S(2)}) copy-start(bf16[128,1152]{1,0:T(8,128)(2,1)S(1)} %get-tuple-element.18.refs_0_) | copy-start | bytes 884740
  19.2 9.4 %collective-permute-start.4 = (bf16[128,1152]{1,0:T(8,128)(2,1)S(1)}, bf16[128,1152]{1,0:T(8,128)(2,1)S(1)}, u32[]{:S(2)}, u32[]{:S(2)}) collective-permute-start(bf16[128,1152]{1,0:T(8,128)(2,1)S(1)} %get-tuple-element.21), channel_id=1, source_target_pairs={{8,16},{16,24},{9,17},{17,25},{10,18},{18,26},{11,19},{19,27},{12,... | collective-permute-start | bytes 884744 | tf_op jit(solution)/shard_map/ppermute | solution.py:371
  20.5 14.9 %collective-permute-start.6 = (bf16[128,1152]{1,0:T(8,128)(2,1)S(1)}, bf16[128,1152]{1,0:T(8,128)(2,1)S(1)}, u32[]{:S(2)}, u32[]{:S(2)}) collective-permute-start(bf16[128,1152]{1,0:T(8,128)(2,1)S(1)} %get-tuple-element.23), channel_id=1, source_target_pairs={{8,24},{9,25},{10,26},{11,27},{12,28},{13,29},{14,30},{15,31}} | collective-permute-start | bytes 884744 | tf_op jit(solution)/shard_map/ppermute | solution.py:372
  23.7 2.7 %copy-start.12 = (bf16[128,1152]{1,0:T(8,128)(2,1)}, bf16[128,1152]{1,0:T(8,128)(2,1)S(1)}, u32[]{:S(2)}) copy-start(bf16[128,1152]{1,0:T(8,128)(2,1)S(1)} %get-tuple-element.20.refs_1_) | copy-start | bytes 884740
  23.7 18.1 %collective-permute-start.5 = (bf16[128,1152]{1,0:T(8,128)(2,1)S(1)}, bf16[128,1152]{1,0:T(8,128)(2,1)S(1)}, u32[]{:S(2)}, u32[]{:S(2)}) collective-permute-start(bf16[128,1152]{1,0:T(8,128)(2,1)S(1)} %get-tuple-element.22), channel_id=1, source_target_pairs={{8,16},{16,24},{9,17},{17,25},{10,18},{18,26},{11,19},{19,27},{12,... | collective-permute-start | bytes 884744 | tf_op jit(solution)/shard_map/ppermute | solution.py:371
  25.1 23.0 %collective-permute-start.7 = (bf16[128,1152]{1,0:T(8,128)(2,1)S(1)}, bf16[128,1152]{1,0:T(8,128)(2,1)S(1)}, u32[]{:S(2)}, u32[]{:S(2)}) collective-permute-start(bf16[128,1152]{1,0:T(8,128)(2,1)S(1)} %get-tuple-element.24), channel_id=1, source_target_pairs={{8,24},{9,25},{10,26},{11,27},{12,28},{13,29},{14,30},{15,31}} | collective-permute-start | bytes 884744 | tf_op jit(solution)/shard_map/ppermute | solution.py:372
  26.4 26.3 %copy-start.2 = (bf16[1,128,2048]{2,1,0:T(8,128)(2,1)S(1)}, bf16[1,128,2048]{2,1,0:T(8,128)(2,1)}, u32[]{:S(2)}) copy-start(bf16[1,128,2048]{2,1,0:T(8,128)(2,1)} %param.9) | copy-start | bytes 1572868
  26.4 26.3 %copy-start.4 = (bf16[1,128,1024]{2,1,0:T(8,128)(2,1)S(1)}, bf16[1,128,1024]{2,1,0:T(8,128)(2,1)}, u32[]{:S(2)}) copy-start(bf16[1,128,1024]{2,1,0:T(8,128)(2,1)} %param.8) | copy-start | bytes 786436
  26.4 27.2 %collective-permute-start.8 = (bf16[2048,256]{1,0:T(8,128)(2,1)}, bf16[2048,256]{1,0:T(8,128)(2,1)}, u32[]{:S(2)}, u32[]{:S(2)}) collective-permute-start(bf16[2048,256]{1,0:T(8,128)(2,1)} %refs_6_.1), channel_id=1, source_target_pairs={{0,1},{1,0},{2,3},{3,2},{4,5},{5,4},{6,7},{7,6},{8,9},{9,8},{10,11... | collective-permute-start | bytes 3145736 | tf_op jit(solution)/shard_map/ppermute | solution.py:80
  28.6 27.5 %copy-start.13 = (bf16[128,1152]{1,0:T(8,128)(2,1)S(1)}, bf16[128,1152]{1,0:T(8,128)(2,1)}, u32[]{:S(2)}) copy-start(bf16[128,1152]{1,0:T(8,128)(2,1)} %copy-done.12) | copy-start | bytes 884740
  28.7 0.7 %copy-start.8 = (bf16[128,1152]{1,0:T(8,128)(2,1)}, bf16[128,1152]{1,0:T(8,128)(2,1)S(1)}, u32[]{:S(2)}) copy-start(bf16[128,1152]{1,0:T(8,128)(2,1)S(1)} %collective-permute-done.4.refs_2_) | copy-start | bytes 884740
  29.4 22.8 %collective-permute-start.13 = (bf16[1024,256]{1,0:T(8,128)(2,1)S(1)}, bf16[1024,256]{1,0:T(8,128)(2,1)}, u32[]{:S(2)}, u32[]{:S(2)}) collective-permute-start(bf16[1024,256]{1,0:T(8,128)(2,1)S(1)} %slice.8), channel_id=1, source_target_pairs={{0,4},{1,5},{2,6},{3,7},{4,0},{5,1},{6,2},{7,3},{8,12},{9,13},{10,... | collective-permute-start | bytes 1572872 | tf_op jit(solution)/shard_map/ppermute | solution.py:80
  35.4 0.7 %copy-start.10 = (bf16[128,1152]{1,0:T(8,128)(2,1)}, bf16[128,1152]{1,0:T(8,128)(2,1)S(1)}, u32[]{:S(2)}) copy-start(bf16[128,1152]{1,0:T(8,128)(2,1)S(1)} %collective-permute-done.6.refs_4_) | copy-start | bytes 884740
  36.2 16.0 %collective-permute-start.14 = (bf16[1024,256]{1,0:T(8,128)(2,1)S(1)}, bf16[1024,256]{1,0:T(8,128)(2,1)}, u32[]{:S(2)}, u32[]{:S(2)}) collective-permute-start(bf16[1024,256]{1,0:T(8,128)(2,1)S(1)} %slice.9), channel_id=1, source_target_pairs={{0,2},{1,3},{2,0},{3,1},{4,6},{5,7},{6,4},{7,5},{8,10},{9,11},{10,... | collective-permute-start | bytes 1572872 | tf_op jit(solution)/shard_map/ppermute | solution.py:80
  41.9 0.7 %copy-start.14 = (bf16[128,1152]{1,0:T(8,128)(2,1)}, bf16[128,1152]{1,0:T(8,128)(2,1)S(1)}, u32[]{:S(2)}) copy-start(bf16[128,1152]{1,0:T(8,128)(2,1)S(1)} %collective-permute-done.5.refs_3_) | copy-start | bytes 884740
  42.6 12.7 %collective-permute-start.10 = (bf16[2048,256]{1,0:T(8,128)(2,1)S(1)}, bf16[2048,256]{1,0:T(8,128)(2,1)}, u32[]{:S(2)}, u32[]{:S(2)}) collective-permute-start(bf16[2048,256]{1,0:T(8,128)(2,1)S(1)} %collective-permute-done.9.refs_8_), channel_id=1, source_target_pairs={{0,1},{1,0},{2,3},{3,2},{4,5},{5,4},{6,7},{7,6},{8,9},{9,8},{10,11... | collective-permute-start | bytes 3145736 | tf_op jit(solution)/shard_map/ppermute | solution.py:80
  48.1 0.7 %copy-start.16 = (bf16[128,1152]{1,0:T(8,128)(2,1)}, bf16[128,1152]{1,0:T(8,128)(2,1)S(1)}, u32[]{:S(2)}) copy-start(bf16[128,1152]{1,0:T(8,128)(2,1)S(1)} %collective-permute-done.7.refs_5_) | copy-start | bytes 884740
  48.8 7.3 %collective-permute-start.12 = (bf16[2048,256]{1,0:T(8,128)(2,1)S(1)}, bf16[2048,256]{1,0:T(8,128)(2,1)}, u32[]{:S(2)}, u32[]{:S(2)}) collective-permute-start(bf16[2048,256]{1,0:T(8,128)(2,1)S(1)} %collective-permute-done.11.refs_10_), channel_id=1, source_target_pairs={{0,1},{1,0},{2,3},{3,2},{4,5},{5,4},{6,7},{7,6},{8,9},{9,8},{10,11... | collective-permute-start | bytes 3145736 | tf_op jit(solution)/shard_map/ppermute | solution.py:80
  52.2 3.2 %collective-permute-start.15 = (bf16[1024,256]{1,0:T(8,128)(2,1)}, bf16[1024,256]{1,0:T(8,128)(2,1)}, u32[]{:S(2)}, u32[]{:S(2)}) collective-permute-start(bf16[1024,256]{1,0:T(8,128)(2,1)} %collective-permute-done.13.refs_12_), channel_id=1, source_target_pairs={{0,1},{1,0},{2,3},{3,2},{4,5},{5,4},{6,7},{7,6},{8,9},{9,8},{10,11... | collective-permute-start | bytes 1572872 | tf_op jit(solution)/shard_map/ppermute | solution.py:80
  52.2 3.9 %collective-permute-start.16 = (bf16[1024,256]{1,0:T(8,128)(2,1)}, bf16[1024,256]{1,0:T(8,128)(2,1)}, u32[]{:S(2)}, u32[]{:S(2)}) collective-permute-start(bf16[1024,256]{1,0:T(8,128)(2,1)} %collective-permute-done.14.refs_13_), channel_id=1, source_target_pairs={{0,1},{1,0},{2,3},{3,2},{4,5},{5,4},{6,7},{7,6},{8,9},{9,8},{10,11... | collective-permute-start | bytes 1572872 | tf_op jit(solution)/shard_map/ppermute | solution.py:80
  52.7 3.4 %copy-start.5 = (bf16[1,128,2048]{2,1,0:T(8,128)(2,1)S(1)}, bf16[1,128,2048]{2,1,0:T(8,128)(2,1)}, u32[]{:S(2)}) copy-start(bf16[1,128,2048]{2,1,0:T(8,128)(2,1)} %param.10) | copy-start | bytes 1572868
  52.7 3.4 %copy-start.7 = (bf16[128,1152]{1,0:T(8,128)(2,1)S(1)}, bf16[128,1152]{1,0:T(8,128)(2,1)}, u32[]{:S(2)}) copy-start(bf16[128,1152]{1,0:T(8,128)(2,1)} %copy-done.6) | copy-start | bytes 884740
  56.1 1.0 %copy-start.9 = (bf16[128,1152]{1,0:T(8,128)(2,1)S(1)}, bf16[128,1152]{1,0:T(8,128)(2,1)}, u32[]{:S(2)}) copy-start(bf16[128,1152]{1,0:T(8,128)(2,1)} %copy-done.8) | copy-start | bytes 884740
  57.1 1.0 %copy-start.11 = (bf16[128,1152]{1,0:T(8,128)(2,1)S(1)}, bf16[128,1152]{1,0:T(8,128)(2,1)}, u32[]{:S(2)}) copy-start(bf16[128,1152]{1,0:T(8,128)(2,1)} %copy-done.10) | copy-start | bytes 884740
  58.0 1.0 %copy-start.15 = (bf16[128,1152]{1,0:T(8,128)(2,1)S(1)}, bf16[128,1152]{1,0:T(8,128)(2,1)}, u32[]{:S(2)}) copy-start(bf16[128,1152]{1,0:T(8,128)(2,1)} %copy-done.14) | copy-start | bytes 884740
  59.0 1.0 %copy-start.17 = (bf16[128,1152]{1,0:T(8,128)(2,1)S(1)}, bf16[128,1152]{1,0:T(8,128)(2,1)}, u32[]{:S(2)}) copy-start(bf16[128,1152]{1,0:T(8,128)(2,1)} %copy-done.16) | copy-start | bytes 884740

commit v3 on v0

--- a/solution.py
+++ b/solution.py
@@ -1,7 +1,12 @@
+import functools
+
 import jax
 import jax.numpy as jnp
 from jax import lax
+from jax.experimental import pallas as pl
+from jax.experimental.pallas import tpu as pltpu
 from jax.sharding import PartitionSpec as P
+
 
 BLOCK = 128
 
@@ -64,6 +69,341 @@
     return outputs.reshape(block_count * BLOCK, value_width)
 
 
+LANES = 128
+
+
+def log_forget(gates):
+    return -jnp.log1p(jnp.exp(-gates))
+
+
+def running_sum(rows):
+    width = rows.shape[1]
+    upto = lax.broadcasted_iota(jnp.int32, (width, width), 0) <= lax.broadcasted_iota(
+        jnp.int32, (width, width), 1
+    )
+    return jnp.dot(
+        rows,
+        upto.astype(jnp.float32),
+        precision=lax.Precision.HIGHEST,
+        preferred_element_type=jnp.float32,
+    )
+
+
+def times_transpose(left, right):
+    return lax.dot_general(
+        left, right, (((1,), (1,)), ((), ())), preferred_element_type=jnp.float32
+    )
+
+
+def three_terms(value):
+    high = value.astype(jnp.bfloat16).astype(jnp.float32)
+    middle = (value - high).astype(jnp.bfloat16).astype(jnp.float32)
+    return [high, middle, value - high - middle]
+
+
+def to_lanes(columns, rows):
+    lane = lax.broadcasted_iota(jnp.int32, (rows, LANES), 1)
+    tile = jnp.zeros((rows, LANES), jnp.float32)
+    for place, column in enumerate(columns):
+        tile = jnp.where(lane == place, column, tile)
+    return tile
+
+
+MIB = 1 << 20
+COUNTS = (2, 2)
+CORE, XBIT, YBIT = 1, 2, 4
+
+
+def pack_kernel(heads, counts, key_ref, value_ref, input_ref, forget_ref, *refs):
+    payloads, copied = refs[:-1], refs[-1]
+    tokens = key_ref.shape[0]
+    key_width, value_width = key_ref.shape[1] // heads, value_ref.shape[1] // heads
+    copies, first = [], 0
+    for place, (payload, count) in enumerate(zip(payloads, counts)):
+        for part, (source, width, start) in enumerate(
+            ((key_ref, key_width, 0), (value_ref, value_width, count * key_width))
+        ):
+            copies.append(
+                pltpu.make_async_copy(
+                    source.at[:, first * width : (first + count) * width],
+                    payload.at[:tokens, start : start + count * width],
+                    copied.at[2 * place + part],
+                )
+            )
+        first += count
+    for copy in copies:
+        copy.start()
+    gates = jnp.concatenate(
+        [input_ref[...].astype(jnp.float32), forget_ref[...].astype(jnp.float32)], axis=0
+    ).astype(jnp.bfloat16)
+    for payload in payloads:
+        payload[tokens:, : gates.shape[1]] = gates
+        payload[tokens:, gates.shape[1] :] = jnp.zeros(
+            (gates.shape[0], payload.shape[1] - gates.shape[1]), jnp.bfloat16
+        )
+    for copy in copies:
+        copy.wait()
+
+
+def gate_rows(payload, heads, tokens):
+    gates = payload[tokens:, :tokens].astype(jnp.float32)
+    running = running_sum(log_forget(gates[heads:]))
+    return gates[:heads] - running, running[:, tokens - 1 :]
+
+
+def two_term_dot(left, right):
+    high = left.astype(jnp.bfloat16)
+    low = (left - high.astype(jnp.float32)).astype(jnp.bfloat16)
+    return jnp.dot(high, right, preferred_element_type=jnp.float32) + jnp.dot(
+        low, right, preferred_element_type=jnp.float32
+    )
+
+
+def home_kernel(heads, first, count, block_ref, earlier_ref, here_ref, query_ref, total_ref, note_ref):
+    tokens = query_ref.shape[0]
+    key_width = query_ref.shape[1] // heads
+    value_width = total_ref.shape[1] // count
+    block = block_ref[0]
+    second = lax.rem(block, 2) == 1
+    level0, end0 = gate_rows(earlier_ref, heads, tokens)
+    level1, _ = gate_rows(here_ref, heads, tokens)
+    top0 = jnp.max(level0, axis=1, keepdims=True)
+    top0 = jnp.where(block == 1, jnp.maximum(top0, 0.0), top0)
+    weight0 = jnp.exp(level0 - top0)
+    state = jnp.where(second, top0 + end0, jnp.where(block == 0, 0.0, -jnp.inf))
+    shift = jnp.where(block == 3, end0, 0.0)
+    causal = lax.broadcasted_iota(jnp.int32, (tokens, tokens), 0) >= lax.broadcasted_iota(
+        jnp.int32, (tokens, tokens), 1
+    )
+    key_scale = key_width ** (-0.5)
+    notes = []
+    for place in range(count):
+        head = first + place
+        pick = slice(head, head + 1)
+        keys = slice(place * key_width, (place + 1) * key_width)
+        start = count * key_width + place * value_width
+        channels = slice(start, start + value_width)
+        rows = query_ref[:, head * key_width : (head + 1) * key_width]
+        masked = jnp.where(causal, level1[pick], -jnp.inf)
+        top = jnp.maximum(jnp.max(masked, axis=1, keepdims=True), state[pick])
+        scores1 = times_transpose(rows, here_ref[:tokens, keys]) * key_scale
+        scores1 = scores1 * jnp.exp(masked - top)
+        scale0 = jnp.where(second, jnp.exp(state[pick] - top), 0.0)
+        scores0 = times_transpose(rows, earlier_ref[:tokens, keys]) * key_scale
+        scores0 = scores0 * weight0[pick] * scale0
+        sums = jnp.sum(scores0 + scores1, axis=1, keepdims=True)
+        total_ref[:, place * value_width : (place + 1) * value_width] = two_term_dot(
+            scores1, here_ref[:tokens, channels]
+        ) + two_term_dot(scores0, earlier_ref[:tokens, channels])
+        notes += [sums, top, shift[pick]]
+    note_ref[...] = to_lanes(notes, tokens)
+
+
+def serve_kernel(
+    heads, first, count, earlier_ref, here_ref, near_ref, far_ref, next_ref, later_ref
+):
+    tokens = near_ref.shape[0]
+    key_width = near_ref.shape[1] // heads
+    value_width = (next_ref.shape[1] - LANES) // count
+    level0, end0 = gate_rows(earlier_ref, heads, tokens)
+    level1, end1 = gate_rows(here_ref, heads, tokens)
+    level = jnp.concatenate([level0, level1 - end0], axis=1)
+    top = jnp.maximum(jnp.max(level, axis=1, keepdims=True), 0.0)
+    weight = jnp.exp(level - top) * (key_width ** (-0.5))
+    reach = top + end0 + end1
+    next_notes, later_notes = [], []
+    for place in range(count):
+        head = first + place
+        pick = slice(head, head + 1)
+        columns = slice(head * key_width, (head + 1) * key_width)
+        keys = slice(place * key_width, (place + 1) * key_width)
+        start = count * key_width + place * value_width
+        channels = slice(start, start + value_width)
+        out = slice(place * value_width, (place + 1) * value_width)
+        key_both = jnp.concatenate([earlier_ref[:tokens, keys], here_ref[:tokens, keys]], axis=0)
+        value_both = jnp.concatenate(
+            [earlier_ref[:tokens, channels], here_ref[:tokens, channels]], axis=0
+        )
+        rows = jnp.concatenate([near_ref[:, columns], far_ref[:, columns]], axis=0)
+        scores = times_transpose(rows, key_both) * weight[pick]
+        sums = jnp.sum(scores, axis=1, keepdims=True)
+        given = jnp.dot(
+            scores.astype(jnp.bfloat16), value_both, preferred_element_type=jnp.float32
+        ).astype(jnp.bfloat16)
+        next_ref[:, out] = given[:tokens]
+        later_ref[:, out] = given[tokens:]
+        next_notes += three_terms(sums[:tokens]) + three_terms(reach[pick])
+        later_notes += three_terms(sums[tokens:]) + three_terms(reach[pick])
+    next_ref[:, count * value_width :] = to_lanes(next_notes, tokens).astype(jnp.bfloat16)
+    later_ref[:, count * value_width :] = to_lanes(later_notes, tokens).astype(jnp.bfloat16)
+
+
+def finish_kernel(plan, counts, place_ref, *refs):
+    chunks, heads, size = len(counts), sum(counts), 1 + 4 * len(counts) + len(plan)
+    out_ref, held, copied = refs[size], refs[size + 1 : -1], refs[-1]
+    copies = [
+        pltpu.make_async_copy(source, target, copied.at[i])
+        for i, (source, target) in enumerate(zip(refs[:size], held))
+    ]
+    for copy in copies:
+        copy.start()
+    for copy in copies[: 1 + 4 * chunks]:
+        copy.wait()
+    gate_ref, parts, pieces = held[0], held[1 : 1 + 4 * chunks], held[1 + 4 * chunks :]
+    totals, notes, nears, fars = (parts[i * chunks : (i + 1) * chunks] for i in range(4))
+    value_width = gate_ref.shape[1] // heads
+    given = place_ref[1] >= 2
+    gated = []
+    for chunk, count in enumerate(counts):
+        tail = slice(count * value_width, count * value_width + LANES)
+        near, far = nears[chunk], fars[chunk]
+        lanes = near[:, tail].astype(jnp.float32) + far[:, tail].astype(jnp.float32)
+        own = notes[chunk][...]
+        for place in range(count):
+            out = slice(place * value_width, (place + 1) * value_width)
+            start = len(gated) * value_width
+            at = 6 * place
+            sums = lanes[:, at : at + 1] + lanes[:, at + 1 : at + 2] + lanes[:, at + 2 : at + 3]
+            at += 3
+            reach = lanes[:, at : at + 1] + lanes[:, at + 1 : at + 2] + lanes[:, at + 2 : at + 3]
+            reach = reach + own[:, 3 * place + 2 : 3 * place + 3]
+            top = own[:, 3 * place + 1 : 3 * place + 2]
+            peak = jnp.where(given, jnp.maximum(top, reach), top)
+            scale = jnp.exp(top - peak)
+            scale_given = jnp.where(given, jnp.exp(reach - peak), 0.0)
+            weight = scale * own[:, 3 * place : 3 * place + 1] + scale_given * sums
+            inverse = 1.0 / jnp.maximum(jnp.abs(weight), 1.0)
+            message = near[:, out].astype(jnp.float32) + far[:, out].astype(jnp.float32)
+            cell = (scale * inverse) * totals[chunk][:, out] + (scale_given * inverse) * message
+            hidden = cell.astype(jnp.bfloat16).astype(jnp.float32)
+            gate = jax.nn.sigmoid(gate_ref[:, start : start + value_width].astype(jnp.float32))
+            gated.append((hidden * gate).astype(jnp.bfloat16))
+    gated = jnp.concatenate(gated, axis=1)
+    sums = {}
+    for (mask, start), piece, copy in zip(plan, pieces, copies[1 + 4 * chunks :]):
+        copy.wait()
+        part = jnp.dot(
+            gated[:, start : start + piece.shape[0]], piece[...], preferred_element_type=jnp.float32
+        )
+        sums[mask] = sums[mask] + part if mask in sums else part
+    width = pieces[0].shape[1]
+    for mask, total in sums.items():
+        start = pl.multiple_of((place_ref[0] ^ mask) * width, width)
+        out_ref[:, pl.ds(start, width)] = total.astype(out_ref.dtype)
+
+
+def kernel_call(kernel, scalars, operands, outs, flops, limit, spaces=(), scratch=()):
+    vmem = pl.BlockSpec(memory_space=pltpu.VMEM)
+    size = sum(x.size * x.dtype.itemsize for x in operands + outs)
+    specs = [pl.BlockSpec(memory_space=pltpu.SMEM)] * len(scalars) + list(spaces)
+    specs += [vmem] * (len(operands) - len(spaces))
+    return pl.pallas_call(
+        kernel,
+        out_shape=outs,
+        in_specs=specs,
+        out_specs=[vmem] * len(outs),
+        scratch_shapes=scratch,
+        compiler_params=pltpu.CompilerParams(vmem_limit_bytes=limit * MIB),
+        cost_estimate=pl.CostEstimate(flops=flops, bytes_accessed=size, transcendentals=0),
+    )(*scalars, *operands)
+
+
+def block_body(queries, key_rows, values, out_gate, input_gate, forget_gate, out_weight):
+    return block_steps(
+        queries[0], key_rows[0], values[0], out_gate[0], input_gate[0], forget_gate[0], out_weight
+    )[None]
+
+
+def block_steps(query, key, value, gate, input_log, forget, out_weight):
+    tokens, heads = query.shape[0], input_log.shape[0]
+    key_width, value_width = query.shape[1] // heads, value.shape[1] // heads
+    block = lax.axis_index("sp").astype(jnp.int32)
+    shape = jax.ShapeDtypeStruct
+    far_memory = pl.BlockSpec(memory_space=pltpu.HBM)
+    device_count = lax.axis_size("dp")
+
+    def swap(piece, bit):
+        return lax.ppermute(piece, "dp", [(i, i ^ bit) for i in range(device_count)])
+
+    near = lax.ppermute(query, "sp", [(2, 1)])
+    far = lax.ppermute(query, "sp", [(3, 1)])
+    payloads = kernel_call(
+        functools.partial(pack_kernel, heads, COUNTS),
+        [],
+        [key, value, input_log, forget],
+        [
+            shape((tokens + 2 * heads, count * (key_width + value_width)), jnp.bfloat16)
+            for count in COUNTS
+        ],
+        0,
+        60,
+        [far_memory] * 2,
+        [pltpu.SemaphoreType.DMA((2 * len(COUNTS),))],
+    )
+    earlier = [lax.ppermute(payload, "sp", [(0, 1), (2, 3)]) for payload in payloads]
+
+    half = out_weight.shape[0] // 2
+    from_x = swap(out_weight, XBIT)
+    from_y = swap(out_weight, YBIT)
+    from_core = swap(out_weight, CORE)
+    top = swap(from_x[:half], YBIT)
+    bottom = swap(from_y[half:], XBIT)
+    pieces = [
+        (0, 0, out_weight),
+        (CORE, 0, from_core),
+        (XBIT, 0, from_x),
+        (XBIT | CORE, 0, swap(from_x, CORE)),
+        (YBIT, 0, from_y),
+        (YBIT | CORE, 0, swap(from_y, CORE)),
+        (XBIT | YBIT, 0, top),
+        (XBIT | YBIT, half, bottom),
+        (XBIT | YBIT | CORE, 0, swap(top, CORE)),
+        (XBIT | YBIT | CORE, half, swap(bottom, CORE)),
+    ]
+
+    totals, notes, nears, fars = [], [], [], []
+    first = 0
+    for chunk, count in enumerate(COUNTS):
+        work = 2 * count * tokens * tokens * (key_width + value_width)
+        message = shape((tokens, count * value_width + LANES), jnp.bfloat16)
+        given_next, given_later = kernel_call(
+            functools.partial(serve_kernel, heads, first, count),
+            [],
+            [earlier[chunk], payloads[chunk], near, far],
+            [message] * 2,
+            4 * work,
+            8,
+        )
+        nears.append(lax.ppermute(given_next, "sp", [(1, 2)]))
+        fars.append(lax.ppermute(given_later, "sp", [(1, 3)]))
+        total, note = kernel_call(
+            functools.partial(home_kernel, heads, first, count),
+            [block.reshape(1)],
+            [earlier[chunk], payloads[chunk], query],
+            [shape((tokens, count * value_width), jnp.float32), shape((tokens, LANES), jnp.float32)],
+            3 * work,
+            8,
+        )
+        totals.append(total)
+        notes.append(note)
+        first += count
+    place = jnp.stack([lax.axis_index("dp").astype(jnp.int32), block])
+    columns = out_weight.shape[1] * device_count
+    operands = [gate, *totals, *notes, *nears, *fars, *(piece for _, _, piece in pieces)]
+    (out,) = kernel_call(
+        functools.partial(finish_kernel, tuple((mask, start) for mask, start, _ in pieces), COUNTS),
+        [place],
+        operands,
+        [shape((tokens, columns), jnp.bfloat16)],
+        2 * tokens * value.shape[1] * columns,
+        60,
+        [far_memory] * len(operands),
+        [pltpu.VMEM(x.shape, x.dtype) for x in operands]
+        + [pltpu.SemaphoreType.DMA((len(operands),))],
+    )
+    return out
+
+
 def body(queries, key_rows, values, out_gate, input_gate, forget_gate, out_weight):
     group_count = lax.axis_size("sp")
     token_count = queries.shape[1]
@@ -118,8 +458,9 @@
 
 
 def solution(mesh):
+    blocks = mesh.shape["sp"] == 4 and mesh.shape["dp"] == 8
     return jax.shard_map(
-        body,
+        block_body if blocks else body,
         mesh=mesh,
         in_specs=(
             P("dp", "sp", None),

time: 122 us -> 68.1 us (0.56)
  the two profiles are of different devices: /device:TPU:0 before, /device:TPU:9 now
where the time goes in v3:
time: 68.1 us; the launch traced here: 67.7 us
  starting transfers between devices  32.8 us (48%)
  waiting for transfers between devices  16.1 us (24%)
  Pallas kernels  14.3 us (21%)
  local copies, waits for them, and re-layouts  3.64 us (5%)
    ppermute x9, starting transfers between devices, swap(): lax.ppermute(piece, 'dp', [(i, i ^ bit) for i in range(device_count)])  16.2 us
    pallas_call x6, Pallas kernels, kernel_call(): pl.pallas_call(kernel, out_shape=outs, in_specs=specs, out_specs=[vmem] *...  14.3 us
    ppermute x2, starting transfers between devices, block_steps(): fars.append(lax.ppermute(given_later, 'sp', [(1, 3)]))  7.12 us
    ppermute x1, waiting for transfers between devices, block_steps(): near = lax.ppermute(query, 'sp', [(2, 1)])  6.47 us
    ppermute x9, waiting for transfers between devices, swap(): lax.ppermute(piece, 'dp', [(i, i ^ bit) for i in range(device_count)])  4.96 us
    ppermute x2, starting transfers between devices, block_steps(): nears.append(lax.ppermute(given_next, 'sp', [(1, 2)]))  4.32 us
    ppermute x1, waiting for transfers between devices, block_steps(): far = lax.ppermute(query, 'sp', [(3, 1)])  2.88 us
    ppermute x2, starting transfers between devices, block_steps(): lax.ppermute(payload, 'sp', [(0, 1), (2, 3)])  2.58 us
  transfers between devices with their start and end apart: 17, of which 4 were waited for; matrix products, arithmetic and copies ran while one was open for 2% of the time, Pallas kernels for 9%

profile of v3, /device:TPU:9, one launch (start us, length us, event | category | flops | bytes accessed | tf_op | source)
XLA Modules:
  0.0 67.7 jit_solution(10029870749525149750)
XLA Ops:
  0.0 1.2 %collective-permute-start.9 = (bf16[2048,256]{1,0:T(8,128)(2,1)}, bf16[2048,256]{1,0:T(8,128)(2,1)S(1)}, u32[]{:S(2)}, u32[]{:S(2)}) collective-permute-start(bf16[2048,256]{1,0:T(8,128)(2,1)} %refs_9_.1), channel_id=1, source_target_pairs={{0,2},{1,3},{2,0},{3,1},{4,6},{5,7},{6,4},{7,5},{8,10},{9,11},{10,... | collective-permute-start | bytes 3145736 | tf_op jit(solution)/shard_map/ppermute | solution.py:326
  1.2 1.2 %collective-permute-start.11 = (bf16[2048,256]{1,0:T(8,128)(2,1)}, bf16[2048,256]{1,0:T(8,128)(2,1)}, u32[]{:S(2)}, u32[]{:S(2)}) collective-permute-start(bf16[2048,256]{1,0:T(8,128)(2,1)} %refs_9_.1), channel_id=1, source_target_pairs={{0,4},{1,5},{2,6},{3,7},{4,0},{5,1},{6,2},{7,3},{8,12},{9,13},{10,... | collective-permute-start | bytes 3145736 | tf_op jit(solution)/shard_map/ppermute | solution.py:326
  2.5 1.3 %collective-permute-start.3 = (bf16[128,1024]{1,0:T(8,128)(2,1)}, bf16[128,1024]{1,0:T(8,128)(2,1)S(1)}, u32[]{:S(2)}, u32[]{:S(2)}) collective-permute-start(bf16[128,1024]{1,0:T(8,128)(2,1)} %bitcast.9), channel_id=1, source_target_pairs={{24,8},{25,9},{26,10},{27,11},{28,12},{29,13},{30,14},{31,15}} | collective-permute-start | bytes 786440 | tf_op jit(solution)/shard_map/ppermute | solution.py:329
  3.7 0.0 copy-start.3
  3.8 2.8 %shard_map.73 = (bf16[136,1536]{1,0:T(8,128)(2,1)}, bf16[136,1536]{1,0:T(8,128)(2,1)}) custom-call(bf16[128,1024]{1,0:T(8,128)(2,1)} %bitcast.15, bf16[128,2048]{1,0:T(8,128)(2,1)} %bitcast.14, bf16[4,128]{1,0:T(4,128)(2,1)} %bitcast.16, bf16[4,128]{1,0:T(4,128)(2,1)} %bitcast.17), custom_call_target="tpu_custom_call" | custom-call | bytes 1624064 | tf_op jit(solution)/shard_map/pallas_call | solution.py:300
  6.6 1.3 %collective-permute-start = (bf16[136,1536]{1,0:T(8,128)(2,1)}, bf16[136,1536]{1,0:T(8,128)(2,1)S(1)}, u32[]{:S(2)}, u32[]{:S(2)}) collective-permute-start(bf16[136,1536]{1,0:T(8,128)(2,1)} %get-tuple-element.15.here_ref), channel_id=1, source_target_pairs={{0,8},{16,24},{1,9},{17,25},{2,10},{18,26},{3,11},{19,27},{4,12},{... | collective-permute-start | bytes 1253384 | tf_op jit(solution)/shard_map/ppermute | solution.py:343
  7.9 1.3 %collective-permute-start.1 = (bf16[136,1536]{1,0:T(8,128)(2,1)}, bf16[136,1536]{1,0:T(8,128)(2,1)S(1)}, u32[]{:S(2)}, u32[]{:S(2)}) collective-permute-start(bf16[136,1536]{1,0:T(8,128)(2,1)} %get-tuple-element.17.here_ref), channel_id=1, source_target_pairs={{0,8},{16,24},{1,9},{17,25},{2,10},{18,26},{3,11},{19,27},{4,12},{... | collective-permute-start | bytes 1253384 | tf_op jit(solution)/shard_map/ppermute | solution.py:343
  9.2 2.9 %collective-permute-done.3.far_ref = bf16[128,1024]{1,0:T(8,128)(2,1)S(1)} collective-permute-done((bf16[128,1024]{1,0:T(8,128)(2,1)}, bf16[128,1024]{1,0:T(8,128)(2,1)S(1)}, u32[]{:S(2)}, u32[]{:S(2)}) %collective-permute-start.3) | collective-permute-done | bytes 262176 | tf_op jit(solution)/shard_map/ppermute | solution.py:329
  12.1 0.0 copy-done.3
  12.1 1.3 %collective-permute-start.2 = (bf16[128,1024]{1,0:T(8,128)(2,1)S(1)}, bf16[128,1024]{1,0:T(8,128)(2,1)S(1)}, u32[]{:S(2)}, u32[]{:S(2)}) collective-permute-start(bf16[128,1024]{1,0:T(8,128)(2,1)S(1)} %bitcast.10), channel_id=1, source_target_pairs={{16,8},{17,9},{18,10},{19,11},{20,12},{21,13},{22,14},{23,15}} | collective-permute-start | bytes 786440 | tf_op jit(solution)/shard_map/ppermute | solution.py:328
  13.4 6.5 %collective-permute-done.2.near_ref = bf16[128,1024]{1,0:T(8,128)(2,1)S(1)} collective-permute-done((bf16[128,1024]{1,0:T(8,128)(2,1)S(1)}, bf16[128,1024]{1,0:T(8,128)(2,1)S(1)}, u32[]{:S(2)}, u32[]{:S(2)}) %collective-permute-start.2) | collective-permute-done | bytes 262176 | tf_op jit(solution)/shard_map/ppermute | solution.py:328
  19.8 0.0 collective-permute-done.earlier_ref
  19.8 0.0 copy-start
  19.8 1.0 %copy-done = bf16[136,1536]{1,0:T(8,128)(2,1)S(1)} copy-done((bf16[136,1536]{1,0:T(8,128)(2,1)S(1)}, bf16[136,1536]{1,0:T(8,128)(2,1)}, u32[]{:S(2)}) %copy-start) | copy-done | bytes 417816
  20.8 0.0 copy-start.2
  20.8 0.7 %shard_map.76 = (bf16[128,1152]{1,0:T(8,128)(2,1)S(1)}, bf16[128,1152]{1,0:T(8,128)(2,1)S(1)}) custom-call(bf16[136,1536]{1,0:T(8,128)(2,1)S(1)} %collective-permute-done.earlier_ref, bf16[136,1536]{1,0:T(8,128)(2,1)S(1)} %copy-done, bf16[128,1024]{1,0:T(8,128)(2,1)S(1)} %collective-permute-done.2.near_ref, bf16[128,1024]{1,0:T(8,128)(2,1)S(1)} %collective-permute-done.3.far_ref), custom_call_target="tpu_custom_call" | custom-call | flops 201326592 | bytes 1949696 | tf_op jit(solution)/shard_map/pallas_call | solution.py:300
  21.6 1.6 %collective-permute-start.4 = (bf16[128,1152]{1,0:T(8,128)(2,1)S(1)}, bf16[128,1152]{1,0:T(8,128)(2,1)S(1)}, u32[]{:S(2)}, u32[]{:S(2)}) collective-permute-start(bf16[128,1152]{1,0:T(8,128)(2,1)S(1)} %get-tuple-element.21), channel_id=1, source_target_pairs={{8,16},{9,17},{10,18},{11,19},{12,20},{13,21},{14,22},{15,23}} | collective-permute-start | bytes 884744 | tf_op jit(solution)/shard_map/ppermute | solution.py:377
  23.2 2.6 %collective-permute-start.6 = (bf16[128,1152]{1,0:T(8,128)(2,1)S(1)}, bf16[128,1152]{1,0:T(8,128)(2,1)S(1)}, u32[]{:S(2)}, u32[]{:S(2)}) collective-permute-start(bf16[128,1152]{1,0:T(8,128)(2,1)S(1)} %get-tuple-element.23), channel_id=1, source_target_pairs={{8,24},{9,25},{10,26},{11,27},{12,28},{13,29},{14,30},{15,31}} | collective-permute-start | bytes 884744 | tf_op jit(solution)/shard_map/ppermute | solution.py:378
  25.8 1.8 %collective-permute-done.1.earlier_ref = bf16[136,1536]{1,0:T(8,128)(2,1)S(1)} collective-permute-done((bf16[136,1536]{1,0:T(8,128)(2,1)}, bf16[136,1536]{1,0:T(8,128)(2,1)S(1)}, u32[]{:S(2)}, u32[]{:S(2)}) %collective-permute-start.1) | collective-permute-done | bytes 417824 | tf_op jit(solution)/shard_map/ppermute | solution.py:343
  27.6 0.0 copy-done.2
  27.6 0.7 %shard_map.77 = (bf16[128,1152]{1,0:T(8,128)(2,1)S(1)}, bf16[128,1152]{1,0:T(8,128)(2,1)S(1)}) custom-call(bf16[136,1536]{1,0:T(8,128)(2,1)S(1)} %collective-permute-done.1.earlier_ref, bf16[136,1536]{1,0:T(8,128)(2,1)S(1)} %copy-done.2, bf16[128,1024]{1,0:T(8,128)(2,1)S(1)} %collective-permute-done.2.near_ref, ...), custom_call_target="tpu_custom_call" | custom-call | flops 201326592 | bytes 1949696 | tf_op jit(solution)/shard_map/pallas_call | solution.py:300
  28.3 2.7 %collective-permute-start.5 = (bf16[128,1152]{1,0:T(8,128)(2,1)S(1)}, bf16[128,1152]{1,0:T(8,128)(2,1)S(1)}, u32[]{:S(2)}, u32[]{:S(2)}) collective-permute-start(bf16[128,1152]{1,0:T(8,128)(2,1)S(1)} %get-tuple-element.22), channel_id=1, source_target_pairs={{8,16},{9,17},{10,18},{11,19},{12,20},{13,21},{14,22},{15,23}} | collective-permute-start | bytes 884744 | tf_op jit(solution)/shard_map/ppermute | solution.py:377
  31.0 0.0 collective-permute-done.9.refs_11_
  31.1 0.0 copy-start.8
  31.1 4.5 %collective-permute-start.7 = (bf16[128,1152]{1,0:T(8,128)(2,1)S(1)}, bf16[128,1152]{1,0:T(8,128)(2,1)S(1)}, u32[]{:S(2)}, u32[]{:S(2)}) collective-permute-start(bf16[128,1152]{1,0:T(8,128)(2,1)S(1)} %get-tuple-element.24), channel_id=1, source_target_pairs={{8,24},{9,25},{10,26},{11,27},{12,28},{13,29},{14,30},{15,31}} | collective-permute-start | bytes 884744 | tf_op jit(solution)/shard_map/ppermute | solution.py:378
  35.6 0.0 collective-permute-done.11.refs_13_
  35.7 4.0 %collective-permute-start.8 = (bf16[2048,256]{1,0:T(8,128)(2,1)}, bf16[2048,256]{1,0:T(8,128)(2,1)}, u32[]{:S(2)}, u32[]{:S(2)}) collective-permute-start(bf16[2048,256]{1,0:T(8,128)(2,1)} %refs_9_.1), channel_id=1, source_target_pairs={{0,1},{1,0},{2,3},{3,2},{4,5},{5,4},{6,7},{7,6},{8,9},{9,8},{10,11... | collective-permute-start | bytes 3145736 | tf_op jit(solution)/shard_map/ppermute | solution.py:326
  39.6 1.1 %slice.9 = bf16[1024,256]{1,0:T(8,128)(2,1)S(1)} slice(bf16[2048,256]{1,0:T(8,128)(2,1)} %collective-permute-done.11.refs_13_), slice={[1024:2048], [0:256]} | slice | bytes 1048576 | tf_op jit(solution)/shard_map/slice | solution.py:350
  40.7 0.0 collective-permute-done.4.refs_5_
  40.7 0.0 copy-start.10
  40.7 0.3 collective-permute-start.13
  41.0 0.0 collective-permute-done.6.refs_7_
  41.0 0.0 copy-start.11
  41.0 0.3 collective-permute-start.14
  41.3 0.0 collective-permute-done.5.refs_6_
  41.3 0.0 copy-done.8
  41.3 0.0 copy-start.12
  41.3 5.0 %collective-permute-start.10 = (bf16[2048,256]{1,0:T(8,128)(2,1)S(1)}, bf16[2048,256]{1,0:T(8,128)(2,1)}, u32[]{:S(2)}, u32[]{:S(2)}) collective-permute-start(bf16[2048,256]{1,0:T(8,128)(2,1)S(1)} %collective-permute-done.9.refs_11_), channel_id=1, source_target_pairs={{0,1},{1,0},{2,3},{3,2},{4,5},{5,4},{6,7},{7,6},{8,9},{9,8},{10,11... | collective-permute-start | bytes 3145736 | tf_op jit(solution)/shard_map/ppermute | solution.py:326
  46.3 0.0 collective-permute-done.7.refs_8_
  46.3 3.2 %collective-permute-start.12 = (bf16[2048,256]{1,0:T(8,128)(2,1)}, bf16[2048,256]{1,0:T(8,128)(2,1)}, u32[]{:S(2)}, u32[]{:S(2)}) collective-permute-start(bf16[2048,256]{1,0:T(8,128)(2,1)} %collective-permute-done.11.refs_13_), channel_id=1, source_target_pairs={{0,1},{1,0},{2,3},{3,2},{4,5},{5,4},{6,7},{7,6},{8,9},{9,8},{10,11... | collective-permute-start | bytes 3145736 | tf_op jit(solution)/shard_map/ppermute | solution.py:326
  49.4 4.9 %collective-permute-done.13.refs_15_ = bf16[1024,256]{1,0:T(8,128)(2,1)S(1)} collective-permute-done((bf16[1024,256]{1,0:T(8,128)(2,1)S(1)}, bf16[1024,256]{1,0:T(8,128)(2,1)S(1)}, u32[]{:S(2)}, u32[]{:S(2)}) %collective-permute-start.13) | collective-permute-done | bytes 524320 | tf_op jit(solution)/shard_map/ppermute | solution.py:326
  54.4 0.8 %collective-permute-start.15 = (bf16[1024,256]{1,0:T(8,128)(2,1)S(1)}, bf16[1024,256]{1,0:T(8,128)(2,1)}, u32[]{:S(2)}, u32[]{:S(2)}) collective-permute-start(bf16[1024,256]{1,0:T(8,128)(2,1)S(1)} %collective-permute-done.13.refs_15_), channel_id=1, source_target_pairs={{0,1},{1,0},{2,3},{3,2},{4,5},{5,4},{6,7},{7,6},{8,9},{9,8},{10,11... | collective-permute-start | bytes 1572872 | tf_op jit(solution)/shard_map/ppermute | solution.py:326
  55.1 0.0 collective-permute-done.14.refs_16_
  55.1 0.0 copy-done.11
  55.1 0.3 collective-permute-start.16
  55.5 0.0 copy-done.12
  55.5 0.0 copy-done.13
  55.5 0.6 pad_add_fusion.place_ref
  56.1 0.9 %shard_map.75 = (f32[128,1024]{1,0:T(8,128)S(1)}, f32[128,128]{1,0:T(8,128)S(1)}) custom-call(s32[1]{0:T(128)} %bitcast.1.block_ref, bf16[136,1536]{1,0:T(8,128)(2,1)S(1)} %collective-permute-done.1.earlier_ref, bf16[136,1536]{1,0:T(8,128)(2,1)S(1)} %copy-done.2, bf16[128,1024]{1,0:T(8,128)(2,1)S(1)} %bitcast.11), custom_call_target="tpu_custom_call" | custom-call | flops 150994944 | bytes 1687552 | tf_op jit(solution)/shard_map/pallas_call | solution.py:300
  57.0 0.0 copy-done.10
  57.0 0.0 copy-done.9
  57.0 0.0 copy-done.1
  57.1 0.9 %shard_map.74 = (f32[128,1024]{1,0:T(8,128)S(1)}, f32[128,128]{1,0:T(8,128)S(1)}) custom-call(s32[1]{0:T(128)} %bitcast.1.block_ref, bf16[136,1536]{1,0:T(8,128)(2,1)S(1)} %collective-permute-done.earlier_ref, bf16[136,1536]{1,0:T(8,128)(2,1)S(1)} %copy-done.1, bf16[128,1024]{1,0:T(8,128)(2,1)S(1)} %bitcast.12), custom_call_target="tpu_custom_call" | custom-call | flops 150994944 | bytes 1687552 | tf_op jit(solution)/shard_map/pallas_call | solution.py:300
  58.0 0.0 copy-done.4
  58.0 0.0 copy-done.6
  58.0 0.0 copy-start.5
  58.0 0.8 %copy-done.5 = f32[128,1024]{1,0:T(8,128)} copy-done((f32[128,1024]{1,0:T(8,128)}, f32[128,1024]{1,0:T(8,128)S(1)}, u32[]{:S(2)}) %copy-start.5) | copy-done | bytes 524312
  58.9 0.6 copy-done.7
  59.5 0.0 collective-permute-done.8.refs_10_
  59.5 0.0 collective-permute-done.15.refs_17_
  59.5 0.0 collective-permute-done.10.refs_12_
  59.5 0.0 collective-permute-done.16.refs_18_
  59.5 0.0 collective-permute-done.12.refs_14_
  59.5 8.1 %shard_map.78 = bf16[128,2048]{1,0:T(8,128)(2,1)} custom-call(s32[2]{0:T(128)} %pad_add_fusion.place_ref, bf16[128,2048]{1,0:T(8,128)(2,1)} %bitcast.13, f32[128,1024]{1,0:T(8,128)} %copy-done.5, f32[128,1024]{1,0:T(8,128)} %copy-done.4, f32[128,128]{1,0:T(8,128)} %copy-done.7, f32[128,128]{1,0:T(8,128)} %copy-done.6, bf16[128,1152]{1,0:T(8,128)(2,1)} %copy-done.10, ...), custom_call_target="tpu_custom_call" | custom-call | flops 1073741824 | bytes 11796480 | tf_op jit(solution)/shard_map/pallas_call | solution.py:300
  (7 shorter events, 0.0 us)
Async XLA Ops:
  0.0 31.0 %collective-permute-start.9 = (bf16[2048,256]{1,0:T(8,128)(2,1)}, bf16[2048,256]{1,0:T(8,128)(2,1)S(1)}, u32[]{:S(2)}, u32[]{:S(2)}) collective-permute-start(bf16[2048,256]{1,0:T(8,128)(2,1)} %refs_9_.1), channel_id=1, source_target_pairs={{0,2},{1,3},{2,0},{3,1},{4,6},{5,7},{6,4},{7,5},{8,10},{9,11},{10,... | collective-permute-start | bytes 3145736 | tf_op jit(solution)/shard_map/ppermute | solution.py:326
  1.2 34.4 %collective-permute-start.11 = (bf16[2048,256]{1,0:T(8,128)(2,1)}, bf16[2048,256]{1,0:T(8,128)(2,1)}, u32[]{:S(2)}, u32[]{:S(2)}) collective-permute-start(bf16[2048,256]{1,0:T(8,128)(2,1)} %refs_9_.1), channel_id=1, source_target_pairs={{0,4},{1,5},{2,6},{3,7},{4,0},{5,1},{6,2},{7,3},{8,12},{9,13},{10,... | collective-permute-start | bytes 3145736 | tf_op jit(solution)/shard_map/ppermute | solution.py:326
  2.5 9.6 %collective-permute-start.3 = (bf16[128,1024]{1,0:T(8,128)(2,1)}, bf16[128,1024]{1,0:T(8,128)(2,1)S(1)}, u32[]{:S(2)}, u32[]{:S(2)}) collective-permute-start(bf16[128,1024]{1,0:T(8,128)(2,1)} %bitcast.9), channel_id=1, source_target_pairs={{24,8},{25,9},{26,10},{27,11},{28,12},{29,13},{30,14},{31,15}} | collective-permute-start | bytes 786440 | tf_op jit(solution)/shard_map/ppermute | solution.py:329
  3.7 8.3 %copy-start.3 = (bf16[1,128,1024]{2,1,0:T(8,128)(2,1)S(1)}, bf16[1,128,1024]{2,1,0:T(8,128)(2,1)}, u32[]{:S(2)}) copy-start(bf16[1,128,1024]{2,1,0:T(8,128)(2,1)} %param.7) | copy-start | bytes 786436
  6.6 13.2 %collective-permute-start = (bf16[136,1536]{1,0:T(8,128)(2,1)}, bf16[136,1536]{1,0:T(8,128)(2,1)S(1)}, u32[]{:S(2)}, u32[]{:S(2)}) collective-permute-start(bf16[136,1536]{1,0:T(8,128)(2,1)} %get-tuple-element.15.here_ref), channel_id=1, source_target_pairs={{0,8},{16,24},{1,9},{17,25},{2,10},{18,26},{3,11},{19,27},{4,12},{... | collective-permute-start | bytes 1253384 | tf_op jit(solution)/shard_map/ppermute | solution.py:343
  7.9 19.7 %collective-permute-start.1 = (bf16[136,1536]{1,0:T(8,128)(2,1)}, bf16[136,1536]{1,0:T(8,128)(2,1)S(1)}, u32[]{:S(2)}, u32[]{:S(2)}) collective-permute-start(bf16[136,1536]{1,0:T(8,128)(2,1)} %get-tuple-element.17.here_ref), channel_id=1, source_target_pairs={{0,8},{16,24},{1,9},{17,25},{2,10},{18,26},{3,11},{19,27},{4,12},{... | collective-permute-start | bytes 1253384 | tf_op jit(solution)/shard_map/ppermute | solution.py:343
  12.1 7.8 %collective-permute-start.2 = (bf16[128,1024]{1,0:T(8,128)(2,1)S(1)}, bf16[128,1024]{1,0:T(8,128)(2,1)S(1)}, u32[]{:S(2)}, u32[]{:S(2)}) collective-permute-start(bf16[128,1024]{1,0:T(8,128)(2,1)S(1)} %bitcast.10), channel_id=1, source_target_pairs={{16,8},{17,9},{18,10},{19,11},{20,12},{21,13},{22,14},{23,15}} | collective-permute-start | bytes 786440 | tf_op jit(solution)/shard_map/ppermute | solution.py:328
  19.8 1.0 %copy-start = (bf16[136,1536]{1,0:T(8,128)(2,1)S(1)}, bf16[136,1536]{1,0:T(8,128)(2,1)}, u32[]{:S(2)}) copy-start(bf16[136,1536]{1,0:T(8,128)(2,1)} %get-tuple-element.15.here_ref) | copy-start | bytes 1253380
  20.8 6.8 %copy-start.2 = (bf16[136,1536]{1,0:T(8,128)(2,1)S(1)}, bf16[136,1536]{1,0:T(8,128)(2,1)}, u32[]{:S(2)}) copy-start(bf16[136,1536]{1,0:T(8,128)(2,1)} %get-tuple-element.17.here_ref) | copy-start | bytes 1253380
  21.6 19.1 %collective-permute-start.4 = (bf16[128,1152]{1,0:T(8,128)(2,1)S(1)}, bf16[128,1152]{1,0:T(8,128)(2,1)S(1)}, u32[]{:S(2)}, u32[]{:S(2)}) collective-permute-start(bf16[128,1152]{1,0:T(8,128)(2,1)S(1)} %get-tuple-element.21), channel_id=1, source_target_pairs={{8,16},{9,17},{10,18},{11,19},{12,20},{13,21},{14,22},{15,23}} | collective-permute-start | bytes 884744 | tf_op jit(solution)/shard_map/ppermute | solution.py:377
  23.2 17.8 %collective-permute-start.6 = (bf16[128,1152]{1,0:T(8,128)(2,1)S(1)}, bf16[128,1152]{1,0:T(8,128)(2,1)S(1)}, u32[]{:S(2)}, u32[]{:S(2)}) collective-permute-start(bf16[128,1152]{1,0:T(8,128)(2,1)S(1)} %get-tuple-element.23), channel_id=1, source_target_pairs={{8,24},{9,25},{10,26},{11,27},{12,28},{13,29},{14,30},{15,31}} | collective-permute-start | bytes 884744 | tf_op jit(solution)/shard_map/ppermute | solution.py:378
  28.3 12.9 %collective-permute-start.5 = (bf16[128,1152]{1,0:T(8,128)(2,1)S(1)}, bf16[128,1152]{1,0:T(8,128)(2,1)S(1)}, u32[]{:S(2)}, u32[]{:S(2)}) collective-permute-start(bf16[128,1152]{1,0:T(8,128)(2,1)S(1)} %get-tuple-element.22), channel_id=1, source_target_pairs={{8,16},{9,17},{10,18},{11,19},{12,20},{13,21},{14,22},{15,23}} | collective-permute-start | bytes 884744 | tf_op jit(solution)/shard_map/ppermute | solution.py:377
  31.1 10.2 %copy-start.8 = (bf16[2048,256]{1,0:T(8,128)(2,1)}, bf16[2048,256]{1,0:T(8,128)(2,1)S(1)}, u32[]{:S(2)}) copy-start(bf16[2048,256]{1,0:T(8,128)(2,1)S(1)} %collective-permute-done.9.refs_11_) | copy-start | bytes 3145732
  31.1 15.2 %collective-permute-start.7 = (bf16[128,1152]{1,0:T(8,128)(2,1)S(1)}, bf16[128,1152]{1,0:T(8,128)(2,1)S(1)}, u32[]{:S(2)}, u32[]{:S(2)}) collective-permute-start(bf16[128,1152]{1,0:T(8,128)(2,1)S(1)} %get-tuple-element.24), channel_id=1, source_target_pairs={{8,24},{9,25},{10,26},{11,27},{12,28},{13,29},{14,30},{15,31}} | collective-permute-start | bytes 884744 | tf_op jit(solution)/shard_map/ppermute | solution.py:378
  35.7 23.8 %collective-permute-start.8 = (bf16[2048,256]{1,0:T(8,128)(2,1)}, bf16[2048,256]{1,0:T(8,128)(2,1)}, u32[]{:S(2)}, u32[]{:S(2)}) collective-permute-start(bf16[2048,256]{1,0:T(8,128)(2,1)} %refs_9_.1), channel_id=1, source_target_pairs={{0,1},{1,0},{2,3},{3,2},{4,5},{5,4},{6,7},{7,6},{8,9},{9,8},{10,11... | collective-permute-start | bytes 3145736 | tf_op jit(solution)/shard_map/ppermute | solution.py:326
  40.7 16.3 %copy-start.10 = (bf16[128,1152]{1,0:T(8,128)(2,1)}, bf16[128,1152]{1,0:T(8,128)(2,1)S(1)}, u32[]{:S(2)}) copy-start(bf16[128,1152]{1,0:T(8,128)(2,1)S(1)} %collective-permute-done.4.refs_5_) | copy-start | bytes 884740
  40.7 13.6 %collective-permute-start.13 = (bf16[1024,256]{1,0:T(8,128)(2,1)S(1)}, bf16[1024,256]{1,0:T(8,128)(2,1)S(1)}, u32[]{:S(2)}, u32[]{:S(2)}) collective-permute-start(bf16[1024,256]{1,0:T(8,128)(2,1)S(1)} %slice.8), channel_id=1, source_target_pairs={{0,4},{1,5},{2,6},{3,7},{4,0},{5,1},{6,2},{7,3},{8,12},{9,13},{10,... | collective-permute-start | bytes 1572872 | tf_op jit(solution)/shard_map/ppermute | solution.py:326
  41.0 14.1 %copy-start.11 = (bf16[128,1152]{1,0:T(8,128)(2,1)}, bf16[128,1152]{1,0:T(8,128)(2,1)S(1)}, u32[]{:S(2)}) copy-start(bf16[128,1152]{1,0:T(8,128)(2,1)S(1)} %collective-permute-done.6.refs_7_) | copy-start | bytes 884740
  41.0 14.1 %collective-permute-start.14 = (bf16[1024,256]{1,0:T(8,128)(2,1)S(1)}, bf16[1024,256]{1,0:T(8,128)(2,1)}, u32[]{:S(2)}, u32[]{:S(2)}) collective-permute-start(bf16[1024,256]{1,0:T(8,128)(2,1)S(1)} %slice.9), channel_id=1, source_target_pairs={{0,2},{1,3},{2,0},{3,1},{4,6},{5,7},{6,4},{7,5},{8,10},{9,11},{10,... | collective-permute-start | bytes 1572872 | tf_op jit(solution)/shard_map/ppermute | solution.py:326
  41.3 14.2 %copy-start.12 = (bf16[128,1152]{1,0:T(8,128)(2,1)}, bf16[128,1152]{1,0:T(8,128)(2,1)S(1)}, u32[]{:S(2)}) copy-start(bf16[128,1152]{1,0:T(8,128)(2,1)S(1)} %collective-permute-done.5.refs_6_) | copy-start | bytes 884740
  41.3 18.2 %collective-permute-start.10 = (bf16[2048,256]{1,0:T(8,128)(2,1)S(1)}, bf16[2048,256]{1,0:T(8,128)(2,1)}, u32[]{:S(2)}, u32[]{:S(2)}) collective-permute-start(bf16[2048,256]{1,0:T(8,128)(2,1)S(1)} %collective-permute-done.9.refs_11_), channel_id=1, source_target_pairs={{0,1},{1,0},{2,3},{3,2},{4,5},{5,4},{6,7},{7,6},{8,9},{9,8},{10,11... | collective-permute-start | bytes 3145736 | tf_op jit(solution)/shard_map/ppermute | solution.py:326
  46.3 9.2 %copy-start.13 = (bf16[128,1152]{1,0:T(8,128)(2,1)}, bf16[128,1152]{1,0:T(8,128)(2,1)S(1)}, u32[]{:S(2)}) copy-start(bf16[128,1152]{1,0:T(8,128)(2,1)S(1)} %collective-permute-done.7.refs_8_) | copy-start | bytes 884740
  46.3 13.2 %collective-permute-start.12 = (bf16[2048,256]{1,0:T(8,128)(2,1)}, bf16[2048,256]{1,0:T(8,128)(2,1)}, u32[]{:S(2)}, u32[]{:S(2)}) collective-permute-start(bf16[2048,256]{1,0:T(8,128)(2,1)} %collective-permute-done.11.refs_13_), channel_id=1, source_target_pairs={{0,1},{1,0},{2,3},{3,2},{4,5},{5,4},{6,7},{7,6},{8,9},{9,8},{10,11... | collective-permute-start | bytes 3145736 | tf_op jit(solution)/shard_map/ppermute | solution.py:326
  54.4 2.7 %copy-start.9 = (bf16[1024,256]{1,0:T(8,128)(2,1)}, bf16[1024,256]{1,0:T(8,128)(2,1)S(1)}, u32[]{:S(2)}) copy-start(bf16[1024,256]{1,0:T(8,128)(2,1)S(1)} %collective-permute-done.13.refs_15_) | copy-start | bytes 1572868
  54.4 5.1 %collective-permute-start.15 = (bf16[1024,256]{1,0:T(8,128)(2,1)S(1)}, bf16[1024,256]{1,0:T(8,128)(2,1)}, u32[]{:S(2)}, u32[]{:S(2)}) collective-permute-start(bf16[1024,256]{1,0:T(8,128)(2,1)S(1)} %collective-permute-done.13.refs_15_), channel_id=1, source_target_pairs={{0,1},{1,0},{2,3},{3,2},{4,5},{5,4},{6,7},{7,6},{8,9},{9,8},{10,11... | collective-permute-start | bytes 1572872 | tf_op jit(solution)/shard_map/ppermute | solution.py:326
  55.1 4.4 %collective-permute-start.16 = (bf16[1024,256]{1,0:T(8,128)(2,1)}, bf16[1024,256]{1,0:T(8,128)(2,1)}, u32[]{:S(2)}, u32[]{:S(2)}) collective-permute-start(bf16[1024,256]{1,0:T(8,128)(2,1)} %collective-permute-done.14.refs_16_), channel_id=1, source_target_pairs={{0,1},{1,0},{2,3},{3,2},{4,5},{5,4},{6,7},{7,6},{8,9},{9,8},{10,11... | collective-permute-start | bytes 1572872 | tf_op jit(solution)/shard_map/ppermute | solution.py:326
  56.1 1.0 %copy-start.1 = (bf16[136,1536]{1,0:T(8,128)(2,1)S(1)}, bf16[136,1536]{1,0:T(8,128)(2,1)}, u32[]{:S(2)}) copy-start(bf16[136,1536]{1,0:T(8,128)(2,1)} %get-tuple-element.15.here_ref) | copy-start | bytes 1253380
  57.1 0.9 %copy-start.4 = (f32[128,1024]{1,0:T(8,128)}, f32[128,1024]{1,0:T(8,128)S(1)}, u32[]{:S(2)}) copy-start(f32[128,1024]{1,0:T(8,128)S(1)} %get-tuple-element.18.refs_2_) | copy-start | bytes 1572868
  57.1 1.0 %copy-start.6 = (f32[128,128]{1,0:T(8,128)}, f32[128,128]{1,0:T(8,128)S(1)}, u32[]{:S(2)}) copy-start(f32[128,128]{1,0:T(8,128)S(1)} %get-tuple-element.20.refs_4_) | copy-start | bytes 196612
  58.0 0.8 %copy-start.5 = (f32[128,1024]{1,0:T(8,128)}, f32[128,1024]{1,0:T(8,128)S(1)}, u32[]{:S(2)}) copy-start(f32[128,1024]{1,0:T(8,128)S(1)} %get-tuple-element.16.refs_1_) | copy-start | bytes 1572868
  58.9 0.6 copy-start.7

commit v4 on v3

--- a/solution.py
+++ b/solution.py
@@ -114,41 +114,17 @@
 CORE, XBIT, YBIT = 1, 2, 4
 
 
-def pack_kernel(heads, counts, key_ref, value_ref, input_ref, forget_ref, *refs):
-    payloads, copied = refs[:-1], refs[-1]
-    tokens = key_ref.shape[0]
-    key_width, value_width = key_ref.shape[1] // heads, value_ref.shape[1] // heads
-    copies, first = [], 0
-    for place, (payload, count) in enumerate(zip(payloads, counts)):
-        for part, (source, width, start) in enumerate(
-            ((key_ref, key_width, 0), (value_ref, value_width, count * key_width))
-        ):
-            copies.append(
-                pltpu.make_async_copy(
-                    source.at[:, first * width : (first + count) * width],
-                    payload.at[:tokens, start : start + count * width],
-                    copied.at[2 * place + part],
-                )
-            )
-        first += count
-    for copy in copies:
-        copy.start()
-    gates = jnp.concatenate(
-        [input_ref[...].astype(jnp.float32), forget_ref[...].astype(jnp.float32)], axis=0
-    ).astype(jnp.bfloat16)
-    for payload in payloads:
-        payload[tokens:, : gates.shape[1]] = gates
-        payload[tokens:, gates.shape[1] :] = jnp.zeros(
-            (gates.shape[0], payload.shape[1] - gates.shape[1]), jnp.bfloat16
-        )
-    for copy in copies:
-        copy.wait()
-
-
-def gate_rows(payload, heads, tokens):
-    gates = payload[tokens:, :tokens].astype(jnp.float32)
-    running = running_sum(log_forget(gates[heads:]))
-    return gates[:heads] - running, running[:, tokens - 1 :]
+def gates_kernel(input_ref, forget_ref, out_ref):
+    running = running_sum(log_forget(forget_ref[...].astype(jnp.float32)))
+    heads, tokens = running.shape
+    level = input_ref[...].astype(jnp.float32) - running
+    decay = jnp.broadcast_to(running[:, tokens - 1 :], (heads, tokens))
+    out_ref[...] = jnp.concatenate([level, decay], axis=0)
+
+
+def levels(ref):
+    heads = ref.shape[0] // 2
+    return ref[:heads, :], ref[heads:, :1]
 
 
 def two_term_dot(left, right):
@@ -159,72 +135,95 @@
     )
 
 
-def home_kernel(heads, first, count, block_ref, earlier_ref, here_ref, query_ref, total_ref, note_ref):
+def own_kernel(counts, gates_ref, key_ref, value_ref, query_ref, *outs):
+    heads = sum(counts)
     tokens = query_ref.shape[0]
-    key_width = query_ref.shape[1] // heads
-    value_width = total_ref.shape[1] // count
-    block = block_ref[0]
+    key_width, value_width = query_ref.shape[1] // heads, value_ref.shape[1] // heads
+    level, _ = levels(gates_ref)
+    causal = lax.broadcasted_iota(jnp.int32, (tokens, tokens), 0) >= lax.broadcasted_iota(
+        jnp.int32, (tokens, tokens), 1
+    )
+    key_scale = key_width ** (-0.5)
+    first = 0
+    for total_ref, note_ref, count in zip(outs[::2], outs[1::2], counts):
+        notes = []
+        for head in range(first, first + count):
+            keys = slice(head * key_width, (head + 1) * key_width)
+            channels = slice(head * value_width, (head + 1) * value_width)
+            out = slice((head - first) * value_width, (head - first + 1) * value_width)
+            masked = jnp.where(causal, level[head : head + 1], -jnp.inf)
+            top = jnp.max(masked, axis=1, keepdims=True)
+            scores = times_transpose(query_ref[:, keys], key_ref[:, keys]) * key_scale
+            scores = scores * jnp.exp(masked - top)
+            total_ref[:, out] = two_term_dot(scores, value_ref[:, channels])
+            notes += [jnp.sum(scores, axis=1, keepdims=True), top]
+        note_ref[...] = to_lanes(notes, tokens)
+        first += count
+
+
+def join_kernel(counts, gates0_ref, key0_ref, value0_ref, query_ref, *refs):
+    chunks, heads = len(counts), sum(counts)
+    tokens = query_ref.shape[0]
+    key_width, value_width = query_ref.shape[1] // heads, value0_ref.shape[1] // heads
+    block = lax.axis_index("sp")
     second = lax.rem(block, 2) == 1
-    level0, end0 = gate_rows(earlier_ref, heads, tokens)
-    level1, _ = gate_rows(here_ref, heads, tokens)
+    level0, end0 = levels(gates0_ref)
     top0 = jnp.max(level0, axis=1, keepdims=True)
     top0 = jnp.where(block == 1, jnp.maximum(top0, 0.0), top0)
-    weight0 = jnp.exp(level0 - top0)
+    weight0 = jnp.exp(level0 - top0) * (key_width ** (-0.5))
     state = jnp.where(second, top0 + end0, jnp.where(block == 0, 0.0, -jnp.inf))
     shift = jnp.where(block == 3, end0, 0.0)
-    causal = lax.broadcasted_iota(jnp.int32, (tokens, tokens), 0) >= lax.broadcasted_iota(
-        jnp.int32, (tokens, tokens), 1
-    )
-    key_scale = key_width ** (-0.5)
-    notes = []
-    for place in range(count):
-        head = first + place
-        pick = slice(head, head + 1)
-        keys = slice(place * key_width, (place + 1) * key_width)
-        start = count * key_width + place * value_width
-        channels = slice(start, start + value_width)
-        rows = query_ref[:, head * key_width : (head + 1) * key_width]
-        masked = jnp.where(causal, level1[pick], -jnp.inf)
-        top = jnp.maximum(jnp.max(masked, axis=1, keepdims=True), state[pick])
-        scores1 = times_transpose(rows, here_ref[:tokens, keys]) * key_scale
-        scores1 = scores1 * jnp.exp(masked - top)
-        scale0 = jnp.where(second, jnp.exp(state[pick] - top), 0.0)
-        scores0 = times_transpose(rows, earlier_ref[:tokens, keys]) * key_scale
-        scores0 = scores0 * weight0[pick] * scale0
-        sums = jnp.sum(scores0 + scores1, axis=1, keepdims=True)
-        total_ref[:, place * value_width : (place + 1) * value_width] = two_term_dot(
-            scores1, here_ref[:tokens, channels]
-        ) + two_term_dot(scores0, earlier_ref[:tokens, channels])
-        notes += [sums, top, shift[pick]]
-    note_ref[...] = to_lanes(notes, tokens)
+    first = 0
+    for chunk, count in enumerate(counts):
+        own_total, own_note, total_ref, note_ref = refs[chunk * 2 : chunk * 2 + 2] + refs[
+            (chunks + chunk) * 2 : (chunks + chunk) * 2 + 2
+        ]
+        own = own_note[...]
+        notes = []
+        for head in range(first, first + count):
+            pick = slice(head, head + 1)
+            keys = slice(head * key_width, (head + 1) * key_width)
+            channels = slice(head * value_width, (head + 1) * value_width)
+            place = head - first
+            out = slice(place * value_width, (place + 1) * value_width)
+            own_top = own[:, 2 * place + 1 : 2 * place + 2]
+            top = jnp.maximum(own_top, state[pick])
+            scale = jnp.exp(own_top - top)
+            scale0 = jnp.where(second, jnp.exp(state[pick] - top), 0.0)
+            scores = times_transpose(query_ref[:, keys], key0_ref[:, keys])
+            scores = scores * weight0[pick] * scale0
+            total_ref[:, out] = scale * own_total[:, out] + two_term_dot(
+                scores, value0_ref[:, channels]
+            )
+            sums = scale * own[:, 2 * place : 2 * place + 1] + jnp.sum(
+                scores, axis=1, keepdims=True
+            )
+            notes += [sums, top, shift[pick]]
+        note_ref[...] = to_lanes(notes, tokens)
+        first += count
 
 
 def serve_kernel(
-    heads, first, count, earlier_ref, here_ref, near_ref, far_ref, next_ref, later_ref
+    heads, first, count, gates0_ref, key0_ref, value0_ref, gates_ref, key_ref, value_ref,
+    near_ref, far_ref, next_ref, later_ref,
 ):
     tokens = near_ref.shape[0]
-    key_width = near_ref.shape[1] // heads
-    value_width = (next_ref.shape[1] - LANES) // count
-    level0, end0 = gate_rows(earlier_ref, heads, tokens)
-    level1, end1 = gate_rows(here_ref, heads, tokens)
+    key_width, value_width = near_ref.shape[1] // heads, value_ref.shape[1] // heads
+    level0, end0 = levels(gates0_ref)
+    level1, end1 = levels(gates_ref)
     level = jnp.concatenate([level0, level1 - end0], axis=1)
     top = jnp.maximum(jnp.max(level, axis=1, keepdims=True), 0.0)
     weight = jnp.exp(level - top) * (key_width ** (-0.5))
     reach = top + end0 + end1
     next_notes, later_notes = [], []
-    for place in range(count):
-        head = first + place
+    for head in range(first, first + count):
         pick = slice(head, head + 1)
-        columns = slice(head * key_width, (head + 1) * key_width)
-        keys = slice(place * key_width, (place + 1) * key_width)
-        start = count * key_width + place * value_width
-        channels = slice(start, start + value_width)
-        out = slice(place * value_width, (place + 1) * value_width)
-        key_both = jnp.concatenate([earlier_ref[:tokens, keys], here_ref[:tokens, keys]], axis=0)
-        value_both = jnp.concatenate(
-            [earlier_ref[:tokens, channels], here_ref[:tokens, channels]], axis=0
-        )
-        rows = jnp.concatenate([near_ref[:, columns], far_ref[:, columns]], axis=0)
+        keys = slice(head * key_width, (head + 1) * key_width)
+        channels = slice(head * value_width, (head + 1) * value_width)
+        out = slice((head - first) * value_width, (head - first + 1) * value_width)
+        key_both = jnp.concatenate([key0_ref[:, keys], key_ref[:, keys]], axis=0)
+        value_both = jnp.concatenate([value0_ref[:, channels], value_ref[:, channels]], axis=0)
+        rows = jnp.concatenate([near_ref[:, keys], far_ref[:, keys]], axis=0)
         scores = times_transpose(rows, key_both) * weight[pick]
         sums = jnp.sum(scores, axis=1, keepdims=True)
         given = jnp.dot(
@@ -238,21 +237,12 @@
     later_ref[:, count * value_width :] = to_lanes(later_notes, tokens).astype(jnp.bfloat16)
 
 
-def finish_kernel(plan, counts, place_ref, *refs):
-    chunks, heads, size = len(counts), sum(counts), 1 + 4 * len(counts) + len(plan)
-    out_ref, held, copied = refs[size], refs[size + 1 : -1], refs[-1]
-    copies = [
-        pltpu.make_async_copy(source, target, copied.at[i])
-        for i, (source, target) in enumerate(zip(refs[:size], held))
-    ]
-    for copy in copies:
-        copy.start()
-    for copy in copies[: 1 + 4 * chunks]:
-        copy.wait()
-    gate_ref, parts, pieces = held[0], held[1 : 1 + 4 * chunks], held[1 + 4 * chunks :]
-    totals, notes, nears, fars = (parts[i * chunks : (i + 1) * chunks] for i in range(4))
+def finish_kernel(plan, counts, gate_ref, *refs):
+    chunks, heads, out_ref = len(counts), sum(counts), refs[-1]
+    totals, notes, nears, fars = (refs[i * chunks : (i + 1) * chunks] for i in range(4))
+    pieces = refs[4 * chunks : -1]
     value_width = gate_ref.shape[1] // heads
-    given = place_ref[1] >= 2
+    given = lax.axis_index("sp") >= 2
     gated = []
     for chunk, count in enumerate(counts):
         tail = slice(count * value_width, count * value_width + LANES)
@@ -280,32 +270,28 @@
             gated.append((hidden * gate).astype(jnp.bfloat16))
     gated = jnp.concatenate(gated, axis=1)
     sums = {}
-    for (mask, start), piece, copy in zip(plan, pieces, copies[1 + 4 * chunks :]):
-        copy.wait()
+    for (mask, start), piece in zip(plan, pieces):
         part = jnp.dot(
             gated[:, start : start + piece.shape[0]], piece[...], preferred_element_type=jnp.float32
         )
         sums[mask] = sums[mask] + part if mask in sums else part
-    width = pieces[0].shape[1]
+    width, device = pieces[0].shape[1], lax.axis_index("dp")
     for mask, total in sums.items():
-        start = pl.multiple_of((place_ref[0] ^ mask) * width, width)
+        start = pl.multiple_of((device ^ mask) * width, width)
         out_ref[:, pl.ds(start, width)] = total.astype(out_ref.dtype)
 
 
-def kernel_call(kernel, scalars, operands, outs, flops, limit, spaces=(), scratch=()):
+def kernel_call(kernel, operands, outs, flops, limit):
     vmem = pl.BlockSpec(memory_space=pltpu.VMEM)
-    size = sum(x.size * x.dtype.itemsize for x in operands + outs)
-    specs = [pl.BlockSpec(memory_space=pltpu.SMEM)] * len(scalars) + list(spaces)
-    specs += [vmem] * (len(operands) - len(spaces))
+    size = sum(x.size * x.dtype.itemsize for x in (*operands, *outs))
     return pl.pallas_call(
         kernel,
         out_shape=outs,
-        in_specs=specs,
+        in_specs=[vmem] * len(operands),
         out_specs=[vmem] * len(outs),
-        scratch_shapes=scratch,
         compiler_params=pltpu.CompilerParams(vmem_limit_bytes=limit * MIB),
         cost_estimate=pl.CostEstimate(flops=flops, bytes_accessed=size, transcendentals=0),
-    )(*scalars, *operands)
+    )(*operands)
 
 
 def block_body(queries, key_rows, values, out_gate, input_gate, forget_gate, out_weight):
@@ -317,30 +303,24 @@
 def block_steps(query, key, value, gate, input_log, forget, out_weight):
     tokens, heads = query.shape[0], input_log.shape[0]
     key_width, value_width = query.shape[1] // heads, value.shape[1] // heads
-    block = lax.axis_index("sp").astype(jnp.int32)
     shape = jax.ShapeDtypeStruct
-    far_memory = pl.BlockSpec(memory_space=pltpu.HBM)
     device_count = lax.axis_size("dp")
 
     def swap(piece, bit):
         return lax.ppermute(piece, "dp", [(i, i ^ bit) for i in range(device_count)])
 
+    (gates,) = kernel_call(
+        gates_kernel, [input_log, forget], [shape((2 * heads, tokens), jnp.float32)], 0, 2
+    )
+    pair = [(0, 1), (2, 3)]
+    earlier = [
+        lax.ppermute(gates, "sp", pair),
+        lax.ppermute(key, "sp", pair),
+        lax.ppermute(value, "sp", pair),
+    ]
+    here = [gates, key, value]
     near = lax.ppermute(query, "sp", [(2, 1)])
     far = lax.ppermute(query, "sp", [(3, 1)])
-    payloads = kernel_call(
-        functools.partial(pack_kernel, heads, COUNTS),
-        [],
-        [key, value, input_log, forget],
-        [
-            shape((tokens + 2 * heads, count * (key_width + value_width)), jnp.bfloat16)
-            for count in COUNTS
-        ],
-        0,
-        60,
-        [far_memory] * 2,
-        [pltpu.SemaphoreType.DMA((2 * len(COUNTS),))],
-    )
-    earlier = [lax.ppermute(payload, "sp", [(0, 1), (2, 3)]) for payload in payloads]
 
     half = out_weight.shape[0] // 2
     from_x = swap(out_weight, XBIT)
@@ -361,45 +341,46 @@
         (XBIT | YBIT | CORE, half, swap(bottom, CORE)),
     ]
 
-    totals, notes, nears, fars = [], [], [], []
+    work = 2 * tokens * tokens * (key_width + value_width)
+    sums = [
+        x
+        for count in COUNTS
+        for x in (
+            shape((tokens, count * value_width), jnp.float32),
+            shape((tokens, LANES), jnp.float32),
+        )
+    ]
+    own = kernel_call(
+        functools.partial(own_kernel, COUNTS), [*here, query], sums, 3 * heads * work // 2, 8
+    )
+    nears, fars = [], []
     first = 0
-    for chunk, count in enumerate(COUNTS):
-        work = 2 * count * tokens * tokens * (key_width + value_width)
+    for count in COUNTS:
         message = shape((tokens, count * value_width + LANES), jnp.bfloat16)
         given_next, given_later = kernel_call(
             functools.partial(serve_kernel, heads, first, count),
-            [],
-            [earlier[chunk], payloads[chunk], near, far],
+            [*earlier, *here, near, far],
             [message] * 2,
-            4 * work,
+            4 * count * work,
             8,
         )
         nears.append(lax.ppermute(given_next, "sp", [(1, 2)]))
         fars.append(lax.ppermute(given_later, "sp", [(1, 3)]))
-        total, note = kernel_call(
-            functools.partial(home_kernel, heads, first, count),
-            [block.reshape(1)],
-            [earlier[chunk], payloads[chunk], query],
-            [shape((tokens, count * value_width), jnp.float32), shape((tokens, LANES), jnp.float32)],
-            3 * work,
-            8,
-        )
-        totals.append(total)
-        notes.append(note)
         first += count
-    place = jnp.stack([lax.axis_index("dp").astype(jnp.int32), block])
+    home = kernel_call(
+        functools.partial(join_kernel, COUNTS),
+        [*earlier, query, *own],
+        sums,
+        3 * heads * work // 2,
+        8,
+    )
     columns = out_weight.shape[1] * device_count
-    operands = [gate, *totals, *notes, *nears, *fars, *(piece for _, _, piece in pieces)]
     (out,) = kernel_call(
         functools.partial(finish_kernel, tuple((mask, start) for mask, start, _ in pieces), COUNTS),
-        [place],
-        operands,
+        [gate, *home[::2], *home[1::2], *nears, *fars, *(piece for _, _, piece in pieces)],
         [shape((tokens, columns), jnp.bfloat16)],
         2 * tokens * value.shape[1] * columns,
-        60,
-        [far_memory] * len(operands),
-        [pltpu.VMEM(x.shape, x.dtype) for x in operands]
-        + [pltpu.SemaphoreType.DMA((len(operands),))],
+        16,
     )
     return out
 

time: 68.1 us -> 74 us (1.087)
  the two profiles are of different devices: /device:TPU:9 before, /device:TPU:25 now
where the time goes in v4:
time: 74 us; the launch traced here: 73.7 us
  waiting for transfers between devices  37.2 us (50%)
  starting transfers between devices  27.5 us (37%)
  Pallas kernels  5.95 us (8%)
  local copies, waits for them, and re-layouts  2.77 us (4%)
    ppermute x2, waiting for transfers between devices, block_steps(): fars.append(lax.ppermute(given_later, 'sp', [(1, 3)]))  16.5 us
    ppermute x9, starting transfers between devices, swap(): lax.ppermute(piece, 'dp', [(i, i ^ bit) for i in range(device_count)])  16.3 us
    ppermute x1, waiting for transfers between devices, block_steps(): lax.ppermute(gates, 'sp', pair)  15.2 us
    pallas_call x6, Pallas kernels, kernel_call(): pl.pallas_call(kernel, out_shape=outs, in_specs=[vmem] * len(operands), o...  5.95 us
    ppermute x1, waiting for transfers between devices, block_steps(): far = lax.ppermute(query, 'sp', [(3, 1)])  3.93 us
    unnamed x18, local copies, waits for them, and re-layouts  2.7 us
    ppermute x1, starting transfers between devices, block_steps(): far = lax.ppermute(query, 'sp', [(3, 1)])  2.59 us
    ppermute x2, starting transfers between devices, block_steps(): fars.append(lax.ppermute(given_later, 'sp', [(1, 3)]))  2.58 us
  transfers between devices with their start and end apart: 18, of which 5 were waited for; matrix products, arithmetic and copies ran while one was open for 0% of the time, Pallas kernels for 4%

profile of v4, /device:TPU:25, one launch (start us, length us, event | category | flops | bytes accessed | tf_op | source)
XLA Modules:
  0.0 73.7 jit_solution(11941141717052017500)
XLA Ops:
  0.0 1.2 %collective-permute-start.10 = (bf16[2048,256]{1,0:T(8,128)(2,1)}, bf16[2048,256]{1,0:T(8,128)(2,1)S(1)}, u32[]{:S(2)}, u32[]{:S(2)}) collective-permute-start(bf16[2048,256]{1,0:T(8,128)(2,1)} %refs_8_.1), channel_id=1, source_target_pairs={{0,2},{1,3},{2,0},{3,1},{4,6},{5,7},{6,4},{7,5},{8,10},{9,11},{10,... | collective-permute-start | bytes 3145736 | tf_op jit(solution)/shard_map/ppermute | solution.py:310
  1.2 1.2 %collective-permute-start.12 = (bf16[2048,256]{1,0:T(8,128)(2,1)}, bf16[2048,256]{1,0:T(8,128)(2,1)S(1)}, u32[]{:S(2)}, u32[]{:S(2)}) collective-permute-start(bf16[2048,256]{1,0:T(8,128)(2,1)} %refs_8_.1), channel_id=1, source_target_pairs={{0,4},{1,5},{2,6},{3,7},{4,0},{5,1},{6,2},{7,3},{8,12},{9,13},{10,... | collective-permute-start | bytes 3145736 | tf_op jit(solution)/shard_map/ppermute | solution.py:310
  2.5 1.3 %collective-permute-start.1 = (bf16[128,1024]{1,0:T(8,128)(2,1)}, bf16[128,1024]{1,0:T(8,128)(2,1)S(1)}, u32[]{:S(2)}, u32[]{:S(2)}) collective-permute-start(bf16[128,1024]{1,0:T(8,128)(2,1)} %bitcast.11), channel_id=1, source_target_pairs={{0,8},{16,24},{1,9},{17,25},{2,10},{18,26},{3,11},{19,27},{4,12},{... | collective-permute-start | bytes 786440 | tf_op jit(solution)/shard_map/ppermute | solution.py:318
  3.7 1.3 %collective-permute-start.2 = (bf16[128,2048]{1,0:T(8,128)(2,1)}, bf16[128,2048]{1,0:T(8,128)(2,1)S(1)}, u32[]{:S(2)}, u32[]{:S(2)}) collective-permute-start(bf16[128,2048]{1,0:T(8,128)(2,1)} %bitcast.7), channel_id=1, source_target_pairs={{0,8},{16,24},{1,9},{17,25},{2,10},{18,26},{3,11},{19,27},{4,12},{... | collective-permute-start | bytes 1572872 | tf_op jit(solution)/shard_map/ppermute | solution.py:319
  5.0 0.0 copy-start.8
  5.0 0.0 copy-start.7
  5.1 0.7 copy-done.8
  5.7 0.0 copy-done.7
  5.7 0.2 shard_map.73.gates_ref
  6.0 1.3 %collective-permute-start = (f32[8,128]{1,0:T(8,128)S(1)}, f32[8,128]{1,0:T(8,128)S(1)}, u32[]{:S(2)}, u32[]{:S(2)}) collective-permute-start(f32[8,128]{1,0:T(8,128)S(1)} %shard_map.73.gates_ref), channel_id=1, source_target_pairs={{0,8},{16,24},{1,9},{17,25},{2,10},{18,26},{3,11},{19,27},{4,12},{... | collective-permute-start | bytes 12296 | tf_op jit(solution)/shard_map/ppermute | solution.py:317
  7.3 15.2 %collective-permute-done.gates0_ref = f32[8,128]{1,0:T(8,128)S(1)} collective-permute-done((f32[8,128]{1,0:T(8,128)S(1)}, f32[8,128]{1,0:T(8,128)S(1)}, u32[]{:S(2)}, u32[]{:S(2)}) %collective-permute-start) | collective-permute-done | bytes 4128 | tf_op jit(solution)/shard_map/ppermute | solution.py:317
  22.5 0.7 collective-permute-start.3
  23.2 0.0 collective-permute-done.1.key0_ref
  23.2 2.6 %collective-permute-start.4 = (bf16[128,1024]{1,0:T(8,128)(2,1)}, bf16[128,1024]{1,0:T(8,128)(2,1)S(1)}, u32[]{:S(2)}, u32[]{:S(2)}) collective-permute-start(bf16[128,1024]{1,0:T(8,128)(2,1)} %bitcast.16), channel_id=1, source_target_pairs={{24,8},{25,9},{26,10},{27,11},{28,12},{29,13},{30,14},{31,15}} | collective-permute-start | bytes 786440 | tf_op jit(solution)/shard_map/ppermute | solution.py:323
  25.8 0.0 collective-permute-done.3.near_ref
  25.8 3.9 %collective-permute-done.4.far_ref = bf16[128,1024]{1,0:T(8,128)(2,1)S(1)} collective-permute-done((bf16[128,1024]{1,0:T(8,128)(2,1)}, bf16[128,1024]{1,0:T(8,128)(2,1)S(1)}, u32[]{:S(2)}, u32[]{:S(2)}) %collective-permute-start.4) | collective-permute-done | bytes 262176 | tf_op jit(solution)/shard_map/ppermute | solution.py:323
  29.7 0.0 collective-permute-done.2.value0_ref
  29.7 0.0 copy-start
  29.7 1.0 %copy-done = bf16[1,128,2048]{2,1,0:T(8,128)(2,1)S(1)} copy-done((bf16[1,128,2048]{2,1,0:T(8,128)(2,1)S(1)}, bf16[1,128,2048]{2,1,0:T(8,128)(2,1)}, u32[]{:S(2)}) %copy-start) | copy-done | bytes 524312
  30.8 0.0 copy-start.2
  30.8 0.9 %copy-done.2 = bf16[1,128,1024]{2,1,0:T(8,128)(2,1)S(1)} copy-done((bf16[1,128,1024]{2,1,0:T(8,128)(2,1)S(1)}, bf16[1,128,1024]{2,1,0:T(8,128)(2,1)}, u32[]{:S(2)}) %copy-start.2) | copy-done | bytes 262168
  31.7 0.5 shard_map.76
  32.3 0.7 collective-permute-start.5
  33.0 0.5 shard_map.77
  33.5 0.0 copy-start.4
  33.5 0.8 %collective-permute-start.6 = (bf16[128,1152]{1,0:T(8,128)(2,1)S(1)}, bf16[128,1152]{1,0:T(8,128)(2,1)S(1)}, u32[]{:S(2)}, u32[]{:S(2)}) collective-permute-start(bf16[128,1152]{1,0:T(8,128)(2,1)S(1)} %get-tuple-element.26), channel_id=1, source_target_pairs={{8,16},{9,17},{10,18},{11,19},{12,20},{13,21},{14,22},{15,23}} | collective-permute-start | bytes 884744 | tf_op jit(solution)/shard_map/ppermute | solution.py:367
  34.3 1.3 %collective-permute-start.7 = (bf16[128,1152]{1,0:T(8,128)(2,1)S(1)}, bf16[128,1152]{1,0:T(8,128)(2,1)S(1)}, u32[]{:S(2)}, u32[]{:S(2)}) collective-permute-start(bf16[128,1152]{1,0:T(8,128)(2,1)S(1)} %get-tuple-element.27), channel_id=1, source_target_pairs={{8,24},{9,25},{10,26},{11,27},{12,28},{13,29},{14,30},{15,31}} | collective-permute-start | bytes 884744 | tf_op jit(solution)/shard_map/ppermute | solution.py:368
  35.6 0.0 collective-permute-done.10.refs_10_
  35.6 1.3 %collective-permute-start.8 = (bf16[128,1152]{1,0:T(8,128)(2,1)S(1)}, bf16[128,1152]{1,0:T(8,128)(2,1)S(1)}, u32[]{:S(2)}, u32[]{:S(2)}) collective-permute-start(bf16[128,1152]{1,0:T(8,128)(2,1)S(1)} %get-tuple-element.28), channel_id=1, source_target_pairs={{8,24},{9,25},{10,26},{11,27},{12,28},{13,29},{14,30},{15,31}} | collective-permute-start | bytes 884744 | tf_op jit(solution)/shard_map/ppermute | solution.py:368
  37.0 0.0 copy-start.1
  37.0 0.0 copy-start.3
  37.0 0.0 copy-start.5
  37.0 0.0 collective-permute-done.12.refs_12_
  37.0 0.0 copy-done.4
  37.0 3.0 %collective-permute-start.9 = (bf16[2048,256]{1,0:T(8,128)(2,1)S(1)}, bf16[2048,256]{1,0:T(8,128)(2,1)S(1)}, u32[]{:S(2)}, u32[]{:S(2)}) collective-permute-start(bf16[2048,256]{1,0:T(8,128)(2,1)S(1)} %copy-done.4), channel_id=1, source_target_pairs={{0,1},{1,0},{2,3},{3,2},{4,5},{5,4},{6,7},{7,6},{8,9},{9,8},{10,11... | collective-permute-start | bytes 3145736 | tf_op jit(solution)/shard_map/ppermute | solution.py:310
  40.1 0.0 collective-permute-done.5.refs_4_
  40.1 0.3 collective-permute-start.14
  40.4 0.0 collective-permute-done.6.refs_5_
  40.4 0.3 collective-permute-start.15
  40.6 16.5 %collective-permute-done.7.refs_6_ = bf16[128,1152]{1,0:T(8,128)(2,1)S(1)} collective-permute-done((bf16[128,1152]{1,0:T(8,128)(2,1)S(1)}, bf16[128,1152]{1,0:T(8,128)(2,1)S(1)}, u32[]{:S(2)}, u32[]{:S(2)}) %collective-permute-start.7) | collective-permute-done | bytes 294944 | tf_op jit(solution)/shard_map/ppermute | solution.py:368
  57.2 6.7 %collective-permute-start.11 = (bf16[2048,256]{1,0:T(8,128)(2,1)S(1)}, bf16[2048,256]{1,0:T(8,128)(2,1)S(1)}, u32[]{:S(2)}, u32[]{:S(2)}) collective-permute-start(bf16[2048,256]{1,0:T(8,128)(2,1)S(1)} %collective-permute-done.10.refs_10_), channel_id=1, source_target_pairs={{0,1},{1,0},{2,3},{3,2},{4,5},{5,4},{6,7},{7,6},{8,9},{9,8},{10,11... | collective-permute-start | bytes 3145736 | tf_op jit(solution)/shard_map/ppermute | solution.py:310
  63.9 0.0 collective-permute-done.8.refs_7_
  63.9 3.2 %collective-permute-start.13 = (bf16[2048,256]{1,0:T(8,128)(2,1)S(1)}, bf16[2048,256]{1,0:T(8,128)(2,1)S(1)}, u32[]{:S(2)}, u32[]{:S(2)}) collective-permute-start(bf16[2048,256]{1,0:T(8,128)(2,1)S(1)} %collective-permute-done.12.refs_12_), channel_id=1, source_target_pairs={{0,1},{1,0},{2,3},{3,2},{4,5},{5,4},{6,7},{7,6},{8,9},{9,8},{10,11... | collective-permute-start | bytes 3145736 | tf_op jit(solution)/shard_map/ppermute | solution.py:310
  67.0 0.0 collective-permute-done.14.refs_14_
  67.0 0.0 collective-permute-start.16
  67.0 0.0 collective-permute-done.15.refs_15_
  67.0 0.5 collective-permute-start.17
  67.5 0.0 copy-done.1
  67.6 0.0 copy-done.3
  67.6 0.0 copy-done.5
  67.6 0.7 shard_map.74
  68.3 0.0 copy-start.6
  68.3 1.1 %shard_map.75 = (f32[128,1024]{1,0:T(8,128)S(1)}, f32[128,128]{1,0:T(8,128)S(1)}, f32[128,1024]{1,0:T(8,128)S(1)}, f32[128,128]{1,0:T(8,128)S(1)}) custom-call(f32[8,128]{1,0:T(8,128)S(1)} %collective-permute-done.gates0_ref, bf16[128,1024]{1,0:T(8,128)(2,1)S(1)} %collective-permute-done.1.key0_ref, bf16[128,2048]{1,0:T(8,128)(2,1)S(1)} %collective-permute-done.2.value0_ref, ...), custom_call_target="tpu_custom_call" | custom-call | flops 150994944 | bytes 3411968 | tf_op jit(solution)/shard_map/pallas_call | solution.py:287
  69.3 0.0 collective-permute-done.9.refs_9_
  69.4 0.7 collective-permute-done.16.refs_16_
  70.1 0.7 %collective-permute-done.17.refs_17_ = bf16[1024,256]{1,0:T(8,128)(2,1)S(1)} collective-permute-done((bf16[1024,256]{1,0:T(8,128)(2,1)S(1)}, bf16[1024,256]{1,0:T(8,128)(2,1)S(1)}, u32[]{:S(2)}, u32[]{:S(2)}) %collective-permute-start.17) | collective-permute-done | bytes 524320 | tf_op jit(solution)/shard_map/ppermute | solution.py:310
  70.8 0.0 collective-permute-done.11.refs_11_
  70.8 0.0 collective-permute-done.13.refs_13_
  70.8 0.0 copy-done.6
  70.8 2.9 %shard_map.78 = bf16[128,2048]{1,0:T(8,128)(2,1)} custom-call(bf16[128,2048]{1,0:T(8,128)(2,1)S(1)} %bitcast.19, f32[128,1024]{1,0:T(8,128)S(1)} %get-tuple-element.21.refs_0_, f32[128,1024]{1,0:T(8,128)S(1)} %get-tuple-element.22.refs_1_, f32[128,128]{1,0:T(8,128)S(1)} %get-tuple-element.23.refs_2_, f32[128,128]{1,0:T(8,128)S(1)} %get-tuple-element.24.refs_3_, ...), custom_call_target="tpu_custom_call" | custom-call | flops 1073741824 | bytes 11796480 | tf_op jit(solution)/shard_map/pallas_call | solution.py:287
  (2 shorter events, 0.1 us)
Async XLA Ops:
  0.0 35.6 %collective-permute-start.10 = (bf16[2048,256]{1,0:T(8,128)(2,1)}, bf16[2048,256]{1,0:T(8,128)(2,1)S(1)}, u32[]{:S(2)}, u32[]{:S(2)}) collective-permute-start(bf16[2048,256]{1,0:T(8,128)(2,1)} %refs_8_.1), channel_id=1, source_target_pairs={{0,2},{1,3},{2,0},{3,1},{4,6},{5,7},{6,4},{7,5},{8,10},{9,11},{10,... | collective-permute-start | bytes 3145736 | tf_op jit(solution)/shard_map/ppermute | solution.py:310
  1.2 35.8 %collective-permute-start.12 = (bf16[2048,256]{1,0:T(8,128)(2,1)}, bf16[2048,256]{1,0:T(8,128)(2,1)S(1)}, u32[]{:S(2)}, u32[]{:S(2)}) collective-permute-start(bf16[2048,256]{1,0:T(8,128)(2,1)} %refs_8_.1), channel_id=1, source_target_pairs={{0,4},{1,5},{2,6},{3,7},{4,0},{5,1},{6,2},{7,3},{8,12},{9,13},{10,... | collective-permute-start | bytes 3145736 | tf_op jit(solution)/shard_map/ppermute | solution.py:310
  2.5 20.7 %collective-permute-start.1 = (bf16[128,1024]{1,0:T(8,128)(2,1)}, bf16[128,1024]{1,0:T(8,128)(2,1)S(1)}, u32[]{:S(2)}, u32[]{:S(2)}) collective-permute-start(bf16[128,1024]{1,0:T(8,128)(2,1)} %bitcast.11), channel_id=1, source_target_pairs={{0,8},{16,24},{1,9},{17,25},{2,10},{18,26},{3,11},{19,27},{4,12},{... | collective-permute-start | bytes 786440 | tf_op jit(solution)/shard_map/ppermute | solution.py:318
  3.7 26.0 %collective-permute-start.2 = (bf16[128,2048]{1,0:T(8,128)(2,1)}, bf16[128,2048]{1,0:T(8,128)(2,1)S(1)}, u32[]{:S(2)}, u32[]{:S(2)}) collective-permute-start(bf16[128,2048]{1,0:T(8,128)(2,1)} %bitcast.7), channel_id=1, source_target_pairs={{0,8},{16,24},{1,9},{17,25},{2,10},{18,26},{3,11},{19,27},{4,12},{... | collective-permute-start | bytes 1572872 | tf_op jit(solution)/shard_map/ppermute | solution.py:319
  5.0 0.7 copy-start.8
  5.0 0.7 copy-start.7
  6.0 16.5 %collective-permute-start = (f32[8,128]{1,0:T(8,128)S(1)}, f32[8,128]{1,0:T(8,128)S(1)}, u32[]{:S(2)}, u32[]{:S(2)}) collective-permute-start(f32[8,128]{1,0:T(8,128)S(1)} %shard_map.73.gates_ref), channel_id=1, source_target_pairs={{0,8},{16,24},{1,9},{17,25},{2,10},{18,26},{3,11},{19,27},{4,12},{... | collective-permute-start | bytes 12296 | tf_op jit(solution)/shard_map/ppermute | solution.py:317
  22.5 3.3 %collective-permute-start.3 = (bf16[128,1024]{1,0:T(8,128)(2,1)}, bf16[128,1024]{1,0:T(8,128)(2,1)S(1)}, u32[]{:S(2)}, u32[]{:S(2)}) collective-permute-start(bf16[128,1024]{1,0:T(8,128)(2,1)} %bitcast.15), channel_id=1, source_target_pairs={{16,8},{17,9},{18,10},{19,11},{20,12},{21,13},{22,14},{23,15}} | collective-permute-start | bytes 786440 | tf_op jit(solution)/shard_map/ppermute | solution.py:322
  23.2 6.5 %collective-permute-start.4 = (bf16[128,1024]{1,0:T(8,128)(2,1)}, bf16[128,1024]{1,0:T(8,128)(2,1)S(1)}, u32[]{:S(2)}, u32[]{:S(2)}) collective-permute-start(bf16[128,1024]{1,0:T(8,128)(2,1)} %bitcast.16), channel_id=1, source_target_pairs={{24,8},{25,9},{26,10},{27,11},{28,12},{29,13},{30,14},{31,15}} | collective-permute-start | bytes 786440 | tf_op jit(solution)/shard_map/ppermute | solution.py:323
  29.7 1.0 %copy-start = (bf16[1,128,2048]{2,1,0:T(8,128)(2,1)S(1)}, bf16[1,128,2048]{2,1,0:T(8,128)(2,1)}, u32[]{:S(2)}) copy-start(bf16[1,128,2048]{2,1,0:T(8,128)(2,1)} %param.9) | copy-start | bytes 1572868
  30.8 0.9 %copy-start.2 = (bf16[1,128,1024]{2,1,0:T(8,128)(2,1)S(1)}, bf16[1,128,1024]{2,1,0:T(8,128)(2,1)}, u32[]{:S(2)}) copy-start(bf16[1,128,1024]{2,1,0:T(8,128)(2,1)} %param.8) | copy-start | bytes 786436
  32.3 7.8 %collective-permute-start.5 = (bf16[128,1152]{1,0:T(8,128)(2,1)S(1)}, bf16[128,1152]{1,0:T(8,128)(2,1)S(1)}, u32[]{:S(2)}, u32[]{:S(2)}) collective-permute-start(bf16[128,1152]{1,0:T(8,128)(2,1)S(1)} %get-tuple-element.25), channel_id=1, source_target_pairs={{8,16},{9,17},{10,18},{11,19},{12,20},{13,21},{14,22},{15,23}} | collective-permute-start | bytes 884744 | tf_op jit(solution)/shard_map/ppermute | solution.py:367
  33.5 3.5 %copy-start.4 = (bf16[2048,256]{1,0:T(8,128)(2,1)S(1)}, bf16[2048,256]{1,0:T(8,128)(2,1)}, u32[]{:S(2)}) copy-start(bf16[2048,256]{1,0:T(8,128)(2,1)} %refs_8_.1) | copy-start | bytes 3145732
  33.5 6.8 %collective-permute-start.6 = (bf16[128,1152]{1,0:T(8,128)(2,1)S(1)}, bf16[128,1152]{1,0:T(8,128)(2,1)S(1)}, u32[]{:S(2)}, u32[]{:S(2)}) collective-permute-start(bf16[128,1152]{1,0:T(8,128)(2,1)S(1)} %get-tuple-element.26), channel_id=1, source_target_pairs={{8,16},{9,17},{10,18},{11,19},{12,20},{13,21},{14,22},{15,23}} | collective-permute-start | bytes 884744 | tf_op jit(solution)/shard_map/ppermute | solution.py:367
  34.3 22.8 %collective-permute-start.7 = (bf16[128,1152]{1,0:T(8,128)(2,1)S(1)}, bf16[128,1152]{1,0:T(8,128)(2,1)S(1)}, u32[]{:S(2)}, u32[]{:S(2)}) collective-permute-start(bf16[128,1152]{1,0:T(8,128)(2,1)S(1)} %get-tuple-element.27), channel_id=1, source_target_pairs={{8,24},{9,25},{10,26},{11,27},{12,28},{13,29},{14,30},{15,31}} | collective-permute-start | bytes 884744 | tf_op jit(solution)/shard_map/ppermute | solution.py:368
  35.6 28.2 %collective-permute-start.8 = (bf16[128,1152]{1,0:T(8,128)(2,1)S(1)}, bf16[128,1152]{1,0:T(8,128)(2,1)S(1)}, u32[]{:S(2)}, u32[]{:S(2)}) collective-permute-start(bf16[128,1152]{1,0:T(8,128)(2,1)S(1)} %get-tuple-element.28), channel_id=1, source_target_pairs={{8,24},{9,25},{10,26},{11,27},{12,28},{13,29},{14,30},{15,31}} | collective-permute-start | bytes 884744 | tf_op jit(solution)/shard_map/ppermute | solution.py:368
  37.0 30.6 %copy-start.1 = (bf16[1,128,2048]{2,1,0:T(8,128)(2,1)S(1)}, bf16[1,128,2048]{2,1,0:T(8,128)(2,1)}, u32[]{:S(2)}) copy-start(bf16[1,128,2048]{2,1,0:T(8,128)(2,1)} %param.9) | copy-start | bytes 1572868
  37.0 30.6 %copy-start.3 = (bf16[1,128,1024]{2,1,0:T(8,128)(2,1)S(1)}, bf16[1,128,1024]{2,1,0:T(8,128)(2,1)}, u32[]{:S(2)}) copy-start(bf16[1,128,1024]{2,1,0:T(8,128)(2,1)} %param.8) | copy-start | bytes 786436
  37.0 30.5 %copy-start.5 = (bf16[1,128,1024]{2,1,0:T(8,128)(2,1)S(1)}, bf16[1,128,1024]{2,1,0:T(8,128)(2,1)}, u32[]{:S(2)}) copy-start(bf16[1,128,1024]{2,1,0:T(8,128)(2,1)} %param.7) | copy-start | bytes 786436
  37.0 32.3 %collective-permute-start.9 = (bf16[2048,256]{1,0:T(8,128)(2,1)S(1)}, bf16[2048,256]{1,0:T(8,128)(2,1)S(1)}, u32[]{:S(2)}, u32[]{:S(2)}) collective-permute-start(bf16[2048,256]{1,0:T(8,128)(2,1)S(1)} %copy-done.4), channel_id=1, source_target_pairs={{0,1},{1,0},{2,3},{3,2},{4,5},{5,4},{6,7},{7,6},{8,9},{9,8},{10,11... | collective-permute-start | bytes 3145736 | tf_op jit(solution)/shard_map/ppermute | solution.py:310
  40.1 27.0 %collective-permute-start.14 = (bf16[1024,256]{1,0:T(8,128)(2,1)S(1)}, bf16[1024,256]{1,0:T(8,128)(2,1)S(1)}, u32[]{:S(2)}, u32[]{:S(2)}) collective-permute-start(bf16[1024,256]{1,0:T(8,128)(2,1)S(1)} %slice.8), channel_id=1, source_target_pairs={{0,4},{1,5},{2,6},{3,7},{4,0},{5,1},{6,2},{7,3},{8,12},{9,13},{10,... | collective-permute-start | bytes 1572872 | tf_op jit(solution)/shard_map/ppermute | solution.py:310
  40.4 26.7 %collective-permute-start.15 = (bf16[1024,256]{1,0:T(8,128)(2,1)S(1)}, bf16[1024,256]{1,0:T(8,128)(2,1)S(1)}, u32[]{:S(2)}, u32[]{:S(2)}) collective-permute-start(bf16[1024,256]{1,0:T(8,128)(2,1)S(1)} %slice.9), channel_id=1, source_target_pairs={{0,2},{1,3},{2,0},{3,1},{4,6},{5,7},{6,4},{7,5},{8,10},{9,11},{10,... | collective-permute-start | bytes 1572872 | tf_op jit(solution)/shard_map/ppermute | solution.py:310
  57.2 13.7 %collective-permute-start.11 = (bf16[2048,256]{1,0:T(8,128)(2,1)S(1)}, bf16[2048,256]{1,0:T(8,128)(2,1)S(1)}, u32[]{:S(2)}, u32[]{:S(2)}) collective-permute-start(bf16[2048,256]{1,0:T(8,128)(2,1)S(1)} %collective-permute-done.10.refs_10_), channel_id=1, source_target_pairs={{0,1},{1,0},{2,3},{3,2},{4,5},{5,4},{6,7},{7,6},{8,9},{9,8},{10,11... | collective-permute-start | bytes 3145736 | tf_op jit(solution)/shard_map/ppermute | solution.py:310
  63.9 7.0 %collective-permute-start.13 = (bf16[2048,256]{1,0:T(8,128)(2,1)S(1)}, bf16[2048,256]{1,0:T(8,128)(2,1)S(1)}, u32[]{:S(2)}, u32[]{:S(2)}) collective-permute-start(bf16[2048,256]{1,0:T(8,128)(2,1)S(1)} %collective-permute-done.12.refs_12_), channel_id=1, source_target_pairs={{0,1},{1,0},{2,3},{3,2},{4,5},{5,4},{6,7},{7,6},{8,9},{9,8},{10,11... | collective-permute-start | bytes 3145736 | tf_op jit(solution)/shard_map/ppermute | solution.py:310
  67.0 3.0 %collective-permute-start.16 = (bf16[1024,256]{1,0:T(8,128)(2,1)S(1)}, bf16[1024,256]{1,0:T(8,128)(2,1)S(1)}, u32[]{:S(2)}, u32[]{:S(2)}) collective-permute-start(bf16[1024,256]{1,0:T(8,128)(2,1)S(1)} %collective-permute-done.14.refs_14_), channel_id=1, source_target_pairs={{0,1},{1,0},{2,3},{3,2},{4,5},{5,4},{6,7},{7,6},{8,9},{9,8},{10,11... | collective-permute-start | bytes 1572872 | tf_op jit(solution)/shard_map/ppermute | solution.py:310
  67.0 3.8 %collective-permute-start.17 = (bf16[1024,256]{1,0:T(8,128)(2,1)S(1)}, bf16[1024,256]{1,0:T(8,128)(2,1)S(1)}, u32[]{:S(2)}, u32[]{:S(2)}) collective-permute-start(bf16[1024,256]{1,0:T(8,128)(2,1)S(1)} %collective-permute-done.15.refs_15_), channel_id=1, source_target_pairs={{0,1},{1,0},{2,3},{3,2},{4,5},{5,4},{6,7},{7,6},{8,9},{9,8},{10,11... | collective-permute-start | bytes 1572872 | tf_op jit(solution)/shard_map/ppermute | solution.py:310
  68.3 2.6 %copy-start.6 = (bf16[1,128,2048]{2,1,0:T(8,128)(2,1)S(1)}, bf16[1,128,2048]{2,1,0:T(8,128)(2,1)}, u32[]{:S(2)}) copy-start(bf16[1,128,2048]{2,1,0:T(8,128)(2,1)} %param.10) | copy-start | bytes 1572868

commit v5 on v4

--- a/solution.py
+++ b/solution.py
@@ -204,9 +204,10 @@
 
 
 def serve_kernel(
-    heads, first, count, gates0_ref, key0_ref, value0_ref, gates_ref, key_ref, value_ref,
-    near_ref, far_ref, next_ref, later_ref,
+    counts, gates0_ref, key0_ref, value0_ref, gates_ref, key_ref, value_ref,
+    near_ref, far_ref, next_ref, later_ref, score_ref,
 ):
+    heads, count = sum(counts), counts[0]
     tokens = near_ref.shape[0]
     key_width, value_width = near_ref.shape[1] // heads, value_ref.shape[1] // heads
     level0, end0 = levels(gates0_ref)
@@ -216,69 +217,115 @@
     weight = jnp.exp(level - top) * (key_width ** (-0.5))
     reach = top + end0 + end1
     next_notes, later_notes = [], []
-    for head in range(first, first + count):
-        pick = slice(head, head + 1)
+    for head in range(heads):
         keys = slice(head * key_width, (head + 1) * key_width)
-        channels = slice(head * value_width, (head + 1) * value_width)
-        out = slice((head - first) * value_width, (head - first + 1) * value_width)
         key_both = jnp.concatenate([key0_ref[:, keys], key_ref[:, keys]], axis=0)
-        value_both = jnp.concatenate([value0_ref[:, channels], value_ref[:, channels]], axis=0)
         rows = jnp.concatenate([near_ref[:, keys], far_ref[:, keys]], axis=0)
-        scores = times_transpose(rows, key_both) * weight[pick]
+        scores = times_transpose(rows, key_both) * weight[head : head + 1]
         sums = jnp.sum(scores, axis=1, keepdims=True)
-        given = jnp.dot(
-            scores.astype(jnp.bfloat16), value_both, preferred_element_type=jnp.float32
-        ).astype(jnp.bfloat16)
-        next_ref[:, out] = given[:tokens]
-        later_ref[:, out] = given[tokens:]
-        next_notes += three_terms(sums[:tokens]) + three_terms(reach[pick])
-        later_notes += three_terms(sums[tokens:]) + three_terms(reach[pick])
+        scores = scores.astype(jnp.bfloat16)
+        if head < count:
+            channels = slice(head * value_width, (head + 1) * value_width)
+            give(scores, value0_ref, value_ref, channels, next_ref, later_ref, channels)
+        else:
+            place = head - count
+            score_ref[:, place * 2 * tokens : (place + 1) * 2 * tokens] = scores
+        terms = three_terms(reach[head : head + 1])
+        next_notes += three_terms(sums[:tokens]) + terms
+        later_notes += three_terms(sums[tokens:]) + terms
     next_ref[:, count * value_width :] = to_lanes(next_notes, tokens).astype(jnp.bfloat16)
     later_ref[:, count * value_width :] = to_lanes(later_notes, tokens).astype(jnp.bfloat16)
 
 
-def finish_kernel(plan, counts, gate_ref, *refs):
-    chunks, heads, out_ref = len(counts), sum(counts), refs[-1]
-    totals, notes, nears, fars = (refs[i * chunks : (i + 1) * chunks] for i in range(4))
-    pieces = refs[4 * chunks : -1]
+def give(scores, value0_ref, value_ref, channels, next_ref, later_ref, out):
+    tokens = value_ref.shape[0]
+    values = jnp.concatenate([value0_ref[:, channels], value_ref[:, channels]], axis=0)
+    given = jnp.dot(scores, values, preferred_element_type=jnp.float32).astype(jnp.bfloat16)
+    next_ref[:, out] = given[:tokens]
+    later_ref[:, out] = given[tokens:]
+
+
+def serve_rest_kernel(first, count, score_ref, value0_ref, value_ref, next_ref, later_ref):
+    width = score_ref.shape[1] // count
+    value_width = next_ref.shape[1] // count
+    for place in range(count):
+        channels = slice((first + place) * value_width, (first + place + 1) * value_width)
+        out = slice(place * value_width, (place + 1) * value_width)
+        scores = score_ref[:, place * width : (place + 1) * width]
+        give(scores, value0_ref, value_ref, channels, next_ref, later_ref, out)
+
+
+def gated_rows(heads, first, count, total_ref, note_ref, near_ref, far_ref, lanes, gate_ref):
     value_width = gate_ref.shape[1] // heads
     given = lax.axis_index("sp") >= 2
+    own = note_ref[...]
     gated = []
-    for chunk, count in enumerate(counts):
-        tail = slice(count * value_width, count * value_width + LANES)
-        near, far = nears[chunk], fars[chunk]
-        lanes = near[:, tail].astype(jnp.float32) + far[:, tail].astype(jnp.float32)
-        own = notes[chunk][...]
-        for place in range(count):
-            out = slice(place * value_width, (place + 1) * value_width)
-            start = len(gated) * value_width
-            at = 6 * place
-            sums = lanes[:, at : at + 1] + lanes[:, at + 1 : at + 2] + lanes[:, at + 2 : at + 3]
-            at += 3
-            reach = lanes[:, at : at + 1] + lanes[:, at + 1 : at + 2] + lanes[:, at + 2 : at + 3]
-            reach = reach + own[:, 3 * place + 2 : 3 * place + 3]
-            top = own[:, 3 * place + 1 : 3 * place + 2]
-            peak = jnp.where(given, jnp.maximum(top, reach), top)
-            scale = jnp.exp(top - peak)
-            scale_given = jnp.where(given, jnp.exp(reach - peak), 0.0)
-            weight = scale * own[:, 3 * place : 3 * place + 1] + scale_given * sums
-            inverse = 1.0 / jnp.maximum(jnp.abs(weight), 1.0)
-            message = near[:, out].astype(jnp.float32) + far[:, out].astype(jnp.float32)
-            cell = (scale * inverse) * totals[chunk][:, out] + (scale_given * inverse) * message
-            hidden = cell.astype(jnp.bfloat16).astype(jnp.float32)
-            gate = jax.nn.sigmoid(gate_ref[:, start : start + value_width].astype(jnp.float32))
-            gated.append((hidden * gate).astype(jnp.bfloat16))
-    gated = jnp.concatenate(gated, axis=1)
+    for place in range(count):
+        out = slice(place * value_width, (place + 1) * value_width)
+        channels = slice((first + place) * value_width, (first + place + 1) * value_width)
+        at = 6 * (first + place)
+        sums = lanes[:, at : at + 1] + lanes[:, at + 1 : at + 2] + lanes[:, at + 2 : at + 3]
+        at += 3
+        reach = lanes[:, at : at + 1] + lanes[:, at + 1 : at + 2] + lanes[:, at + 2 : at + 3]
+        reach = reach + own[:, 3 * place + 2 : 3 * place + 3]
+        top = own[:, 3 * place + 1 : 3 * place + 2]
+        peak = jnp.where(given, jnp.maximum(top, reach), top)
+        scale = jnp.exp(top - peak)
+        scale_given = jnp.where(given, jnp.exp(reach - peak), 0.0)
+        weight = scale * own[:, 3 * place : 3 * place + 1] + scale_given * sums
+        inverse = 1.0 / jnp.maximum(jnp.abs(weight), 1.0)
+        message = near_ref[:, out].astype(jnp.float32) + far_ref[:, out].astype(jnp.float32)
+        cell = (scale * inverse) * total_ref[:, out] + (scale_given * inverse) * message
+        hidden = cell.astype(jnp.bfloat16).astype(jnp.float32)
+        gate = jax.nn.sigmoid(gate_ref[:, channels].astype(jnp.float32))
+        gated.append((hidden * gate).astype(jnp.bfloat16))
+    return jnp.concatenate(gated, axis=1)
+
+
+def product(left, right):
+    return jnp.dot(left, right, preferred_element_type=jnp.float32)
+
+
+def first_kernel(counts, gate_ref, total_ref, note_ref, near_ref, far_ref, *refs):
+    pieces, gated_ref, lane_ref, part_ref = refs[:-3], refs[-3], refs[-2], refs[-1]
+    rows = gated_ref.shape[1]
+    lanes = near_ref[:, rows:].astype(jnp.float32) + far_ref[:, rows:].astype(jnp.float32)
+    lane_ref[...] = lanes
+    gated = gated_rows(
+        sum(counts), 0, counts[0], total_ref, note_ref, near_ref, far_ref, lanes, gate_ref
+    )
+    gated_ref[...] = gated
+    width = pieces[0].shape[1]
+    for place, piece in enumerate(pieces):
+        part_ref[:, place * width : (place + 1) * width] = product(gated, piece[:rows, :])
+
+
+def finish_kernel(
+    counts, whole, plan, gate_ref, total_ref, note_ref, near_ref, far_ref, gated_ref, lane_ref,
+    part_ref, *refs,
+):
+    pieces, out_ref = refs[:-1], refs[-1]
+    rows, device = gated_ref.shape[1], lax.axis_index("dp")
+    width = pieces[0].shape[1]
+    gated = gated_rows(
+        sum(counts), counts[0], counts[1], total_ref, note_ref, near_ref, far_ref,
+        lane_ref[...], gate_ref,
+    )
+
+    def put(mask, columns):
+        start = pl.multiple_of((device ^ mask) * width, width)
+        out_ref[:, pl.ds(start, width)] = columns.astype(out_ref.dtype)
+
+    for place, (mask, piece) in enumerate(zip(whole, pieces)):
+        part = part_ref[:, place * width : (place + 1) * width]
+        put(mask, part + product(gated, piece[rows:, :]))
+    both = jnp.concatenate([gated_ref[...], gated], axis=1)
     sums = {}
-    for (mask, start), piece in zip(plan, pieces):
-        part = jnp.dot(
-            gated[:, start : start + piece.shape[0]], piece[...], preferred_element_type=jnp.float32
-        )
+    for (mask, start), piece in zip(plan, pieces[len(whole) :]):
+        part = product(both[:, start : start + piece.shape[0]], piece[...])
         sums[mask] = sums[mask] + part if mask in sums else part
-    width, device = pieces[0].shape[1], lax.axis_index("dp")
-    for mask, total in sums.items():
-        start = pl.multiple_of((device ^ mask) * width, width)
-        out_ref[:, pl.ds(start, width)] = total.astype(out_ref.dtype)
+    for mask, columns in sums.items():
+        put(mask, columns)
 
 
 def kernel_call(kernel, operands, outs, flops, limit):
@@ -328,17 +375,19 @@
     from_core = swap(out_weight, CORE)
     top = swap(from_x[:half], YBIT)
     bottom = swap(from_y[half:], XBIT)
-    pieces = [
-        (0, 0, out_weight),
-        (CORE, 0, from_core),
-        (XBIT, 0, from_x),
-        (XBIT | CORE, 0, swap(from_x, CORE)),
-        (YBIT, 0, from_y),
-        (YBIT | CORE, 0, swap(from_y, CORE)),
-        (XBIT | YBIT, 0, top),
-        (XBIT | YBIT, half, bottom),
-        (XBIT | YBIT | CORE, 0, swap(top, CORE)),
-        (XBIT | YBIT | CORE, half, swap(bottom, CORE)),
+    whole = {
+        0: out_weight,
+        CORE: from_core,
+        XBIT: from_x,
+        XBIT | CORE: swap(from_x, CORE),
+        YBIT: from_y,
+        YBIT | CORE: swap(from_y, CORE),
+    }
+    corner = [
+        ((XBIT | YBIT, 0), top),
+        ((XBIT | YBIT, half), bottom),
+        ((XBIT | YBIT | CORE, 0), swap(top, CORE)),
+        ((XBIT | YBIT | CORE, half), swap(bottom, CORE)),
     ]
 
     work = 2 * tokens * tokens * (key_width + value_width)
@@ -353,20 +402,25 @@
     own = kernel_call(
         functools.partial(own_kernel, COUNTS), [*here, query], sums, 3 * heads * work // 2, 8
     )
-    nears, fars = [], []
-    first = 0
-    for count in COUNTS:
-        message = shape((tokens, count * value_width + LANES), jnp.bfloat16)
-        given_next, given_later = kernel_call(
-            functools.partial(serve_kernel, heads, first, count),
-            [*earlier, *here, near, far],
-            [message] * 2,
-            4 * count * work,
-            8,
-        )
-        nears.append(lax.ppermute(given_next, "sp", [(1, 2)]))
-        fars.append(lax.ppermute(given_later, "sp", [(1, 3)]))
-        first += count
+    first, rest = COUNTS
+    message = shape((tokens, first * value_width + LANES), jnp.bfloat16)
+    given_next, given_later, scores = kernel_call(
+        functools.partial(serve_kernel, COUNTS),
+        [*earlier, *here, near, far],
+        [message, message, shape((2 * tokens, rest * 2 * tokens), jnp.bfloat16)],
+        4 * heads * work,
+        8,
+    )
+    message = shape((tokens, rest * value_width), jnp.bfloat16)
+    rest_next, rest_later = kernel_call(
+        functools.partial(serve_rest_kernel, first, rest),
+        [scores, earlier[2], value],
+        [message] * 2,
+        2 * rest * work,
+        8,
+    )
+    nears = [lax.ppermute(given_next, "sp", [(1, 2)]), lax.ppermute(rest_next, "sp", [(1, 2)])]
+    fars = [lax.ppermute(given_later, "sp", [(1, 3)]), lax.ppermute(rest_later, "sp", [(1, 3)])]
     home = kernel_call(
         functools.partial(join_kernel, COUNTS),
         [*earlier, query, *own],
@@ -374,13 +428,27 @@
         3 * heads * work // 2,
         8,
     )
-    columns = out_weight.shape[1] * device_count
+    width = out_weight.shape[1]
+    kept = kernel_call(
+        functools.partial(first_kernel, COUNTS),
+        [gate, *home[:2], nears[0], fars[0], *whole.values()],
+        [
+            shape((tokens, first * value_width), jnp.bfloat16),
+            shape((tokens, LANES), jnp.float32),
+            shape((tokens, len(whole) * width), jnp.float32),
+        ],
+        2 * tokens * first * value_width * len(whole) * width,
+        10,
+    )
     (out,) = kernel_call(
-        functools.partial(finish_kernel, tuple((mask, start) for mask, start, _ in pieces), COUNTS),
-        [gate, *home[::2], *home[1::2], *nears, *fars, *(piece for _, _, piece in pieces)],
-        [shape((tokens, columns), jnp.bfloat16)],
-        2 * tokens * value.shape[1] * columns,
-        16,
+        functools.partial(finish_kernel, COUNTS, tuple(whole), tuple(place for place, _ in corner)),
+        [
+            gate, *home[2:], nears[1], fars[1], *kept, *whole.values(),
+            *(piece for _, piece in corner),
+        ],
+        [shape((tokens, width * device_count), jnp.bfloat16)],
+        2 * tokens * rest * value_width * width * device_count,
+        12,
     )
     return out
 

time: 74 us -> 81.1 us (1.096)
  waiting for transfers between devices: 37.2 us -> 45.8 us
  starting transfers between devices: 27.5 us -> 25.6 us
    ppermute x9, waiting for transfers between devices: 1.48 us -> 6.09 us  [swap(): lax.ppermute(piece, 'dp', [(i, i ^ bit) for i in range(device_count)])]
    ppermute x4, waiting for transfers between devices: 16.6 us -> 20.5 us  [the longest x1 12.7 us: block_steps(): lax.ppermute(given_later, 'sp', [(1, 3)])]
    ppermute x9, starting transfers between devices: 16.3 us -> 14.5 us  [swap(): lax.ppermute(piece, 'dp', [(i, i ^ bit) for i in range(device_count)])]
    pallas_call x6 -> x7, Pallas kernels: 5.95 us -> 6.45 us  [kernel_call(): pl.pallas_call(kernel, out_shape=outs, in_specs=[vmem] * len(operands), o...]
  transfers between devices with their start and end apart: 18 -> 18, of which waited for: 5 -> 6; matrix products, arithmetic and copies ran while one was open for 0% -> 0% of each run, Pallas kernels for 4% -> 5%
where the time goes in v5:
time: 81.1 us; the launch traced here: 80.8 us
  waiting for transfers between devices  45.8 us (56%)
  starting transfers between devices  25.6 us (32%)
  Pallas kernels  6.45 us (8%)
  local copies, waits for them, and re-layouts  2.77 us (3%)
    ppermute x1, waiting for transfers between devices, block_steps(): lax.ppermute(gates, 'sp', pair)  15.2 us
    ppermute x9, starting transfers between devices, swap(): lax.ppermute(piece, 'dp', [(i, i ^ bit) for i in range(device_count)])  14.5 us
    ppermute x1, waiting for transfers between devices, block_steps(): lax.ppermute(given_later, 'sp', [(1, 3)])  12.7 us
    ppermute x1, waiting for transfers between devices, block_steps(): lax.ppermute(rest_later, 'sp', [(1, 3)])  7.81 us
    pallas_call x7, Pallas kernels, kernel_call(): pl.pallas_call(kernel, out_shape=outs, in_specs=[vmem] * len(operands), o...  6.45 us
    ppermute x9, waiting for transfers between devices, swap(): lax.ppermute(piece, 'dp', [(i, i ^ bit) for i in range(device_count)])  6.09 us
    ppermute x1, waiting for transfers between devices, block_steps(): far = lax.ppermute(query, 'sp', [(3, 1)])  3.93 us
    unnamed x18, local copies, waits for them, and re-layouts  2.69 us
  transfers between devices with their start and end apart: 18, of which 6 were waited for; matrix products, arithmetic and copies ran while one was open for 0% of the time, Pallas kernels for 5%

profile of v5, /device:TPU:25, one launch (start us, length us, event | category | flops | bytes accessed | tf_op | source)
XLA Modules:
  0.0 80.8 jit_solution(14400158063604097818)
XLA Ops:
  0.0 1.2 %collective-permute-start.10 = (bf16[2048,256]{1,0:T(8,128)(2,1)}, bf16[2048,256]{1,0:T(8,128)(2,1)S(1)}, u32[]{:S(2)}, u32[]{:S(2)}) collective-permute-start(bf16[2048,256]{1,0:T(8,128)(2,1)} %refs_0_.3), channel_id=1, source_target_pairs={{0,2},{1,3},{2,0},{3,1},{4,6},{5,7},{6,4},{7,5},{8,10},{9,11},{10,... | collective-permute-start | bytes 3145736 | tf_op jit(solution)/shard_map/ppermute | solution.py:357
  1.2 1.2 %collective-permute-start.12 = (bf16[2048,256]{1,0:T(8,128)(2,1)}, bf16[2048,256]{1,0:T(8,128)(2,1)S(1)}, u32[]{:S(2)}, u32[]{:S(2)}) collective-permute-start(bf16[2048,256]{1,0:T(8,128)(2,1)} %refs_0_.3), channel_id=1, source_target_pairs={{0,4},{1,5},{2,6},{3,7},{4,0},{5,1},{6,2},{7,3},{8,12},{9,13},{10,... | collective-permute-start | bytes 3145736 | tf_op jit(solution)/shard_map/ppermute | solution.py:357
  2.5 1.3 %collective-permute-start.1 = (bf16[128,1024]{1,0:T(8,128)(2,1)}, bf16[128,1024]{1,0:T(8,128)(2,1)S(1)}, u32[]{:S(2)}, u32[]{:S(2)}) collective-permute-start(bf16[128,1024]{1,0:T(8,128)(2,1)} %bitcast.17), channel_id=1, source_target_pairs={{0,8},{16,24},{1,9},{17,25},{2,10},{18,26},{3,11},{19,27},{4,12},{... | collective-permute-start | bytes 786440 | tf_op jit(solution)/shard_map/ppermute | solution.py:365
  3.7 1.3 %collective-permute-start.2 = (bf16[128,2048]{1,0:T(8,128)(2,1)}, bf16[128,2048]{1,0:T(8,128)(2,1)S(1)}, u32[]{:S(2)}, u32[]{:S(2)}) collective-permute-start(bf16[128,2048]{1,0:T(8,128)(2,1)} %bitcast.7), channel_id=1, source_target_pairs={{0,8},{16,24},{1,9},{17,25},{2,10},{18,26},{3,11},{19,27},{4,12},{... | collective-permute-start | bytes 1572872 | tf_op jit(solution)/shard_map/ppermute | solution.py:366
  5.0 0.0 copy-start.8
  5.0 0.0 copy-start.7
  5.1 0.7 copy-done.8
  5.7 0.0 copy-done.7
  5.7 0.2 shard_map.73.gates_ref
  6.0 1.3 %collective-permute-start = (f32[8,128]{1,0:T(8,128)S(1)}, f32[8,128]{1,0:T(8,128)S(1)}, u32[]{:S(2)}, u32[]{:S(2)}) collective-permute-start(f32[8,128]{1,0:T(8,128)S(1)} %shard_map.73.gates_ref), channel_id=1, source_target_pairs={{0,8},{16,24},{1,9},{17,25},{2,10},{18,26},{3,11},{19,27},{4,12},{... | collective-permute-start | bytes 12296 | tf_op jit(solution)/shard_map/ppermute | solution.py:364
  7.3 15.2 %collective-permute-done.gates0_ref = f32[8,128]{1,0:T(8,128)S(1)} collective-permute-done((f32[8,128]{1,0:T(8,128)S(1)}, f32[8,128]{1,0:T(8,128)S(1)}, u32[]{:S(2)}, u32[]{:S(2)}) %collective-permute-start) | collective-permute-done | bytes 4128 | tf_op jit(solution)/shard_map/ppermute | solution.py:364
  22.5 0.7 collective-permute-start.3
  23.2 0.0 collective-permute-done.1.key0_ref
  23.2 2.6 %collective-permute-start.4 = (bf16[128,1024]{1,0:T(8,128)(2,1)}, bf16[128,1024]{1,0:T(8,128)(2,1)S(1)}, u32[]{:S(2)}, u32[]{:S(2)}) collective-permute-start(bf16[128,1024]{1,0:T(8,128)(2,1)} %bitcast.14), channel_id=1, source_target_pairs={{24,8},{25,9},{26,10},{27,11},{28,12},{29,13},{30,14},{31,15}} | collective-permute-start | bytes 786440 | tf_op jit(solution)/shard_map/ppermute | solution.py:370
  25.8 0.0 collective-permute-done.3.near_ref
  25.8 3.9 %collective-permute-done.4.far_ref = bf16[128,1024]{1,0:T(8,128)(2,1)S(1)} collective-permute-done((bf16[128,1024]{1,0:T(8,128)(2,1)}, bf16[128,1024]{1,0:T(8,128)(2,1)S(1)}, u32[]{:S(2)}, u32[]{:S(2)}) %collective-permute-start.4) | collective-permute-done | bytes 262176 | tf_op jit(solution)/shard_map/ppermute | solution.py:370
  29.7 0.0 collective-permute-done.2.value0_ref
  29.7 0.0 copy-start
  29.7 1.0 %copy-done = bf16[1,128,2048]{2,1,0:T(8,128)(2,1)S(1)} copy-done((bf16[1,128,2048]{2,1,0:T(8,128)(2,1)S(1)}, bf16[1,128,2048]{2,1,0:T(8,128)(2,1)}, u32[]{:S(2)}) %copy-start) | copy-done | bytes 524312
  30.8 0.0 copy-start.5
  30.8 0.9 %copy-done.5 = bf16[1,128,1024]{2,1,0:T(8,128)(2,1)S(1)} copy-done((bf16[1,128,1024]{2,1,0:T(8,128)(2,1)S(1)}, bf16[1,128,1024]{2,1,0:T(8,128)(2,1)}, u32[]{:S(2)}) %copy-start.5) | copy-done | bytes 262168
  31.7 0.0 copy-start.2
  31.7 0.7 shard_map.76
  32.4 0.7 collective-permute-start.7
  33.1 1.3 %collective-permute-start.8 = (bf16[128,1152]{1,0:T(8,128)(2,1)S(1)}, bf16[128,1152]{1,0:T(8,128)(2,1)S(1)}, u32[]{:S(2)}, u32[]{:S(2)}) collective-permute-start(bf16[128,1152]{1,0:T(8,128)(2,1)S(1)} %get-tuple-element.33), channel_id=1, source_target_pairs={{8,24},{9,25},{10,26},{11,27},{12,28},{13,29},{14,30},{15,31}} | collective-permute-start | bytes 884744 | tf_op jit(solution)/shard_map/ppermute | solution.py:423
  34.4 0.0 copy-done.2
  34.4 3.0 %collective-permute-start.9 = (bf16[2048,256]{1,0:T(8,128)(2,1)S(1)}, bf16[2048,256]{1,0:T(8,128)(2,1)S(1)}, u32[]{:S(2)}, u32[]{:S(2)}) collective-permute-start(bf16[2048,256]{1,0:T(8,128)(2,1)S(1)} %copy-done.2), channel_id=1, source_target_pairs={{0,1},{1,0},{2,3},{3,2},{4,5},{5,4},{6,7},{7,6},{8,9},{9,8},{10,11... | collective-permute-start | bytes 3145736 | tf_op jit(solution)/shard_map/ppermute | solution.py:357
  37.4 0.0 collective-permute-done.10.refs_2_
  37.4 0.1 collective-permute-start.11
  37.5 0.0 collective-permute-done.12.refs_4_
  37.5 0.4 collective-permute-start.13
  38.0 0.0 copy-start.1
  38.0 0.0 collective-permute-done.7.near_ref
  38.0 0.3 collective-permute-start.14
  38.3 12.7 %collective-permute-done.8.far_ref = bf16[128,1152]{1,0:T(8,128)(2,1)S(1)} collective-permute-done((bf16[128,1152]{1,0:T(8,128)(2,1)S(1)}, bf16[128,1152]{1,0:T(8,128)(2,1)S(1)}, u32[]{:S(2)}, u32[]{:S(2)}) %collective-permute-start.8) | collective-permute-done | bytes 294944 | tf_op jit(solution)/shard_map/ppermute | solution.py:423
  51.0 0.3 collective-permute-start.15
  51.3 0.2 collective-permute-done.14.refs_6_
  51.5 3.6 %collective-permute-start.16 = (bf16[1024,256]{1,0:T(8,128)(2,1)S(1)}, bf16[1024,256]{1,0:T(8,128)(2,1)S(1)}, u32[]{:S(2)}, u32[]{:S(2)}) collective-permute-start(bf16[1024,256]{1,0:T(8,128)(2,1)S(1)} %collective-permute-done.14.refs_6_), channel_id=1, source_target_pairs={{0,1},{1,0},{2,3},{3,2},{4,5},{5,4},{6,7},{7,6},{8,9},{9,8},{10,11... | collective-permute-start | bytes 1572872 | tf_op jit(solution)/shard_map/ppermute | solution.py:357
  55.1 5.9 %collective-permute-done.15.refs_7_ = bf16[1024,256]{1,0:T(8,128)(2,1)S(1)} collective-permute-done((bf16[1024,256]{1,0:T(8,128)(2,1)S(1)}, bf16[1024,256]{1,0:T(8,128)(2,1)S(1)}, u32[]{:S(2)}, u32[]{:S(2)}) %collective-permute-start.15) | collective-permute-done | bytes 524320 | tf_op jit(solution)/shard_map/ppermute | solution.py:357
  61.0 4.4 %collective-permute-start.17 = (bf16[1024,256]{1,0:T(8,128)(2,1)S(1)}, bf16[1024,256]{1,0:T(8,128)(2,1)S(1)}, u32[]{:S(2)}, u32[]{:S(2)}) collective-permute-start(bf16[1024,256]{1,0:T(8,128)(2,1)S(1)} %collective-permute-done.15.refs_7_), channel_id=1, source_target_pairs={{0,1},{1,0},{2,3},{3,2},{4,5},{5,4},{6,7},{7,6},{8,9},{9,8},{10,11... | collective-permute-start | bytes 1572872 | tf_op jit(solution)/shard_map/ppermute | solution.py:357
  65.4 0.0 copy-done.1
  65.4 0.0 copy-start.4
  65.4 0.0 copy-start.6
  65.4 0.3 shard_map.77
  65.7 0.0 collective-permute-done.9.refs_1_
  65.7 0.7 collective-permute-start.5
  66.4 0.0 collective-permute-done.11.refs_3_
  66.4 1.3 %collective-permute-start.6 = (bf16[128,1024]{1,0:T(8,128)(2,1)S(1)}, bf16[128,1024]{1,0:T(8,128)(2,1)S(1)}, u32[]{:S(2)}, u32[]{:S(2)}) collective-permute-start(bf16[128,1024]{1,0:T(8,128)(2,1)S(1)} %get-tuple-element.29), channel_id=1, source_target_pairs={{8,24},{9,25},{10,26},{11,27},{12,28},{13,29},{14,30},{15,31}} | collective-permute-start | bytes 786440 | tf_op jit(solution)/shard_map/ppermute | solution.py:423
  67.7 0.0 copy-done.4
  67.7 0.0 copy-done.6
  67.7 0.7 shard_map.74
  68.4 0.0 copy-start.3
  68.4 1.1 %shard_map.75 = (f32[128,1024]{1,0:T(8,128)S(1)}, f32[128,128]{1,0:T(8,128)S(1)}, f32[128,1024]{1,0:T(8,128)S(1)}, f32[128,128]{1,0:T(8,128)S(1)}) custom-call(f32[8,128]{1,0:T(8,128)S(1)} %collective-permute-done.gates0_ref, bf16[128,1024]{1,0:T(8,128)(2,1)S(1)} %collective-permute-done.1.key0_ref, bf16[128,2048]{1,0:T(8,128)(2,1)S(1)} %collective-permute-done.2.value0_ref, ...), custom_call_target="tpu_custom_call" | custom-call | flops 150994944 | bytes 3411968 | tf_op jit(solution)/shard_map/pallas_call | solution.py:334
  69.5 0.0 collective-permute-done.13.refs_5_
  69.5 0.0 copy-done.3
  69.5 1.2 %shard_map.78 = (bf16[128,1024]{1,0:T(8,128)(2,1)S(1)}, f32[128,128]{1,0:T(8,128)S(1)}, f32[128,1536]{1,0:T(8,128)S(1)}) custom-call(bf16[128,2048]{1,0:T(8,128)(2,1)S(1)} %bitcast.11, f32[128,1024]{1,0:T(8,128)S(1)} %get-tuple-element.30.total_ref, f32[128,128]{1,0:T(8,128)S(1)} %get-tuple-element.31.note_ref, ...), custom_call_target="tpu_custom_call" | custom-call | flops 402653184 | bytes 9109504 | tf_op jit(solution)/shard_map/pallas_call | solution.py:334
  70.7 0.0 collective-permute-done.5.near_ref
  70.7 7.8 %collective-permute-done.6.far_ref = bf16[128,1024]{1,0:T(8,128)(2,1)S(1)} collective-permute-done((bf16[128,1024]{1,0:T(8,128)(2,1)S(1)}, bf16[128,1024]{1,0:T(8,128)(2,1)S(1)}, u32[]{:S(2)}, u32[]{:S(2)}) %collective-permute-start.6) | collective-permute-done | bytes 262176 | tf_op jit(solution)/shard_map/ppermute | solution.py:423
  78.5 0.0 collective-permute-done.16.refs_8_
  78.5 0.0 collective-permute-done.17.refs_9_
  78.5 2.3 %shard_map.79 = bf16[128,2048]{1,0:T(8,128)(2,1)} custom-call(bf16[128,2048]{1,0:T(8,128)(2,1)S(1)} %bitcast.12, f32[128,1024]{1,0:T(8,128)S(1)} %get-tuple-element.25.total_ref, f32[128,128]{1,0:T(8,128)S(1)} %get-tuple-element.26.note_ref, bf16[128,1024]{1,0:T(8,128)(2,1)S(1)} %collective-permute-done.5.near_ref, ...), custom_call_target="tpu_custom_call" | custom-call | flops 536870912 | bytes 11665408 | tf_op jit(solution)/shard_map/pallas_call | solution.py:334
  (2 shorter events, 0.1 us)
Async XLA Ops:
  0.0 37.4 %collective-permute-start.10 = (bf16[2048,256]{1,0:T(8,128)(2,1)}, bf16[2048,256]{1,0:T(8,128)(2,1)S(1)}, u32[]{:S(2)}, u32[]{:S(2)}) collective-permute-start(bf16[2048,256]{1,0:T(8,128)(2,1)} %refs_0_.3), channel_id=1, source_target_pairs={{0,2},{1,3},{2,0},{3,1},{4,6},{5,7},{6,4},{7,5},{8,10},{9,11},{10,... | collective-permute-start | bytes 3145736 | tf_op jit(solution)/shard_map/ppermute | solution.py:357
  1.2 36.3 %collective-permute-start.12 = (bf16[2048,256]{1,0:T(8,128)(2,1)}, bf16[2048,256]{1,0:T(8,128)(2,1)S(1)}, u32[]{:S(2)}, u32[]{:S(2)}) collective-permute-start(bf16[2048,256]{1,0:T(8,128)(2,1)} %refs_0_.3), channel_id=1, source_target_pairs={{0,4},{1,5},{2,6},{3,7},{4,0},{5,1},{6,2},{7,3},{8,12},{9,13},{10,... | collective-permute-start | bytes 3145736 | tf_op jit(solution)/shard_map/ppermute | solution.py:357
  2.5 20.7 %collective-permute-start.1 = (bf16[128,1024]{1,0:T(8,128)(2,1)}, bf16[128,1024]{1,0:T(8,128)(2,1)S(1)}, u32[]{:S(2)}, u32[]{:S(2)}) collective-permute-start(bf16[128,1024]{1,0:T(8,128)(2,1)} %bitcast.17), channel_id=1, source_target_pairs={{0,8},{16,24},{1,9},{17,25},{2,10},{18,26},{3,11},{19,27},{4,12},{... | collective-permute-start | bytes 786440 | tf_op jit(solution)/shard_map/ppermute | solution.py:365
  3.7 26.0 %collective-permute-start.2 = (bf16[128,2048]{1,0:T(8,128)(2,1)}, bf16[128,2048]{1,0:T(8,128)(2,1)S(1)}, u32[]{:S(2)}, u32[]{:S(2)}) collective-permute-start(bf16[128,2048]{1,0:T(8,128)(2,1)} %bitcast.7), channel_id=1, source_target_pairs={{0,8},{16,24},{1,9},{17,25},{2,10},{18,26},{3,11},{19,27},{4,12},{... | collective-permute-start | bytes 1572872 | tf_op jit(solution)/shard_map/ppermute | solution.py:366
  5.0 0.7 copy-start.8
  5.0 0.7 copy-start.7
  6.0 16.5 %collective-permute-start = (f32[8,128]{1,0:T(8,128)S(1)}, f32[8,128]{1,0:T(8,128)S(1)}, u32[]{:S(2)}, u32[]{:S(2)}) collective-permute-start(f32[8,128]{1,0:T(8,128)S(1)} %shard_map.73.gates_ref), channel_id=1, source_target_pairs={{0,8},{16,24},{1,9},{17,25},{2,10},{18,26},{3,11},{19,27},{4,12},{... | collective-permute-start | bytes 12296 | tf_op jit(solution)/shard_map/ppermute | solution.py:364
  22.5 3.3 %collective-permute-start.3 = (bf16[128,1024]{1,0:T(8,128)(2,1)}, bf16[128,1024]{1,0:T(8,128)(2,1)S(1)}, u32[]{:S(2)}, u32[]{:S(2)}) collective-permute-start(bf16[128,1024]{1,0:T(8,128)(2,1)} %bitcast.13), channel_id=1, source_target_pairs={{16,8},{17,9},{18,10},{19,11},{20,12},{21,13},{22,14},{23,15}} | collective-permute-start | bytes 786440 | tf_op jit(solution)/shard_map/ppermute | solution.py:369
  23.2 6.5 %collective-permute-start.4 = (bf16[128,1024]{1,0:T(8,128)(2,1)}, bf16[128,1024]{1,0:T(8,128)(2,1)S(1)}, u32[]{:S(2)}, u32[]{:S(2)}) collective-permute-start(bf16[128,1024]{1,0:T(8,128)(2,1)} %bitcast.14), channel_id=1, source_target_pairs={{24,8},{25,9},{26,10},{27,11},{28,12},{29,13},{30,14},{31,15}} | collective-permute-start | bytes 786440 | tf_op jit(solution)/shard_map/ppermute | solution.py:370
  29.7 1.0 %copy-start = (bf16[1,128,2048]{2,1,0:T(8,128)(2,1)S(1)}, bf16[1,128,2048]{2,1,0:T(8,128)(2,1)}, u32[]{:S(2)}) copy-start(bf16[1,128,2048]{2,1,0:T(8,128)(2,1)} %param.9) | copy-start | bytes 1572868
  30.8 0.9 %copy-start.5 = (bf16[1,128,1024]{2,1,0:T(8,128)(2,1)S(1)}, bf16[1,128,1024]{2,1,0:T(8,128)(2,1)}, u32[]{:S(2)}) copy-start(bf16[1,128,1024]{2,1,0:T(8,128)(2,1)} %param.8) | copy-start | bytes 786436
  31.7 2.7 %copy-start.2 = (bf16[2048,256]{1,0:T(8,128)(2,1)S(1)}, bf16[2048,256]{1,0:T(8,128)(2,1)}, u32[]{:S(2)}) copy-start(bf16[2048,256]{1,0:T(8,128)(2,1)} %refs_0_.3) | copy-start | bytes 3145732
  32.4 5.6 %collective-permute-start.7 = (bf16[128,1152]{1,0:T(8,128)(2,1)S(1)}, bf16[128,1152]{1,0:T(8,128)(2,1)S(1)}, u32[]{:S(2)}, u32[]{:S(2)}) collective-permute-start(bf16[128,1152]{1,0:T(8,128)(2,1)S(1)} %get-tuple-element.32), channel_id=1, source_target_pairs={{8,16},{9,17},{10,18},{11,19},{12,20},{13,21},{14,22},{15,23}} | collective-permute-start | bytes 884744 | tf_op jit(solution)/shard_map/ppermute | solution.py:422
  33.1 17.9 %collective-permute-start.8 = (bf16[128,1152]{1,0:T(8,128)(2,1)S(1)}, bf16[128,1152]{1,0:T(8,128)(2,1)S(1)}, u32[]{:S(2)}, u32[]{:S(2)}) collective-permute-start(bf16[128,1152]{1,0:T(8,128)(2,1)S(1)} %get-tuple-element.33), channel_id=1, source_target_pairs={{8,24},{9,25},{10,26},{11,27},{12,28},{13,29},{14,30},{15,31}} | collective-permute-start | bytes 884744 | tf_op jit(solution)/shard_map/ppermute | solution.py:423
  34.4 31.2 %collective-permute-start.9 = (bf16[2048,256]{1,0:T(8,128)(2,1)S(1)}, bf16[2048,256]{1,0:T(8,128)(2,1)S(1)}, u32[]{:S(2)}, u32[]{:S(2)}) collective-permute-start(bf16[2048,256]{1,0:T(8,128)(2,1)S(1)} %copy-done.2), channel_id=1, source_target_pairs={{0,1},{1,0},{2,3},{3,2},{4,5},{5,4},{6,7},{7,6},{8,9},{9,8},{10,11... | collective-permute-start | bytes 3145736 | tf_op jit(solution)/shard_map/ppermute | solution.py:357
  37.4 29.0 %collective-permute-start.11 = (bf16[2048,256]{1,0:T(8,128)(2,1)S(1)}, bf16[2048,256]{1,0:T(8,128)(2,1)S(1)}, u32[]{:S(2)}, u32[]{:S(2)}) collective-permute-start(bf16[2048,256]{1,0:T(8,128)(2,1)S(1)} %collective-permute-done.10.refs_2_), channel_id=1, source_target_pairs={{0,1},{1,0},{2,3},{3,2},{4,5},{5,4},{6,7},{7,6},{8,9},{9,8},{10,11... | collective-permute-start | bytes 3145736 | tf_op jit(solution)/shard_map/ppermute | solution.py:357
  37.5 32.0 %collective-permute-start.13 = (bf16[2048,256]{1,0:T(8,128)(2,1)S(1)}, bf16[2048,256]{1,0:T(8,128)(2,1)S(1)}, u32[]{:S(2)}, u32[]{:S(2)}) collective-permute-start(bf16[2048,256]{1,0:T(8,128)(2,1)S(1)} %collective-permute-done.12.refs_4_), channel_id=1, source_target_pairs={{0,1},{1,0},{2,3},{3,2},{4,5},{5,4},{6,7},{7,6},{8,9},{9,8},{10,11... | collective-permute-start | bytes 3145736 | tf_op jit(solution)/shard_map/ppermute | solution.py:357
  38.0 27.4 %copy-start.1 = (bf16[1,128,2048]{2,1,0:T(8,128)(2,1)S(1)}, bf16[1,128,2048]{2,1,0:T(8,128)(2,1)}, u32[]{:S(2)}) copy-start(bf16[1,128,2048]{2,1,0:T(8,128)(2,1)} %param.9) | copy-start | bytes 1572868
  38.0 13.5 %collective-permute-start.14 = (bf16[1024,256]{1,0:T(8,128)(2,1)S(1)}, bf16[1024,256]{1,0:T(8,128)(2,1)S(1)}, u32[]{:S(2)}, u32[]{:S(2)}) collective-permute-start(bf16[1024,256]{1,0:T(8,128)(2,1)S(1)} %slice.8), channel_id=1, source_target_pairs={{0,4},{1,5},{2,6},{3,7},{4,0},{5,1},{6,2},{7,3},{8,12},{9,13},{10,... | collective-permute-start | bytes 1572872 | tf_op jit(solution)/shard_map/ppermute | solution.py:357
  51.0 9.9 %collective-permute-start.15 = (bf16[1024,256]{1,0:T(8,128)(2,1)S(1)}, bf16[1024,256]{1,0:T(8,128)(2,1)S(1)}, u32[]{:S(2)}, u32[]{:S(2)}) collective-permute-start(bf16[1024,256]{1,0:T(8,128)(2,1)S(1)} %slice.9), channel_id=1, source_target_pairs={{0,2},{1,3},{2,0},{3,1},{4,6},{5,7},{6,4},{7,5},{8,10},{9,11},{10,... | collective-permute-start | bytes 1572872 | tf_op jit(solution)/shard_map/ppermute | solution.py:357
  51.5 27.0 %collective-permute-start.16 = (bf16[1024,256]{1,0:T(8,128)(2,1)S(1)}, bf16[1024,256]{1,0:T(8,128)(2,1)S(1)}, u32[]{:S(2)}, u32[]{:S(2)}) collective-permute-start(bf16[1024,256]{1,0:T(8,128)(2,1)S(1)} %collective-permute-done.14.refs_6_), channel_id=1, source_target_pairs={{0,1},{1,0},{2,3},{3,2},{4,5},{5,4},{6,7},{7,6},{8,9},{9,8},{10,11... | collective-permute-start | bytes 1572872 | tf_op jit(solution)/shard_map/ppermute | solution.py:357
  61.0 17.6 %collective-permute-start.17 = (bf16[1024,256]{1,0:T(8,128)(2,1)S(1)}, bf16[1024,256]{1,0:T(8,128)(2,1)S(1)}, u32[]{:S(2)}, u32[]{:S(2)}) collective-permute-start(bf16[1024,256]{1,0:T(8,128)(2,1)S(1)} %collective-permute-done.15.refs_7_), channel_id=1, source_target_pairs={{0,1},{1,0},{2,3},{3,2},{4,5},{5,4},{6,7},{7,6},{8,9},{9,8},{10,11... | collective-permute-start | bytes 1572872 | tf_op jit(solution)/shard_map/ppermute | solution.py:357
  65.4 2.3 %copy-start.4 = (bf16[1,128,1024]{2,1,0:T(8,128)(2,1)S(1)}, bf16[1,128,1024]{2,1,0:T(8,128)(2,1)}, u32[]{:S(2)}) copy-start(bf16[1,128,1024]{2,1,0:T(8,128)(2,1)} %param.7) | copy-start | bytes 786436
  65.4 2.3 %copy-start.6 = (bf16[1,128,1024]{2,1,0:T(8,128)(2,1)S(1)}, bf16[1,128,1024]{2,1,0:T(8,128)(2,1)}, u32[]{:S(2)}) copy-start(bf16[1,128,1024]{2,1,0:T(8,128)(2,1)} %param.8) | copy-start | bytes 786436
  65.7 5.0 %collective-permute-start.5 = (bf16[128,1024]{1,0:T(8,128)(2,1)S(1)}, bf16[128,1024]{1,0:T(8,128)(2,1)S(1)}, u32[]{:S(2)}, u32[]{:S(2)}) collective-permute-start(bf16[128,1024]{1,0:T(8,128)(2,1)S(1)} %get-tuple-element.28), channel_id=1, source_target_pairs={{8,16},{9,17},{10,18},{11,19},{12,20},{13,21},{14,22},{15,23}} | collective-permute-start | bytes 786440 | tf_op jit(solution)/shard_map/ppermute | solution.py:422
  66.4 12.1 %collective-permute-start.6 = (bf16[128,1024]{1,0:T(8,128)(2,1)S(1)}, bf16[128,1024]{1,0:T(8,128)(2,1)S(1)}, u32[]{:S(2)}, u32[]{:S(2)}) collective-permute-start(bf16[128,1024]{1,0:T(8,128)(2,1)S(1)} %get-tuple-element.29), channel_id=1, source_target_pairs={{8,24},{9,25},{10,26},{11,27},{12,28},{13,29},{14,30},{15,31}} | collective-permute-start | bytes 786440 | tf_op jit(solution)/shard_map/ppermute | solution.py:423
  68.4 1.1 %copy-start.3 = (bf16[1,128,2048]{2,1,0:T(8,128)(2,1)S(1)}, bf16[1,128,2048]{2,1,0:T(8,128)(2,1)}, u32[]{:S(2)}) copy-start(bf16[1,128,2048]{2,1,0:T(8,128)(2,1)} %param.10) | copy-start | bytes 1572868

commit v6 on v5

--- a/solution.py
+++ b/solution.py
@@ -161,10 +161,11 @@
         first += count
 
 
-def join_kernel(counts, gates0_ref, key0_ref, value0_ref, query_ref, *refs):
+def join_kernel(counts, gates0_ref, key0_ref, *refs):
     chunks, heads = len(counts), sum(counts)
+    values0, query_ref, refs = refs[:chunks], refs[chunks], refs[chunks + 1 :]
     tokens = query_ref.shape[0]
-    key_width, value_width = query_ref.shape[1] // heads, value0_ref.shape[1] // heads
+    key_width, value_width = query_ref.shape[1] // heads, values0[0].shape[1] // counts[0]
     block = lax.axis_index("sp")
     second = lax.rem(block, 2) == 1
     level0, end0 = levels(gates0_ref)
@@ -183,7 +184,6 @@
         for head in range(first, first + count):
             pick = slice(head, head + 1)
             keys = slice(head * key_width, (head + 1) * key_width)
-            channels = slice(head * value_width, (head + 1) * value_width)
             place = head - first
             out = slice(place * value_width, (place + 1) * value_width)
             own_top = own[:, 2 * place + 1 : 2 * place + 2]
@@ -193,7 +193,7 @@
             scores = times_transpose(query_ref[:, keys], key0_ref[:, keys])
             scores = scores * weight0[pick] * scale0
             total_ref[:, out] = scale * own_total[:, out] + two_term_dot(
-                scores, value0_ref[:, channels]
+                scores, values0[chunk][:, out]
             )
             sums = scale * own[:, 2 * place : 2 * place + 1] + jnp.sum(
                 scores, axis=1, keepdims=True
@@ -226,7 +226,7 @@
         scores = scores.astype(jnp.bfloat16)
         if head < count:
             channels = slice(head * value_width, (head + 1) * value_width)
-            give(scores, value0_ref, value_ref, channels, next_ref, later_ref, channels)
+            give(scores, value0_ref[:, channels], value_ref[:, channels], next_ref, later_ref, channels)
         else:
             place = head - count
             score_ref[:, place * 2 * tokens : (place + 1) * 2 * tokens] = scores
@@ -237,9 +237,9 @@
     later_ref[:, count * value_width :] = to_lanes(later_notes, tokens).astype(jnp.bfloat16)
 
 
-def give(scores, value0_ref, value_ref, channels, next_ref, later_ref, out):
-    tokens = value_ref.shape[0]
-    values = jnp.concatenate([value0_ref[:, channels], value_ref[:, channels]], axis=0)
+def give(scores, value0, value1, next_ref, later_ref, out):
+    tokens = value1.shape[0]
+    values = jnp.concatenate([value0, value1], axis=0)
     given = jnp.dot(scores, values, preferred_element_type=jnp.float32).astype(jnp.bfloat16)
     next_ref[:, out] = given[:tokens]
     later_ref[:, out] = given[tokens:]
@@ -252,7 +252,7 @@
         channels = slice((first + place) * value_width, (first + place + 1) * value_width)
         out = slice(place * value_width, (place + 1) * value_width)
         scores = score_ref[:, place * width : (place + 1) * width]
-        give(scores, value0_ref, value_ref, channels, next_ref, later_ref, out)
+        give(scores, value0_ref[:, out], value_ref[:, channels], next_ref, later_ref, out)
 
 
 def gated_rows(heads, first, count, total_ref, note_ref, near_ref, far_ref, lanes, gate_ref):
@@ -360,10 +360,11 @@
         gates_kernel, [input_log, forget], [shape((2 * heads, tokens), jnp.float32)], 0, 2
     )
     pair = [(0, 1), (2, 3)]
-    earlier = [
-        lax.ppermute(gates, "sp", pair),
-        lax.ppermute(key, "sp", pair),
-        lax.ppermute(value, "sp", pair),
+    first, rest = COUNTS
+    split = first * value_width
+    earlier = [lax.ppermute(gates, "sp", pair), lax.ppermute(key, "sp", pair)]
+    values0 = [
+        lax.ppermute(value[:, :split], "sp", pair), lax.ppermute(value[:, split:], "sp", pair)
     ]
     here = [gates, key, value]
     near = lax.ppermute(query, "sp", [(2, 1)])
@@ -402,11 +403,10 @@
     own = kernel_call(
         functools.partial(own_kernel, COUNTS), [*here, query], sums, 3 * heads * work // 2, 8
     )
-    first, rest = COUNTS
     message = shape((tokens, first * value_width + LANES), jnp.bfloat16)
     given_next, given_later, scores = kernel_call(
         functools.partial(serve_kernel, COUNTS),
-        [*earlier, *here, near, far],
+        [*earlier, values0[0], *here, near, far],
         [message, message, shape((2 * tokens, rest * 2 * tokens), jnp.bfloat16)],
         4 * heads * work,
         8,
@@ -414,7 +414,7 @@
     message = shape((tokens, rest * value_width), jnp.bfloat16)
     rest_next, rest_later = kernel_call(
         functools.partial(serve_rest_kernel, first, rest),
-        [scores, earlier[2], value],
+        [scores, values0[1], value],
         [message] * 2,
         2 * rest * work,
         8,
@@ -423,7 +423,7 @@
     fars = [lax.ppermute(given_later, "sp", [(1, 3)]), lax.ppermute(rest_later, "sp", [(1, 3)])]
     home = kernel_call(
         functools.partial(join_kernel, COUNTS),
-        [*earlier, query, *own],
+        [*earlier, *values0, query, *own],
         sums,
         3 * heads * work // 2,
         8,

time: 81.1 us -> 74.4 us (0.917)
  waiting for transfers between devices: 45.8 us -> 40 us
  local copies, waits for them, and re-layouts: 2.77 us -> 1.25 us
    ppermute x3 -> x4, waiting for transfers between devices: 15.2 us -> 10.9 us  [the longest x2 10.1 us: block_steps(): earlier = [lax.ppermute(gates, 'sp', pair), lax.ppermute(key, 'sp', pair)]]
    unnamed x18 -> x14, local copies, waits for them, and re-layouts: 2.69 us -> 0.03 us
    ppermute x1, waiting for transfers between devices: 3.93 us -> 2.3 us  [block_steps(): far = lax.ppermute(query, 'sp', [(3, 1)])]
    ppermute x3 -> x4, starting transfers between devices: 3.87 us -> 5.3 us  [the longest x2 2.59 us: block_steps(): earlier = [lax.ppermute(gates, 'sp', pair), lax.ppermute(key, 'sp', pair)]]
    ppermute x9, waiting for transfers between devices: 6.09 us -> 7.44 us  [swap(): lax.ppermute(piece, 'dp', [(i, i ^ bit) for i in range(device_count)])]
    slice x0 -> x1, local copies, waits for them, and re-layouts: none -> 1.15 us  [block_steps(): value[:, split:]]
    ppermute x1, waiting for transfers between devices: 12.7 us -> 11.6 us  [block_steps(): lax.ppermute(given_later, 'sp', [(1, 3)])]
  transfers between devices with their start and end apart: 18 -> 19, of which waited for: 6 -> 7; matrix products, arithmetic and copies ran while one was open for 0% -> 2% of each run, Pallas kernels for 5% -> 6%
where the time goes in v6:
time: 74.4 us; the launch traced here: 74.2 us
  waiting for transfers between devices  40 us (54%)
  starting transfers between devices  26.2 us (35%)
  Pallas kernels  6.4 us (9%)
  local copies, waits for them, and re-layouts  1.25 us (2%)
    ppermute x9, starting transfers between devices, swap(): lax.ppermute(piece, 'dp', [(i, i ^ bit) for i in range(device_count)])  13.7 us
    ppermute x1, waiting for transfers between devices, block_steps(): lax.ppermute(given_later, 'sp', [(1, 3)])  11.6 us
    ppermute x2, waiting for transfers between devices, block_steps(): earlier = [lax.ppermute(gates, 'sp', pair), lax.ppermute(key, 'sp', pair)]  10.1 us
    ppermute x1, waiting for transfers between devices, block_steps(): lax.ppermute(rest_later, 'sp', [(1, 3)])  7.86 us
    ppermute x9, waiting for transfers between devices, swap(): lax.ppermute(piece, 'dp', [(i, i ^ bit) for i in range(device_count)])  7.44 us
    pallas_call x7, Pallas kernels, kernel_call(): pl.pallas_call(kernel, out_shape=outs, in_specs=[vmem] * len(operands), o...  6.4 us
    ppermute x1, starting transfers between devices, block_steps(): far = lax.ppermute(query, 'sp', [(3, 1)])  2.59 us
    ppermute x2, starting transfers between devices, block_steps(): earlier = [lax.ppermute(gates, 'sp', pair), lax.ppermute(key, 'sp', pair)]  2.59 us
  transfers between devices with their start and end apart: 19, of which 7 were waited for; matrix products, arithmetic and copies ran while one was open for 2% of the time, Pallas kernels for 6%

profile of v6, /device:TPU:25, one launch (start us, length us, event | category | flops | bytes accessed | tf_op | source)
XLA Modules:
  0.0 74.2 jit_solution(1220488253111935065)
XLA Ops:
  0.0 1.2 %collective-permute-start.11 = (bf16[2048,256]{1,0:T(8,128)(2,1)}, bf16[2048,256]{1,0:T(8,128)(2,1)S(1)}, u32[]{:S(2)}, u32[]{:S(2)}) collective-permute-start(bf16[2048,256]{1,0:T(8,128)(2,1)} %refs_0_.3), channel_id=1, source_target_pairs={{0,2},{1,3},{2,0},{3,1},{4,6},{5,7},{6,4},{7,5},{8,10},{9,11},{10,... | collective-permute-start | bytes 3145736 | tf_op jit(solution)/shard_map/ppermute | solution.py:357
  1.2 1.2 %collective-permute-start.13 = (bf16[2048,256]{1,0:T(8,128)(2,1)}, bf16[2048,256]{1,0:T(8,128)(2,1)S(1)}, u32[]{:S(2)}, u32[]{:S(2)}) collective-permute-start(bf16[2048,256]{1,0:T(8,128)(2,1)} %refs_0_.3), channel_id=1, source_target_pairs={{0,4},{1,5},{2,6},{3,7},{4,0},{5,1},{6,2},{7,3},{8,12},{9,13},{10,... | collective-permute-start | bytes 3145736 | tf_op jit(solution)/shard_map/ppermute | solution.py:357
  2.5 0.0 copy-start.3
  2.5 0.0 copy-start.5
  2.5 0.0 copy-start.6
  2.5 0.0 copy-start.4
  2.5 0.0 copy-start
  2.5 1.2 %fusion = (bf16[128,1024]{1,0:T(8,128)(2,1)S(1)}, bf16[128,1024]{1,0:T(8,128)(2,1)S(1)}) fusion(bf16[128,2048]{1,0:T(8,128)(2,1)} %bitcast.7), kind=kLoop, calls=%fused_computation | loop fusion | bytes 1048576 | tf_op jit(solution)/shard_map/slice | solution.py:367
  3.6 0.0 copy-start.1
  3.6 1.4 %collective-permute-start.2 = (bf16[128,1024]{1,0:T(8,128)(2,1)S(1)}, bf16[128,1024]{1,0:T(8,128)(2,1)S(1)}, u32[]{:S(2)}, u32[]{:S(2)}) collective-permute-start(bf16[128,1024]{1,0:T(8,128)(2,1)S(1)} %get-tuple-element.38), channel_id=1, source_target_pairs={{0,8},{16,24},{1,9},{17,25},{2,10},{18,26},{3,11},{19,27},{4,12},{... | collective-permute-start | bytes 786440 | tf_op jit(solution)/shard_map/ppermute | solution.py:367
  5.1 0.0 copy-done.3
  5.1 1.3 %collective-permute-start.1 = (bf16[128,1024]{1,0:T(8,128)(2,1)S(1)}, bf16[128,1024]{1,0:T(8,128)(2,1)S(1)}, u32[]{:S(2)}, u32[]{:S(2)}) collective-permute-start(bf16[128,1024]{1,0:T(8,128)(2,1)S(1)} %bitcast.13), channel_id=1, source_target_pairs={{0,8},{16,24},{1,9},{17,25},{2,10},{18,26},{3,11},{19,27},{4,12},{... | collective-permute-start | bytes 786440 | tf_op jit(solution)/shard_map/ppermute | solution.py:365
  6.4 0.0 copy-done.5
  6.4 0.0 copy-done.6
  6.4 0.2 shard_map.73.gates_ref
  6.6 1.3 %collective-permute-start = (f32[8,128]{1,0:T(8,128)S(1)}, f32[8,128]{1,0:T(8,128)S(1)}, u32[]{:S(2)}, u32[]{:S(2)}) collective-permute-start(f32[8,128]{1,0:T(8,128)S(1)} %shard_map.73.gates_ref), channel_id=1, source_target_pairs={{0,8},{16,24},{1,9},{17,25},{2,10},{18,26},{3,11},{19,27},{4,12},{... | collective-permute-start | bytes 12296 | tf_op jit(solution)/shard_map/ppermute | solution.py:365
  7.9 10.1 %collective-permute-done.gates0_ref = f32[8,128]{1,0:T(8,128)S(1)} collective-permute-done((f32[8,128]{1,0:T(8,128)S(1)}, f32[8,128]{1,0:T(8,128)S(1)}, u32[]{:S(2)}, u32[]{:S(2)}) %collective-permute-start) | collective-permute-done | bytes 4128 | tf_op jit(solution)/shard_map/ppermute | solution.py:365
  18.0 0.0 copy-done.4
  18.0 0.7 collective-permute-start.4
  18.7 0.0 collective-permute-done.2.refs_0_.value0_ref
  18.7 2.6 %collective-permute-start.5 = (bf16[128,1024]{1,0:T(8,128)(2,1)S(1)}, bf16[128,1024]{1,0:T(8,128)(2,1)S(1)}, u32[]{:S(2)}, u32[]{:S(2)}) collective-permute-start(bf16[128,1024]{1,0:T(8,128)(2,1)S(1)} %bitcast.17), channel_id=1, source_target_pairs={{24,8},{25,9},{26,10},{27,11},{28,12},{29,13},{30,14},{31,15}} | collective-permute-start | bytes 786440 | tf_op jit(solution)/shard_map/ppermute | solution.py:371
  21.3 0.0 collective-permute-done.1.key0_ref
  21.3 1.3 %collective-permute-start.3 = (bf16[128,1024]{1,0:T(8,128)(2,1)S(1)}, bf16[128,1024]{1,0:T(8,128)(2,1)S(1)}, u32[]{:S(2)}, u32[]{:S(2)}) collective-permute-start(bf16[128,1024]{1,0:T(8,128)(2,1)S(1)} %get-tuple-element.37), channel_id=1, source_target_pairs={{0,8},{16,24},{1,9},{17,25},{2,10},{18,26},{3,11},{19,27},{4,12},{... | collective-permute-start | bytes 786440 | tf_op jit(solution)/shard_map/ppermute | solution.py:367
  22.6 0.0 collective-permute-done.4.near_ref
  22.6 2.3 %collective-permute-done.5.far_ref = bf16[128,1024]{1,0:T(8,128)(2,1)S(1)} collective-permute-done((bf16[128,1024]{1,0:T(8,128)(2,1)S(1)}, bf16[128,1024]{1,0:T(8,128)(2,1)S(1)}, u32[]{:S(2)}, u32[]{:S(2)}) %collective-permute-start.5) | collective-permute-done | bytes 262176 | tf_op jit(solution)/shard_map/ppermute | solution.py:371
  24.9 0.0 copy-done
  24.9 0.7 shard_map.76
  25.6 0.7 collective-permute-start.8
  26.3 1.3 %collective-permute-start.9 = (bf16[128,1152]{1,0:T(8,128)(2,1)S(1)}, bf16[128,1152]{1,0:T(8,128)(2,1)S(1)}, u32[]{:S(2)}, u32[]{:S(2)}) collective-permute-start(bf16[128,1152]{1,0:T(8,128)(2,1)S(1)} %get-tuple-element.33), channel_id=1, source_target_pairs={{8,24},{9,25},{10,26},{11,27},{12,28},{13,29},{14,30},{15,31}} | collective-permute-start | bytes 884744 | tf_op jit(solution)/shard_map/ppermute | solution.py:423
  27.6 0.8 %collective-permute-done.3.refs_1_.value0_ref = bf16[128,1024]{1,0:T(8,128)(2,1)S(1)} collective-permute-done((bf16[128,1024]{1,0:T(8,128)(2,1)S(1)}, bf16[128,1024]{1,0:T(8,128)(2,1)S(1)}, u32[]{:S(2)}, u32[]{:S(2)}) %collective-permute-start.3) | collective-permute-done | bytes 262176 | tf_op jit(solution)/shard_map/ppermute | solution.py:367
  28.4 0.0 copy-done.1
  28.4 3.5 %collective-permute-start.10 = (bf16[2048,256]{1,0:T(8,128)(2,1)S(1)}, bf16[2048,256]{1,0:T(8,128)(2,1)S(1)}, u32[]{:S(2)}, u32[]{:S(2)}) collective-permute-start(bf16[2048,256]{1,0:T(8,128)(2,1)S(1)} %copy-done.1), channel_id=1, source_target_pairs={{0,1},{1,0},{2,3},{3,2},{4,5},{5,4},{6,7},{7,6},{8,9},{9,8},{10,11... | collective-permute-start | bytes 3145736 | tf_op jit(solution)/shard_map/ppermute | solution.py:357
  31.9 0.0 collective-permute-done.11.refs_2_
  31.9 0.1 collective-permute-start.12
  32.0 0.0 collective-permute-done.13.refs_4_
  32.0 0.4 collective-permute-start.14
  32.5 0.0 collective-permute-done.8.near_ref
  32.5 0.3 collective-permute-start.15
  32.8 11.6 %collective-permute-done.9.far_ref = bf16[128,1152]{1,0:T(8,128)(2,1)S(1)} collective-permute-done((bf16[128,1152]{1,0:T(8,128)(2,1)S(1)}, bf16[128,1152]{1,0:T(8,128)(2,1)S(1)}, u32[]{:S(2)}, u32[]{:S(2)}) %collective-permute-start.9) | collective-permute-done | bytes 294944 | tf_op jit(solution)/shard_map/ppermute | solution.py:423
  44.4 0.3 collective-permute-start.16
  44.7 1.4 %collective-permute-done.15.refs_6_ = bf16[1024,256]{1,0:T(8,128)(2,1)S(1)} collective-permute-done((bf16[1024,256]{1,0:T(8,128)(2,1)S(1)}, bf16[1024,256]{1,0:T(8,128)(2,1)S(1)}, u32[]{:S(2)}, u32[]{:S(2)}) %collective-permute-start.15) | collective-permute-done | bytes 524320 | tf_op jit(solution)/shard_map/ppermute | solution.py:357
  46.0 2.4 %collective-permute-start.17 = (bf16[1024,256]{1,0:T(8,128)(2,1)S(1)}, bf16[1024,256]{1,0:T(8,128)(2,1)S(1)}, u32[]{:S(2)}, u32[]{:S(2)}) collective-permute-start(bf16[1024,256]{1,0:T(8,128)(2,1)S(1)} %collective-permute-done.15.refs_6_), channel_id=1, source_target_pairs={{0,1},{1,0},{2,3},{3,2},{4,5},{5,4},{6,7},{7,6},{8,9},{9,8},{10,11... | collective-permute-start | bytes 1572872 | tf_op jit(solution)/shard_map/ppermute | solution.py:357
  48.4 6.1 %collective-permute-done.16.refs_7_ = bf16[1024,256]{1,0:T(8,128)(2,1)S(1)} collective-permute-done((bf16[1024,256]{1,0:T(8,128)(2,1)S(1)}, bf16[1024,256]{1,0:T(8,128)(2,1)S(1)}, u32[]{:S(2)}, u32[]{:S(2)}) %collective-permute-start.16) | collective-permute-done | bytes 524320 | tf_op jit(solution)/shard_map/ppermute | solution.py:357
  54.5 4.3 %collective-permute-start.18 = (bf16[1024,256]{1,0:T(8,128)(2,1)S(1)}, bf16[1024,256]{1,0:T(8,128)(2,1)S(1)}, u32[]{:S(2)}, u32[]{:S(2)}) collective-permute-start(bf16[1024,256]{1,0:T(8,128)(2,1)S(1)} %collective-permute-done.16.refs_7_), channel_id=1, source_target_pairs={{0,1},{1,0},{2,3},{3,2},{4,5},{5,4},{6,7},{7,6},{8,9},{9,8},{10,11... | collective-permute-start | bytes 1572872 | tf_op jit(solution)/shard_map/ppermute | solution.py:357
  58.8 0.3 shard_map.77
  59.1 0.0 collective-permute-done.10.refs_1_
  59.1 0.7 collective-permute-start.6
  59.8 0.0 collective-permute-done.12.refs_3_
  59.8 1.3 %collective-permute-start.7 = (bf16[128,1024]{1,0:T(8,128)(2,1)S(1)}, bf16[128,1024]{1,0:T(8,128)(2,1)S(1)}, u32[]{:S(2)}, u32[]{:S(2)}) collective-permute-start(bf16[128,1024]{1,0:T(8,128)(2,1)S(1)} %get-tuple-element.29), channel_id=1, source_target_pairs={{8,24},{9,25},{10,26},{11,27},{12,28},{13,29},{14,30},{15,31}} | collective-permute-start | bytes 786440 | tf_op jit(solution)/shard_map/ppermute | solution.py:423
  61.1 0.7 shard_map.74
  61.8 0.0 copy-start.2
  61.8 1.1 %shard_map.75 = (f32[128,1024]{1,0:T(8,128)S(1)}, f32[128,128]{1,0:T(8,128)S(1)}, f32[128,1024]{1,0:T(8,128)S(1)}, f32[128,128]{1,0:T(8,128)S(1)}) custom-call(f32[8,128]{1,0:T(8,128)S(1)} %collective-permute-done.gates0_ref, bf16[128,1024]{1,0:T(8,128)(2,1)S(1)} %collective-permute-done.1.key0_ref, ...), custom_call_target="tpu_custom_call" | custom-call | flops 150994944 | bytes 3411968 | tf_op jit(solution)/shard_map/pallas_call | solution.py:334
  62.9 0.0 collective-permute-done.14.refs_5_
  62.9 0.0 copy-done.2
  62.9 1.2 %shard_map.78 = (bf16[128,1024]{1,0:T(8,128)(2,1)S(1)}, f32[128,128]{1,0:T(8,128)S(1)}, f32[128,1536]{1,0:T(8,128)S(1)}) custom-call(bf16[128,2048]{1,0:T(8,128)(2,1)S(1)} %bitcast.11, f32[128,1024]{1,0:T(8,128)S(1)} %get-tuple-element.30.total_ref, f32[128,128]{1,0:T(8,128)S(1)} %get-tuple-element.31.note_ref, ...), custom_call_target="tpu_custom_call" | custom-call | flops 402653184 | bytes 9109504 | tf_op jit(solution)/shard_map/pallas_call | solution.py:334
  64.0 0.0 collective-permute-done.6.near_ref
  64.1 7.9 %collective-permute-done.7.far_ref = bf16[128,1024]{1,0:T(8,128)(2,1)S(1)} collective-permute-done((bf16[128,1024]{1,0:T(8,128)(2,1)S(1)}, bf16[128,1024]{1,0:T(8,128)(2,1)S(1)}, u32[]{:S(2)}, u32[]{:S(2)}) %collective-permute-start.7) | collective-permute-done | bytes 262176 | tf_op jit(solution)/shard_map/ppermute | solution.py:423
  71.9 0.0 collective-permute-done.17.refs_8_
  71.9 0.0 collective-permute-done.18.refs_9_
  71.9 2.2 %shard_map.79 = bf16[128,2048]{1,0:T(8,128)(2,1)} custom-call(bf16[128,2048]{1,0:T(8,128)(2,1)S(1)} %bitcast.12, f32[128,1024]{1,0:T(8,128)S(1)} %get-tuple-element.25.total_ref, f32[128,128]{1,0:T(8,128)S(1)} %get-tuple-element.26.note_ref, bf16[128,1024]{1,0:T(8,128)(2,1)S(1)} %collective-permute-done.6.near_ref, ...), custom_call_target="tpu_custom_call" | custom-call | flops 536870912 | bytes 11665408 | tf_op jit(solution)/shard_map/pallas_call | solution.py:334
  (2 shorter events, 0.1 us)
Async XLA Ops:
  0.0 31.9 %collective-permute-start.11 = (bf16[2048,256]{1,0:T(8,128)(2,1)}, bf16[2048,256]{1,0:T(8,128)(2,1)S(1)}, u32[]{:S(2)}, u32[]{:S(2)}) collective-permute-start(bf16[2048,256]{1,0:T(8,128)(2,1)} %refs_0_.3), channel_id=1, source_target_pairs={{0,2},{1,3},{2,0},{3,1},{4,6},{5,7},{6,4},{7,5},{8,10},{9,11},{10,... | collective-permute-start | bytes 3145736 | tf_op jit(solution)/shard_map/ppermute | solution.py:357
  1.2 30.8 %collective-permute-start.13 = (bf16[2048,256]{1,0:T(8,128)(2,1)}, bf16[2048,256]{1,0:T(8,128)(2,1)S(1)}, u32[]{:S(2)}, u32[]{:S(2)}) collective-permute-start(bf16[2048,256]{1,0:T(8,128)(2,1)} %refs_0_.3), channel_id=1, source_target_pairs={{0,4},{1,5},{2,6},{3,7},{4,0},{5,1},{6,2},{7,3},{8,12},{9,13},{10,... | collective-permute-start | bytes 3145736 | tf_op jit(solution)/shard_map/ppermute | solution.py:357
  2.5 2.6 %copy-start.3 = (bf16[1,128,1024]{2,1,0:T(8,128)(2,1)S(1)}, bf16[1,128,1024]{2,1,0:T(8,128)(2,1)}, u32[]{:S(2)}) copy-start(bf16[1,128,1024]{2,1,0:T(8,128)(2,1)} %param.8) | copy-start | bytes 786436
  2.5 3.9 %copy-start.5 = (bf16[1,4,128]{2,1,0:T(4,128)(2,1)S(1)}, bf16[1,4,128]{2,1,0:T(4,128)(2,1)}, u32[]{:S(2)}) copy-start(bf16[1,4,128]{2,1,0:T(4,128)(2,1)} %param.11) | copy-start | bytes 3076
  2.5 3.9 %copy-start.6 = (bf16[1,4,128]{2,1,0:T(4,128)(2,1)S(1)}, bf16[1,4,128]{2,1,0:T(4,128)(2,1)}, u32[]{:S(2)}) copy-start(bf16[1,4,128]{2,1,0:T(4,128)(2,1)} %param.12) | copy-start | bytes 3076
  2.5 15.5 %copy-start.4 = (bf16[1,128,1024]{2,1,0:T(8,128)(2,1)S(1)}, bf16[1,128,1024]{2,1,0:T(8,128)(2,1)}, u32[]{:S(2)}) copy-start(bf16[1,128,1024]{2,1,0:T(8,128)(2,1)} %param.7) | copy-start | bytes 786436
  2.5 22.4 %copy-start = (bf16[1,128,2048]{2,1,0:T(8,128)(2,1)S(1)}, bf16[1,128,2048]{2,1,0:T(8,128)(2,1)}, u32[]{:S(2)}) copy-start(bf16[1,128,2048]{2,1,0:T(8,128)(2,1)} %param.9) | copy-start | bytes 1572868
  3.6 24.8 %copy-start.1 = (bf16[2048,256]{1,0:T(8,128)(2,1)S(1)}, bf16[2048,256]{1,0:T(8,128)(2,1)}, u32[]{:S(2)}) copy-start(bf16[2048,256]{1,0:T(8,128)(2,1)} %refs_0_.3) | copy-start | bytes 3145732
  3.6 15.0 %collective-permute-start.2 = (bf16[128,1024]{1,0:T(8,128)(2,1)S(1)}, bf16[128,1024]{1,0:T(8,128)(2,1)S(1)}, u32[]{:S(2)}, u32[]{:S(2)}) collective-permute-start(bf16[128,1024]{1,0:T(8,128)(2,1)S(1)} %get-tuple-element.38), channel_id=1, source_target_pairs={{0,8},{16,24},{1,9},{17,25},{2,10},{18,26},{3,11},{19,27},{4,12},{... | collective-permute-start | bytes 786440 | tf_op jit(solution)/shard_map/ppermute | solution.py:367
  5.1 16.2 %collective-permute-start.1 = (bf16[128,1024]{1,0:T(8,128)(2,1)S(1)}, bf16[128,1024]{1,0:T(8,128)(2,1)S(1)}, u32[]{:S(2)}, u32[]{:S(2)}) collective-permute-start(bf16[128,1024]{1,0:T(8,128)(2,1)S(1)} %bitcast.13), channel_id=1, source_target_pairs={{0,8},{16,24},{1,9},{17,25},{2,10},{18,26},{3,11},{19,27},{4,12},{... | collective-permute-start | bytes 786440 | tf_op jit(solution)/shard_map/ppermute | solution.py:365
  6.6 11.4 %collective-permute-start = (f32[8,128]{1,0:T(8,128)S(1)}, f32[8,128]{1,0:T(8,128)S(1)}, u32[]{:S(2)}, u32[]{:S(2)}) collective-permute-start(f32[8,128]{1,0:T(8,128)S(1)} %shard_map.73.gates_ref), channel_id=1, source_target_pairs={{0,8},{16,24},{1,9},{17,25},{2,10},{18,26},{3,11},{19,27},{4,12},{... | collective-permute-start | bytes 12296 | tf_op jit(solution)/shard_map/ppermute | solution.py:365
  18.0 4.6 %collective-permute-start.4 = (bf16[128,1024]{1,0:T(8,128)(2,1)S(1)}, bf16[128,1024]{1,0:T(8,128)(2,1)S(1)}, u32[]{:S(2)}, u32[]{:S(2)}) collective-permute-start(bf16[128,1024]{1,0:T(8,128)(2,1)S(1)} %bitcast.16), channel_id=1, source_target_pairs={{16,8},{17,9},{18,10},{19,11},{20,12},{21,13},{22,14},{23,15}} | collective-permute-start | bytes 786440 | tf_op jit(solution)/shard_map/ppermute | solution.py:370
  18.7 6.2 %collective-permute-start.5 = (bf16[128,1024]{1,0:T(8,128)(2,1)S(1)}, bf16[128,1024]{1,0:T(8,128)(2,1)S(1)}, u32[]{:S(2)}, u32[]{:S(2)}) collective-permute-start(bf16[128,1024]{1,0:T(8,128)(2,1)S(1)} %bitcast.17), channel_id=1, source_target_pairs={{24,8},{25,9},{26,10},{27,11},{28,12},{29,13},{30,14},{31,15}} | collective-permute-start | bytes 786440 | tf_op jit(solution)/shard_map/ppermute | solution.py:371
  21.3 7.1 %collective-permute-start.3 = (bf16[128,1024]{1,0:T(8,128)(2,1)S(1)}, bf16[128,1024]{1,0:T(8,128)(2,1)S(1)}, u32[]{:S(2)}, u32[]{:S(2)}) collective-permute-start(bf16[128,1024]{1,0:T(8,128)(2,1)S(1)} %get-tuple-element.37), channel_id=1, source_target_pairs={{0,8},{16,24},{1,9},{17,25},{2,10},{18,26},{3,11},{19,27},{4,12},{... | collective-permute-start | bytes 786440 | tf_op jit(solution)/shard_map/ppermute | solution.py:367
  25.6 6.9 %collective-permute-start.8 = (bf16[128,1152]{1,0:T(8,128)(2,1)S(1)}, bf16[128,1152]{1,0:T(8,128)(2,1)S(1)}, u32[]{:S(2)}, u32[]{:S(2)}) collective-permute-start(bf16[128,1152]{1,0:T(8,128)(2,1)S(1)} %get-tuple-element.32), channel_id=1, source_target_pairs={{8,16},{9,17},{10,18},{11,19},{12,20},{13,21},{14,22},{15,23}} | collective-permute-start | bytes 884744 | tf_op jit(solution)/shard_map/ppermute | solution.py:422
  26.3 18.1 %collective-permute-start.9 = (bf16[128,1152]{1,0:T(8,128)(2,1)S(1)}, bf16[128,1152]{1,0:T(8,128)(2,1)S(1)}, u32[]{:S(2)}, u32[]{:S(2)}) collective-permute-start(bf16[128,1152]{1,0:T(8,128)(2,1)S(1)} %get-tuple-element.33), channel_id=1, source_target_pairs={{8,24},{9,25},{10,26},{11,27},{12,28},{13,29},{14,30},{15,31}} | collective-permute-start | bytes 884744 | tf_op jit(solution)/shard_map/ppermute | solution.py:423
  28.4 30.7 %collective-permute-start.10 = (bf16[2048,256]{1,0:T(8,128)(2,1)S(1)}, bf16[2048,256]{1,0:T(8,128)(2,1)S(1)}, u32[]{:S(2)}, u32[]{:S(2)}) collective-permute-start(bf16[2048,256]{1,0:T(8,128)(2,1)S(1)} %copy-done.1), channel_id=1, source_target_pairs={{0,1},{1,0},{2,3},{3,2},{4,5},{5,4},{6,7},{7,6},{8,9},{9,8},{10,11... | collective-permute-start | bytes 3145736 | tf_op jit(solution)/shard_map/ppermute | solution.py:357
  31.9 27.8 %collective-permute-start.12 = (bf16[2048,256]{1,0:T(8,128)(2,1)S(1)}, bf16[2048,256]{1,0:T(8,128)(2,1)S(1)}, u32[]{:S(2)}, u32[]{:S(2)}) collective-permute-start(bf16[2048,256]{1,0:T(8,128)(2,1)S(1)} %collective-permute-done.11.refs_2_), channel_id=1, source_target_pairs={{0,1},{1,0},{2,3},{3,2},{4,5},{5,4},{6,7},{7,6},{8,9},{9,8},{10,11... | collective-permute-start | bytes 3145736 | tf_op jit(solution)/shard_map/ppermute | solution.py:357
  32.0 30.9 %collective-permute-start.14 = (bf16[2048,256]{1,0:T(8,128)(2,1)S(1)}, bf16[2048,256]{1,0:T(8,128)(2,1)S(1)}, u32[]{:S(2)}, u32[]{:S(2)}) collective-permute-start(bf16[2048,256]{1,0:T(8,128)(2,1)S(1)} %collective-permute-done.13.refs_4_), channel_id=1, source_target_pairs={{0,1},{1,0},{2,3},{3,2},{4,5},{5,4},{6,7},{7,6},{8,9},{9,8},{10,11... | collective-permute-start | bytes 3145736 | tf_op jit(solution)/shard_map/ppermute | solution.py:357
  32.5 13.5 %collective-permute-start.15 = (bf16[1024,256]{1,0:T(8,128)(2,1)S(1)}, bf16[1024,256]{1,0:T(8,128)(2,1)S(1)}, u32[]{:S(2)}, u32[]{:S(2)}) collective-permute-start(bf16[1024,256]{1,0:T(8,128)(2,1)S(1)} %slice.18), channel_id=1, source_target_pairs={{0,4},{1,5},{2,6},{3,7},{4,0},{5,1},{6,2},{7,3},{8,12},{9,13},{10,... | collective-permute-start | bytes 1572872 | tf_op jit(solution)/shard_map/ppermute | solution.py:357
  44.4 10.0 %collective-permute-start.16 = (bf16[1024,256]{1,0:T(8,128)(2,1)S(1)}, bf16[1024,256]{1,0:T(8,128)(2,1)S(1)}, u32[]{:S(2)}, u32[]{:S(2)}) collective-permute-start(bf16[1024,256]{1,0:T(8,128)(2,1)S(1)} %slice.19), channel_id=1, source_target_pairs={{0,2},{1,3},{2,0},{3,1},{4,6},{5,7},{6,4},{7,5},{8,10},{9,11},{10,... | collective-permute-start | bytes 1572872 | tf_op jit(solution)/shard_map/ppermute | solution.py:357
  46.0 25.9 %collective-permute-start.17 = (bf16[1024,256]{1,0:T(8,128)(2,1)S(1)}, bf16[1024,256]{1,0:T(8,128)(2,1)S(1)}, u32[]{:S(2)}, u32[]{:S(2)}) collective-permute-start(bf16[1024,256]{1,0:T(8,128)(2,1)S(1)} %collective-permute-done.15.refs_6_), channel_id=1, source_target_pairs={{0,1},{1,0},{2,3},{3,2},{4,5},{5,4},{6,7},{7,6},{8,9},{9,8},{10,11... | collective-permute-start | bytes 1572872 | tf_op jit(solution)/shard_map/ppermute | solution.py:357
  54.5 17.5 %collective-permute-start.18 = (bf16[1024,256]{1,0:T(8,128)(2,1)S(1)}, bf16[1024,256]{1,0:T(8,128)(2,1)S(1)}, u32[]{:S(2)}, u32[]{:S(2)}) collective-permute-start(bf16[1024,256]{1,0:T(8,128)(2,1)S(1)} %collective-permute-done.16.refs_7_), channel_id=1, source_target_pairs={{0,1},{1,0},{2,3},{3,2},{4,5},{5,4},{6,7},{7,6},{8,9},{9,8},{10,11... | collective-permute-start | bytes 1572872 | tf_op jit(solution)/shard_map/ppermute | solution.py:357
  59.1 5.0 %collective-permute-start.6 = (bf16[128,1024]{1,0:T(8,128)(2,1)S(1)}, bf16[128,1024]{1,0:T(8,128)(2,1)S(1)}, u32[]{:S(2)}, u32[]{:S(2)}) collective-permute-start(bf16[128,1024]{1,0:T(8,128)(2,1)S(1)} %get-tuple-element.28), channel_id=1, source_target_pairs={{8,16},{9,17},{10,18},{11,19},{12,20},{13,21},{14,22},{15,23}} | collective-permute-start | bytes 786440 | tf_op jit(solution)/shard_map/ppermute | solution.py:422
  59.8 12.1 %collective-permute-start.7 = (bf16[128,1024]{1,0:T(8,128)(2,1)S(1)}, bf16[128,1024]{1,0:T(8,128)(2,1)S(1)}, u32[]{:S(2)}, u32[]{:S(2)}) collective-permute-start(bf16[128,1024]{1,0:T(8,128)(2,1)S(1)} %get-tuple-element.29), channel_id=1, source_target_pairs={{8,24},{9,25},{10,26},{11,27},{12,28},{13,29},{14,30},{15,31}} | collective-permute-start | bytes 786440 | tf_op jit(solution)/shard_map/ppermute | solution.py:423
  61.8 1.1 %copy-start.2 = (bf16[1,128,2048]{2,1,0:T(8,128)(2,1)S(1)}, bf16[1,128,2048]{2,1,0:T(8,128)(2,1)}, u32[]{:S(2)}) copy-start(bf16[1,128,2048]{2,1,0:T(8,128)(2,1)} %param.10) | copy-start | bytes 1572868

commit v7 on v6

--- a/solution.py
+++ b/solution.py
@@ -301,7 +301,7 @@
 
 
 def finish_kernel(
-    counts, whole, plan, gate_ref, total_ref, note_ref, near_ref, far_ref, gated_ref, lane_ref,
+    counts, whole, last, gate_ref, total_ref, note_ref, near_ref, far_ref, gated_ref, lane_ref,
     part_ref, *refs,
 ):
     pieces, out_ref = refs[:-1], refs[-1]
@@ -312,20 +312,17 @@
         lane_ref[...], gate_ref,
     )
 
-    def put(mask, columns):
+    def put(masks, columns):
+        mask = jnp.where(device & CORE, masks[1], masks[0])
         start = pl.multiple_of((device ^ mask) * width, width)
         out_ref[:, pl.ds(start, width)] = columns.astype(out_ref.dtype)
 
-    for place, (mask, piece) in enumerate(zip(whole, pieces)):
+    for place, (masks, piece) in enumerate(zip(whole, pieces)):
         part = part_ref[:, place * width : (place + 1) * width]
-        put(mask, part + product(gated, piece[rows:, :]))
+        put(masks, part + product(gated, piece[rows:, :]))
     both = jnp.concatenate([gated_ref[...], gated], axis=1)
-    sums = {}
-    for (mask, start), piece in zip(plan, pieces[len(whole) :]):
-        part = product(both[:, start : start + piece.shape[0]], piece[...])
-        sums[mask] = sums[mask] + part if mask in sums else part
-    for mask, columns in sums.items():
-        put(mask, columns)
+    for masks, piece in zip(last, pieces[len(whole) :]):
+        put(masks, product(both, piece[...]))
 
 
 def kernel_call(kernel, operands, outs, flops, limit):
@@ -370,26 +367,25 @@
     near = lax.ppermute(query, "sp", [(2, 1)])
     far = lax.ppermute(query, "sp", [(3, 1)])
 
-    half = out_weight.shape[0] // 2
-    from_x = swap(out_weight, XBIT)
-    from_y = swap(out_weight, YBIT)
-    from_core = swap(out_weight, CORE)
-    top = swap(from_x[:half], YBIT)
-    bottom = swap(from_y[half:], XBIT)
+    def cross(piece, even, odd):
+        pairs = [(i, i ^ (odd if i & CORE else even)) for i in range(device_count)]
+        return lax.ppermute(piece, "dp", pairs)
+
+    side_a = cross(out_weight, XBIT, YBIT)
+    side_b = cross(out_weight, YBIT, XBIT)
+    corner = cross(side_a, YBIT, XBIT)
     whole = {
-        0: out_weight,
-        CORE: from_core,
-        XBIT: from_x,
-        XBIT | CORE: swap(from_x, CORE),
-        YBIT: from_y,
-        YBIT | CORE: swap(from_y, CORE),
+        (0, 0): out_weight,
+        (CORE, CORE): swap(out_weight, CORE),
+        (XBIT, YBIT): side_a,
+        (YBIT | CORE, XBIT | CORE): swap(side_a, CORE),
+        (YBIT, XBIT): side_b,
+        (XBIT | CORE, YBIT | CORE): swap(side_b, CORE),
     }
-    corner = [
-        ((XBIT | YBIT, 0), top),
-        ((XBIT | YBIT, half), bottom),
-        ((XBIT | YBIT | CORE, 0), swap(top, CORE)),
-        ((XBIT | YBIT | CORE, half), swap(bottom, CORE)),
-    ]
+    last = {
+        (XBIT | YBIT,) * 2: corner,
+        (XBIT | YBIT | CORE,) * 2: swap(corner, CORE),
+    }
 
     work = 2 * tokens * tokens * (key_width + value_width)
     sums = [
@@ -441,10 +437,10 @@
         10,
     )
     (out,) = kernel_call(
-        functools.partial(finish_kernel, COUNTS, tuple(whole), tuple(place for place, _ in corner)),
+        functools.partial(finish_kernel, COUNTS, tuple(whole), tuple(last)),
         [
             gate, *home[2:], nears[1], fars[1], *kept, *whole.values(),
-            *(piece for _, piece in corner),
+            *last.values(),
         ],
         [shape((tokens, width * device_count), jnp.bfloat16)],
         2 * tokens * rest * value_width * width * device_count,

time: 74.4 us -> 92.4 us (1.24)
  the two profiles are of different devices: /device:TPU:25 before, /device:TPU:24 now
where the time goes in v7:
time: 92.4 us; the launch traced here: 92.1 us
  waiting for transfers between devices  66.4 us (72%)
  starting transfers between devices  17 us (18%)
  Pallas kernels  6.39 us (7%)
  local copies, waits for them, and re-layouts  2.09 us (2%)
    ppermute x3, waiting for transfers between devices, cross(): return lax.ppermute(piece, 'dp', pairs)  23.1 us
    ppermute x1, waiting for transfers between devices, block_steps(): lax.ppermute(given_later, 'sp', [(1, 3)])  19.2 us
    ppermute x2, waiting for transfers between devices, block_steps(): earlier = [lax.ppermute(gates, 'sp', pair), lax.ppermute(key, 'sp', pair)]  8.89 us
    ppermute x1, waiting for transfers between devices, block_steps(): lax.ppermute(value[:, split:], 'sp', pair)  8.01 us
    pallas_call x7, Pallas kernels, kernel_call(): pl.pallas_call(kernel, out_shape=outs, in_specs=[vmem] * len(operands), o...  6.39 us
    ppermute x1, waiting for transfers between devices, block_steps(): lax.ppermute(rest_later, 'sp', [(1, 3)])  4.62 us
    ppermute x3, starting transfers between devices, cross(): return lax.ppermute(piece, 'dp', pairs)  3.73 us
    ppermute x1, starting transfers between devices, block_steps(): far = lax.ppermute(query, 'sp', [(3, 1)])  2.87 us
  transfers between devices with their start and end apart: 17, of which 6 were waited for; matrix products, arithmetic and copies ran while one was open for 1% of the time, Pallas kernels for 5%

profile of v7, /device:TPU:24, one launch (start us, length us, event | category | flops | bytes accessed | tf_op | source)
XLA Modules:
  0.0 92.1 jit_solution(16014787714071529509)
XLA Ops:
  0.0 1.5 %collective-permute-start.11 = (bf16[2048,256]{1,0:T(8,128)(2,1)}, bf16[2048,256]{1,0:T(8,128)(2,1)S(1)}, u32[]{:S(2)}, u32[]{:S(2)}) collective-permute-start(bf16[2048,256]{1,0:T(8,128)(2,1)} %refs_0_.3), channel_id=1, source_target_pairs={{0,2},{1,5},{2,0},{3,7},{4,6},{5,1},{6,4},{7,3},{8,10},{9,13},{10,... | collective-permute-start | bytes 3145736 | tf_op jit(solution)/shard_map/ppermute | solution.py:372
  1.5 1.5 %collective-permute-start.13 = (bf16[2048,256]{1,0:T(8,128)(2,1)}, bf16[2048,256]{1,0:T(8,128)(2,1)S(1)}, u32[]{:S(2)}, u32[]{:S(2)}) collective-permute-start(bf16[2048,256]{1,0:T(8,128)(2,1)} %refs_0_.3), channel_id=1, source_target_pairs={{0,4},{1,3},{2,6},{3,1},{4,0},{5,7},{6,2},{7,5},{8,12},{9,11},{10,... | collective-permute-start | bytes 3145736 | tf_op jit(solution)/shard_map/ppermute | solution.py:372
  3.0 23.1 %collective-permute-done.11.refs_2_ = bf16[2048,256]{1,0:T(8,128)(2,1)S(1)} collective-permute-done((bf16[2048,256]{1,0:T(8,128)(2,1)}, bf16[2048,256]{1,0:T(8,128)(2,1)S(1)}, u32[]{:S(2)}, u32[]{:S(2)}) %collective-permute-start.11) | collective-permute-done | bytes 1048608 | tf_op jit(solution)/shard_map/ppermute | solution.py:372
  26.1 0.7 collective-permute-start.15
  26.9 0.0 copy-start.3
  26.9 0.0 copy-start.6
  26.9 0.0 copy-start.4
  26.9 0.0 copy-start
  26.9 1.2 %fusion = (bf16[128,1024]{1,0:T(8,128)(2,1)S(1)}, bf16[128,1024]{1,0:T(8,128)(2,1)S(1)}) fusion(bf16[128,2048]{1,0:T(8,128)(2,1)} %bitcast.7), kind=kLoop, calls=%fused_computation | loop fusion | bytes 1048576 | tf_op jit(solution)/shard_map/slice | solution.py:364
  28.0 1.3 %collective-permute-start.2 = (bf16[128,1024]{1,0:T(8,128)(2,1)S(1)}, bf16[128,1024]{1,0:T(8,128)(2,1)S(1)}, u32[]{:S(2)}, u32[]{:S(2)}) collective-permute-start(bf16[128,1024]{1,0:T(8,128)(2,1)S(1)} %get-tuple-element.38), channel_id=1, source_target_pairs={{0,8},{16,24},{1,9},{17,25},{2,10},{18,26},{3,11},{19,27},{4,12},{... | collective-permute-start | bytes 786440 | tf_op jit(solution)/shard_map/ppermute | solution.py:364
  29.3 0.0 copy-done.3
  29.3 1.3 %collective-permute-start.1 = (bf16[128,1024]{1,0:T(8,128)(2,1)S(1)}, bf16[128,1024]{1,0:T(8,128)(2,1)S(1)}, u32[]{:S(2)}, u32[]{:S(2)}) collective-permute-start(bf16[128,1024]{1,0:T(8,128)(2,1)S(1)} %bitcast.13), channel_id=1, source_target_pairs={{0,8},{16,24},{1,9},{17,25},{2,10},{18,26},{3,11},{19,27},{4,12},{... | collective-permute-start | bytes 786440 | tf_op jit(solution)/shard_map/ppermute | solution.py:362
  30.6 0.0 copy-start.5
  30.6 0.0 copy-done.6
  30.7 0.7 copy-done.5
  31.3 0.2 shard_map.73.gates_ref
  31.5 1.3 %collective-permute-start = (f32[8,128]{1,0:T(8,128)S(1)}, f32[8,128]{1,0:T(8,128)S(1)}, u32[]{:S(2)}, u32[]{:S(2)}) collective-permute-start(f32[8,128]{1,0:T(8,128)S(1)} %shard_map.73.gates_ref), channel_id=1, source_target_pairs={{0,8},{16,24},{1,9},{17,25},{2,10},{18,26},{3,11},{19,27},{4,12},{... | collective-permute-start | bytes 12296 | tf_op jit(solution)/shard_map/ppermute | solution.py:362
  32.8 8.9 %collective-permute-done.gates0_ref = f32[8,128]{1,0:T(8,128)S(1)} collective-permute-done((f32[8,128]{1,0:T(8,128)S(1)}, f32[8,128]{1,0:T(8,128)S(1)}, u32[]{:S(2)}, u32[]{:S(2)}) %collective-permute-start) | collective-permute-done | bytes 4128 | tf_op jit(solution)/shard_map/ppermute | solution.py:362
  41.7 0.0 copy-done.4
  41.7 0.7 collective-permute-start.4
  42.4 0.0 collective-permute-done.2.refs_0_.value0_ref
  42.4 2.9 %collective-permute-start.5 = (bf16[128,1024]{1,0:T(8,128)(2,1)S(1)}, bf16[128,1024]{1,0:T(8,128)(2,1)S(1)}, u32[]{:S(2)}, u32[]{:S(2)}) collective-permute-start(bf16[128,1024]{1,0:T(8,128)(2,1)S(1)} %bitcast.17), channel_id=1, source_target_pairs={{24,8},{25,9},{26,10},{27,11},{28,12},{29,13},{30,14},{31,15}} | collective-permute-start | bytes 786440 | tf_op jit(solution)/shard_map/ppermute | solution.py:368
  45.3 0.0 collective-permute-done.1.key0_ref
  45.3 0.1 collective-permute-start.10
  45.4 0.0 collective-permute-done.4.near_ref
  45.4 1.3 %collective-permute-start.3 = (bf16[128,1024]{1,0:T(8,128)(2,1)S(1)}, bf16[128,1024]{1,0:T(8,128)(2,1)S(1)}, u32[]{:S(2)}, u32[]{:S(2)}) collective-permute-start(bf16[128,1024]{1,0:T(8,128)(2,1)S(1)} %get-tuple-element.37), channel_id=1, source_target_pairs={{0,8},{16,24},{1,9},{17,25},{2,10},{18,26},{3,11},{19,27},{4,12},{... | collective-permute-start | bytes 786440 | tf_op jit(solution)/shard_map/ppermute | solution.py:364
  46.7 2.5 %collective-permute-done.5.far_ref = bf16[128,1024]{1,0:T(8,128)(2,1)S(1)} collective-permute-done((bf16[128,1024]{1,0:T(8,128)(2,1)S(1)}, bf16[128,1024]{1,0:T(8,128)(2,1)S(1)}, u32[]{:S(2)}, u32[]{:S(2)}) %collective-permute-start.5) | collective-permute-done | bytes 262176 | tf_op jit(solution)/shard_map/ppermute | solution.py:368
  49.2 0.0 collective-permute-start.12
  49.2 0.0 collective-permute-done.13.refs_4_
  49.2 0.5 collective-permute-start.14
  49.7 0.0 collective-permute-done.15.refs_6_
  49.7 0.1 collective-permute-start.16
  49.8 0.0 copy-done
  49.8 0.7 shard_map.76
  50.5 8.0 %collective-permute-done.3.refs_1_.value0_ref = bf16[128,1024]{1,0:T(8,128)(2,1)S(1)} collective-permute-done((bf16[128,1024]{1,0:T(8,128)(2,1)S(1)}, bf16[128,1024]{1,0:T(8,128)(2,1)S(1)}, u32[]{:S(2)}, u32[]{:S(2)}) %collective-permute-start.3) | collective-permute-done | bytes 262176 | tf_op jit(solution)/shard_map/ppermute | solution.py:364
  58.5 0.7 collective-permute-start.8
  59.2 0.0 collective-permute-done.8.near_ref
  59.2 1.3 %collective-permute-start.9 = (bf16[128,1152]{1,0:T(8,128)(2,1)S(1)}, bf16[128,1152]{1,0:T(8,128)(2,1)S(1)}, u32[]{:S(2)}, u32[]{:S(2)}) collective-permute-start(bf16[128,1152]{1,0:T(8,128)(2,1)S(1)} %get-tuple-element.33), channel_id=1, source_target_pairs={{8,24},{9,25},{10,26},{11,27},{12,28},{13,29},{14,30},{15,31}} | collective-permute-start | bytes 884744 | tf_op jit(solution)/shard_map/ppermute | solution.py:419
  60.5 0.3 shard_map.77
  60.8 19.2 %collective-permute-done.9.far_ref = bf16[128,1152]{1,0:T(8,128)(2,1)S(1)} collective-permute-done((bf16[128,1152]{1,0:T(8,128)(2,1)S(1)}, bf16[128,1152]{1,0:T(8,128)(2,1)S(1)}, u32[]{:S(2)}, u32[]{:S(2)}) %collective-permute-start.9) | collective-permute-done | bytes 294944 | tf_op jit(solution)/shard_map/ppermute | solution.py:419
  80.0 0.7 collective-permute-start.6
  80.7 0.0 collective-permute-done.10.refs_1_
  80.7 1.3 %collective-permute-start.7 = (bf16[128,1024]{1,0:T(8,128)(2,1)S(1)}, bf16[128,1024]{1,0:T(8,128)(2,1)S(1)}, u32[]{:S(2)}, u32[]{:S(2)}) collective-permute-start(bf16[128,1024]{1,0:T(8,128)(2,1)S(1)} %get-tuple-element.29), channel_id=1, source_target_pairs={{8,24},{9,25},{10,26},{11,27},{12,28},{13,29},{14,30},{15,31}} | collective-permute-start | bytes 786440 | tf_op jit(solution)/shard_map/ppermute | solution.py:419
  82.0 0.7 shard_map.74
  82.7 0.0 copy-start.1
  82.7 0.0 copy-start.2
  82.7 1.1 %shard_map.75 = (f32[128,1024]{1,0:T(8,128)S(1)}, f32[128,128]{1,0:T(8,128)S(1)}, f32[128,1024]{1,0:T(8,128)S(1)}, f32[128,128]{1,0:T(8,128)S(1)}) custom-call(f32[8,128]{1,0:T(8,128)S(1)} %collective-permute-done.gates0_ref, bf16[128,1024]{1,0:T(8,128)(2,1)S(1)} %collective-permute-done.1.key0_ref, ...), custom_call_target="tpu_custom_call" | custom-call | flops 150994944 | bytes 3411968 | tf_op jit(solution)/shard_map/pallas_call | solution.py:331
  83.8 0.0 collective-permute-done.12.refs_3_
  83.8 0.0 collective-permute-done.14.refs_5_
  83.8 0.1 copy-done.1
  83.9 0.1 copy-done.2
  84.1 1.1 %shard_map.78 = (bf16[128,1024]{1,0:T(8,128)(2,1)S(1)}, f32[128,128]{1,0:T(8,128)S(1)}, f32[128,1536]{1,0:T(8,128)S(1)}) custom-call(bf16[128,2048]{1,0:T(8,128)(2,1)S(1)} %bitcast.11, f32[128,1024]{1,0:T(8,128)S(1)} %get-tuple-element.30.total_ref, f32[128,128]{1,0:T(8,128)S(1)} %get-tuple-element.31.note_ref, ...), custom_call_target="tpu_custom_call" | custom-call | flops 402653184 | bytes 9109504 | tf_op jit(solution)/shard_map/pallas_call | solution.py:331
  85.2 0.0 collective-permute-done.6.near_ref
  85.2 4.6 %collective-permute-done.7.far_ref = bf16[128,1024]{1,0:T(8,128)(2,1)S(1)} collective-permute-done((bf16[128,1024]{1,0:T(8,128)(2,1)S(1)}, bf16[128,1024]{1,0:T(8,128)(2,1)S(1)}, u32[]{:S(2)}, u32[]{:S(2)}) %collective-permute-start.7) | collective-permute-done | bytes 262176 | tf_op jit(solution)/shard_map/ppermute | solution.py:419
  89.9 0.0 collective-permute-done.16.refs_7_
  89.9 2.2 %shard_map.79 = bf16[128,2048]{1,0:T(8,128)(2,1)} custom-call(bf16[128,2048]{1,0:T(8,128)(2,1)S(1)} %bitcast.12, f32[128,1024]{1,0:T(8,128)S(1)} %get-tuple-element.25.total_ref, f32[128,128]{1,0:T(8,128)S(1)} %get-tuple-element.26.note_ref, bf16[128,1024]{1,0:T(8,128)(2,1)S(1)} %collective-permute-done.6.near_ref, ...), custom_call_target="tpu_custom_call" | custom-call | flops 536870912 | bytes 11665408 | tf_op jit(solution)/shard_map/pallas_call | solution.py:331
Async XLA Ops:
  0.0 26.1 %collective-permute-start.11 = (bf16[2048,256]{1,0:T(8,128)(2,1)}, bf16[2048,256]{1,0:T(8,128)(2,1)S(1)}, u32[]{:S(2)}, u32[]{:S(2)}) collective-permute-start(bf16[2048,256]{1,0:T(8,128)(2,1)} %refs_0_.3), channel_id=1, source_target_pairs={{0,2},{1,5},{2,0},{3,7},{4,6},{5,1},{6,4},{7,3},{8,10},{9,13},{10,... | collective-permute-start | bytes 3145736 | tf_op jit(solution)/shard_map/ppermute | solution.py:372
  1.5 47.7 %collective-permute-start.13 = (bf16[2048,256]{1,0:T(8,128)(2,1)}, bf16[2048,256]{1,0:T(8,128)(2,1)S(1)}, u32[]{:S(2)}, u32[]{:S(2)}) collective-permute-start(bf16[2048,256]{1,0:T(8,128)(2,1)} %refs_0_.3), channel_id=1, source_target_pairs={{0,4},{1,3},{2,6},{3,1},{4,0},{5,7},{6,2},{7,5},{8,12},{9,11},{10,... | collective-permute-start | bytes 3145736 | tf_op jit(solution)/shard_map/ppermute | solution.py:372
  26.1 23.6 %collective-permute-start.15 = (bf16[2048,256]{1,0:T(8,128)(2,1)S(1)}, bf16[2048,256]{1,0:T(8,128)(2,1)S(1)}, u32[]{:S(2)}, u32[]{:S(2)}) collective-permute-start(bf16[2048,256]{1,0:T(8,128)(2,1)S(1)} %collective-permute-done.11.refs_2_), channel_id=1, source_target_pairs={{0,4},{1,3},{2,6},{3,1},{4,0},{5,7},{6,2},{7,5},{8,12},{9,11},{10,... | collective-permute-start | bytes 3145736 | tf_op jit(solution)/shard_map/ppermute | solution.py:372
  26.9 2.5 %copy-start.3 = (bf16[1,128,1024]{2,1,0:T(8,128)(2,1)S(1)}, bf16[1,128,1024]{2,1,0:T(8,128)(2,1)}, u32[]{:S(2)}) copy-start(bf16[1,128,1024]{2,1,0:T(8,128)(2,1)} %param.8) | copy-start | bytes 786436
  26.9 3.8 %copy-start.6 = (bf16[1,4,128]{2,1,0:T(4,128)(2,1)S(1)}, bf16[1,4,128]{2,1,0:T(4,128)(2,1)}, u32[]{:S(2)}) copy-start(bf16[1,4,128]{2,1,0:T(4,128)(2,1)} %param.12) | copy-start | bytes 3076
  26.9 14.9 %copy-start.4 = (bf16[1,128,1024]{2,1,0:T(8,128)(2,1)S(1)}, bf16[1,128,1024]{2,1,0:T(8,128)(2,1)}, u32[]{:S(2)}) copy-start(bf16[1,128,1024]{2,1,0:T(8,128)(2,1)} %param.7) | copy-start | bytes 786436
  26.9 22.9 %copy-start = (bf16[1,128,2048]{2,1,0:T(8,128)(2,1)S(1)}, bf16[1,128,2048]{2,1,0:T(8,128)(2,1)}, u32[]{:S(2)}) copy-start(bf16[1,128,2048]{2,1,0:T(8,128)(2,1)} %param.9) | copy-start | bytes 1572868
  28.0 14.4 %collective-permute-start.2 = (bf16[128,1024]{1,0:T(8,128)(2,1)S(1)}, bf16[128,1024]{1,0:T(8,128)(2,1)S(1)}, u32[]{:S(2)}, u32[]{:S(2)}) collective-permute-start(bf16[128,1024]{1,0:T(8,128)(2,1)S(1)} %get-tuple-element.38), channel_id=1, source_target_pairs={{0,8},{16,24},{1,9},{17,25},{2,10},{18,26},{3,11},{19,27},{4,12},{... | collective-permute-start | bytes 786440 | tf_op jit(solution)/shard_map/ppermute | solution.py:364
  29.3 16.0 %collective-permute-start.1 = (bf16[128,1024]{1,0:T(8,128)(2,1)S(1)}, bf16[128,1024]{1,0:T(8,128)(2,1)S(1)}, u32[]{:S(2)}, u32[]{:S(2)}) collective-permute-start(bf16[128,1024]{1,0:T(8,128)(2,1)S(1)} %bitcast.13), channel_id=1, source_target_pairs={{0,8},{16,24},{1,9},{17,25},{2,10},{18,26},{3,11},{19,27},{4,12},{... | collective-permute-start | bytes 786440 | tf_op jit(solution)/shard_map/ppermute | solution.py:362
  30.6 0.7 copy-start.5
  31.5 10.2 %collective-permute-start = (f32[8,128]{1,0:T(8,128)S(1)}, f32[8,128]{1,0:T(8,128)S(1)}, u32[]{:S(2)}, u32[]{:S(2)}) collective-permute-start(f32[8,128]{1,0:T(8,128)S(1)} %shard_map.73.gates_ref), channel_id=1, source_target_pairs={{0,8},{16,24},{1,9},{17,25},{2,10},{18,26},{3,11},{19,27},{4,12},{... | collective-permute-start | bytes 12296 | tf_op jit(solution)/shard_map/ppermute | solution.py:362
  41.7 3.7 %collective-permute-start.4 = (bf16[128,1024]{1,0:T(8,128)(2,1)S(1)}, bf16[128,1024]{1,0:T(8,128)(2,1)S(1)}, u32[]{:S(2)}, u32[]{:S(2)}) collective-permute-start(bf16[128,1024]{1,0:T(8,128)(2,1)S(1)} %bitcast.16), channel_id=1, source_target_pairs={{16,8},{17,9},{18,10},{19,11},{20,12},{21,13},{22,14},{23,15}} | collective-permute-start | bytes 786440 | tf_op jit(solution)/shard_map/ppermute | solution.py:367
  42.4 6.8 %collective-permute-start.5 = (bf16[128,1024]{1,0:T(8,128)(2,1)S(1)}, bf16[128,1024]{1,0:T(8,128)(2,1)S(1)}, u32[]{:S(2)}, u32[]{:S(2)}) collective-permute-start(bf16[128,1024]{1,0:T(8,128)(2,1)S(1)} %bitcast.17), channel_id=1, source_target_pairs={{24,8},{25,9},{26,10},{27,11},{28,12},{29,13},{30,14},{31,15}} | collective-permute-start | bytes 786440 | tf_op jit(solution)/shard_map/ppermute | solution.py:368
  45.3 35.4 %collective-permute-start.10 = (bf16[2048,256]{1,0:T(8,128)(2,1)}, bf16[2048,256]{1,0:T(8,128)(2,1)S(1)}, u32[]{:S(2)}, u32[]{:S(2)}) collective-permute-start(bf16[2048,256]{1,0:T(8,128)(2,1)} %refs_0_.3), channel_id=1, source_target_pairs={{0,1},{1,0},{2,3},{3,2},{4,5},{5,4},{6,7},{7,6},{8,9},{9,8},{10,11... | collective-permute-start | bytes 3145736 | tf_op jit(solution)/shard_map/ppermute | solution.py:354
  45.4 13.1 %collective-permute-start.3 = (bf16[128,1024]{1,0:T(8,128)(2,1)S(1)}, bf16[128,1024]{1,0:T(8,128)(2,1)S(1)}, u32[]{:S(2)}, u32[]{:S(2)}) collective-permute-start(bf16[128,1024]{1,0:T(8,128)(2,1)S(1)} %get-tuple-element.37), channel_id=1, source_target_pairs={{0,8},{16,24},{1,9},{17,25},{2,10},{18,26},{3,11},{19,27},{4,12},{... | collective-permute-start | bytes 786440 | tf_op jit(solution)/shard_map/ppermute | solution.py:364
  49.2 34.6 %collective-permute-start.12 = (bf16[2048,256]{1,0:T(8,128)(2,1)S(1)}, bf16[2048,256]{1,0:T(8,128)(2,1)S(1)}, u32[]{:S(2)}, u32[]{:S(2)}) collective-permute-start(bf16[2048,256]{1,0:T(8,128)(2,1)S(1)} %collective-permute-done.11.refs_2_), channel_id=1, source_target_pairs={{0,1},{1,0},{2,3},{3,2},{4,5},{5,4},{6,7},{7,6},{8,9},{9,8},{10,11... | collective-permute-start | bytes 3145736 | tf_op jit(solution)/shard_map/ppermute | solution.py:354
  49.2 34.6 %collective-permute-start.14 = (bf16[2048,256]{1,0:T(8,128)(2,1)S(1)}, bf16[2048,256]{1,0:T(8,128)(2,1)S(1)}, u32[]{:S(2)}, u32[]{:S(2)}) collective-permute-start(bf16[2048,256]{1,0:T(8,128)(2,1)S(1)} %collective-permute-done.13.refs_4_), channel_id=1, source_target_pairs={{0,1},{1,0},{2,3},{3,2},{4,5},{5,4},{6,7},{7,6},{8,9},{9,8},{10,11... | collective-permute-start | bytes 3145736 | tf_op jit(solution)/shard_map/ppermute | solution.py:354
  49.7 40.1 %collective-permute-start.16 = (bf16[2048,256]{1,0:T(8,128)(2,1)S(1)}, bf16[2048,256]{1,0:T(8,128)(2,1)S(1)}, u32[]{:S(2)}, u32[]{:S(2)}) collective-permute-start(bf16[2048,256]{1,0:T(8,128)(2,1)S(1)} %collective-permute-done.15.refs_6_), channel_id=1, source_target_pairs={{0,1},{1,0},{2,3},{3,2},{4,5},{5,4},{6,7},{7,6},{8,9},{9,8},{10,11... | collective-permute-start | bytes 3145736 | tf_op jit(solution)/shard_map/ppermute | solution.py:354
  58.5 0.7 collective-permute-start.8
  59.2 20.8 %collective-permute-start.9 = (bf16[128,1152]{1,0:T(8,128)(2,1)S(1)}, bf16[128,1152]{1,0:T(8,128)(2,1)S(1)}, u32[]{:S(2)}, u32[]{:S(2)}) collective-permute-start(bf16[128,1152]{1,0:T(8,128)(2,1)S(1)} %get-tuple-element.33), channel_id=1, source_target_pairs={{8,24},{9,25},{10,26},{11,27},{12,28},{13,29},{14,30},{15,31}} | collective-permute-start | bytes 884744 | tf_op jit(solution)/shard_map/ppermute | solution.py:419
  80.0 5.2 %collective-permute-start.6 = (bf16[128,1024]{1,0:T(8,128)(2,1)S(1)}, bf16[128,1024]{1,0:T(8,128)(2,1)S(1)}, u32[]{:S(2)}, u32[]{:S(2)}) collective-permute-start(bf16[128,1024]{1,0:T(8,128)(2,1)S(1)} %get-tuple-element.28), channel_id=1, source_target_pairs={{8,16},{9,17},{10,18},{11,19},{12,20},{13,21},{14,22},{15,23}} | collective-permute-start | bytes 786440 | tf_op jit(solution)/shard_map/ppermute | solution.py:418
  80.7 9.2 %collective-permute-start.7 = (bf16[128,1024]{1,0:T(8,128)(2,1)S(1)}, bf16[128,1024]{1,0:T(8,128)(2,1)S(1)}, u32[]{:S(2)}, u32[]{:S(2)}) collective-permute-start(bf16[128,1024]{1,0:T(8,128)(2,1)S(1)} %get-tuple-element.29), channel_id=1, source_target_pairs={{8,24},{9,25},{10,26},{11,27},{12,28},{13,29},{14,30},{15,31}} | collective-permute-start | bytes 786440 | tf_op jit(solution)/shard_map/ppermute | solution.py:419
  82.7 1.2 %copy-start.1 = (bf16[2048,256]{1,0:T(8,128)(2,1)S(1)}, bf16[2048,256]{1,0:T(8,128)(2,1)}, u32[]{:S(2)}) copy-start(bf16[2048,256]{1,0:T(8,128)(2,1)} %refs_0_.3) | copy-start | bytes 3145732
  82.7 1.3 %copy-start.2 = (bf16[1,128,2048]{2,1,0:T(8,128)(2,1)S(1)}, bf16[1,128,2048]{2,1,0:T(8,128)(2,1)}, u32[]{:S(2)}) copy-start(bf16[1,128,2048]{2,1,0:T(8,128)(2,1)} %param.10) | copy-start | bytes 1572868

commit v8 on v0

--- a/solution.py
+++ b/solution.py
@@ -1,7 +1,12 @@
+import functools
+
 import jax
 import jax.numpy as jnp
 from jax import lax
+from jax.experimental import pallas as pl
+from jax.experimental.pallas import tpu as pltpu
 from jax.sharding import PartitionSpec as P
+
 
 BLOCK = 128
 
@@ -64,6 +69,391 @@
     return outputs.reshape(block_count * BLOCK, value_width)
 
 
+LANES = 128
+
+
+def log_forget(gates):
+    return -jnp.log1p(jnp.exp(-gates))
+
+
+def running_sum(rows):
+    width = rows.shape[1]
+    upto = lax.broadcasted_iota(jnp.int32, (width, width), 0) <= lax.broadcasted_iota(
+        jnp.int32, (width, width), 1
+    )
+    return jnp.dot(
+        rows,
+        upto.astype(jnp.float32),
+        precision=lax.Precision.HIGHEST,
+        preferred_element_type=jnp.float32,
+    )
+
+
+def times_transpose(left, right):
+    return lax.dot_general(
+        left, right, (((1,), (1,)), ((), ())), preferred_element_type=jnp.float32
+    )
+
+
+def three_terms(value):
+    high = value.astype(jnp.bfloat16).astype(jnp.float32)
+    middle = (value - high).astype(jnp.bfloat16).astype(jnp.float32)
+    return [high, middle, value - high - middle]
+
+
+def to_lanes(columns, rows):
+    lane = lax.broadcasted_iota(jnp.int32, (rows, LANES), 1)
+    tile = jnp.zeros((rows, LANES), jnp.float32)
+    for place, column in enumerate(columns):
+        tile = jnp.where(lane == place, column, tile)
+    return tile
+
+
+MIB = 1 << 20
+CORE, XBIT, YBIT = 1, 2, 4
+
+
+def gate_levels(payloads, tokens):
+    gates = [payload[tokens:, :tokens].astype(jnp.float32) for payload in payloads]
+    heads = gates[0].shape[0] // 2
+    running = running_sum(log_forget(jnp.concatenate([g[heads:] for g in gates], axis=0)))
+    parts = []
+    for place, gate in enumerate(gates):
+        sums = running[place * heads : (place + 1) * heads]
+        parts.append((gate[:heads] - sums, sums[:, tokens - 1 :]))
+    return parts
+
+
+def two_term_dot(left, right):
+    high = left.astype(jnp.bfloat16)
+    low = (left - high.astype(jnp.float32)).astype(jnp.bfloat16)
+    return jnp.dot(high, right, preferred_element_type=jnp.float32) + jnp.dot(
+        low, right, preferred_element_type=jnp.float32
+    )
+
+
+def half_slices(place, key_width, value_width, count):
+    start = count * key_width + place * value_width
+    return (
+        slice(place * key_width, (place + 1) * key_width),
+        slice(start, start + value_width),
+        slice(place * value_width, (place + 1) * value_width),
+    )
+
+
+def own_kernel(count, low_ref, high_ref, query_ref, *outs):
+    tokens, key_width = query_ref.shape[0], query_ref.shape[1] // (2 * count)
+    value_width = low_ref.shape[1] // count - key_width
+    ((level, _),) = gate_levels([low_ref], tokens)
+    causal = lax.broadcasted_iota(jnp.int32, (tokens, tokens), 0) >= lax.broadcasted_iota(
+        jnp.int32, (tokens, tokens), 1
+    )
+    for half, payload in enumerate((low_ref, high_ref)):
+        total_ref, note_ref = outs[2 * half : 2 * half + 2]
+        notes = []
+        for place in range(count):
+            head = half * count + place
+            keys, channels, out = half_slices(place, key_width, value_width, count)
+            masked = jnp.where(causal, level[head : head + 1], -jnp.inf)
+            top = jnp.max(masked, axis=1, keepdims=True)
+            rows = query_ref[:, head * key_width : (head + 1) * key_width]
+            scores = times_transpose(rows, payload[:tokens, keys]) * (key_width ** (-0.5))
+            scores = scores * jnp.exp(masked - top)
+            total_ref[:, out] = two_term_dot(scores, payload[:tokens, channels])
+            notes += [jnp.sum(scores, axis=1, keepdims=True), top]
+        note_ref[...] = to_lanes(notes, tokens)
+
+
+def join_kernel(count, pair_ref, before_ref, last_ref, query_ref, *refs):
+    tokens, key_width = query_ref.shape[0], query_ref.shape[1] // (2 * count)
+    value_width = pair_ref.shape[1] // count - key_width
+    block = lax.axis_index("sp")
+    second, both = lax.rem(block, 2) == 1, block == 2
+    upper = (block == 1) | both
+    start = jnp.where(block == 0, 0.0, -jnp.inf)
+    (level, end), (level0, end0), (level1, end1) = gate_levels(
+        [pair_ref, before_ref, last_ref], tokens
+    )
+    top = jnp.max(level, axis=1, keepdims=True)
+    top = jnp.where(block == 1, jnp.maximum(top, 0.0), top)
+    end0 = jnp.where(both, end0, 0.0)
+    level1 = level1 - end0
+    top1 = jnp.maximum(jnp.max(level1, axis=1, keepdims=True), 0.0)
+    top1 = jnp.where(both, jnp.maximum(top1, jnp.max(level0, axis=1, keepdims=True)), top1)
+    weight0 = jnp.where(both, jnp.exp(level0 - top1), 0.0)
+    cases = (
+        (
+            [pair_ref],
+            jnp.exp(level - top),
+            second,
+            jnp.where(second, top + end, start),
+            jnp.where(block == 3, end, 0.0),
+        ),
+        (
+            [before_ref, last_ref],
+            jnp.concatenate([weight0, jnp.exp(level1 - top1)], axis=1),
+            upper,
+            jnp.where(upper, top1 + end0 + end1, start),
+            jnp.zeros_like(end),
+        ),
+    )
+    for half, (payloads, weight, valid, state, shift) in enumerate(cases):
+        own_total, own_note, total_ref, note_ref = (
+            refs[2 * half], refs[2 * half + 1], refs[2 * half + 4], refs[2 * half + 5]
+        )
+        own = own_note[...]
+        notes = []
+        for place in range(count):
+            head = half * count + place
+            pick = slice(head, head + 1)
+            keys, channels, out = half_slices(place, key_width, value_width, count)
+            own_top = own[:, 2 * place + 1 : 2 * place + 2]
+            peak = jnp.maximum(own_top, state[pick])
+            scale = jnp.exp(own_top - peak)
+            scale0 = jnp.where(valid, jnp.exp(state[pick] - peak), 0.0) * (key_width ** (-0.5))
+            key_all = jnp.concatenate([p[:tokens, keys] for p in payloads], axis=0)
+            value_all = jnp.concatenate([p[:tokens, channels] for p in payloads], axis=0)
+            rows = query_ref[:, head * key_width : (head + 1) * key_width]
+            scores = times_transpose(rows, key_all) * weight[pick] * scale0
+            total_ref[:, out] = scale * own_total[:, out] + two_term_dot(scores, value_all)
+            sums = scale * own[:, 2 * place : 2 * place + 1] + jnp.sum(
+                scores, axis=1, keepdims=True
+            )
+            notes += [sums, peak, shift[pick]]
+        note_ref[...] = to_lanes(notes, tokens)
+
+
+def answer(count, half, payloads, rows_refs, out_refs):
+    tokens, key_width = rows_refs[0].shape[0], rows_refs[0].shape[1] // (2 * count)
+    value_width = payloads[0].shape[1] // count - key_width
+    levels, shift = [], 0.0
+    for level, end in gate_levels(payloads, tokens):
+        levels.append(level - shift)
+        shift = shift + end
+    level = jnp.concatenate(levels, axis=1)
+    top = jnp.maximum(jnp.max(level, axis=1, keepdims=True), 0.0)
+    weight = jnp.exp(level - top) * (key_width ** (-0.5))
+    reach = top + shift
+    notes = [[] for _ in out_refs]
+    for place in range(count):
+        pick = slice(half * count + place, half * count + place + 1)
+        keys, channels, out = half_slices(place, key_width, value_width, count)
+        key_all = jnp.concatenate([p[:tokens, keys] for p in payloads], axis=0)
+        value_all = jnp.concatenate([p[:tokens, channels] for p in payloads], axis=0)
+        columns = slice(pick.start * key_width, pick.stop * key_width)
+        rows = jnp.concatenate([ref[:, columns] for ref in rows_refs], axis=0)
+        scores = times_transpose(rows, key_all) * weight[pick]
+        sums = jnp.sum(scores, axis=1, keepdims=True)
+        given = product(scores.astype(jnp.bfloat16), value_all).astype(jnp.bfloat16)
+        for i, ref in enumerate(out_refs):
+            here = slice(i * tokens, (i + 1) * tokens)
+            ref[:, out] = given[here]
+            notes[i] += three_terms(sums[here]) + three_terms(reach[pick])
+    for ref, note in zip(out_refs, notes):
+        ref[:, count * value_width :] = to_lanes(note, tokens).astype(jnp.bfloat16)
+
+
+def serve_low_kernel(count, pair_ref, low_ref, near_ref, far_ref, next_ref, later_ref):
+    answer(count, 0, [pair_ref, low_ref], [near_ref, far_ref], [next_ref, later_ref])
+
+
+def serve_high_kernel(count, before_ref, last_ref, high_ref, near_ref, next_ref):
+    answer(count, 1, [before_ref, last_ref, high_ref], [near_ref], [next_ref])
+
+
+def gated_rows(count, half, given, message, total_ref, note_ref, gate_ref):
+    value_width = total_ref.shape[1] // count
+    own = note_ref[...]
+    lanes = message(slice(count * value_width, count * value_width + LANES))
+    gated = []
+    for place in range(count):
+        out = slice(place * value_width, (place + 1) * value_width)
+        start = (half * count + place) * value_width
+        at = 6 * place
+        sums = lanes[:, at : at + 1] + lanes[:, at + 1 : at + 2] + lanes[:, at + 2 : at + 3]
+        at += 3
+        reach = lanes[:, at : at + 1] + lanes[:, at + 1 : at + 2] + lanes[:, at + 2 : at + 3]
+        reach = reach + own[:, 3 * place + 2 : 3 * place + 3]
+        top = own[:, 3 * place + 1 : 3 * place + 2]
+        peak = jnp.where(given, jnp.maximum(top, reach), top)
+        scale = jnp.exp(top - peak)
+        scale_given = jnp.where(given, jnp.exp(reach - peak), 0.0)
+        weight = scale * own[:, 3 * place : 3 * place + 1] + scale_given * sums
+        inverse = 1.0 / jnp.maximum(jnp.abs(weight), 1.0)
+        cell = (scale * inverse) * total_ref[:, out] + (scale_given * inverse) * message(out)
+        hidden = cell.astype(jnp.bfloat16).astype(jnp.float32)
+        gate = jax.nn.sigmoid(gate_ref[:, start : start + value_width].astype(jnp.float32))
+        gated.append((hidden * gate).astype(jnp.bfloat16))
+    return jnp.concatenate(gated, axis=1)
+
+
+def product(left, right):
+    return jnp.dot(left, right, preferred_element_type=jnp.float32)
+
+
+def first_kernel(count, gate_ref, total_ref, note_ref, next_ref, *refs):
+    pieces, gated_ref, part_ref = refs[:-2], refs[-2], refs[-1]
+    rows = gated_ref.shape[1]
+
+    def message(columns):
+        return next_ref[:, columns].astype(jnp.float32)
+
+    given = lax.axis_index("sp") == 3
+    gated = gated_rows(count, 1, given, message, total_ref, note_ref, gate_ref)
+    gated_ref[...] = gated
+    width = pieces[0].shape[1]
+    for place, piece in enumerate(pieces):
+        part_ref[:, place * width : (place + 1) * width] = product(gated, piece[rows:, :])
+
+
+def finish_kernel(
+    count, whole, last, gate_ref, total_ref, note_ref, next_ref, later_ref, gated_ref, part_ref, *refs
+):
+    pieces, out_ref = refs[:-1], refs[-1]
+    rows, device = gated_ref.shape[1], lax.axis_index("dp")
+    width = pieces[0].shape[1]
+
+    def message(columns):
+        return next_ref[:, columns].astype(jnp.float32) + later_ref[:, columns].astype(jnp.float32)
+
+    gated = gated_rows(count, 0, lax.axis_index("sp") >= 2, message, total_ref, note_ref, gate_ref)
+
+    def put(masks, columns):
+        mask = jnp.where(device & CORE, masks[1], masks[0])
+        start = pl.multiple_of((device ^ mask) * width, width)
+        out_ref[:, pl.ds(start, width)] = columns.astype(out_ref.dtype)
+
+    for place, (masks, piece) in enumerate(zip(whole, pieces)):
+        part = part_ref[:, place * width : (place + 1) * width]
+        put(masks, part + product(gated, piece[:rows, :]))
+    both = jnp.concatenate([gated, gated_ref[...]], axis=1)
+    for masks, piece in zip(last, pieces[len(whole) :]):
+        put(masks, product(both, piece[...]))
+
+
+def kernel_call(kernel, operands, outs, flops, limit):
+    vmem = pl.BlockSpec(memory_space=pltpu.VMEM)
+    size = sum(x.size * x.dtype.itemsize for x in (*operands, *outs))
+    return pl.pallas_call(
+        kernel,
+        out_shape=outs,
+        in_specs=[vmem] * len(operands),
+        out_specs=[vmem] * len(outs),
+        compiler_params=pltpu.CompilerParams(vmem_limit_bytes=limit * MIB),
+        cost_estimate=pl.CostEstimate(flops=flops, bytes_accessed=size, transcendentals=0),
+    )(*operands)
+
+
+def block_body(queries, key_rows, values, out_gate, input_gate, forget_gate, out_weight):
+    return block_steps(
+        queries[0], key_rows[0], values[0], out_gate[0], input_gate[0], forget_gate[0], out_weight
+    )[None]
+
+
+def block_steps(query, key, value, gate, input_log, forget, out_weight):
+    tokens, heads = query.shape[0], input_log.shape[0]
+    key_width, value_width = query.shape[1] // heads, value.shape[1] // heads
+    shape = jax.ShapeDtypeStruct
+    device_count = lax.axis_size("dp")
+
+    def swap(piece, bit):
+        return lax.ppermute(piece, "dp", [(i, i ^ bit) for i in range(device_count)])
+
+    count = heads // 2
+    gates = jnp.concatenate([input_log, forget], axis=0)
+
+    def payload(half):
+        wide = key.shape[1] // 2
+        tall = value.shape[1] // 2
+        parts = [
+            key[:, half * wide : (half + 1) * wide],
+            value[:, half * tall : (half + 1) * tall],
+        ]
+        below = jnp.pad(gates, ((0, 0), (0, wide + tall - tokens)))
+        return jnp.concatenate([jnp.concatenate(parts, axis=1), below], axis=0)
+
+    high = payload(1)
+    low = payload(0)
+    last = lax.ppermute(high, "sp", [(0, 1), (1, 2)])
+    near = lax.ppermute(query, "sp", [(2, 1), (3, 2)])
+    far = lax.ppermute(query, "sp", [(3, 1)])
+    pair = lax.ppermute(low, "sp", [(0, 1), (2, 3)])
+    before = lax.ppermute(last, "sp", [(1, 2)])
+
+    def cross(piece, even, odd):
+        pairs = [(i, i ^ (odd if i & CORE else even)) for i in range(device_count)]
+        return lax.ppermute(piece, "dp", pairs)
+
+    side_a = cross(out_weight, XBIT, YBIT)
+    side_b = cross(out_weight, YBIT, XBIT)
+    corner = cross(side_a, YBIT, XBIT)
+    whole = {
+        (0, 0): out_weight,
+        (CORE, CORE): swap(out_weight, CORE),
+        (XBIT, YBIT): side_a,
+        (YBIT | CORE, XBIT | CORE): swap(side_a, CORE),
+        (YBIT, XBIT): side_b,
+        (XBIT | CORE, YBIT | CORE): swap(side_b, CORE),
+    }
+    corners = {
+        (XBIT | YBIT,) * 2: corner,
+        (XBIT | YBIT | CORE,) * 2: swap(corner, CORE),
+    }
+
+    work = 2 * tokens * tokens * (key_width + value_width)
+    sums = [
+        shape((tokens, count * value_width), jnp.float32),
+        shape((tokens, LANES), jnp.float32),
+    ] * 2
+    own = kernel_call(
+        functools.partial(own_kernel, count), [low, high, query], sums, 3 * heads * work // 2, 8
+    )
+    message = shape((tokens, count * value_width + LANES), jnp.bfloat16)
+    given_next, given_later = kernel_call(
+        functools.partial(serve_low_kernel, count),
+        [pair, low, near, far],
+        [message] * 2,
+        4 * count * work,
+        8,
+    )
+    (given_high,) = kernel_call(
+        functools.partial(serve_high_kernel, count),
+        [before, last, high, near],
+        [message],
+        3 * count * work,
+        8,
+    )
+    from_next = lax.ppermute(given_next, "sp", [(1, 2)])
+    from_later = lax.ppermute(given_later, "sp", [(1, 3)])
+    from_high = lax.ppermute(given_high, "sp", [(2, 3)])
+    home = kernel_call(
+        functools.partial(join_kernel, count),
+        [pair, before, last, query, *own],
+        sums,
+        3 * heads * work // 2,
+        8,
+    )
+    width = out_weight.shape[1]
+    kept = kernel_call(
+        functools.partial(first_kernel, count),
+        [gate, *home[2:], from_high, *whole.values()],
+        [
+            shape((tokens, count * value_width), jnp.bfloat16),
+            shape((tokens, len(whole) * width), jnp.float32),
+        ],
+        2 * tokens * count * value_width * len(whole) * width,
+        10,
+    )
+    (out,) = kernel_call(
+        functools.partial(finish_kernel, count, tuple(whole), tuple(corners)),
+        [gate, *home[:2], from_next, from_later, *kept, *whole.values(), *corners.values()],
+        [shape((tokens, width * device_count), jnp.bfloat16)],
+        2 * tokens * count * value_width * width * device_count,
+        12,
+    )
+    return out
+
+
 def body(queries, key_rows, values, out_gate, input_gate, forget_gate, out_weight):
     group_count = lax.axis_size("sp")
     token_count = queries.shape[1]
@@ -118,8 +508,9 @@
 
 
 def solution(mesh):
+    blocks = mesh.shape["sp"] == 4 and mesh.shape["dp"] == 8
     return jax.shard_map(
-        body,
+        block_body if blocks else body,
         mesh=mesh,
         in_specs=(
             P("dp", "sp", None),

time: 122 us -> 85.7 us (0.70)
  the two profiles are of different devices: /device:TPU:0 before, /device:TPU:24 now
where the time goes in v8:
time: 85.7 us; the launch traced here: 85.4 us
  waiting for transfers between devices  50.3 us (59%)
  starting transfers between devices  25.8 us (30%)
  Pallas kernels  7.79 us (9%)
  local copies, waits for them, and re-layouts  1.23 us (1%)
    ppermute x3, waiting for transfers between devices, cross(): return lax.ppermute(piece, 'dp', pairs)  22.1 us
    ppermute x1, starting transfers between devices, block_steps(): far = lax.ppermute(query, 'sp', [(3, 1)])  12.7 us
    ppermute x1, waiting for transfers between devices, block_steps(): pair = lax.ppermute(low, 'sp', [(0, 1), (2, 3)])  11.8 us
    pallas_call x6, Pallas kernels, kernel_call(): pl.pallas_call(kernel, out_shape=outs, in_specs=[vmem] * len(operands), o...  7.79 us
    ppermute x1, waiting for transfers between devices, block_steps(): from_high = lax.ppermute(given_high, 'sp', [(2, 3)])  7.56 us
    ppermute x1, waiting for transfers between devices, block_steps(): from_later = lax.ppermute(given_later, 'sp', [(1, 3)])  5.16 us
    ppermute x1, waiting for transfers between devices, block_steps(): far = lax.ppermute(query, 'sp', [(3, 1)])  3.76 us
    ppermute x3, starting transfers between devices, cross(): return lax.ppermute(piece, 'dp', pairs)  3.73 us
  transfers between devices with their start and end apart: 15, of which 5 were waited for; matrix products, arithmetic and copies ran while one was open for 1% of the time, Pallas kernels for 6%

profile of v8, /device:TPU:24, one launch (start us, length us, event | category | flops | bytes accessed | tf_op | source)
XLA Modules:
  0.0 85.4 jit_solution(13081794935576628883)
XLA Ops:
  0.0 0.0 copy-start.3
  0.0 1.5 %collective-permute-start.9 = (bf16[2048,256]{1,0:T(8,128)(2,1)}, bf16[2048,256]{1,0:T(8,128)(2,1)S(1)}, u32[]{:S(2)}, u32[]{:S(2)}) collective-permute-start(bf16[2048,256]{1,0:T(8,128)(2,1)} %refs_0_.3), channel_id=1, source_target_pairs={{0,2},{1,5},{2,0},{3,7},{4,6},{5,1},{6,4},{7,3},{8,10},{9,13},{10,... | collective-permute-start | bytes 3145736 | tf_op jit(solution)/shard_map/ppermute | solution.py:385
  1.5 1.5 %collective-permute-start.11 = (bf16[2048,256]{1,0:T(8,128)(2,1)}, bf16[2048,256]{1,0:T(8,128)(2,1)S(1)}, u32[]{:S(2)}, u32[]{:S(2)}) collective-permute-start(bf16[2048,256]{1,0:T(8,128)(2,1)} %refs_0_.3), channel_id=1, source_target_pairs={{0,4},{1,3},{2,6},{3,1},{4,0},{5,7},{6,2},{7,5},{8,12},{9,11},{10,... | collective-permute-start | bytes 3145736 | tf_op jit(solution)/shard_map/ppermute | solution.py:385
  3.0 1.0 %fusion.4 = (bf16[128,512]{1,0:T(8,128)(2,1)S(1)}, bf16[128,512]{1,0:T(8,128)(2,1)S(1)}) fusion(bf16[128,1024]{1,0:T(8,128)(2,1)} %bitcast.14), kind=kLoop, calls=%fused_computation.7 | loop fusion | bytes 524288 | tf_op jit(solution)/shard_map/slice | solution.py:369
  4.0 0.0 copy-done.3
  4.0 0.0 copy-start.4
  4.0 0.0 copy-start.5
  4.1 0.0 copy-start
  4.1 22.0 %collective-permute-done.9.refs_2_ = bf16[2048,256]{1,0:T(8,128)(2,1)S(1)} collective-permute-done((bf16[2048,256]{1,0:T(8,128)(2,1)}, bf16[2048,256]{1,0:T(8,128)(2,1)S(1)}, u32[]{:S(2)}, u32[]{:S(2)}) %collective-permute-start.9) | collective-permute-done | bytes 1048608 | tf_op jit(solution)/shard_map/ppermute | solution.py:385
  26.1 0.7 collective-permute-start.13
  26.9 0.0 copy-done.4
  26.9 0.0 copy-done.5
  26.9 0.0 copy-start.2
  26.9 0.1 pad_maximum_fusion
  27.0 0.7 collective-permute-start.1
  27.6 0.2 copy-done.2
  27.8 2.8 %collective-permute-start.3 = (bf16[128,1024]{1,0:T(8,128)(2,1)S(1)}, bf16[128,1024]{1,0:T(8,128)(2,1)S(1)}, u32[]{:S(2)}, u32[]{:S(2)}) collective-permute-start(bf16[128,1024]{1,0:T(8,128)(2,1)S(1)} %bitcast.9), channel_id=1, source_target_pairs={{16,8},{24,16},{17,9},{25,17},{18,10},{26,18},{19,11},{27,19},{20,... | collective-permute-start | bytes 786440 | tf_op jit(solution)/shard_map/ppermute | solution.py:378
  30.6 0.0 collective-permute-done.1.last_ref
  30.7 0.7 collective-permute-start.2
  31.3 12.7 %collective-permute-start.4 = (bf16[128,1024]{1,0:T(8,128)(2,1)S(1)}, bf16[128,1024]{1,0:T(8,128)(2,1)S(1)}, u32[]{:S(2)}, u32[]{:S(2)}) collective-permute-start(bf16[128,1024]{1,0:T(8,128)(2,1)S(1)} %bitcast.10), channel_id=1, source_target_pairs={{24,8},{25,9},{26,10},{27,11},{28,12},{29,13},{30,14},{31,15}} | collective-permute-start | bytes 786440 | tf_op jit(solution)/shard_map/ppermute | solution.py:379
  44.1 0.0 collective-permute-done.3.near_ref
  44.1 0.0 copy-done
  44.1 0.1 collective-permute-start.8
  44.2 3.8 %collective-permute-done.4.far_ref = bf16[128,1024]{1,0:T(8,128)(2,1)S(1)} collective-permute-done((bf16[128,1024]{1,0:T(8,128)(2,1)S(1)}, bf16[128,1024]{1,0:T(8,128)(2,1)S(1)}, u32[]{:S(2)}, u32[]{:S(2)}) %collective-permute-start.4) | collective-permute-done | bytes 262176 | tf_op jit(solution)/shard_map/ppermute | solution.py:379
  47.9 0.0 collective-permute-start.10
  47.9 0.0 collective-permute-done.11.refs_4_
  47.9 0.5 collective-permute-start.12
  48.4 0.0 collective-permute-done.13.refs_6_
  48.4 0.1 collective-permute-start.14
  48.5 0.0 collective-permute-done.2.before_ref
  48.5 1.3 %collective-permute-start = (bf16[136,1536]{1,0:T(8,128)(2,1)S(1)}, bf16[136,1536]{1,0:T(8,128)(2,1)S(1)}, u32[]{:S(2)}, u32[]{:S(2)}) collective-permute-start(bf16[136,1536]{1,0:T(8,128)(2,1)S(1)} %get-tuple-element.34.low_ref), channel_id=1, source_target_pairs={{0,8},{16,24},{1,9},{17,25},{2,10},{18,26},{3,11},{19,27},{4,12},{... | collective-permute-start | bytes 1253384 | tf_op jit(solution)/shard_map/ppermute | solution.py:380
  49.8 0.8 shard_map.76
  50.6 11.8 %collective-permute-done.pair_ref = bf16[136,1536]{1,0:T(8,128)(2,1)S(1)} collective-permute-done((bf16[136,1536]{1,0:T(8,128)(2,1)S(1)}, bf16[136,1536]{1,0:T(8,128)(2,1)S(1)}, u32[]{:S(2)}, u32[]{:S(2)}) %collective-permute-start) | collective-permute-done | bytes 417824 | tf_op jit(solution)/shard_map/ppermute | solution.py:380
  62.4 1.3 %collective-permute-start.7 = (bf16[128,1152]{1,0:T(8,128)(2,1)S(1)}, bf16[128,1152]{1,0:T(8,128)(2,1)S(1)}, u32[]{:S(2)}, u32[]{:S(2)}) collective-permute-start(bf16[128,1152]{1,0:T(8,128)(2,1)S(1)} %shard_map.76), channel_id=1, source_target_pairs={{16,24},{17,25},{18,26},{19,27},{20,28},{21,29},{22,30},{23,31}} | collective-permute-start | bytes 884744 | tf_op jit(solution)/shard_map/ppermute | solution.py:428
  63.7 0.8 shard_map.75
  64.5 0.0 collective-permute-done.8.refs_1_
  64.5 0.7 collective-permute-start.5
  65.2 7.6 %collective-permute-done.7.next_ref = bf16[128,1152]{1,0:T(8,128)(2,1)S(1)} collective-permute-done((bf16[128,1152]{1,0:T(8,128)(2,1)S(1)}, bf16[128,1152]{1,0:T(8,128)(2,1)S(1)}, u32[]{:S(2)}, u32[]{:S(2)}) %collective-permute-start.7) | collective-permute-done | bytes 294944 | tf_op jit(solution)/shard_map/ppermute | solution.py:428
  72.8 1.3 %collective-permute-start.6 = (bf16[128,1152]{1,0:T(8,128)(2,1)S(1)}, bf16[128,1152]{1,0:T(8,128)(2,1)S(1)}, u32[]{:S(2)}, u32[]{:S(2)}) collective-permute-start(bf16[128,1152]{1,0:T(8,128)(2,1)S(1)} %get-tuple-element.24), channel_id=1, source_target_pairs={{8,24},{9,25},{10,26},{11,27},{12,28},{13,29},{14,30},{15,31}} | collective-permute-start | bytes 884744 | tf_op jit(solution)/shard_map/ppermute | solution.py:427
  74.1 1.1 %shard_map.73 = (f32[128,1024]{1,0:T(8,128)S(1)}, f32[128,128]{1,0:T(8,128)S(1)}, f32[128,1024]{1,0:T(8,128)S(1)}, f32[128,128]{1,0:T(8,128)S(1)}) custom-call(bf16[136,1536]{1,0:T(8,128)(2,1)S(1)} %get-tuple-element.34.low_ref, bf16[136,1536]{1,0:T(8,128)(2,1)S(1)} %get-tuple-element.33.high_ref, bf16[128,1024]{1,0:T(8,128)(2,1)S(1)} %bitcast.11), custom_call_target="tpu_custom_call" | custom-call | flops 150994944 | bytes 2277376 | tf_op jit(solution)/shard_map/pallas_call | solution.py:337
  75.2 0.0 copy-start.1
  75.2 1.6 %shard_map.74 = (f32[128,1024]{1,0:T(8,128)S(1)}, f32[128,128]{1,0:T(8,128)S(1)}, f32[128,1024]{1,0:T(8,128)S(1)}, f32[128,128]{1,0:T(8,128)S(1)}) custom-call(bf16[136,1536]{1,0:T(8,128)(2,1)S(1)} %collective-permute-done.pair_ref, bf16[136,1536]{1,0:T(8,128)(2,1)S(1)} %collective-permute-done.2.before_ref, ...), custom_call_target="tpu_custom_call" | custom-call | flops 150994944 | bytes 3874816 | tf_op jit(solution)/shard_map/pallas_call | solution.py:337
  76.8 0.0 collective-permute-done.10.refs_3_
  76.8 0.0 collective-permute-done.12.refs_5_
  76.9 0.0 copy-done.1
  76.9 1.2 %shard_map.77 = (bf16[128,1024]{1,0:T(8,128)(2,1)S(1)}, f32[128,1536]{1,0:T(8,128)S(1)}) custom-call(bf16[128,2048]{1,0:T(8,128)(2,1)S(1)} %bitcast.7, f32[128,1024]{1,0:T(8,128)S(1)} %get-tuple-element.25.total_ref, f32[128,128]{1,0:T(8,128)S(1)} %get-tuple-element.26.note_ref, bf16[128,1152]{1,0:T(8,128)(2,1)S(1)} %collective-permute-done.7.next_ref, ...), custom_call_target="tpu_custom_call" | custom-call | flops 402653184 | bytes 8749056 | tf_op jit(solution)/shard_map/pallas_call | solution.py:337
  78.0 0.0 collective-permute-done.5.next_ref
  78.0 5.2 %collective-permute-done.6.later_ref = bf16[128,1152]{1,0:T(8,128)(2,1)S(1)} collective-permute-done((bf16[128,1152]{1,0:T(8,128)(2,1)S(1)}, bf16[128,1152]{1,0:T(8,128)(2,1)S(1)}, u32[]{:S(2)}, u32[]{:S(2)}) %collective-permute-start.6) | collective-permute-done | bytes 294944 | tf_op jit(solution)/shard_map/ppermute | solution.py:427
  83.2 0.0 collective-permute-done.14.refs_7_
  83.2 2.2 %shard_map.78 = bf16[128,2048]{1,0:T(8,128)(2,1)} custom-call(bf16[128,2048]{1,0:T(8,128)(2,1)S(1)} %bitcast.8, f32[128,1024]{1,0:T(8,128)S(1)} %get-tuple-element.21.total_ref, f32[128,128]{1,0:T(8,128)S(1)} %get-tuple-element.22.note_ref, bf16[128,1152]{1,0:T(8,128)(2,1)S(1)} %collective-permute-done.5.next_ref, ...), custom_call_target="tpu_custom_call" | custom-call | flops 536870912 | bytes 11665408 | tf_op jit(solution)/shard_map/pallas_call | solution.py:337
  (2 shorter events, 0.0 us)
Async XLA Ops:
  0.0 4.0 %copy-start.3 = (bf16[1,128,2048]{2,1,0:T(8,128)(2,1)S(1)}, bf16[1,128,2048]{2,1,0:T(8,128)(2,1)}, u32[]{:S(2)}) copy-start(bf16[1,128,2048]{2,1,0:T(8,128)(2,1)} %param.9) | copy-start | bytes 1572868
  0.0 26.1 %collective-permute-start.9 = (bf16[2048,256]{1,0:T(8,128)(2,1)}, bf16[2048,256]{1,0:T(8,128)(2,1)S(1)}, u32[]{:S(2)}, u32[]{:S(2)}) collective-permute-start(bf16[2048,256]{1,0:T(8,128)(2,1)} %refs_0_.3), channel_id=1, source_target_pairs={{0,2},{1,5},{2,0},{3,7},{4,6},{5,1},{6,4},{7,3},{8,10},{9,13},{10,... | collective-permute-start | bytes 3145736 | tf_op jit(solution)/shard_map/ppermute | solution.py:385
  1.5 46.4 %collective-permute-start.11 = (bf16[2048,256]{1,0:T(8,128)(2,1)}, bf16[2048,256]{1,0:T(8,128)(2,1)S(1)}, u32[]{:S(2)}, u32[]{:S(2)}) collective-permute-start(bf16[2048,256]{1,0:T(8,128)(2,1)} %refs_0_.3), channel_id=1, source_target_pairs={{0,4},{1,3},{2,6},{3,1},{4,0},{5,7},{6,2},{7,5},{8,12},{9,11},{10,... | collective-permute-start | bytes 3145736 | tf_op jit(solution)/shard_map/ppermute | solution.py:385
  4.0 22.8 %copy-start.4 = (bf16[1,4,128]{2,1,0:T(4,128)(2,1)S(1)}, bf16[1,4,128]{2,1,0:T(4,128)(2,1)}, u32[]{:S(2)}) copy-start(bf16[1,4,128]{2,1,0:T(4,128)(2,1)} %param.12) | copy-start | bytes 3076
  4.0 22.8 %copy-start.5 = (bf16[1,4,128]{2,1,0:T(4,128)(2,1)S(1)}, bf16[1,4,128]{2,1,0:T(4,128)(2,1)}, u32[]{:S(2)}) copy-start(bf16[1,4,128]{2,1,0:T(4,128)(2,1)} %param.11) | copy-start | bytes 3076
  4.1 40.0 %copy-start = (bf16[2048,256]{1,0:T(8,128)(2,1)S(1)}, bf16[2048,256]{1,0:T(8,128)(2,1)}, u32[]{:S(2)}) copy-start(bf16[2048,256]{1,0:T(8,128)(2,1)} %refs_0_.3) | copy-start | bytes 3145732
  26.1 22.3 %collective-permute-start.13 = (bf16[2048,256]{1,0:T(8,128)(2,1)S(1)}, bf16[2048,256]{1,0:T(8,128)(2,1)S(1)}, u32[]{:S(2)}, u32[]{:S(2)}) collective-permute-start(bf16[2048,256]{1,0:T(8,128)(2,1)S(1)} %collective-permute-done.9.refs_2_), channel_id=1, source_target_pairs={{0,4},{1,3},{2,6},{3,1},{4,0},{5,7},{6,2},{7,5},{8,12},{9,11},{10,... | collective-permute-start | bytes 3145736 | tf_op jit(solution)/shard_map/ppermute | solution.py:385
  26.9 1.0 %copy-start.2 = (bf16[1,128,1024]{2,1,0:T(8,128)(2,1)S(1)}, bf16[1,128,1024]{2,1,0:T(8,128)(2,1)}, u32[]{:S(2)}) copy-start(bf16[1,128,1024]{2,1,0:T(8,128)(2,1)} %param.7) | copy-start | bytes 786436
  27.0 3.7 %collective-permute-start.1 = (bf16[136,1536]{1,0:T(8,128)(2,1)S(1)}, bf16[136,1536]{1,0:T(8,128)(2,1)S(1)}, u32[]{:S(2)}, u32[]{:S(2)}) collective-permute-start(bf16[136,1536]{1,0:T(8,128)(2,1)S(1)} %get-tuple-element.33.high_ref), channel_id=1, source_target_pairs={{0,8},{8,16},{1,9},{9,17},{2,10},{10,18},{3,11},{11,19},{4,12},{12... | collective-permute-start | bytes 1253384 | tf_op jit(solution)/shard_map/ppermute | solution.py:377
  27.8 16.2 %collective-permute-start.3 = (bf16[128,1024]{1,0:T(8,128)(2,1)S(1)}, bf16[128,1024]{1,0:T(8,128)(2,1)S(1)}, u32[]{:S(2)}, u32[]{:S(2)}) collective-permute-start(bf16[128,1024]{1,0:T(8,128)(2,1)S(1)} %bitcast.9), channel_id=1, source_target_pairs={{16,8},{24,16},{17,9},{25,17},{18,10},{26,18},{19,11},{27,19},{20,... | collective-permute-start | bytes 786440 | tf_op jit(solution)/shard_map/ppermute | solution.py:378
  30.7 17.9 %collective-permute-start.2 = (bf16[136,1536]{1,0:T(8,128)(2,1)S(1)}, bf16[136,1536]{1,0:T(8,128)(2,1)S(1)}, u32[]{:S(2)}, u32[]{:S(2)}) collective-permute-start(bf16[136,1536]{1,0:T(8,128)(2,1)S(1)} %collective-permute-done.1.last_ref), channel_id=1, source_target_pairs={{8,16},{9,17},{10,18},{11,19},{12,20},{13,21},{14,22},{15,23}} | collective-permute-start | bytes 1253384 | tf_op jit(solution)/shard_map/ppermute | solution.py:381
  31.3 16.6 %collective-permute-start.4 = (bf16[128,1024]{1,0:T(8,128)(2,1)S(1)}, bf16[128,1024]{1,0:T(8,128)(2,1)S(1)}, u32[]{:S(2)}, u32[]{:S(2)}) collective-permute-start(bf16[128,1024]{1,0:T(8,128)(2,1)S(1)} %bitcast.10), channel_id=1, source_target_pairs={{24,8},{25,9},{26,10},{27,11},{28,12},{29,13},{30,14},{31,15}} | collective-permute-start | bytes 786440 | tf_op jit(solution)/shard_map/ppermute | solution.py:379
  44.1 20.4 %collective-permute-start.8 = (bf16[2048,256]{1,0:T(8,128)(2,1)S(1)}, bf16[2048,256]{1,0:T(8,128)(2,1)S(1)}, u32[]{:S(2)}, u32[]{:S(2)}) collective-permute-start(bf16[2048,256]{1,0:T(8,128)(2,1)S(1)} %copy-done), channel_id=1, source_target_pairs={{0,1},{1,0},{2,3},{3,2},{4,5},{5,4},{6,7},{7,6},{8,9},{9,8},{10,11... | collective-permute-start | bytes 3145736 | tf_op jit(solution)/shard_map/ppermute | solution.py:360
  47.9 28.9 %collective-permute-start.10 = (bf16[2048,256]{1,0:T(8,128)(2,1)S(1)}, bf16[2048,256]{1,0:T(8,128)(2,1)S(1)}, u32[]{:S(2)}, u32[]{:S(2)}) collective-permute-start(bf16[2048,256]{1,0:T(8,128)(2,1)S(1)} %collective-permute-done.9.refs_2_), channel_id=1, source_target_pairs={{0,1},{1,0},{2,3},{3,2},{4,5},{5,4},{6,7},{7,6},{8,9},{9,8},{10,11... | collective-permute-start | bytes 3145736 | tf_op jit(solution)/shard_map/ppermute | solution.py:360
  47.9 28.9 %collective-permute-start.12 = (bf16[2048,256]{1,0:T(8,128)(2,1)S(1)}, bf16[2048,256]{1,0:T(8,128)(2,1)S(1)}, u32[]{:S(2)}, u32[]{:S(2)}) collective-permute-start(bf16[2048,256]{1,0:T(8,128)(2,1)S(1)} %collective-permute-done.11.refs_4_), channel_id=1, source_target_pairs={{0,1},{1,0},{2,3},{3,2},{4,5},{5,4},{6,7},{7,6},{8,9},{9,8},{10,11... | collective-permute-start | bytes 3145736 | tf_op jit(solution)/shard_map/ppermute | solution.py:360
  48.4 34.7 %collective-permute-start.14 = (bf16[2048,256]{1,0:T(8,128)(2,1)S(1)}, bf16[2048,256]{1,0:T(8,128)(2,1)S(1)}, u32[]{:S(2)}, u32[]{:S(2)}) collective-permute-start(bf16[2048,256]{1,0:T(8,128)(2,1)S(1)} %collective-permute-done.13.refs_6_), channel_id=1, source_target_pairs={{0,1},{1,0},{2,3},{3,2},{4,5},{5,4},{6,7},{7,6},{8,9},{9,8},{10,11... | collective-permute-start | bytes 3145736 | tf_op jit(solution)/shard_map/ppermute | solution.py:360
  48.5 13.9 %collective-permute-start = (bf16[136,1536]{1,0:T(8,128)(2,1)S(1)}, bf16[136,1536]{1,0:T(8,128)(2,1)S(1)}, u32[]{:S(2)}, u32[]{:S(2)}) collective-permute-start(bf16[136,1536]{1,0:T(8,128)(2,1)S(1)} %get-tuple-element.34.low_ref), channel_id=1, source_target_pairs={{0,8},{16,24},{1,9},{17,25},{2,10},{18,26},{3,11},{19,27},{4,12},{... | collective-permute-start | bytes 1253384 | tf_op jit(solution)/shard_map/ppermute | solution.py:380
  62.4 10.4 %collective-permute-start.7 = (bf16[128,1152]{1,0:T(8,128)(2,1)S(1)}, bf16[128,1152]{1,0:T(8,128)(2,1)S(1)}, u32[]{:S(2)}, u32[]{:S(2)}) collective-permute-start(bf16[128,1152]{1,0:T(8,128)(2,1)S(1)} %shard_map.76), channel_id=1, source_target_pairs={{16,24},{17,25},{18,26},{19,27},{20,28},{21,29},{22,30},{23,31}} | collective-permute-start | bytes 884744 | tf_op jit(solution)/shard_map/ppermute | solution.py:428
  64.5 13.5 %collective-permute-start.5 = (bf16[128,1152]{1,0:T(8,128)(2,1)S(1)}, bf16[128,1152]{1,0:T(8,128)(2,1)S(1)}, u32[]{:S(2)}, u32[]{:S(2)}) collective-permute-start(bf16[128,1152]{1,0:T(8,128)(2,1)S(1)} %get-tuple-element.23), channel_id=1, source_target_pairs={{8,16},{9,17},{10,18},{11,19},{12,20},{13,21},{14,22},{15,23}} | collective-permute-start | bytes 884744 | tf_op jit(solution)/shard_map/ppermute | solution.py:426
  72.8 10.4 %collective-permute-start.6 = (bf16[128,1152]{1,0:T(8,128)(2,1)S(1)}, bf16[128,1152]{1,0:T(8,128)(2,1)S(1)}, u32[]{:S(2)}, u32[]{:S(2)}) collective-permute-start(bf16[128,1152]{1,0:T(8,128)(2,1)S(1)} %get-tuple-element.24), channel_id=1, source_target_pairs={{8,24},{9,25},{10,26},{11,27},{12,28},{13,29},{14,30},{15,31}} | collective-permute-start | bytes 884744 | tf_op jit(solution)/shard_map/ppermute | solution.py:427
  75.2 1.7 %copy-start.1 = (bf16[1,128,2048]{2,1,0:T(8,128)(2,1)S(1)}, bf16[1,128,2048]{2,1,0:T(8,128)(2,1)}, u32[]{:S(2)}) copy-start(bf16[1,128,2048]{2,1,0:T(8,128)(2,1)} %param.10) | copy-start | bytes 1572868

commit v9 on v8

--- a/solution.py
+++ b/solution.py
@@ -261,14 +261,15 @@
     answer(count, 1, [before_ref, last_ref, high_ref], [near_ref], [next_ref])
 
 
-def gated_rows(count, half, given, message, total_ref, note_ref, gate_ref):
-    value_width = total_ref.shape[1] // count
-    own = note_ref[...]
+def gated_rows(count, half, given, message, totals, notes, gate_ref):
+    value_width = totals[0].shape[1] // count
+    low = half == 0
+    own = jnp.where(low, notes[0][...], notes[1][...])
     lanes = message(slice(count * value_width, count * value_width + LANES))
     gated = []
     for place in range(count):
         out = slice(place * value_width, (place + 1) * value_width)
-        start = (half * count + place) * value_width
+        start = pl.multiple_of((half * count + place) * value_width, value_width)
         at = 6 * place
         sums = lanes[:, at : at + 1] + lanes[:, at + 1 : at + 2] + lanes[:, at + 2 : at + 3]
         at += 3
@@ -280,9 +281,10 @@
         scale_given = jnp.where(given, jnp.exp(reach - peak), 0.0)
         weight = scale * own[:, 3 * place : 3 * place + 1] + scale_given * sums
         inverse = 1.0 / jnp.maximum(jnp.abs(weight), 1.0)
-        cell = (scale * inverse) * total_ref[:, out] + (scale_given * inverse) * message(out)
+        total = jnp.where(low, totals[0][:, out], totals[1][:, out])
+        cell = (scale * inverse) * total + (scale_given * inverse) * message(out)
         hidden = cell.astype(jnp.bfloat16).astype(jnp.float32)
-        gate = jax.nn.sigmoid(gate_ref[:, start : start + value_width].astype(jnp.float32))
+        gate = jax.nn.sigmoid(gate_ref[:, pl.ds(start, value_width)].astype(jnp.float32))
         gated.append((hidden * gate).astype(jnp.bfloat16))
     return jnp.concatenate(gated, axis=1)
 
@@ -291,32 +293,47 @@
     return jnp.dot(left, right, preferred_element_type=jnp.float32)
 
 
-def first_kernel(count, gate_ref, total_ref, note_ref, next_ref, *refs):
+def first_half():
+    return jnp.where(lax.axis_index("sp") == 3, 0, 1)
+
+
+def rows_of(piece, half, rows):
+    return piece[pl.ds(pl.multiple_of(half * rows, rows), rows), :]
+
+
+def first_kernel(count, gate_ref, low_ref, low_note, high_ref, high_note, later_ref, *refs):
     pieces, gated_ref, part_ref = refs[:-2], refs[-2], refs[-1]
-    rows = gated_ref.shape[1]
+    rows, half = gated_ref.shape[1], first_half()
 
     def message(columns):
-        return next_ref[:, columns].astype(jnp.float32)
+        return later_ref[:, columns].astype(jnp.float32)
 
     given = lax.axis_index("sp") == 3
-    gated = gated_rows(count, 1, given, message, total_ref, note_ref, gate_ref)
+    totals, notes = (low_ref, high_ref), (low_note, high_note)
+    gated = gated_rows(count, half, given, message, totals, notes, gate_ref)
     gated_ref[...] = gated
     width = pieces[0].shape[1]
     for place, piece in enumerate(pieces):
-        part_ref[:, place * width : (place + 1) * width] = product(gated, piece[rows:, :])
+        part_ref[:, place * width : (place + 1) * width] = product(
+            gated, rows_of(piece, half, rows)
+        )
 
 
 def finish_kernel(
-    count, whole, last, gate_ref, total_ref, note_ref, next_ref, later_ref, gated_ref, part_ref, *refs
+    count, whole, last, gate_ref, low_ref, low_note, high_ref, high_note, next_ref, nextx_ref,
+    gated_ref, part_ref, *refs,
 ):
     pieces, out_ref = refs[:-1], refs[-1]
     rows, device = gated_ref.shape[1], lax.axis_index("dp")
     width = pieces[0].shape[1]
+    half = first_half()
 
     def message(columns):
-        return next_ref[:, columns].astype(jnp.float32) + later_ref[:, columns].astype(jnp.float32)
-
-    gated = gated_rows(count, 0, lax.axis_index("sp") >= 2, message, total_ref, note_ref, gate_ref)
+        return next_ref[:, columns].astype(jnp.float32) + nextx_ref[:, columns].astype(jnp.float32)
+
+    given = lax.axis_index("sp") >= 2
+    totals, notes = (low_ref, high_ref), (low_note, high_note)
+    gated = gated_rows(count, 1 - half, given, message, totals, notes, gate_ref)
 
     def put(masks, columns):
         mask = jnp.where(device & CORE, masks[1], masks[0])
@@ -325,10 +342,10 @@
 
     for place, (masks, piece) in enumerate(zip(whole, pieces)):
         part = part_ref[:, place * width : (place + 1) * width]
-        put(masks, part + product(gated, piece[:rows, :]))
-    both = jnp.concatenate([gated, gated_ref[...]], axis=1)
+        put(masks, part + product(gated, rows_of(piece, 1 - half, rows)))
     for masks, piece in zip(last, pieces[len(whole) :]):
-        put(masks, product(both, piece[...]))
+        part = product(gated_ref[...], rows_of(piece, half, rows))
+        put(masks, part + product(gated, rows_of(piece, 1 - half, rows)))
 
 
 def kernel_call(kernel, operands, outs, flops, limit):
@@ -436,7 +453,7 @@
     width = out_weight.shape[1]
     kept = kernel_call(
         functools.partial(first_kernel, count),
-        [gate, *home[2:], from_high, *whole.values()],
+        [gate, *home, from_later, *whole.values()],
         [
             shape((tokens, count * value_width), jnp.bfloat16),
             shape((tokens, len(whole) * width), jnp.float32),
@@ -446,7 +463,7 @@
     )
     (out,) = kernel_call(
         functools.partial(finish_kernel, count, tuple(whole), tuple(corners)),
-        [gate, *home[:2], from_next, from_later, *kept, *whole.values(), *corners.values()],
+        [gate, *home, from_next, from_high, *kept, *whole.values(), *corners.values()],
         [shape((tokens, width * device_count), jnp.bfloat16)],
         2 * tokens * count * value_width * width * device_count,
         12,

time: 85.7 us -> 76.3 us (0.89)
  starting transfers between devices: 25.8 us -> 16 us
    ppermute x1, waiting for transfers between devices: 5.16 us -> 22.5 us  [block_steps(): from_later = lax.ppermute(given_later, 'sp', [(1, 3)])]
    ppermute x1, waiting for transfers between devices: 11.8 us -> 0.01 us  [block_steps(): pair = lax.ppermute(low, 'sp', [(0, 1), (2, 3)])]
    ppermute x1, starting transfers between devices: 12.7 us -> 2.25 us  [block_steps(): far = lax.ppermute(query, 'sp', [(3, 1)])]
    ppermute x1, waiting for transfers between devices: 7.56 us -> 3.29 us  [block_steps(): from_high = lax.ppermute(given_high, 'sp', [(2, 3)])]
    ppermute x1, waiting for transfers between devices: 3.76 us -> 0.01 us  [block_steps(): far = lax.ppermute(query, 'sp', [(3, 1)])]
    ppermute x3, waiting for transfers between devices: 22.1 us -> 24.3 us  [cross(): return lax.ppermute(piece, 'dp', pairs)]
    ppermute x3, starting transfers between devices: 3.73 us -> 5.61 us  [cross(): return lax.ppermute(piece, 'dp', pairs)]
    ppermute x1, starting transfers between devices: 2.8 us -> 1.31 us  [block_steps(): near = lax.ppermute(query, 'sp', [(2, 1), (3, 2)])]
  transfers between devices with their start and end apart: 15 -> 15, of which waited for: 5 -> 4; matrix products, arithmetic and copies ran while one was open for 1% -> 1% of each run, Pallas kernels for 6% -> 7%
where the time goes in v9:
time: 76.3 us; the launch traced here: 76 us
  waiting for transfers between devices  50.1 us (66%)
  starting transfers between devices  16 us (21%)
  Pallas kernels  7.84 us (10%)
  local copies, waits for them, and re-layouts  1.74 us (2%)
    ppermute x3, waiting for transfers between devices, cross(): return lax.ppermute(piece, 'dp', pairs)  24.3 us
    ppermute x1, waiting for transfers between devices, block_steps(): from_later = lax.ppermute(given_later, 'sp', [(1, 3)])  22.5 us
    pallas_call x6, Pallas kernels, kernel_call(): pl.pallas_call(kernel, out_shape=outs, in_specs=[vmem] * len(operands), o...  7.84 us
    ppermute x3, starting transfers between devices, cross(): return lax.ppermute(piece, 'dp', pairs)  5.61 us
    ppermute x1, waiting for transfers between devices, block_steps(): from_high = lax.ppermute(given_high, 'sp', [(2, 3)])  3.29 us
    ppermute x1, starting transfers between devices, block_steps(): far = lax.ppermute(query, 'sp', [(3, 1)])  2.25 us
  transfers between devices with their start and end apart: 15, of which 4 were waited for; matrix products, arithmetic and copies ran while one was open for 1% of the time, Pallas kernels for 7%

profile of v9, /device:TPU:24, one launch (start us, length us, event | category | flops | bytes accessed | tf_op | source)
XLA Modules:
  0.0 76.0 jit_solution(9773016279170392001)
XLA Ops:
  0.0 0.0 copy-start.3
  0.0 1.5 %collective-permute-start.9 = (bf16[2048,256]{1,0:T(8,128)(2,1)}, bf16[2048,256]{1,0:T(8,128)(2,1)S(1)}, u32[]{:S(2)}, u32[]{:S(2)}) collective-permute-start(bf16[2048,256]{1,0:T(8,128)(2,1)} %refs_0_.3), channel_id=1, source_target_pairs={{0,2},{1,5},{2,0},{3,7},{4,6},{5,1},{6,4},{7,3},{8,10},{9,13},{10,... | collective-permute-start | bytes 3145736 | tf_op jit(solution)/shard_map/ppermute | solution.py:402
  1.5 2.2 %collective-permute-start.4 = (bf16[128,1024]{1,0:T(8,128)(2,1)}, bf16[128,1024]{1,0:T(8,128)(2,1)S(1)}, u32[]{:S(2)}, u32[]{:S(2)}) collective-permute-start(bf16[128,1024]{1,0:T(8,128)(2,1)} %bitcast.9), channel_id=1, source_target_pairs={{24,8},{25,9},{26,10},{27,11},{28,12},{29,13},{30,14},{31,15}} | collective-permute-start | bytes 786440 | tf_op jit(solution)/shard_map/ppermute | solution.py:396
  3.7 1.3 %collective-permute-start.3 = (bf16[128,1024]{1,0:T(8,128)(2,1)}, bf16[128,1024]{1,0:T(8,128)(2,1)S(1)}, u32[]{:S(2)}, u32[]{:S(2)}) collective-permute-start(bf16[128,1024]{1,0:T(8,128)(2,1)} %bitcast.10), channel_id=1, source_target_pairs={{16,8},{24,16},{17,9},{25,17},{18,10},{26,18},{19,11},{27,19},{20,... | collective-permute-start | bytes 786440 | tf_op jit(solution)/shard_map/ppermute | solution.py:395
  5.1 1.6 %collective-permute-start.11 = (bf16[2048,256]{1,0:T(8,128)(2,1)}, bf16[2048,256]{1,0:T(8,128)(2,1)S(1)}, u32[]{:S(2)}, u32[]{:S(2)}) collective-permute-start(bf16[2048,256]{1,0:T(8,128)(2,1)} %refs_0_.3), channel_id=1, source_target_pairs={{0,4},{1,3},{2,6},{3,1},{4,0},{5,7},{6,2},{7,5},{8,12},{9,11},{10,... | collective-permute-start | bytes 3145736 | tf_op jit(solution)/shard_map/ppermute | solution.py:402
  6.6 0.0 copy-start.5
  6.7 1.0 %fusion.4 = (bf16[128,512]{1,0:T(8,128)(2,1)S(1)}, bf16[128,512]{1,0:T(8,128)(2,1)S(1)}) fusion(bf16[128,1024]{1,0:T(8,128)(2,1)} %bitcast.14), kind=kLoop, calls=%fused_computation.7 | loop fusion | bytes 524288 | tf_op jit(solution)/shard_map/slice | solution.py:386
  7.7 15.1 %collective-permute-done.9.refs_2_ = bf16[2048,256]{1,0:T(8,128)(2,1)S(1)} collective-permute-done((bf16[2048,256]{1,0:T(8,128)(2,1)}, bf16[2048,256]{1,0:T(8,128)(2,1)S(1)}, u32[]{:S(2)}, u32[]{:S(2)}) %collective-permute-start.9) | collective-permute-done | bytes 1048608 | tf_op jit(solution)/shard_map/ppermute | solution.py:402
  22.8 2.5 %collective-permute-start.13 = (bf16[2048,256]{1,0:T(8,128)(2,1)S(1)}, bf16[2048,256]{1,0:T(8,128)(2,1)S(1)}, u32[]{:S(2)}, u32[]{:S(2)}) collective-permute-start(bf16[2048,256]{1,0:T(8,128)(2,1)S(1)} %collective-permute-done.9.refs_2_), channel_id=1, source_target_pairs={{0,4},{1,3},{2,6},{3,1},{4,0},{5,7},{6,2},{7,5},{8,12},{9,11},{10,... | collective-permute-start | bytes 3145736 | tf_op jit(solution)/shard_map/ppermute | solution.py:402
  25.3 0.0 copy-start.4
  25.3 0.0 copy-done.5
  25.3 0.7 copy-done.4
  26.0 0.0 copy-done.3
  26.1 0.0 copy-start
  26.1 0.1 pad_maximum_fusion
  26.1 0.8 %collective-permute-start.1 = (bf16[136,1536]{1,0:T(8,128)(2,1)S(1)}, bf16[136,1536]{1,0:T(8,128)(2,1)S(1)}, u32[]{:S(2)}, u32[]{:S(2)}) collective-permute-start(bf16[136,1536]{1,0:T(8,128)(2,1)S(1)} %get-tuple-element.33.high_ref), channel_id=1, source_target_pairs={{0,8},{8,16},{1,9},{9,17},{2,10},{10,18},{3,11},{11,19},{4,12},{12... | collective-permute-start | bytes 1253384 | tf_op jit(solution)/shard_map/ppermute | solution.py:394
  27.0 0.0 collective-permute-done.4.far_ref
  27.0 1.3 %collective-permute-start = (bf16[136,1536]{1,0:T(8,128)(2,1)S(1)}, bf16[136,1536]{1,0:T(8,128)(2,1)S(1)}, u32[]{:S(2)}, u32[]{:S(2)}) collective-permute-start(bf16[136,1536]{1,0:T(8,128)(2,1)S(1)} %get-tuple-element.34.low_ref), channel_id=1, source_target_pairs={{0,8},{16,24},{1,9},{17,25},{2,10},{18,26},{3,11},{19,27},{4,12},{... | collective-permute-start | bytes 1253384 | tf_op jit(solution)/shard_map/ppermute | solution.py:397
  28.3 0.0 collective-permute-done.3.near_ref
  28.3 0.0 copy-done
  28.3 0.1 collective-permute-start.8
  28.4 0.0 collective-permute-done.11.refs_4_
  28.4 0.5 collective-permute-start.12
  28.9 0.0 collective-permute-done.1.last_ref
  28.9 0.1 collective-permute-start.10
  29.0 9.1 %collective-permute-done.13.refs_6_ = bf16[2048,256]{1,0:T(8,128)(2,1)S(1)} collective-permute-done((bf16[2048,256]{1,0:T(8,128)(2,1)S(1)}, bf16[2048,256]{1,0:T(8,128)(2,1)S(1)}, u32[]{:S(2)}, u32[]{:S(2)}) %collective-permute-start.13) | collective-permute-done | bytes 1048608 | tf_op jit(solution)/shard_map/ppermute | solution.py:402
  38.1 0.0 collective-permute-start.14
  38.1 0.0 collective-permute-done.pair_ref
  38.1 0.7 collective-permute-start.2
  38.8 0.8 %shard_map.75 = (bf16[128,1152]{1,0:T(8,128)(2,1)S(1)}, bf16[128,1152]{1,0:T(8,128)(2,1)S(1)}) custom-call(bf16[136,1536]{1,0:T(8,128)(2,1)S(1)} %collective-permute-done.pair_ref, bf16[136,1536]{1,0:T(8,128)(2,1)S(1)} %get-tuple-element.34.low_ref, bf16[128,1024]{1,0:T(8,128)(2,1)S(1)} %collective-permute-done.3.near_ref, ...), custom_call_target="tpu_custom_call" | custom-call | flops 201326592 | bytes 1949696 | tf_op jit(solution)/shard_map/pallas_call | solution.py:354
  39.6 0.0 collective-permute-done.2.before_ref
  39.6 0.0 copy-start.2
  39.6 1.4 %collective-permute-start.7 = (bf16[128,1152]{1,0:T(8,128)(2,1)S(1)}, bf16[128,1152]{1,0:T(8,128)(2,1)S(1)}, u32[]{:S(2)}, u32[]{:S(2)}) collective-permute-start(bf16[128,1152]{1,0:T(8,128)(2,1)S(1)} %get-tuple-element.26), channel_id=1, source_target_pairs={{8,24},{9,25},{10,26},{11,27},{12,28},{13,29},{14,30},{15,31}} | collective-permute-start | bytes 884744 | tf_op jit(solution)/shard_map/ppermute | solution.py:444
  41.1 0.8 %shard_map.76 = bf16[128,1152]{1,0:T(8,128)(2,1)S(1)} custom-call(bf16[136,1536]{1,0:T(8,128)(2,1)S(1)} %collective-permute-done.2.before_ref, bf16[136,1536]{1,0:T(8,128)(2,1)S(1)} %collective-permute-done.1.last_ref, bf16[136,1536]{1,0:T(8,128)(2,1)S(1)} %get-tuple-element.33.high_ref, bf16[128,1024]{1,0:T(8,128)(2,1)S(1)} %collective-permute-done.3.near_ref), custom_call_target="tpu_custom_call" | custom-call | flops 150994944 | bytes 1810432 | tf_op jit(solution)/shard_map/pallas_call | solution.py:354
  41.9 22.5 %collective-permute-done.7.later_ref = bf16[128,1152]{1,0:T(8,128)(2,1)S(1)} collective-permute-done((bf16[128,1152]{1,0:T(8,128)(2,1)S(1)}, bf16[128,1152]{1,0:T(8,128)(2,1)S(1)}, u32[]{:S(2)}, u32[]{:S(2)}) %collective-permute-start.7) | collective-permute-done | bytes 294944 | tf_op jit(solution)/shard_map/ppermute | solution.py:444
  64.4 0.7 collective-permute-start.5
  65.1 0.0 collective-permute-done.8.refs_1_
  65.1 1.3 %collective-permute-start.6 = (bf16[128,1152]{1,0:T(8,128)(2,1)S(1)}, bf16[128,1152]{1,0:T(8,128)(2,1)S(1)}, u32[]{:S(2)}, u32[]{:S(2)}) collective-permute-start(bf16[128,1152]{1,0:T(8,128)(2,1)S(1)} %shard_map.76), channel_id=1, source_target_pairs={{16,24},{17,25},{18,26},{19,27},{20,28},{21,29},{22,30},{23,31}} | collective-permute-start | bytes 884744 | tf_op jit(solution)/shard_map/ppermute | solution.py:445
  66.4 0.0 copy-done.2
  66.4 1.1 %shard_map.73 = (f32[128,1024]{1,0:T(8,128)S(1)}, f32[128,128]{1,0:T(8,128)S(1)}, f32[128,1024]{1,0:T(8,128)S(1)}, f32[128,128]{1,0:T(8,128)S(1)}) custom-call(bf16[136,1536]{1,0:T(8,128)(2,1)S(1)} %get-tuple-element.34.low_ref, bf16[136,1536]{1,0:T(8,128)(2,1)S(1)} %get-tuple-element.33.high_ref, bf16[128,1024]{1,0:T(8,128)(2,1)S(1)} %bitcast.11), custom_call_target="tpu_custom_call" | custom-call | flops 150994944 | bytes 2277376 | tf_op jit(solution)/shard_map/pallas_call | solution.py:354
  67.5 0.0 copy-start.1
  67.5 1.6 %shard_map.74 = (f32[128,1024]{1,0:T(8,128)S(1)}, f32[128,128]{1,0:T(8,128)S(1)}, f32[128,1024]{1,0:T(8,128)S(1)}, f32[128,128]{1,0:T(8,128)S(1)}) custom-call(bf16[136,1536]{1,0:T(8,128)(2,1)S(1)} %collective-permute-done.pair_ref, bf16[136,1536]{1,0:T(8,128)(2,1)S(1)} %collective-permute-done.2.before_ref, ...), custom_call_target="tpu_custom_call" | custom-call | flops 150994944 | bytes 3874816 | tf_op jit(solution)/shard_map/pallas_call | solution.py:354
  69.2 0.0 collective-permute-done.12.refs_5_
  69.2 0.0 collective-permute-done.10.refs_3_
  69.2 0.0 copy-done.1
  69.2 1.2 %shard_map.77 = (bf16[128,1024]{1,0:T(8,128)(2,1)S(1)}, f32[128,1536]{1,0:T(8,128)S(1)}) custom-call(bf16[128,2048]{1,0:T(8,128)(2,1)S(1)} %bitcast.7, f32[128,1024]{1,0:T(8,128)S(1)} %get-tuple-element.21.low_ref, f32[128,128]{1,0:T(8,128)S(1)} %get-tuple-element.22.low_note, f32[128,1024]{1,0:T(8,128)S(1)} %get-tuple-element.23.high_ref, ...), custom_call_target="tpu_custom_call" | custom-call | flops 402653184 | bytes 9338880 | tf_op jit(solution)/shard_map/pallas_call | solution.py:354
  70.4 0.0 collective-permute-done.5.next_ref
  70.4 3.3 %collective-permute-done.6.nextx_ref = bf16[128,1152]{1,0:T(8,128)(2,1)S(1)} collective-permute-done((bf16[128,1152]{1,0:T(8,128)(2,1)S(1)}, bf16[128,1152]{1,0:T(8,128)(2,1)S(1)}, u32[]{:S(2)}, u32[]{:S(2)}) %collective-permute-start.6) | collective-permute-done | bytes 294944 | tf_op jit(solution)/shard_map/ppermute | solution.py:445
  73.7 0.0 collective-permute-done.14.refs_7_
  73.7 2.3 %shard_map.78 = bf16[128,2048]{1,0:T(8,128)(2,1)} custom-call(bf16[128,2048]{1,0:T(8,128)(2,1)S(1)} %bitcast.8, f32[128,1024]{1,0:T(8,128)S(1)} %get-tuple-element.21.low_ref, f32[128,128]{1,0:T(8,128)S(1)} %get-tuple-element.22.low_note, f32[128,1024]{1,0:T(8,128)S(1)} %get-tuple-element.23.high_ref, f32[128,128]{1,0:T(8,128)S(1)} %get-tuple-element.24.high_note, ...), custom_call_target="tpu_custom_call" | custom-call | flops 536870912 | bytes 12255232 | tf_op jit(solution)/shard_map/pallas_call | solution.py:354
  (2 shorter events, 0.0 us)
Async XLA Ops:
  0.0 26.0 %copy-start.3 = (bf16[1,128,2048]{2,1,0:T(8,128)(2,1)S(1)}, bf16[1,128,2048]{2,1,0:T(8,128)(2,1)}, u32[]{:S(2)}) copy-start(bf16[1,128,2048]{2,1,0:T(8,128)(2,1)} %param.9) | copy-start | bytes 1572868
  0.0 22.8 %collective-permute-start.9 = (bf16[2048,256]{1,0:T(8,128)(2,1)}, bf16[2048,256]{1,0:T(8,128)(2,1)S(1)}, u32[]{:S(2)}, u32[]{:S(2)}) collective-permute-start(bf16[2048,256]{1,0:T(8,128)(2,1)} %refs_0_.3), channel_id=1, source_target_pairs={{0,2},{1,5},{2,0},{3,7},{4,6},{5,1},{6,4},{7,3},{8,10},{9,13},{10,... | collective-permute-start | bytes 3145736 | tf_op jit(solution)/shard_map/ppermute | solution.py:402
  1.5 25.5 %collective-permute-start.4 = (bf16[128,1024]{1,0:T(8,128)(2,1)}, bf16[128,1024]{1,0:T(8,128)(2,1)S(1)}, u32[]{:S(2)}, u32[]{:S(2)}) collective-permute-start(bf16[128,1024]{1,0:T(8,128)(2,1)} %bitcast.9), channel_id=1, source_target_pairs={{24,8},{25,9},{26,10},{27,11},{28,12},{29,13},{30,14},{31,15}} | collective-permute-start | bytes 786440 | tf_op jit(solution)/shard_map/ppermute | solution.py:396
  3.7 24.5 %collective-permute-start.3 = (bf16[128,1024]{1,0:T(8,128)(2,1)}, bf16[128,1024]{1,0:T(8,128)(2,1)S(1)}, u32[]{:S(2)}, u32[]{:S(2)}) collective-permute-start(bf16[128,1024]{1,0:T(8,128)(2,1)} %bitcast.10), channel_id=1, source_target_pairs={{16,8},{24,16},{17,9},{25,17},{18,10},{26,18},{19,11},{27,19},{20,... | collective-permute-start | bytes 786440 | tf_op jit(solution)/shard_map/ppermute | solution.py:395
  5.1 23.3 %collective-permute-start.11 = (bf16[2048,256]{1,0:T(8,128)(2,1)}, bf16[2048,256]{1,0:T(8,128)(2,1)S(1)}, u32[]{:S(2)}, u32[]{:S(2)}) collective-permute-start(bf16[2048,256]{1,0:T(8,128)(2,1)} %refs_0_.3), channel_id=1, source_target_pairs={{0,4},{1,3},{2,6},{3,1},{4,0},{5,7},{6,2},{7,5},{8,12},{9,11},{10,... | collective-permute-start | bytes 3145736 | tf_op jit(solution)/shard_map/ppermute | solution.py:402
  6.6 18.7 %copy-start.5 = (bf16[1,4,128]{2,1,0:T(4,128)(2,1)S(1)}, bf16[1,4,128]{2,1,0:T(4,128)(2,1)}, u32[]{:S(2)}) copy-start(bf16[1,4,128]{2,1,0:T(4,128)(2,1)} %param.11) | copy-start | bytes 3076
  22.8 15.3 %collective-permute-start.13 = (bf16[2048,256]{1,0:T(8,128)(2,1)S(1)}, bf16[2048,256]{1,0:T(8,128)(2,1)S(1)}, u32[]{:S(2)}, u32[]{:S(2)}) collective-permute-start(bf16[2048,256]{1,0:T(8,128)(2,1)S(1)} %collective-permute-done.9.refs_2_), channel_id=1, source_target_pairs={{0,4},{1,3},{2,6},{3,1},{4,0},{5,7},{6,2},{7,5},{8,12},{9,11},{10,... | collective-permute-start | bytes 3145736 | tf_op jit(solution)/shard_map/ppermute | solution.py:402
  25.3 0.7 copy-start.4
  26.1 2.2 %copy-start = (bf16[2048,256]{1,0:T(8,128)(2,1)S(1)}, bf16[2048,256]{1,0:T(8,128)(2,1)}, u32[]{:S(2)}) copy-start(bf16[2048,256]{1,0:T(8,128)(2,1)} %refs_0_.3) | copy-start | bytes 3145732
  26.1 2.7 %collective-permute-start.1 = (bf16[136,1536]{1,0:T(8,128)(2,1)S(1)}, bf16[136,1536]{1,0:T(8,128)(2,1)S(1)}, u32[]{:S(2)}, u32[]{:S(2)}) collective-permute-start(bf16[136,1536]{1,0:T(8,128)(2,1)S(1)} %get-tuple-element.33.high_ref), channel_id=1, source_target_pairs={{0,8},{8,16},{1,9},{9,17},{2,10},{10,18},{3,11},{11,19},{4,12},{12... | collective-permute-start | bytes 1253384 | tf_op jit(solution)/shard_map/ppermute | solution.py:394
  27.0 11.1 %collective-permute-start = (bf16[136,1536]{1,0:T(8,128)(2,1)S(1)}, bf16[136,1536]{1,0:T(8,128)(2,1)S(1)}, u32[]{:S(2)}, u32[]{:S(2)}) collective-permute-start(bf16[136,1536]{1,0:T(8,128)(2,1)S(1)} %get-tuple-element.34.low_ref), channel_id=1, source_target_pairs={{0,8},{16,24},{1,9},{17,25},{2,10},{18,26},{3,11},{19,27},{4,12},{... | collective-permute-start | bytes 1253384 | tf_op jit(solution)/shard_map/ppermute | solution.py:397
  28.3 36.8 %collective-permute-start.8 = (bf16[2048,256]{1,0:T(8,128)(2,1)S(1)}, bf16[2048,256]{1,0:T(8,128)(2,1)S(1)}, u32[]{:S(2)}, u32[]{:S(2)}) collective-permute-start(bf16[2048,256]{1,0:T(8,128)(2,1)S(1)} %copy-done), channel_id=1, source_target_pairs={{0,1},{1,0},{2,3},{3,2},{4,5},{5,4},{6,7},{7,6},{8,9},{9,8},{10,11... | collective-permute-start | bytes 3145736 | tf_op jit(solution)/shard_map/ppermute | solution.py:377
  28.4 40.8 %collective-permute-start.12 = (bf16[2048,256]{1,0:T(8,128)(2,1)S(1)}, bf16[2048,256]{1,0:T(8,128)(2,1)S(1)}, u32[]{:S(2)}, u32[]{:S(2)}) collective-permute-start(bf16[2048,256]{1,0:T(8,128)(2,1)S(1)} %collective-permute-done.11.refs_4_), channel_id=1, source_target_pairs={{0,1},{1,0},{2,3},{3,2},{4,5},{5,4},{6,7},{7,6},{8,9},{9,8},{10,11... | collective-permute-start | bytes 3145736 | tf_op jit(solution)/shard_map/ppermute | solution.py:377
  28.9 40.3 %collective-permute-start.10 = (bf16[2048,256]{1,0:T(8,128)(2,1)S(1)}, bf16[2048,256]{1,0:T(8,128)(2,1)S(1)}, u32[]{:S(2)}, u32[]{:S(2)}) collective-permute-start(bf16[2048,256]{1,0:T(8,128)(2,1)S(1)} %collective-permute-done.9.refs_2_), channel_id=1, source_target_pairs={{0,1},{1,0},{2,3},{3,2},{4,5},{5,4},{6,7},{7,6},{8,9},{9,8},{10,11... | collective-permute-start | bytes 3145736 | tf_op jit(solution)/shard_map/ppermute | solution.py:377
  38.1 35.6 %collective-permute-start.14 = (bf16[2048,256]{1,0:T(8,128)(2,1)S(1)}, bf16[2048,256]{1,0:T(8,128)(2,1)S(1)}, u32[]{:S(2)}, u32[]{:S(2)}) collective-permute-start(bf16[2048,256]{1,0:T(8,128)(2,1)S(1)} %collective-permute-done.13.refs_6_), channel_id=1, source_target_pairs={{0,1},{1,0},{2,3},{3,2},{4,5},{5,4},{6,7},{7,6},{8,9},{9,8},{10,11... | collective-permute-start | bytes 3145736 | tf_op jit(solution)/shard_map/ppermute | solution.py:377
  38.1 1.5 %collective-permute-start.2 = (bf16[136,1536]{1,0:T(8,128)(2,1)S(1)}, bf16[136,1536]{1,0:T(8,128)(2,1)S(1)}, u32[]{:S(2)}, u32[]{:S(2)}) collective-permute-start(bf16[136,1536]{1,0:T(8,128)(2,1)S(1)} %collective-permute-done.1.last_ref), channel_id=1, source_target_pairs={{8,16},{9,17},{10,18},{11,19},{12,20},{13,21},{14,22},{15,23}} | collective-permute-start | bytes 1253384 | tf_op jit(solution)/shard_map/ppermute | solution.py:398
  39.6 26.8 %copy-start.2 = (bf16[1,128,1024]{2,1,0:T(8,128)(2,1)S(1)}, bf16[1,128,1024]{2,1,0:T(8,128)(2,1)}, u32[]{:S(2)}) copy-start(bf16[1,128,1024]{2,1,0:T(8,128)(2,1)} %param.7) | copy-start | bytes 786436
  39.6 24.8 %collective-permute-start.7 = (bf16[128,1152]{1,0:T(8,128)(2,1)S(1)}, bf16[128,1152]{1,0:T(8,128)(2,1)S(1)}, u32[]{:S(2)}, u32[]{:S(2)}) collective-permute-start(bf16[128,1152]{1,0:T(8,128)(2,1)S(1)} %get-tuple-element.26), channel_id=1, source_target_pairs={{8,24},{9,25},{10,26},{11,27},{12,28},{13,29},{14,30},{15,31}} | collective-permute-start | bytes 884744 | tf_op jit(solution)/shard_map/ppermute | solution.py:444
  64.4 6.0 %collective-permute-start.5 = (bf16[128,1152]{1,0:T(8,128)(2,1)S(1)}, bf16[128,1152]{1,0:T(8,128)(2,1)S(1)}, u32[]{:S(2)}, u32[]{:S(2)}) collective-permute-start(bf16[128,1152]{1,0:T(8,128)(2,1)S(1)} %get-tuple-element.25), channel_id=1, source_target_pairs={{8,16},{9,17},{10,18},{11,19},{12,20},{13,21},{14,22},{15,23}} | collective-permute-start | bytes 884744 | tf_op jit(solution)/shard_map/ppermute | solution.py:443
  65.1 8.6 %collective-permute-start.6 = (bf16[128,1152]{1,0:T(8,128)(2,1)S(1)}, bf16[128,1152]{1,0:T(8,128)(2,1)S(1)}, u32[]{:S(2)}, u32[]{:S(2)}) collective-permute-start(bf16[128,1152]{1,0:T(8,128)(2,1)S(1)} %shard_map.76), channel_id=1, source_target_pairs={{16,24},{17,25},{18,26},{19,27},{20,28},{21,29},{22,30},{23,31}} | collective-permute-start | bytes 884744 | tf_op jit(solution)/shard_map/ppermute | solution.py:445
  67.5 1.7 %copy-start.1 = (bf16[1,128,2048]{2,1,0:T(8,128)(2,1)S(1)}, bf16[1,128,2048]{2,1,0:T(8,128)(2,1)}, u32[]{:S(2)}) copy-start(bf16[1,128,2048]{2,1,0:T(8,128)(2,1)} %param.10) | copy-start | bytes 1572868

commit v10 on v9

--- a/solution.py
+++ b/solution.py
@@ -70,6 +70,7 @@
 
 
 LANES = 128
+NOTES = 8
 
 
 def log_forget(gates):
@@ -247,10 +248,17 @@
         given = product(scores.astype(jnp.bfloat16), value_all).astype(jnp.bfloat16)
         for i, ref in enumerate(out_refs):
             here = slice(i * tokens, (i + 1) * tokens)
-            ref[:, out] = given[here]
+            ref[:tokens, out] = given[here]
             notes[i] += three_terms(sums[here]) + three_terms(reach[pick])
+            notes[i] += [jnp.zeros((1, 1), jnp.float32)] * (NOTES - 6)
     for ref, note in zip(out_refs, notes):
-        ref[:, count * value_width :] = to_lanes(note, tokens).astype(jnp.bfloat16)
+        rows = jnp.transpose(to_lanes(note, tokens))
+        for place in range(count):
+            group = slice(place * tokens, (place + 1) * tokens)
+            ref[tokens:, group] = rows[place * NOTES : (place + 1) * NOTES].astype(jnp.bfloat16)
+        ref[tokens:, count * tokens :] = jnp.zeros(
+            (NOTES, ref.shape[1] - count * tokens), jnp.bfloat16
+        )
 
 
 def serve_low_kernel(count, pair_ref, low_ref, near_ref, far_ref, next_ref, later_ref):
@@ -265,12 +273,18 @@
     value_width = totals[0].shape[1] // count
     low = half == 0
     own = jnp.where(low, notes[0][...], notes[1][...])
-    lanes = message(slice(count * value_width, count * value_width + LANES))
+    tokens = totals[0].shape[0]
+    tiles = [
+        message(slice(tokens, None), slice(place * tokens, (place + 1) * tokens))
+        for place in range(count)
+    ]
+    tiles.append(jnp.zeros((LANES - count * NOTES, tokens), jnp.float32))
+    lanes = jnp.transpose(jnp.concatenate(tiles, axis=0))
     gated = []
     for place in range(count):
         out = slice(place * value_width, (place + 1) * value_width)
         start = pl.multiple_of((half * count + place) * value_width, value_width)
-        at = 6 * place
+        at = NOTES * place
         sums = lanes[:, at : at + 1] + lanes[:, at + 1 : at + 2] + lanes[:, at + 2 : at + 3]
         at += 3
         reach = lanes[:, at : at + 1] + lanes[:, at + 1 : at + 2] + lanes[:, at + 2 : at + 3]
@@ -282,7 +296,7 @@
         weight = scale * own[:, 3 * place : 3 * place + 1] + scale_given * sums
         inverse = 1.0 / jnp.maximum(jnp.abs(weight), 1.0)
         total = jnp.where(low, totals[0][:, out], totals[1][:, out])
-        cell = (scale * inverse) * total + (scale_given * inverse) * message(out)
+        cell = (scale * inverse) * total + (scale_given * inverse) * message(slice(0, tokens), out)
         hidden = cell.astype(jnp.bfloat16).astype(jnp.float32)
         gate = jax.nn.sigmoid(gate_ref[:, pl.ds(start, value_width)].astype(jnp.float32))
         gated.append((hidden * gate).astype(jnp.bfloat16))
@@ -305,8 +319,8 @@
     pieces, gated_ref, part_ref = refs[:-2], refs[-2], refs[-1]
     rows, half = gated_ref.shape[1], first_half()
 
-    def message(columns):
-        return later_ref[:, columns].astype(jnp.float32)
+    def message(rows, columns):
+        return later_ref[rows, columns].astype(jnp.float32)
 
     given = lax.axis_index("sp") == 3
     totals, notes = (low_ref, high_ref), (low_note, high_note)
@@ -328,8 +342,10 @@
     width = pieces[0].shape[1]
     half = first_half()
 
-    def message(columns):
-        return next_ref[:, columns].astype(jnp.float32) + nextx_ref[:, columns].astype(jnp.float32)
+    def message(rows, columns):
+        return next_ref[rows, columns].astype(jnp.float32) + nextx_ref[rows, columns].astype(
+            jnp.float32
+        )
 
     given = lax.axis_index("sp") >= 2
     totals, notes = (low_ref, high_ref), (low_note, high_note)
@@ -425,7 +441,7 @@
     own = kernel_call(
         functools.partial(own_kernel, count), [low, high, query], sums, 3 * heads * work // 2, 8
     )
-    message = shape((tokens, count * value_width + LANES), jnp.bfloat16)
+    message = shape((tokens + NOTES, count * value_width), jnp.bfloat16)
     given_next, given_later = kernel_call(
         functools.partial(serve_low_kernel, count),
         [pair, low, near, far],

time: 76.3 us -> 75.6 us (level)
  waiting for transfers between devices: 50.1 us -> 49.3 us
  transfers between devices with their start and end apart: 15 -> 15, of which waited for: 4 -> 4; matrix products, arithmetic and copies ran while one was open for 1% -> 1% of each run, Pallas kernels for 7% -> 8%
where the time goes in v10:
time: 75.6 us; the launch traced here: 75.4 us
  waiting for transfers between devices  49.3 us (65%)
  starting transfers between devices  16 us (21%)
  Pallas kernels  7.99 us (11%)
  local copies, waits for them, and re-layouts  1.74 us (2%)
    ppermute x3, waiting for transfers between devices, cross(): return lax.ppermute(piece, 'dp', pairs)  24.3 us
    ppermute x1, waiting for transfers between devices, block_steps(): from_later = lax.ppermute(given_later, 'sp', [(1, 3)])  22 us
    pallas_call x6, Pallas kernels, kernel_call(): pl.pallas_call(kernel, out_shape=outs, in_specs=[vmem] * len(operands), o...  7.99 us
    ppermute x3, starting transfers between devices, cross(): return lax.ppermute(piece, 'dp', pairs)  5.61 us
    ppermute x1, waiting for transfers between devices, block_steps(): from_high = lax.ppermute(given_high, 'sp', [(2, 3)])  3.05 us
    ppermute x1, starting transfers between devices, block_steps(): far = lax.ppermute(query, 'sp', [(3, 1)])  2.25 us
  transfers between devices with their start and end apart: 15, of which 4 were waited for; matrix products, arithmetic and copies ran while one was open for 1% of the time, Pallas kernels for 8%

profile of v10, /device:TPU:24, one launch (start us, length us, event | category | flops | bytes accessed | tf_op | source)
XLA Modules:
  0.0 75.4 jit_solution(4689225465479169148)
XLA Ops:
  0.0 0.0 copy-start.3
  0.0 1.5 %collective-permute-start.9 = (bf16[2048,256]{1,0:T(8,128)(2,1)}, bf16[2048,256]{1,0:T(8,128)(2,1)S(1)}, u32[]{:S(2)}, u32[]{:S(2)}) collective-permute-start(bf16[2048,256]{1,0:T(8,128)(2,1)} %refs_0_.3), channel_id=1, source_target_pairs={{0,2},{1,5},{2,0},{3,7},{4,6},{5,1},{6,4},{7,3},{8,10},{9,13},{10,... | collective-permute-start | bytes 3145736 | tf_op jit(solution)/shard_map/ppermute | solution.py:418
  1.5 2.2 %collective-permute-start.4 = (bf16[128,1024]{1,0:T(8,128)(2,1)}, bf16[128,1024]{1,0:T(8,128)(2,1)S(1)}, u32[]{:S(2)}, u32[]{:S(2)}) collective-permute-start(bf16[128,1024]{1,0:T(8,128)(2,1)} %bitcast.9), channel_id=1, source_target_pairs={{24,8},{25,9},{26,10},{27,11},{28,12},{29,13},{30,14},{31,15}} | collective-permute-start | bytes 786440 | tf_op jit(solution)/shard_map/ppermute | solution.py:412
  3.7 1.3 %collective-permute-start.3 = (bf16[128,1024]{1,0:T(8,128)(2,1)}, bf16[128,1024]{1,0:T(8,128)(2,1)S(1)}, u32[]{:S(2)}, u32[]{:S(2)}) collective-permute-start(bf16[128,1024]{1,0:T(8,128)(2,1)} %bitcast.10), channel_id=1, source_target_pairs={{16,8},{24,16},{17,9},{25,17},{18,10},{26,18},{19,11},{27,19},{20,... | collective-permute-start | bytes 786440 | tf_op jit(solution)/shard_map/ppermute | solution.py:411
  5.1 1.6 %collective-permute-start.11 = (bf16[2048,256]{1,0:T(8,128)(2,1)}, bf16[2048,256]{1,0:T(8,128)(2,1)S(1)}, u32[]{:S(2)}, u32[]{:S(2)}) collective-permute-start(bf16[2048,256]{1,0:T(8,128)(2,1)} %refs_0_.3), channel_id=1, source_target_pairs={{0,4},{1,3},{2,6},{3,1},{4,0},{5,7},{6,2},{7,5},{8,12},{9,11},{10,... | collective-permute-start | bytes 3145736 | tf_op jit(solution)/shard_map/ppermute | solution.py:418
  6.6 0.0 copy-start.5
  6.7 1.0 %fusion.4 = (bf16[128,512]{1,0:T(8,128)(2,1)S(1)}, bf16[128,512]{1,0:T(8,128)(2,1)S(1)}) fusion(bf16[128,1024]{1,0:T(8,128)(2,1)} %bitcast.14), kind=kLoop, calls=%fused_computation.7 | loop fusion | bytes 524288 | tf_op jit(solution)/shard_map/slice | solution.py:402
  7.7 15.1 %collective-permute-done.9.refs_2_ = bf16[2048,256]{1,0:T(8,128)(2,1)S(1)} collective-permute-done((bf16[2048,256]{1,0:T(8,128)(2,1)}, bf16[2048,256]{1,0:T(8,128)(2,1)S(1)}, u32[]{:S(2)}, u32[]{:S(2)}) %collective-permute-start.9) | collective-permute-done | bytes 1048608 | tf_op jit(solution)/shard_map/ppermute | solution.py:418
  22.8 2.5 %collective-permute-start.13 = (bf16[2048,256]{1,0:T(8,128)(2,1)S(1)}, bf16[2048,256]{1,0:T(8,128)(2,1)S(1)}, u32[]{:S(2)}, u32[]{:S(2)}) collective-permute-start(bf16[2048,256]{1,0:T(8,128)(2,1)S(1)} %collective-permute-done.9.refs_2_), channel_id=1, source_target_pairs={{0,4},{1,3},{2,6},{3,1},{4,0},{5,7},{6,2},{7,5},{8,12},{9,11},{10,... | collective-permute-start | bytes 3145736 | tf_op jit(solution)/shard_map/ppermute | solution.py:418
  25.3 0.0 copy-start.4
  25.3 0.0 copy-done.5
  25.3 0.7 copy-done.4
  26.0 0.0 copy-done.3
  26.1 0.0 copy-start
  26.1 0.1 pad_maximum_fusion
  26.1 0.8 %collective-permute-start.1 = (bf16[136,1536]{1,0:T(8,128)(2,1)S(1)}, bf16[136,1536]{1,0:T(8,128)(2,1)S(1)}, u32[]{:S(2)}, u32[]{:S(2)}) collective-permute-start(bf16[136,1536]{1,0:T(8,128)(2,1)S(1)} %get-tuple-element.33.high_ref), channel_id=1, source_target_pairs={{0,8},{8,16},{1,9},{9,17},{2,10},{10,18},{3,11},{11,19},{4,12},{12... | collective-permute-start | bytes 1253384 | tf_op jit(solution)/shard_map/ppermute | solution.py:410
  27.0 0.0 collective-permute-done.4.far_ref
  27.0 1.3 %collective-permute-start = (bf16[136,1536]{1,0:T(8,128)(2,1)S(1)}, bf16[136,1536]{1,0:T(8,128)(2,1)S(1)}, u32[]{:S(2)}, u32[]{:S(2)}) collective-permute-start(bf16[136,1536]{1,0:T(8,128)(2,1)S(1)} %get-tuple-element.34.low_ref), channel_id=1, source_target_pairs={{0,8},{16,24},{1,9},{17,25},{2,10},{18,26},{3,11},{19,27},{4,12},{... | collective-permute-start | bytes 1253384 | tf_op jit(solution)/shard_map/ppermute | solution.py:413
  28.3 0.0 collective-permute-done.3.near_ref
  28.3 0.0 copy-done
  28.3 0.1 collective-permute-start.8
  28.4 0.0 collective-permute-done.11.refs_4_
  28.4 0.5 collective-permute-start.12
  28.9 0.0 collective-permute-done.1.last_ref
  28.9 0.1 collective-permute-start.10
  29.0 9.1 %collective-permute-done.13.refs_6_ = bf16[2048,256]{1,0:T(8,128)(2,1)S(1)} collective-permute-done((bf16[2048,256]{1,0:T(8,128)(2,1)S(1)}, bf16[2048,256]{1,0:T(8,128)(2,1)S(1)}, u32[]{:S(2)}, u32[]{:S(2)}) %collective-permute-start.13) | collective-permute-done | bytes 1048608 | tf_op jit(solution)/shard_map/ppermute | solution.py:418
  38.1 0.0 collective-permute-start.14
  38.1 0.0 collective-permute-done.pair_ref
  38.1 0.7 collective-permute-start.2
  38.8 0.8 %shard_map.75 = (bf16[136,1024]{1,0:T(8,128)(2,1)S(1)}, bf16[136,1024]{1,0:T(8,128)(2,1)S(1)}) custom-call(bf16[136,1536]{1,0:T(8,128)(2,1)S(1)} %collective-permute-done.pair_ref, bf16[136,1536]{1,0:T(8,128)(2,1)S(1)} %get-tuple-element.34.low_ref, bf16[128,1024]{1,0:T(8,128)(2,1)S(1)} %collective-permute-done.3.near_ref, ...), custom_call_target="tpu_custom_call" | custom-call | flops 201326592 | bytes 1916928 | tf_op jit(solution)/shard_map/pallas_call | solution.py:370
  39.6 0.0 collective-permute-done.2.before_ref
  39.6 0.0 copy-start.2
  39.6 1.4 %collective-permute-start.7 = (bf16[136,1024]{1,0:T(8,128)(2,1)S(1)}, bf16[136,1024]{1,0:T(8,128)(2,1)S(1)}, u32[]{:S(2)}, u32[]{:S(2)}) collective-permute-start(bf16[136,1024]{1,0:T(8,128)(2,1)S(1)} %get-tuple-element.26), channel_id=1, source_target_pairs={{8,24},{9,25},{10,26},{11,27},{12,28},{13,29},{14,30},{15,31}} | collective-permute-start | bytes 835592 | tf_op jit(solution)/shard_map/ppermute | solution.py:460
  41.1 0.8 %shard_map.76 = bf16[136,1024]{1,0:T(8,128)(2,1)S(1)} custom-call(bf16[136,1536]{1,0:T(8,128)(2,1)S(1)} %collective-permute-done.2.before_ref, bf16[136,1536]{1,0:T(8,128)(2,1)S(1)} %collective-permute-done.1.last_ref, bf16[136,1536]{1,0:T(8,128)(2,1)S(1)} %get-tuple-element.33.high_ref, bf16[128,1024]{1,0:T(8,128)(2,1)S(1)} %collective-permute-done.3.near_ref), custom_call_target="tpu_custom_call" | custom-call | flops 150994944 | bytes 1794048 | tf_op jit(solution)/shard_map/pallas_call | solution.py:370
  41.9 22.0 %collective-permute-done.7.later_ref = bf16[136,1024]{1,0:T(8,128)(2,1)S(1)} collective-permute-done((bf16[136,1024]{1,0:T(8,128)(2,1)S(1)}, bf16[136,1024]{1,0:T(8,128)(2,1)S(1)}, u32[]{:S(2)}, u32[]{:S(2)}) %collective-permute-start.7) | collective-permute-done | bytes 278560 | tf_op jit(solution)/shard_map/ppermute | solution.py:460
  63.9 0.7 collective-permute-start.5
  64.6 0.0 collective-permute-done.8.refs_1_
  64.6 1.3 %collective-permute-start.6 = (bf16[136,1024]{1,0:T(8,128)(2,1)S(1)}, bf16[136,1024]{1,0:T(8,128)(2,1)S(1)}, u32[]{:S(2)}, u32[]{:S(2)}) collective-permute-start(bf16[136,1024]{1,0:T(8,128)(2,1)S(1)} %shard_map.76), channel_id=1, source_target_pairs={{16,24},{17,25},{18,26},{19,27},{20,28},{21,29},{22,30},{23,31}} | collective-permute-start | bytes 835592 | tf_op jit(solution)/shard_map/ppermute | solution.py:461
  65.9 0.0 copy-done.2
  65.9 1.1 %shard_map.73 = (f32[128,1024]{1,0:T(8,128)S(1)}, f32[128,128]{1,0:T(8,128)S(1)}, f32[128,1024]{1,0:T(8,128)S(1)}, f32[128,128]{1,0:T(8,128)S(1)}) custom-call(bf16[136,1536]{1,0:T(8,128)(2,1)S(1)} %get-tuple-element.34.low_ref, bf16[136,1536]{1,0:T(8,128)(2,1)S(1)} %get-tuple-element.33.high_ref, bf16[128,1024]{1,0:T(8,128)(2,1)S(1)} %bitcast.11), custom_call_target="tpu_custom_call" | custom-call | flops 150994944 | bytes 2277376 | tf_op jit(solution)/shard_map/pallas_call | solution.py:370
  67.0 0.0 copy-start.1
  67.0 1.6 %shard_map.74 = (f32[128,1024]{1,0:T(8,128)S(1)}, f32[128,128]{1,0:T(8,128)S(1)}, f32[128,1024]{1,0:T(8,128)S(1)}, f32[128,128]{1,0:T(8,128)S(1)}) custom-call(bf16[136,1536]{1,0:T(8,128)(2,1)S(1)} %collective-permute-done.pair_ref, bf16[136,1536]{1,0:T(8,128)(2,1)S(1)} %collective-permute-done.2.before_ref, ...), custom_call_target="tpu_custom_call" | custom-call | flops 150994944 | bytes 3874816 | tf_op jit(solution)/shard_map/pallas_call | solution.py:370
  68.7 0.0 collective-permute-done.12.refs_5_
  68.7 0.0 collective-permute-done.10.refs_3_
  68.7 0.0 copy-done.1
  68.7 1.3 %shard_map.77 = (bf16[128,1024]{1,0:T(8,128)(2,1)S(1)}, f32[128,1536]{1,0:T(8,128)S(1)}) custom-call(bf16[128,2048]{1,0:T(8,128)(2,1)S(1)} %bitcast.7, f32[128,1024]{1,0:T(8,128)S(1)} %get-tuple-element.21.low_ref, f32[128,128]{1,0:T(8,128)S(1)} %get-tuple-element.22.low_note, f32[128,1024]{1,0:T(8,128)S(1)} %get-tuple-element.23.high_ref, ...), custom_call_target="tpu_custom_call" | custom-call | flops 402653184 | bytes 9322496 | tf_op jit(solution)/shard_map/pallas_call | solution.py:370
  70.0 0.0 collective-permute-done.5.next_ref
  70.0 3.0 %collective-permute-done.6.nextx_ref = bf16[136,1024]{1,0:T(8,128)(2,1)S(1)} collective-permute-done((bf16[136,1024]{1,0:T(8,128)(2,1)S(1)}, bf16[136,1024]{1,0:T(8,128)(2,1)S(1)}, u32[]{:S(2)}, u32[]{:S(2)}) %collective-permute-start.6) | collective-permute-done | bytes 278560 | tf_op jit(solution)/shard_map/ppermute | solution.py:461
  73.0 0.0 collective-permute-done.14.refs_7_
  73.0 2.3 %shard_map.78 = bf16[128,2048]{1,0:T(8,128)(2,1)} custom-call(bf16[128,2048]{1,0:T(8,128)(2,1)S(1)} %bitcast.8, f32[128,1024]{1,0:T(8,128)S(1)} %get-tuple-element.21.low_ref, f32[128,128]{1,0:T(8,128)S(1)} %get-tuple-element.22.low_note, f32[128,1024]{1,0:T(8,128)S(1)} %get-tuple-element.23.high_ref, f32[128,128]{1,0:T(8,128)S(1)} %get-tuple-element.24.high_note, ...), custom_call_target="tpu_custom_call" | custom-call | flops 536870912 | bytes 12222464 | tf_op jit(solution)/shard_map/pallas_call | solution.py:370
  (2 shorter events, 0.0 us)
Async XLA Ops:
  0.0 26.0 %copy-start.3 = (bf16[1,128,2048]{2,1,0:T(8,128)(2,1)S(1)}, bf16[1,128,2048]{2,1,0:T(8,128)(2,1)}, u32[]{:S(2)}) copy-start(bf16[1,128,2048]{2,1,0:T(8,128)(2,1)} %param.9) | copy-start | bytes 1572868
  0.0 22.8 %collective-permute-start.9 = (bf16[2048,256]{1,0:T(8,128)(2,1)}, bf16[2048,256]{1,0:T(8,128)(2,1)S(1)}, u32[]{:S(2)}, u32[]{:S(2)}) collective-permute-start(bf16[2048,256]{1,0:T(8,128)(2,1)} %refs_0_.3), channel_id=1, source_target_pairs={{0,2},{1,5},{2,0},{3,7},{4,6},{5,1},{6,4},{7,3},{8,10},{9,13},{10,... | collective-permute-start | bytes 3145736 | tf_op jit(solution)/shard_map/ppermute | solution.py:418
  1.5 25.5 %collective-permute-start.4 = (bf16[128,1024]{1,0:T(8,128)(2,1)}, bf16[128,1024]{1,0:T(8,128)(2,1)S(1)}, u32[]{:S(2)}, u32[]{:S(2)}) collective-permute-start(bf16[128,1024]{1,0:T(8,128)(2,1)} %bitcast.9), channel_id=1, source_target_pairs={{24,8},{25,9},{26,10},{27,11},{28,12},{29,13},{30,14},{31,15}} | collective-permute-start | bytes 786440 | tf_op jit(solution)/shard_map/ppermute | solution.py:412
  3.7 24.5 %collective-permute-start.3 = (bf16[128,1024]{1,0:T(8,128)(2,1)}, bf16[128,1024]{1,0:T(8,128)(2,1)S(1)}, u32[]{:S(2)}, u32[]{:S(2)}) collective-permute-start(bf16[128,1024]{1,0:T(8,128)(2,1)} %bitcast.10), channel_id=1, source_target_pairs={{16,8},{24,16},{17,9},{25,17},{18,10},{26,18},{19,11},{27,19},{20,... | collective-permute-start | bytes 786440 | tf_op jit(solution)/shard_map/ppermute | solution.py:411
  5.1 23.3 %collective-permute-start.11 = (bf16[2048,256]{1,0:T(8,128)(2,1)}, bf16[2048,256]{1,0:T(8,128)(2,1)S(1)}, u32[]{:S(2)}, u32[]{:S(2)}) collective-permute-start(bf16[2048,256]{1,0:T(8,128)(2,1)} %refs_0_.3), channel_id=1, source_target_pairs={{0,4},{1,3},{2,6},{3,1},{4,0},{5,7},{6,2},{7,5},{8,12},{9,11},{10,... | collective-permute-start | bytes 3145736 | tf_op jit(solution)/shard_map/ppermute | solution.py:418
  6.6 18.7 %copy-start.5 = (bf16[1,4,128]{2,1,0:T(4,128)(2,1)S(1)}, bf16[1,4,128]{2,1,0:T(4,128)(2,1)}, u32[]{:S(2)}) copy-start(bf16[1,4,128]{2,1,0:T(4,128)(2,1)} %param.11) | copy-start | bytes 3076
  22.8 15.3 %collective-permute-start.13 = (bf16[2048,256]{1,0:T(8,128)(2,1)S(1)}, bf16[2048,256]{1,0:T(8,128)(2,1)S(1)}, u32[]{:S(2)}, u32[]{:S(2)}) collective-permute-start(bf16[2048,256]{1,0:T(8,128)(2,1)S(1)} %collective-permute-done.9.refs_2_), channel_id=1, source_target_pairs={{0,4},{1,3},{2,6},{3,1},{4,0},{5,7},{6,2},{7,5},{8,12},{9,11},{10,... | collective-permute-start | bytes 3145736 | tf_op jit(solution)/shard_map/ppermute | solution.py:418
  25.3 0.7 copy-start.4
  26.1 2.2 %copy-start = (bf16[2048,256]{1,0:T(8,128)(2,1)S(1)}, bf16[2048,256]{1,0:T(8,128)(2,1)}, u32[]{:S(2)}) copy-start(bf16[2048,256]{1,0:T(8,128)(2,1)} %refs_0_.3) | copy-start | bytes 3145732
  26.1 2.7 %collective-permute-start.1 = (bf16[136,1536]{1,0:T(8,128)(2,1)S(1)}, bf16[136,1536]{1,0:T(8,128)(2,1)S(1)}, u32[]{:S(2)}, u32[]{:S(2)}) collective-permute-start(bf16[136,1536]{1,0:T(8,128)(2,1)S(1)} %get-tuple-element.33.high_ref), channel_id=1, source_target_pairs={{0,8},{8,16},{1,9},{9,17},{2,10},{10,18},{3,11},{11,19},{4,12},{12... | collective-permute-start | bytes 1253384 | tf_op jit(solution)/shard_map/ppermute | solution.py:410
  27.0 11.1 %collective-permute-start = (bf16[136,1536]{1,0:T(8,128)(2,1)S(1)}, bf16[136,1536]{1,0:T(8,128)(2,1)S(1)}, u32[]{:S(2)}, u32[]{:S(2)}) collective-permute-start(bf16[136,1536]{1,0:T(8,128)(2,1)S(1)} %get-tuple-element.34.low_ref), channel_id=1, source_target_pairs={{0,8},{16,24},{1,9},{17,25},{2,10},{18,26},{3,11},{19,27},{4,12},{... | collective-permute-start | bytes 1253384 | tf_op jit(solution)/shard_map/ppermute | solution.py:413
  28.3 36.3 %collective-permute-start.8 = (bf16[2048,256]{1,0:T(8,128)(2,1)S(1)}, bf16[2048,256]{1,0:T(8,128)(2,1)S(1)}, u32[]{:S(2)}, u32[]{:S(2)}) collective-permute-start(bf16[2048,256]{1,0:T(8,128)(2,1)S(1)} %copy-done), channel_id=1, source_target_pairs={{0,1},{1,0},{2,3},{3,2},{4,5},{5,4},{6,7},{7,6},{8,9},{9,8},{10,11... | collective-permute-start | bytes 3145736 | tf_op jit(solution)/shard_map/ppermute | solution.py:393
  28.4 40.3 %collective-permute-start.12 = (bf16[2048,256]{1,0:T(8,128)(2,1)S(1)}, bf16[2048,256]{1,0:T(8,128)(2,1)S(1)}, u32[]{:S(2)}, u32[]{:S(2)}) collective-permute-start(bf16[2048,256]{1,0:T(8,128)(2,1)S(1)} %collective-permute-done.11.refs_4_), channel_id=1, source_target_pairs={{0,1},{1,0},{2,3},{3,2},{4,5},{5,4},{6,7},{7,6},{8,9},{9,8},{10,11... | collective-permute-start | bytes 3145736 | tf_op jit(solution)/shard_map/ppermute | solution.py:393
  28.9 39.8 %collective-permute-start.10 = (bf16[2048,256]{1,0:T(8,128)(2,1)S(1)}, bf16[2048,256]{1,0:T(8,128)(2,1)S(1)}, u32[]{:S(2)}, u32[]{:S(2)}) collective-permute-start(bf16[2048,256]{1,0:T(8,128)(2,1)S(1)} %collective-permute-done.9.refs_2_), channel_id=1, source_target_pairs={{0,1},{1,0},{2,3},{3,2},{4,5},{5,4},{6,7},{7,6},{8,9},{9,8},{10,11... | collective-permute-start | bytes 3145736 | tf_op jit(solution)/shard_map/ppermute | solution.py:393
  38.1 34.9 %collective-permute-start.14 = (bf16[2048,256]{1,0:T(8,128)(2,1)S(1)}, bf16[2048,256]{1,0:T(8,128)(2,1)S(1)}, u32[]{:S(2)}, u32[]{:S(2)}) collective-permute-start(bf16[2048,256]{1,0:T(8,128)(2,1)S(1)} %collective-permute-done.13.refs_6_), channel_id=1, source_target_pairs={{0,1},{1,0},{2,3},{3,2},{4,5},{5,4},{6,7},{7,6},{8,9},{9,8},{10,11... | collective-permute-start | bytes 3145736 | tf_op jit(solution)/shard_map/ppermute | solution.py:393
  38.1 1.5 %collective-permute-start.2 = (bf16[136,1536]{1,0:T(8,128)(2,1)S(1)}, bf16[136,1536]{1,0:T(8,128)(2,1)S(1)}, u32[]{:S(2)}, u32[]{:S(2)}) collective-permute-start(bf16[136,1536]{1,0:T(8,128)(2,1)S(1)} %collective-permute-done.1.last_ref), channel_id=1, source_target_pairs={{8,16},{9,17},{10,18},{11,19},{12,20},{13,21},{14,22},{15,23}} | collective-permute-start | bytes 1253384 | tf_op jit(solution)/shard_map/ppermute | solution.py:414
  39.6 26.3 %copy-start.2 = (bf16[1,128,1024]{2,1,0:T(8,128)(2,1)S(1)}, bf16[1,128,1024]{2,1,0:T(8,128)(2,1)}, u32[]{:S(2)}) copy-start(bf16[1,128,1024]{2,1,0:T(8,128)(2,1)} %param.7) | copy-start | bytes 786436
  39.6 24.3 %collective-permute-start.7 = (bf16[136,1024]{1,0:T(8,128)(2,1)S(1)}, bf16[136,1024]{1,0:T(8,128)(2,1)S(1)}, u32[]{:S(2)}, u32[]{:S(2)}) collective-permute-start(bf16[136,1024]{1,0:T(8,128)(2,1)S(1)} %get-tuple-element.26), channel_id=1, source_target_pairs={{8,24},{9,25},{10,26},{11,27},{12,28},{13,29},{14,30},{15,31}} | collective-permute-start | bytes 835592 | tf_op jit(solution)/shard_map/ppermute | solution.py:460
  63.9 6.1 %collective-permute-start.5 = (bf16[136,1024]{1,0:T(8,128)(2,1)S(1)}, bf16[136,1024]{1,0:T(8,128)(2,1)S(1)}, u32[]{:S(2)}, u32[]{:S(2)}) collective-permute-start(bf16[136,1024]{1,0:T(8,128)(2,1)S(1)} %get-tuple-element.25), channel_id=1, source_target_pairs={{8,16},{9,17},{10,18},{11,19},{12,20},{13,21},{14,22},{15,23}} | collective-permute-start | bytes 835592 | tf_op jit(solution)/shard_map/ppermute | solution.py:459
  64.6 8.4 %collective-permute-start.6 = (bf16[136,1024]{1,0:T(8,128)(2,1)S(1)}, bf16[136,1024]{1,0:T(8,128)(2,1)S(1)}, u32[]{:S(2)}, u32[]{:S(2)}) collective-permute-start(bf16[136,1024]{1,0:T(8,128)(2,1)S(1)} %shard_map.76), channel_id=1, source_target_pairs={{16,24},{17,25},{18,26},{19,27},{20,28},{21,29},{22,30},{23,31}} | collective-permute-start | bytes 835592 | tf_op jit(solution)/shard_map/ppermute | solution.py:461
  67.0 1.7 %copy-start.1 = (bf16[1,128,2048]{2,1,0:T(8,128)(2,1)S(1)}, bf16[1,128,2048]{2,1,0:T(8,128)(2,1)}, u32[]{:S(2)}) copy-start(bf16[1,128,2048]{2,1,0:T(8,128)(2,1)} %param.10) | copy-start | bytes 1572868
